TPU v7x, 512 devices: a whole 4x4x16 slice. The times are simulated.
512 devices in a mesh: sp: 16 (over y, x), tp: 32 (over z, core).
Axes of the slice: x: 4, y: 4, z: 16, core: 2. Of those that a mesh axis runs over, the one named last changes fastest.
Arguments:
- tokens: bfloat16 [3, 8192, 4096], P(None, 'sp', 'tp'), may hold values from -6 to 6
- new_token: bfloat16 [3, 1, 4096], P(None, None, 'tp'), may hold values from -6 to 6
- query_weight: bfloat16 [4096, 4096], P(None, 'tp'), may hold values from -0.09375 to 0.09375
- key_weight: bfloat16 [4096, 4096], P(None, 'tp'), may hold values from -0.09375 to 0.09375
- value_weight: bfloat16 [4096, 4096], P(None, 'tp'), may hold values from -0.09375 to 0.09375
- log_decay: float32 [64], P('tp'), may hold values from -0.034 to 0
Outputs:
- state: bfloat16 [3, 64, 64, 64], P(None, 'tp', 'sp')
- read: bfloat16 [3, 4096], P(None, 'tp')
All inputs are finite; a program needn't handle non-finite values.
Results may differ from a plain program's by a relative error of at most 0.012.
Values may be sent and summed in bfloat16 or wider, within the bound.
No kernel may reach another device: no remote copies, remote signals or barrier semaphores. Data moves between devices by JAX's collectives and lax.ppermute only.
A program may use at most 64 MiB of HBM per device.

v0:
```python
import jax
import jax.numpy as jnp
from jax import lax
from jax.sharding import PartitionSpec as P

HD = 64


def cut_along(value, dim, count):
    dims = value.shape
    tiles = value.reshape(*dims[:dim], count, dims[dim] // count, *dims[dim + 1 :])
    return jnp.moveaxis(tiles, dim, 0)


def sent_and_summed(value, axis, dim):
    tiles = cut_along(value, dim, lax.axis_size(axis))
    arrived = lax.all_to_all(tiles, axis, split_axis=0, concat_axis=0, tiled=True)
    return arrived.sum(axis=0)


def from_everyone(value, axis):
    copies = jnp.broadcast_to(value, (lax.axis_size(axis), *value.shape))
    return lax.all_to_all(copies, axis, split_axis=0, concat_axis=0, tiled=True)


def over_copies(value, axis):
    everything = from_everyone(value, axis)
    return jnp.sum(everything, axis=0)


def rotate(values, positions):
    half_dim = values.shape[-1] // 2
    inverse = 10000.0 ** (-jnp.arange(half_dim, dtype=jnp.float32) / half_dim)
    angles = positions.astype(jnp.float32)[:, None, None] * inverse[None, None, :]
    cosine = jnp.cos(angles)
    sine_part = jnp.sin(angles)
    first = values[..., :half_dim]
    second = values[..., half_dim:]
    return jnp.concatenate(
        [first * cosine - second * sine_part, first * sine_part + second * cosine], axis=-1
    )


def group_norm(output):
    centered = output - jnp.mean(output, axis=-1, keepdims=True)
    return centered * lax.rsqrt(jnp.mean(centered * centered, axis=-1, keepdims=True) + 1e-05)


def body(tokens, new_token, query_weight, key_weight, value_weight, log_decay):
    sequences, span_len, _ = tokens.shape
    head_count = log_decay.shape[0]
    inner = head_count * HD
    groups = lax.axis_size("sp")
    own_index = lax.axis_index("sp")
    key_scale = HD ** (-0.5)
    row_weights = jnp.concatenate([key_weight, value_weight], axis=1)
    all_weights = jnp.concatenate([key_weight, value_weight, query_weight], axis=1)
    row_piece = lax.all_gather(tokens, "tp", axis=2, tiled=True)
    new_piece = lax.all_gather(new_token, "tp", axis=2, tiled=True)
    row_total = jnp.dot(row_piece, row_weights, preferred_element_type=jnp.float32)
    new_total = jnp.dot(new_piece, all_weights, preferred_element_type=jnp.float32)
    row_total = row_total.reshape(sequences, span_len, 2, head_count, HD)
    offsets = own_index * span_len + jnp.arange(span_len, dtype=jnp.int32)
    key_rows = (rotate(row_total[:, :, 0], offsets) * key_scale).astype(jnp.bfloat16)
    value_rows = row_total[:, :, 1].astype(jnp.bfloat16)
    to_end = (span_len - 1 - jnp.arange(span_len, dtype=jnp.int32)).astype(jnp.float32)
    decay_rows = jnp.exp(to_end[:, None] * log_decay[None, :])
    weighted = (key_rows.astype(jnp.float32) * decay_rows[None, :, :, None]).astype(jnp.bfloat16)
    span_state = jnp.einsum(
        "sthk,sthv->shkv", weighted, value_rows, preferred_element_type=jnp.float32
    )
    carried_state = jnp.exp(log_decay * (span_len * (groups - 1 - own_index)).astype(jnp.float32))
    scaled_state = span_state * carried_state[None, :, None, None]
    state_rows = sent_and_summed(scaled_state, "sp", 2)
    new_total = new_total.reshape(sequences, 1, 3, head_count, HD)
    new_position = jnp.full((1,), groups * span_len, jnp.int32)
    fresh_key = (rotate(new_total[:, :, 0], new_position) * key_scale).astype(jnp.bfloat16)[:, 0]
    new_value = new_total[:, 0, 1].astype(jnp.bfloat16)
    new_query = rotate(new_total[:, :, 2], new_position).astype(jnp.bfloat16)[:, 0]
    query_entries = new_query.astype(jnp.float32)
    decay_one = jnp.exp(log_decay)[None, :, None]
    partial_read = (
        jnp.einsum("shkv,shk->shv", scaled_state, query_entries, precision=lax.Precision.HIGHEST)
        * decay_one
    )
    summed = over_copies(partial_read, "sp")
    own_term = jnp.sum(
        query_entries * fresh_key.astype(jnp.float32), axis=-1, keepdims=True
    ) * new_value.astype(jnp.float32)
    normed = group_norm(summed + own_term)
    return (state_rows.astype(jnp.bfloat16), normed.reshape(sequences, inner).astype(jnp.bfloat16))


def solution(mesh):
    return jax.shard_map(
        body,
        mesh=mesh,
        in_specs=(
            P(None, "sp", "tp"),
            P(None, None, "tp"),
            P(None, "tp"),
            P(None, "tp"),
            P(None, "tp"),
            P("tp"),
        ),
        out_specs=(P(None, "tp", "sp", None), P(None, "tp")),
        check_vma=False,
    )
```

profile of v0, /device:TPU:1, one launch (start us, length us, event | category | flops | bytes accessed | tf_op | source)
XLA Modules:
  0.0 171.5 jit_solution(1786247637780565341)
XLA Ops:
  7.2 0.7 all-gather.2.cloned.1.call-update
  7.9 1.5 copy.27
  9.4 1.4 copy.26
  10.8 37.7 %all_gather.7 = bf16[3,1,4096]{2,0,1:T(4,128)(2,1)S(1)} all-gather(bf16[3,1,128]{2,0,1:T(4,128)(2,1)S(1)} %copy-done.3), channel_id=1, replica_groups=mesh['sp'=16,'tp'=32] {'tp'}, dimensions={2}, use_global_device_ids=true | all-gather | bytes 25344 | tf_op jit(solution)/shard_map/all_gather | solution.py:59
  48.5 1.8 %fusion.9 = f32[3,384]{1,0:T(4,128)S(1)} fusion(bf16[4096,128]{1,0:T(8,128)(2,1)} %param.8, bf16[4096,128]{1,0:T(8,128)(2,1)S(1)} %copy-done, bf16[4096,128]{1,0:T(8,128)(2,1)S(1)} %copy-done.1, bf16[3,1,4096]{2,0,1:T(4,128)(2,1)S(1)} %all_gather.7), kind=kOutput, calls=%fused_computation.11 | convolution fusion | flops 18874368 | bytes 3174912 | tf_op jit(solution)/shard_map/dot_general | solution.py:61
  50.3 0.1 reshape.207
  50.7 0.3 multiply_cosine_fusion
  51.0 79.8 %all-gather.2.cloned.1.call-done = bf16[3,512,4096]{2,1,0:T(8,128)(2,1)} async-done(((bf16[3,512,128]{2,1,0:T(8,128)(2,1)}), bf16[3,512,4096]{2,1,0:T(8,128)(2,1)}) %all-gather.2.cloned.1.call-update) | async-done | bytes 12582928 | tf_op jit(solution)/shard_map/all_gather | solution.py:58
  130.8 6.8 %fusion.6 = f32[256,3,512]{2,0,1:T(8,128)S(1)} fusion(bf16[3,512,4096]{2,1,0:T(8,128)(2,1)} %all-gather.2.cloned.1.call-done, bf16[4096,128]{0,1:T(8,128)(2,1)S(1)} %copy.27, bf16[4096,128]{0,1:T(8,128)(2,1)} %copy.26), kind=kOutput, calls=%fused_computation.7 | convolution fusion | flops 3225419776 | bytes 16252928 | tf_op jit(solution)/shard_map/dot_general | solution.py:60
  137.7 0.1 multiply_subtract_fusion
  137.8 0.3 convolution_multiply_fusion
  138.1 0.2 fusion.22
  138.4 0.7 reshape.215
  139.1 7.3 %all-to-all-start.1 = ((f32[16,1,384]{2,1,0:T(1,128)}), f32[16,1,384]{2,1,0:T(1,128)S(1)}, u32[]{:S(2)}, u32[]{:S(2)}) async-start(f32[16,1,384]{2,1,0:T(1,128)} %reshape.215), calls=%async_computation.1 | async-start | bytes 49152 | tf_op jit(solution)/shard_map/all_to_all | solution.py:23
  146.4 0.2 multiply_reduce_fusion.1
  146.6 0.1 mul.280
  146.7 0.1 reshape.208
  146.8 0.8 reshape.213
  147.7 5.2 %all-to-all-done.1 = f32[16,1,384]{2,1,0:T(1,128)S(1)} async-done(((f32[16,1,384]{2,1,0:T(1,128)}), f32[16,1,384]{2,1,0:T(1,128)S(1)}, u32[]{:S(2)}, u32[]{:S(2)}) %all-to-all-start.1) | async-done | bytes 24608 | tf_op jit(solution)/shard_map/all_to_all | solution.py:23
  152.8 3.5 %all-to-all-start = ((f32[16,1,1536]{2,1,0:T(1,128)}), f32[16,1,1536]{2,1,0:T(1,128)S(1)}, u32[]{:S(2)}, u32[]{:S(2)}) async-start(f32[16,1,1536]{2,1,0:T(1,128)} %reshape.213), calls=%async_computation | async-start | bytes 196608 | tf_op jit(solution)/shard_map/all_to_all | solution.py:17
  156.4 0.5 broadcast.164
  156.9 0.7 reduce.1
  157.6 0.1 reshape.216
  157.7 0.2 fusion.32
  158.0 0.2 multiply_reduce_fusion
  158.2 0.1 mul.285
  158.4 0.1 sub.42
  158.4 0.6 multiply_convert_fusion.2
  159.0 4.0 %all-to-all-done = f32[16,1,1536]{2,1,0:T(1,128)S(1)} async-done(((f32[16,1,1536]{2,1,0:T(1,128)}), f32[16,1,1536]{2,1,0:T(1,128)S(1)}, u32[]{:S(2)}, u32[]{:S(2)}) %all-to-all-start) | async-done | bytes 98336 | tf_op jit(solution)/shard_map/all_to_all | solution.py:17
  163.0 0.9 reduce
  163.9 0.1 reshape.214
  164.0 0.7 reduce_sum.47
  (30 shorter events, 0.9 us)
Async XLA Ops:
  7.2 41.3 %copy-start = (bf16[4096,128]{1,0:T(8,128)(2,1)S(1)}, bf16[4096,128]{1,0:T(8,128)(2,1)}, u32[]{:S(2)}) copy-start(bf16[4096,128]{1,0:T(8,128)(2,1)} %param.10) | copy-start | bytes 3145732
  7.2 2.3 %copy-start.1 = (bf16[4096,128]{1,0:T(8,128)(2,1)S(1)}, bf16[4096,128]{1,0:T(8,128)(2,1)}, u32[]{:S(2)}) copy-start(bf16[4096,128]{1,0:T(8,128)(2,1)} %param.9) | copy-start | bytes 3145732
  7.2 3.6 %copy-start.3 = (bf16[3,1,128]{2,0,1:T(4,128)(2,1)S(1)}, bf16[3,1,128]{2,0,1:T(4,128)(2,1)}, u32[]{:S(2)}) copy-start(bf16[3,1,128]{2,0,1:T(4,128)(2,1)} %param.7) | copy-start | bytes 2308
  7.2 123.6 %all-gather.2.cloned.1.call-start = ((), (), s32[]{:S(2)}) async-start(), calls=%async_computation.2 | async-start | bytes 12976128 | tf_op jit(solution)/shard_map/all_gather | solution.py:58
  48.5 2.1 %copy-start.2 = (f32[2]{0:T(128)S(1)}, f32[2]{0:T(128)}, u32[]{:S(2)}) copy-start(f32[2]{0:T(128)} %param.11) | copy-start | bytes 28
  139.1 13.7 %all-to-all-start.1 = ((f32[16,1,384]{2,1,0:T(1,128)}), f32[16,1,384]{2,1,0:T(1,128)S(1)}, u32[]{:S(2)}, u32[]{:S(2)}) async-start(f32[16,1,384]{2,1,0:T(1,128)} %reshape.215), calls=%async_computation.1 | async-start | bytes 49152 | tf_op jit(solution)/shard_map/all_to_all | solution.py:23
  152.8 10.1 %all-to-all-start = ((f32[16,1,1536]{2,1,0:T(1,128)}), f32[16,1,1536]{2,1,0:T(1,128)S(1)}, u32[]{:S(2)}, u32[]{:S(2)}) async-start(f32[16,1,1536]{2,1,0:T(1,128)} %reshape.213), calls=%async_computation | async-start | bytes 196608 | tf_op jit(solution)/shard_map/all_to_all | solution.py:17
Sparse Core Ops, SparseCore 0:
  10.0 120.7 all-gather.1
where the time goes:
time: 173 us; the launch traced here: 172 us
  waiting for transfers between devices  89.6 us (52%)
  blocking collectives  37.7 us (22%)
  between operations  14.2 us (8%)
  starting transfers between devices  10.8 us (6%)
  matrix products  9.01 us (5%)
  local copies, waits for them, and re-layouts  5.97 us (3%)
  other arithmetic  4.18 us (2%)
    all_gather x1, waiting for transfers between devices, body(): row_piece = lax.all_gather(tokens, 'tp', axis=2, tiled=True)  79.8 us
    all_gather x1, blocking collectives, body(): new_piece = lax.all_gather(new_token, 'tp', axis=2, tiled=True)  37.7 us
    all_to_all x1, starting transfers between devices, from_everyone(): return lax.all_to_all(copies, axis, split_axis=0, concat_axis=0, tiled=True)  7.27 us
    dot_general x1, matrix products, body(): jnp.dot(row_piece, row_weights, preferred_element_type=jnp.float32)  6.76 us
    all_to_all x1, waiting for transfers between devices, from_everyone(): return lax.all_to_all(copies, axis, split_axis=0, concat_axis=0, tiled=True)  5.18 us
    unnamed x14, local copies, waits for them, and re-layouts  4.6 us
    all_to_all x1, waiting for transfers between devices, sent_and_summed(): lax.all_to_all(tiles, axis, split_axis=0, concat_axis=0, tiled=True)  3.96 us
    all_to_all x1, starting transfers between devices, sent_and_summed(): lax.all_to_all(tiles, axis, split_axis=0, concat_axis=0, tiled=True)  3.51 us
  transfers between devices with their start and end apart: 3, of which 3 were waited for; matrix products, arithmetic and copies ran while one was open for 5% of the time, Pallas kernels for 0%

commit v1 on v0

v1 whole, which is shorter than its diff:
```python
import jax
import jax.numpy as jnp
from jax import lax
from jax.experimental import pallas as pl
from jax.experimental.pallas import tpu as pltpu
from jax.sharding import PartitionSpec as P

HD = 64
EPS = 1e-05
STEP = 8


def swap_halves(values):
    lanes = values.shape[-1]
    lane = lax.broadcasted_iota(jnp.int32, values.shape, len(values.shape) - 1)
    quarter = HD // 2
    back = pltpu.roll(values, lanes - quarter, len(values.shape) - 1)
    ahead = pltpu.roll(values, quarter, len(values.shape) - 1)
    return jnp.where(lane % HD < quarter, back, ahead)


def state_kernel(
    x_ref, kw_ref, vw_ref, cos_ref, sin_ref, decay_ref, carried_ref, query_ref, one_ref, out_ref, acc
):
    prompt = pl.program_id(0)
    step = pl.program_id(1)
    blocks = [x_ref[i, 0] for i in range(STEP)]
    both = jnp.concatenate(blocks, axis=1)
    width = both.shape[1]
    at = pl.ds(pl.multiple_of(step * width, width), width)
    weights = jnp.concatenate([kw_ref[at, :], vw_ref[at, :]], axis=1)
    part = jnp.dot(both, weights, preferred_element_type=jnp.float32)

    @pl.when(step == 0)
    def _():
        acc[...] = part

    @pl.when(step > 0)
    def _():
        acc[...] += part

    @pl.when(step == pl.num_programs(1) - 1)
    def _():
        inner = kw_ref.shape[1]
        total = acc[...]
        keys = total[:, :inner]
        values = total[:, inner:].astype(jnp.bfloat16)
        keys = (keys * cos_ref[...] + swap_halves(keys) * sin_ref[...]).astype(jnp.bfloat16)
        weighted = (keys.astype(jnp.float32) * decay_ref[...]).astype(jnp.bfloat16)
        full = lax.dot_general(
            weighted, values, (((0,), (0,)), ((), ())), preferred_element_type=jnp.float32
        )
        lane = lax.broadcasted_iota(jnp.int32, (HD, inner), 1)
        state = jnp.where(lane < HD, full[:HD], full[HD:]) * carried_ref[...]
        read = jnp.sum(state * query_ref[0], axis=0, keepdims=True) * one_ref[...]
        groups = out_ref.shape[0]
        keep = HD // groups
        count = out_ref.shape[1] // (keep + 1)
        for s in range(count):

            @pl.when(prompt == s)
            def _():
                for g in range(groups):
                    out_ref[g, s * keep : (s + 1) * keep, :] = state[g * keep : (g + 1) * keep]
                    out_ref[g, count * keep + s : count * keep + s + 1, :] = read


def span_states(gathered, key_weight, value_weight, cosine, sine, decay, carried, query, one, groups):
    devices, prompts, span_len, width = gathered.shape
    inner = key_weight.shape[1]
    keep = HD // groups
    out_rows = prompts * (keep + 1)
    whole = pl.BlockSpec(memory_space=pltpu.VMEM)
    return pl.pallas_call(
        state_kernel,
        grid=(prompts, devices // STEP),
        in_specs=[
            pl.BlockSpec((STEP, 1, span_len, width), lambda s, k: (k, s, 0, 0)),
            whole,
            whole,
            whole,
            whole,
            whole,
            whole,
            pl.BlockSpec((1, HD, inner), lambda s, k: (s, 0, 0)),
            whole,
        ],
        out_specs=pl.BlockSpec((groups, out_rows, inner), lambda s, k: (0, 0, 0)),
        out_shape=jax.ShapeDtypeStruct((groups, out_rows, inner), jnp.float32),
        scratch_shapes=[pltpu.VMEM((span_len, 2 * inner), jnp.float32)],
        compiler_params=pltpu.CompilerParams(
            dimension_semantics=("arbitrary", "arbitrary"), vmem_limit_bytes=53 * 1024 * 1024
        ),
        name="span_states",
    )(gathered, key_weight, value_weight, cosine, sine, decay, carried, query, one)


def finish_kernel(arrived_ref, own_ref, state_ref, read_ref):
    total = jnp.sum(arrived_ref[...], axis=0)
    prompts, heads, keep, _ = state_ref.shape
    for s in range(prompts):
        for h in range(heads):
            state_ref[s, h] = total[s * keep : (s + 1) * keep, h * HD : (h + 1) * HD].astype(
                jnp.bfloat16
            )
    raw = total[prompts * keep :] + own_ref[...]
    lane = lax.broadcasted_iota(jnp.int32, raw.shape, 1)

    def per_head(values):
        result = jnp.zeros_like(values)
        for h in range(heads):
            here = lane // HD == h
            mean = jnp.sum(jnp.where(here, values, 0.0), axis=1, keepdims=True) / HD
            result = jnp.where(here, mean, result)
        return result

    centered = raw - per_head(raw)
    spread = per_head(centered * centered)
    read_ref[...] = (centered * lax.rsqrt(spread + EPS)).astype(jnp.bfloat16)


def finish(arrived, own_term, heads, keep):
    prompts, inner = own_term.shape
    whole = pl.BlockSpec(memory_space=pltpu.VMEM)
    return pl.pallas_call(
        finish_kernel,
        in_specs=[whole, whole],
        out_specs=[whole, whole],
        out_shape=[
            jax.ShapeDtypeStruct((prompts, heads, keep, HD), jnp.bfloat16),
            jax.ShapeDtypeStruct((prompts, inner), jnp.bfloat16),
        ],
        compiler_params=pltpu.CompilerParams(vmem_limit_bytes=4 * 1024 * 1024),
        name="finish",
    )(arrived, own_term)


def angles_at(positions, heads):
    half_dim = HD // 2
    inverse = 10000.0 ** (-jnp.arange(half_dim, dtype=jnp.float32) / half_dim)
    angles = positions.astype(jnp.float32)[:, None] * inverse[None, :]
    cosine = jnp.cos(angles)
    sine = jnp.sin(angles)
    cosine = jnp.tile(jnp.concatenate([cosine, cosine], axis=1), (1, heads))
    sine = jnp.tile(jnp.concatenate([-sine, sine], axis=1), (1, heads))
    return cosine, sine


def rotate(values, cosine, sine):
    half_dim = HD // 2
    swapped = values.reshape(values.shape[0], -1, 2, half_dim)[:, :, ::-1].reshape(values.shape)
    return values * cosine + swapped * sine


def body(tokens, new_token, query_weight, key_weight, value_weight, log_decay):
    prompts, span_len, width = tokens.shape
    heads = log_decay.shape[0]
    inner = heads * HD
    groups = lax.axis_size("sp")
    own_index = lax.axis_index("sp")
    key_scale = HD ** (-0.5)

    gathered = lax.all_gather(tokens, "tp", axis=0, tiled=False)
    fresh = lax.all_gather(new_token[:, 0], "tp", axis=0, tiled=False)

    local = jnp.arange(span_len, dtype=jnp.int32)
    cosine, sine = angles_at(own_index * span_len + local, heads)
    to_end = (span_len - 1 - local).astype(jnp.float32)
    lane_decay = jnp.repeat(log_decay, HD)
    decay_rows = jnp.exp(to_end[:, None] * lane_decay[None, :])
    distance = (span_len * (groups - 1 - own_index)).astype(jnp.float32)
    carried = jnp.exp(lane_decay * distance)[None, :]
    one = jnp.exp(lane_decay)[None, :]

    all_weights = jnp.concatenate([key_weight, value_weight, query_weight], axis=1)
    fresh = jnp.moveaxis(fresh, 0, 1).reshape(prompts, -1)
    new_total = jnp.dot(fresh, all_weights, preferred_element_type=jnp.float32)
    new_cosine, new_sine = angles_at(jnp.full((1,), groups * span_len, jnp.int32), heads)
    new_key = (rotate(new_total[:, :inner], new_cosine, new_sine) * key_scale).astype(jnp.bfloat16)
    new_value = new_total[:, inner : 2 * inner].astype(jnp.bfloat16).astype(jnp.float32)
    new_query = rotate(new_total[:, 2 * inner :], new_cosine, new_sine).astype(jnp.bfloat16)
    new_query = new_query.astype(jnp.float32)
    score = jnp.sum(
        (new_query * new_key.astype(jnp.float32)).reshape(prompts, heads, HD), axis=-1, keepdims=True
    )
    own_term = (score * new_value.reshape(prompts, heads, HD)).reshape(prompts, inner)
    query = jnp.swapaxes(new_query.reshape(prompts, heads, HD), 1, 2)
    query = jnp.repeat(query, HD, axis=2)

    messages = span_states(
        gathered,
        key_weight,
        value_weight,
        cosine * key_scale,
        sine * key_scale,
        decay_rows,
        carried,
        query,
        one,
        groups,
    )
    arrived = lax.all_to_all(messages, "sp", split_axis=0, concat_axis=0, tiled=True)
    return tuple(finish(arrived, own_term, heads, HD // groups))


def solution(mesh):
    return jax.shard_map(
        body,
        mesh=mesh,
        in_specs=(
            P(None, "sp", "tp"),
            P(None, None, "tp"),
            P(None, "tp"),
            P(None, "tp"),
            P(None, "tp"),
            P("tp"),
        ),
        out_specs=(P(None, "tp", "sp", None), P(None, "tp")),
        check_vma=False,
    )
```

time: 173 us -> 138 us (0.80)
  waiting for transfers between devices: 89.6 us -> 57.2 us
  Pallas kernels: 0 us -> 14.5 us
  matrix products: 9.01 us -> 2.44 us
  starting transfers between devices: 10.8 us -> 6.84 us
  local copies, waits for them, and re-layouts: 5.97 us -> 2.84 us
  other arithmetic: 4.18 us -> 1.71 us
    all_gather x1, waiting for transfers between devices: 79.8 us -> 49.7 us  [body(): gathered = lax.all_gather(tokens, 'tp', axis=0, tiled=False)]
    pallas_call x0 -> x2, Pallas kernels: none -> 14.5 us  [the longest x1 13.8 us: span_states(): pl.pallas_call(state_kernel, grid=(prompts, devices // STEP), in_specs=[p...]
    dot_general x4 -> x1, matrix products: 9.01 us -> 2.44 us  [body(): new_total = jnp.dot(fresh, all_weights, preferred_element_type=jnp.float32)]
    all_to_all x2 -> x1, starting transfers between devices: 10.8 us -> 6.8 us  [body(): lax.all_to_all(messages, 'sp', split_axis=0, concat_axis=0, tiled=True)]
    unnamed x14 -> x3, local copies, waits for them, and re-layouts: 4.6 us -> 0.69 us
    all_to_all x2 -> x1, waiting for transfers between devices: 9.13 us -> 6.83 us  [body(): lax.all_to_all(messages, 'sp', split_axis=0, concat_axis=0, tiled=True)]
  transfers between devices with their start and end apart: 3 -> 2, of which waited for: 3 -> 2; matrix products, arithmetic and copies ran while one was open for 5% -> 5% of each run, Pallas kernels for 0% -> 0%
where the time goes in v1:
time: 138 us
  waiting for transfers between devices  57.2 us (41%)
  blocking collectives  38 us (28%)
  Pallas kernels  14.5 us (11%)
  between operations  14.2 us (10%)
  starting transfers between devices  6.84 us (5%)
  local copies, waits for them, and re-layouts  2.84 us (2%)
  matrix products  2.44 us (2%)
  other arithmetic  1.71 us (1%)
    all_gather x1, waiting for transfers between devices, body(): gathered = lax.all_gather(tokens, 'tp', axis=0, tiled=False)  49.7 us
    all_gather x1, blocking collectives, body(): fresh = lax.all_gather(new_token[:, 0], 'tp', axis=0, tiled=False)  38 us
    pallas_call x1, Pallas kernels, span_states(): pl.pallas_call(state_kernel, grid=(prompts, devices // STEP), in_specs=[p...  13.8 us
    all_to_all x1, waiting for transfers between devices, body(): lax.all_to_all(messages, 'sp', split_axis=0, concat_axis=0, tiled=True)  6.83 us
    all_to_all x1, starting transfers between devices, body(): lax.all_to_all(messages, 'sp', split_axis=0, concat_axis=0, tiled=True)  6.8 us
  transfers between devices with their start and end apart: 2, of which 2 were waited for; matrix products, arithmetic and copies ran while one was open for 5% of the time, Pallas kernels for 0%

profile of v1, /device:TPU:1, one launch (start us, length us, event | category | flops | bytes accessed | tf_op | source)
XLA Modules:
  0.0 137.8 jit_solution(2635889893870370107)
XLA Ops:
  7.2 0.7 all-gather.4.cloned.1.call-update
  7.9 0.7 copy.12
  8.6 38.0 %all-gather.1 = bf16[96,1,128]{2,1,0:T(2,128)(2,1)S(1)} all-gather(bf16[3,1,128]{2,1,0:T(2,128)(2,1)S(1)} %copy.12), channel_id=3, replica_groups=mesh['sp'=16,'tp'=32] {'tp'}, dimensions={0}, use_global_device_ids=true | all-gather | bytes 25344 | tf_op jit(solution)/shard_map/all_gather | solution.py:164
  46.6 0.1 reduce
  46.7 2.4 %fusion.7 = f32[3,384]{1,0:T(4,128)S(1)} fusion(bf16[4096,128]{1,0:T(8,128)(2,1)} %param.8, bf16[4096,128]{1,0:T(8,128)(2,1)} %vw_ref.1, bf16[4096,128]{1,0:T(8,128)(2,1)} %kw_ref.1, bf16[32,3,128]{2,1,0:T(4,128)(2,1)S(1)} %reshape.137), kind=kOutput, calls=%fused_computation.7 | convolution fusion | flops 18874368 | bytes 3174912 | tf_op jit(solution)/shard_map/dot_general | solution.py:177
  49.2 0.1 reshape.129
  49.3 0.1 reshape.130
  49.4 0.1 reshape.133
  49.5 0.1 reshape.134
  49.7 0.1 maximum_bitcast_fusion.1
  49.7 0.1 tile.43
  49.9 0.1 maximum_bitcast_fusion
  50.0 0.1 tile.40
  50.1 0.1 reshape.131
  50.1 0.1 copy.13
  50.3 0.3 broadcast_in_dim.19
  50.5 0.2 reshape.132.query_ref
  50.7 0.3 fusion.11
  51.1 0.1 copy.14.cos_ref
  51.3 0.1 copy.15.sin_ref
  51.5 0.1 exp.33.carried_ref
  51.6 0.1 exp.35.one_ref
  51.8 0.1 mul.144
  51.9 0.1 reshape.135
  52.0 0.1 fusion
  52.0 0.1 mul.162
  52.1 0.9 multiply_exponential_fusion.decay_ref
  53.0 49.7 %all-gather.4.cloned.1.call-done = bf16[96,512,128]{2,1,0:T(8,128)(2,1)} async-done(((bf16[3,512,128]{2,1,0:T(8,128)(2,1)}), bf16[96,512,128]{2,1,0:T(8,128)(2,1)}) %all-gather.4.cloned.1.call-update) | async-done | bytes 12582928 | tf_op jit(solution)/shard_map/all_gather | solution.py:163
  102.7 13.8 %span_states.1 = f32[16,15,128]{2,1,0:T(8,128)} custom-call(bf16[32,3,512,128]{3,2,1,0:T(8,128)(2,1)} %bitcast.16, bf16[4096,128]{1,0:T(8,128)(2,1)} %kw_ref.1, bf16[4096,128]{1,0:T(8,128)(2,1)} %vw_ref.1, f32[512,128]{1,0:T(8,128)S(1)} %copy.14.cos_ref, f32[512,128]{1,0:T(8,128)S(1)} %copy.15.sin_ref, f32[512,128]{1,0:T(8,128)} %multiply_exponential_fusion.decay_ref, ...), custom_call_target="tpu_custom_call" | custom-call | tf_op jit(solution)/shard_map/span_states/pallas_call | solution.py:74
  116.5 6.8 %all-to-all-start = ((f32[16,15,128]{2,1,0:T(8,128)}), f32[16,15,128]{2,1,0:T(8,128)S(1)}, u32[]{:S(2)}, u32[]{:S(2)}) async-start(f32[16,15,128]{2,1,0:T(8,128)} %span_states.1), calls=%async_computation | async-start | bytes 262144 | tf_op jit(solution)/shard_map/all_to_all | solution.py:202
  123.3 6.8 %all-to-all-done.arrived_ref = f32[16,15,128]{2,1,0:T(8,128)S(1)} async-done(((f32[16,15,128]{2,1,0:T(8,128)}), f32[16,15,128]{2,1,0:T(8,128)S(1)}, u32[]{:S(2)}, u32[]{:S(2)}) %all-to-all-start) | async-done | bytes 122912 | tf_op jit(solution)/shard_map/all_to_all | solution.py:202
  130.1 0.8 finish.1
  (23 shorter events, 0.6 us)
Async XLA Ops:
  7.2 44.2 %copy-start = (f32[2]{0:T(128)S(1)}, f32[2]{0:T(128)}, u32[]{:S(2)}) copy-start(f32[2]{0:T(128)} %param.11) | copy-start | bytes 28
  7.2 95.6 %all-gather.4.cloned.1.call-start = ((), (), s32[]{:S(2)}) async-start(), calls=%async_computation.1 | async-start | bytes 12976128 | tf_op jit(solution)/shard_map/all_gather | solution.py:163
  116.5 13.7 %all-to-all-start = ((f32[16,15,128]{2,1,0:T(8,128)}), f32[16,15,128]{2,1,0:T(8,128)S(1)}, u32[]{:S(2)}, u32[]{:S(2)}) async-start(f32[16,15,128]{2,1,0:T(8,128)} %span_states.1), calls=%async_computation | async-start | bytes 262144 | tf_op jit(solution)/shard_map/all_to_all | solution.py:202
Sparse Core Ops, SparseCore 0:
  10.1 92.5 all-gather.3

commit v2 on v1

--- a/solution.py
+++ b/solution.py
@@ -7,7 +7,7 @@
 
 HD = 64
 EPS = 1e-05
-STEP = 8
+STEP = 16
 
 
 def swap_halves(values):
@@ -20,29 +20,45 @@
 
 
 def state_kernel(
-    x_ref, kw_ref, vw_ref, cos_ref, sin_ref, decay_ref, carried_ref, query_ref, one_ref, out_ref, acc
+    x_ref,
+    kw_ref,
+    vw_ref,
+    cos_ref,
+    sin_ref,
+    decay_ref,
+    carried_ref,
+    query_ref,
+    one_ref,
+    out_ref,
+    held,
+    arrived,
 ):
-    prompt = pl.program_id(0)
-    step = pl.program_id(1)
-    blocks = [x_ref[i, 0] for i in range(STEP)]
-    both = jnp.concatenate(blocks, axis=1)
-    width = both.shape[1]
-    at = pl.ds(pl.multiple_of(step * width, width), width)
-    weights = jnp.concatenate([kw_ref[at, :], vw_ref[at, :]], axis=1)
-    part = jnp.dot(both, weights, preferred_element_type=jnp.float32)
-
-    @pl.when(step == 0)
-    def _():
-        acc[...] = part
-
-    @pl.when(step > 0)
-    def _():
-        acc[...] += part
-
-    @pl.when(step == pl.num_programs(1) - 1)
-    def _():
-        inner = kw_ref.shape[1]
-        total = acc[...]
+    devices, prompts, _, width = x_ref.shape
+    inner = kw_ref.shape[1]
+    groups = out_ref.shape[0]
+    keep = HD // groups
+    pieces = devices // STEP
+    copies = [
+        pltpu.make_async_copy(
+            x_ref.at[pl.ds(k * STEP, STEP), s],
+            held.at[s, pl.ds(k * STEP, STEP)],
+            arrived.at[s * pieces + k],
+        )
+        for s in range(prompts)
+        for k in range(pieces)
+    ]
+    for copy in copies:
+        copy.start()
+    lane = lax.broadcasted_iota(jnp.int32, (HD, inner), 1)
+    for s in range(prompts):
+        total = None
+        for k in range(pieces):
+            copies[s * pieces + k].wait()
+            both = jnp.concatenate([held[s, k * STEP + i] for i in range(STEP)], axis=1)
+            at = pl.ds(k * STEP * width, STEP * width)
+            weights = jnp.concatenate([kw_ref[at, :], vw_ref[at, :]], axis=1)
+            part = jnp.dot(both, weights, preferred_element_type=jnp.float32)
+            total = part if total is None else total + part
         keys = total[:, :inner]
         values = total[:, inner:].astype(jnp.bfloat16)
         keys = (keys * cos_ref[...] + swap_halves(keys) * sin_ref[...]).astype(jnp.bfloat16)
@@ -50,47 +66,28 @@
         full = lax.dot_general(
             weighted, values, (((0,), (0,)), ((), ())), preferred_element_type=jnp.float32
         )
-        lane = lax.broadcasted_iota(jnp.int32, (HD, inner), 1)
         state = jnp.where(lane < HD, full[:HD], full[HD:]) * carried_ref[...]
-        read = jnp.sum(state * query_ref[0], axis=0, keepdims=True) * one_ref[...]
-        groups = out_ref.shape[0]
-        keep = HD // groups
-        count = out_ref.shape[1] // (keep + 1)
-        for s in range(count):
-
-            @pl.when(prompt == s)
-            def _():
-                for g in range(groups):
-                    out_ref[g, s * keep : (s + 1) * keep, :] = state[g * keep : (g + 1) * keep]
-                    out_ref[g, count * keep + s : count * keep + s + 1, :] = read
+        read = jnp.sum(state * query_ref[s], axis=0, keepdims=True) * one_ref[...]
+        for g in range(groups):
+            out_ref[g, s * keep : (s + 1) * keep, :] = state[g * keep : (g + 1) * keep]
+            out_ref[g, prompts * keep + s : prompts * keep + s + 1, :] = read
 
 
 def span_states(gathered, key_weight, value_weight, cosine, sine, decay, carried, query, one, groups):
     devices, prompts, span_len, width = gathered.shape
     inner = key_weight.shape[1]
     keep = HD // groups
-    out_rows = prompts * (keep + 1)
     whole = pl.BlockSpec(memory_space=pltpu.VMEM)
     return pl.pallas_call(
         state_kernel,
-        grid=(prompts, devices // STEP),
-        in_specs=[
-            pl.BlockSpec((STEP, 1, span_len, width), lambda s, k: (k, s, 0, 0)),
-            whole,
-            whole,
-            whole,
-            whole,
-            whole,
-            whole,
-            pl.BlockSpec((1, HD, inner), lambda s, k: (s, 0, 0)),
-            whole,
+        in_specs=[pl.BlockSpec(memory_space=pltpu.HBM)] + [whole] * 8,
+        out_specs=whole,
+        out_shape=jax.ShapeDtypeStruct((groups, prompts * (keep + 1), inner), jnp.float32),
+        scratch_shapes=[
+            pltpu.VMEM((prompts, devices, span_len, width), gathered.dtype),
+            pltpu.SemaphoreType.DMA((prompts * (devices // STEP),)),
         ],
-        out_specs=pl.BlockSpec((groups, out_rows, inner), lambda s, k: (0, 0, 0)),
-        out_shape=jax.ShapeDtypeStruct((groups, out_rows, inner), jnp.float32),
-        scratch_shapes=[pltpu.VMEM((span_len, 2 * inner), jnp.float32)],
-        compiler_params=pltpu.CompilerParams(
-            dimension_semantics=("arbitrary", "arbitrary"), vmem_limit_bytes=53 * 1024 * 1024
-        ),
+        compiler_params=pltpu.CompilerParams(vmem_limit_bytes=53 * 1024 * 1024),
         name="span_states",
     )(gathered, key_weight, value_weight, cosine, sine, decay, carried, query, one)
 

time: 138 us -> 136 us (0.986)
  Pallas kernels: 14.5 us -> 12.4 us
    pallas_call x1, Pallas kernels: 13.8 us -> 11.6 us  [span_states(): pl.pallas_call(state_kernel, in_specs=[pl.BlockSpec(memory_space=pltpu.HB...]
where the time goes in v2:
time: 136 us
  waiting for transfers between devices  57.2 us (42%)
  blocking collectives  38 us (28%)
  between operations  14.2 us (10%)
  Pallas kernels  12.4 us (9%)
  starting transfers between devices  6.85 us (5%)
  local copies, waits for them, and re-layouts  2.84 us (2%)
  matrix products  2.44 us (2%)
  other arithmetic  1.71 us (1%)
    all_gather x1, waiting for transfers between devices, body(): gathered = lax.all_gather(tokens, 'tp', axis=0, tiled=False)  49.7 us
    all_gather x1, blocking collectives, body(): fresh = lax.all_gather(new_token[:, 0], 'tp', axis=0, tiled=False)  38 us
    pallas_call x1, Pallas kernels, span_states(): pl.pallas_call(state_kernel, in_specs=[pl.BlockSpec(memory_space=pltpu.HB...  11.6 us
    all_to_all x1, waiting for transfers between devices, body(): lax.all_to_all(messages, 'sp', split_axis=0, concat_axis=0, tiled=True)  6.83 us
    all_to_all x1, starting transfers between devices, body(): lax.all_to_all(messages, 'sp', split_axis=0, concat_axis=0, tiled=True)  6.82 us
  transfers between devices with their start and end apart: 2, of which 2 were waited for; matrix products, arithmetic and copies ran while one was open for 5% of the time, Pallas kernels for 0%

profile of v2, /device:TPU:1, one launch (start us, length us, event | category | flops | bytes accessed | tf_op | source)
XLA Modules:
  0.0 135.7 jit_solution(14036020078071457162)
XLA Ops:
  7.2 0.7 all-gather.4.cloned.1.call-update
  7.9 0.7 copy.12
  8.6 38.0 %all-gather.1 = bf16[96,1,128]{2,1,0:T(2,128)(2,1)S(1)} all-gather(bf16[3,1,128]{2,1,0:T(2,128)(2,1)S(1)} %copy.12), channel_id=3, replica_groups=mesh['sp'=16,'tp'=32] {'tp'}, dimensions={0}, use_global_device_ids=true | all-gather | bytes 25344 | tf_op jit(solution)/shard_map/all_gather | solution.py:161
  46.6 0.1 reduce
  46.7 2.4 %fusion.7 = f32[3,384]{1,0:T(4,128)S(1)} fusion(bf16[4096,128]{1,0:T(8,128)(2,1)} %param.8, bf16[4096,128]{1,0:T(8,128)(2,1)} %vw_ref.1, bf16[4096,128]{1,0:T(8,128)(2,1)} %kw_ref.1, bf16[32,3,128]{2,1,0:T(4,128)(2,1)S(1)} %reshape.137), kind=kOutput, calls=%fused_computation.7 | convolution fusion | flops 18874368 | bytes 3174912 | tf_op jit(solution)/shard_map/dot_general | solution.py:174
  49.2 0.1 reshape.129
  49.3 0.1 reshape.130
  49.4 0.1 reshape.133
  49.5 0.1 reshape.134
  49.7 0.1 maximum_bitcast_fusion.1
  49.7 0.1 tile.43
  49.9 0.1 maximum_bitcast_fusion
  50.0 0.1 tile.40
  50.1 0.1 reshape.131
  50.1 0.1 copy.13
  50.3 0.3 broadcast_in_dim.19
  50.5 0.2 reshape.132.query_ref
  50.7 0.3 fusion.11
  51.1 0.1 copy.14.cos_ref
  51.3 0.1 copy.15.sin_ref
  51.5 0.1 exp.33.carried_ref
  51.6 0.1 exp.35.one_ref
  51.8 0.1 mul.144
  51.9 0.1 reshape.135
  52.0 0.1 fusion
  52.0 0.1 mul.162
  52.1 0.9 multiply_exponential_fusion.decay_ref
  53.0 49.7 %all-gather.4.cloned.1.call-done = bf16[96,512,128]{2,1,0:T(8,128)(2,1)} async-done(((bf16[3,512,128]{2,1,0:T(8,128)(2,1)}), bf16[96,512,128]{2,1,0:T(8,128)(2,1)}) %all-gather.4.cloned.1.call-update) | async-done | bytes 12582928 | tf_op jit(solution)/shard_map/all_gather | solution.py:160
  102.7 11.6 %span_states.1 = f32[16,15,128]{2,1,0:T(8,128)} custom-call(bf16[32,3,512,128]{3,2,1,0:T(8,128)(2,1)} %bitcast.16, bf16[4096,128]{1,0:T(8,128)(2,1)} %kw_ref.1, bf16[4096,128]{1,0:T(8,128)(2,1)} %vw_ref.1, f32[512,128]{1,0:T(8,128)S(1)} %copy.14.cos_ref, f32[512,128]{1,0:T(8,128)S(1)} %copy.15.sin_ref, f32[512,128]{1,0:T(8,128)} %multiply_exponential_fusion.decay_ref, ...), custom_call_target="tpu_custom_call" | custom-call | tf_op jit(solution)/shard_map/span_states/pallas_call | solution.py:81
  114.4 6.8 %all-to-all-start = ((f32[16,15,128]{2,1,0:T(8,128)}), f32[16,15,128]{2,1,0:T(8,128)S(1)}, u32[]{:S(2)}, u32[]{:S(2)}) async-start(f32[16,15,128]{2,1,0:T(8,128)} %span_states.1), calls=%async_computation | async-start | bytes 262144 | tf_op jit(solution)/shard_map/all_to_all | solution.py:199
  121.2 6.8 %all-to-all-done.arrived_ref = f32[16,15,128]{2,1,0:T(8,128)S(1)} async-done(((f32[16,15,128]{2,1,0:T(8,128)}), f32[16,15,128]{2,1,0:T(8,128)S(1)}, u32[]{:S(2)}, u32[]{:S(2)}) %all-to-all-start) | async-done | bytes 122912 | tf_op jit(solution)/shard_map/all_to_all | solution.py:199
  128.0 0.8 finish.1
  (23 shorter events, 0.6 us)
Async XLA Ops:
  7.2 44.2 %copy-start = (f32[2]{0:T(128)S(1)}, f32[2]{0:T(128)}, u32[]{:S(2)}) copy-start(f32[2]{0:T(128)} %param.11) | copy-start | bytes 28
  7.2 95.6 %all-gather.4.cloned.1.call-start = ((), (), s32[]{:S(2)}) async-start(), calls=%async_computation.1 | async-start | bytes 12976128 | tf_op jit(solution)/shard_map/all_gather | solution.py:160
  114.4 13.7 %all-to-all-start = ((f32[16,15,128]{2,1,0:T(8,128)}), f32[16,15,128]{2,1,0:T(8,128)S(1)}, u32[]{:S(2)}, u32[]{:S(2)}) async-start(f32[16,15,128]{2,1,0:T(8,128)} %span_states.1), calls=%async_computation | async-start | bytes 262144 | tf_op jit(solution)/shard_map/all_to_all | solution.py:199
Sparse Core Ops, SparseCore 0:
  10.1 92.5 all-gather.3

commit v3 on v2

v3 whole, which is shorter than its diff:
```python
import jax
import jax.numpy as jnp
from jax import lax
from jax.experimental import pallas as pl
from jax.experimental.pallas import tpu as pltpu
from jax.sharding import PartitionSpec as P

HD = 64
EPS = 1e-05
EXTRA = 16


def swap_halves(values):
    lanes = values.shape[-1]
    lane = lax.broadcasted_iota(jnp.int32, values.shape, len(values.shape) - 1)
    quarter = HD // 2
    back = pltpu.roll(values, lanes - quarter, len(values.shape) - 1)
    ahead = pltpu.roll(values, quarter, len(values.shape) - 1)
    return jnp.where(lane % HD < quarter, back, ahead)


def state_kernel(
    total_ref,
    arrived_ref,
    query_ref,
    last_a_ref,
    last_b_ref,
    weight_ref,
    query_weight_ref,
    cos_ref,
    sin_ref,
    decay_ref,
    carried_ref,
    one_ref,
    new_cos_ref,
    new_sin_ref,
    out_ref,
    own_ref,
):
    span_len, inner = decay_ref.shape
    rows = last_a_ref.shape[0] - EXTRA
    prompts = rows // span_len
    groups = out_ref.shape[0]
    keep = HD // groups
    key_scale = HD ** (-0.5)
    lane = lax.broadcasted_iota(jnp.int32, (HD, inner), 1)

    def projected(start, count):
        at = pl.ds(start, count)
        last = jnp.concatenate([last_a_ref[at, :], last_b_ref[at, :]], axis=1)
        part = jnp.dot(last, weight_ref[...], preferred_element_type=jnp.float32)
        return total_ref[at, :] + arrived_ref[at, :] + part

    fresh = projected(rows, EXTRA)
    last = jnp.concatenate([last_a_ref[rows:, :], last_b_ref[rows:, :]], axis=1)
    query = query_ref[...] + arrived_ref[rows + EXTRA :, :inner]
    query += jnp.dot(last, query_weight_ref[...], preferred_element_type=jnp.float32)
    query = query * new_cos_ref[...] + swap_halves(query) * new_sin_ref[...]
    query = query.astype(jnp.bfloat16).astype(jnp.float32)
    new_key = fresh[:, :inner]
    new_key = (new_key * new_cos_ref[...] + swap_halves(new_key) * new_sin_ref[...]) * key_scale
    new_key = new_key.astype(jnp.bfloat16).astype(jnp.float32)
    new_value = fresh[:, inner:].astype(jnp.bfloat16).astype(jnp.float32)
    products = query * new_key
    new_lane = lax.broadcasted_iota(jnp.int32, products.shape, 1)
    score = jnp.zeros_like(products)
    for h in range(inner // HD):
        here = new_lane // HD == h
        score = jnp.where(
            here, jnp.sum(jnp.where(here, products, 0.0), axis=1, keepdims=True), score
        )
    own_ref[...] = score * new_value
    columns = jnp.transpose(query)

    for s in range(prompts):
        total = projected(s * span_len, span_len)
        keys = total[:, :inner]
        values = total[:, inner:].astype(jnp.bfloat16)
        keys = (keys * cos_ref[...] + swap_halves(keys) * sin_ref[...]).astype(jnp.bfloat16)
        weighted = (keys.astype(jnp.float32) * decay_ref[...]).astype(jnp.bfloat16)
        full = lax.dot_general(
            weighted, values, (((0,), (0,)), ((), ())), preferred_element_type=jnp.float32
        )
        state = jnp.where(lane < HD, full[:HD], full[HD:]) * carried_ref[...]
        entries = jnp.where(lane < HD, columns[:HD, s : s + 1], columns[HD:, s : s + 1])
        read = jnp.sum(state * entries, axis=0, keepdims=True) * one_ref[...]
        for g in range(groups):
            out_ref[g, s * keep : (s + 1) * keep, :] = state[g * keep : (g + 1) * keep]
            out_ref[g, prompts * keep + s : prompts * keep + s + 1, :] = read


def span_states(prompts, groups, decay, *operands):
    inner = decay.shape[1]
    keep = HD // groups
    whole = pl.BlockSpec(memory_space=pltpu.VMEM)
    return pl.pallas_call(
        state_kernel,
        in_specs=[whole] * len(operands),
        out_specs=[whole, whole],
        out_shape=[
            jax.ShapeDtypeStruct((groups, prompts * (keep + 1), inner), jnp.float32),
            jax.ShapeDtypeStruct((EXTRA, inner), jnp.float32),
        ],
        compiler_params=pltpu.CompilerParams(vmem_limit_bytes=24 * 1024 * 1024),
        name="span_states",
    )(*operands)


def finish_kernel(arrived_ref, own_ref, state_ref, read_ref):
    total = jnp.sum(arrived_ref[...], axis=0)
    prompts, heads, keep, _ = state_ref.shape
    for s in range(prompts):
        for h in range(heads):
            state_ref[s, h] = total[s * keep : (s + 1) * keep, h * HD : (h + 1) * HD].astype(
                jnp.bfloat16
            )
    raw = total[prompts * keep :] + own_ref[:prompts, :]
    lane = lax.broadcasted_iota(jnp.int32, raw.shape, 1)

    def per_head(values):
        result = jnp.zeros_like(values)
        for h in range(heads):
            here = lane // HD == h
            mean = jnp.sum(jnp.where(here, values, 0.0), axis=1, keepdims=True) / HD
            result = jnp.where(here, mean, result)
        return result

    centered = raw - per_head(raw)
    spread = per_head(centered * centered)
    read_ref[...] = (centered * lax.rsqrt(spread + EPS)).astype(jnp.bfloat16)


def finish(arrived, own_term, prompts, heads, keep):
    inner = own_term.shape[1]
    whole = pl.BlockSpec(memory_space=pltpu.VMEM)
    return pl.pallas_call(
        finish_kernel,
        in_specs=[whole, whole],
        out_specs=[whole, whole],
        out_shape=[
            jax.ShapeDtypeStruct((prompts, heads, keep, HD), jnp.bfloat16),
            jax.ShapeDtypeStruct((prompts, inner), jnp.bfloat16),
        ],
        compiler_params=pltpu.CompilerParams(vmem_limit_bytes=4 * 1024 * 1024),
        name="finish",
    )(arrived, own_term)


def angles_at(positions, heads):
    half_dim = HD // 2
    inverse = 10000.0 ** (-jnp.arange(half_dim, dtype=jnp.float32) / half_dim)
    angles = positions.astype(jnp.float32)[:, None] * inverse[None, :]
    cosine = jnp.cos(angles)
    sine = jnp.sin(angles)
    cosine = jnp.tile(jnp.concatenate([cosine, cosine], axis=1), (1, heads))
    sine = jnp.tile(jnp.concatenate([-sine, sine], axis=1), (1, heads))
    return cosine, sine


def body(tokens, new_token, query_weight, key_weight, value_weight, log_decay):
    prompts, span_len, width = tokens.shape
    heads = log_decay.shape[0]
    inner = heads * HD
    groups = lax.axis_size("sp")
    own_index = lax.axis_index("sp")
    tp_index = lax.axis_index("tp")
    planes = lax.axis_size("tp") // 2
    plane = tp_index // 2
    core = tp_index % 2
    toward = 1 - 2 * core
    rows = prompts * span_len
    key_scale = HD ** (-0.5)

    partner = [(i, i ^ 1) for i in range(2 * planes)]
    onward = [
        (2 * z + c, 2 * ((z + (1 if c == 0 else -1)) % planes) + c)
        for z in range(planes)
        for c in range(2)
    ]

    fresh = jnp.concatenate(
        [new_token[:, 0], jnp.zeros((EXTRA - prompts, width), new_token.dtype)], axis=0
    )
    chain_a = jnp.concatenate([tokens.reshape(rows, width), fresh], axis=0)
    chain_b = lax.ppermute(chain_a, "tp", partner)

    def other(weights):
        return lax.ppermute(weights, "tp", partner)

    main_weights = jnp.concatenate([key_weight, value_weight], axis=1)
    all_weights = jnp.concatenate(
        [main_weights, other(key_weight), other(value_weight)], axis=1
    ).reshape(2 * planes, width, 4 * inner)
    main_weights = main_weights.reshape(2 * planes, width, 2 * inner)
    own_query = query_weight.reshape(2 * planes, width, inner)
    all_query = jnp.concatenate([query_weight, other(query_weight)], axis=1)
    all_query = all_query.reshape(2 * planes, width, 2 * inner)

    def places(offset):
        at = (plane - offset * toward) % planes
        return 2 * at + core, 2 * at + 1 - core

    def block(weights, at):
        return lax.dynamic_index_in_dim(weights, at, 0, keepdims=False)

    def project(a, b, offset, weights, queries):
        at_a, at_b = places(offset)
        main = jnp.dot(a, block(weights, at_a), preferred_element_type=jnp.float32)
        main = main + jnp.dot(b, block(weights, at_b), preferred_element_type=jnp.float32)
        query = jnp.dot(a[rows:], block(queries, at_a), preferred_element_type=jnp.float32)
        query = query + jnp.dot(b[rows:], block(queries, at_b), preferred_element_type=jnp.float32)
        return main, query

    own_main, own_query_rows = project(chain_a, chain_b, 0, main_weights, own_query)
    reach = planes // 2
    main = query = None
    for step in range(1, reach):
        chain_a = lax.ppermute(chain_a, "tp", onward)
        chain_b = lax.ppermute(chain_b, "tp", onward)
        more, more_query = project(chain_a, chain_b, step, all_weights, all_query)
        main = more if main is None else main + more
        query = more_query if query is None else query + more_query
        main, query = lax.optimization_barrier((main, query))
    last_a = lax.ppermute(chain_a, "tp", onward)
    last_b = lax.ppermute(chain_b, "tp", onward)

    outgoing = jnp.concatenate(
        [main[:, 2 * inner :], jnp.concatenate([query[:, inner:]] * 2, axis=1)], axis=0
    )
    arrived = lax.ppermute(outgoing, "tp", partner)
    own_main = own_main + main[:, : 2 * inner]
    own_query_rows = own_query_rows + query[:, :inner]
    at_a, at_b = places(reach)
    last_weights = jnp.concatenate([block(main_weights, at_a), block(main_weights, at_b)], axis=0)
    last_query = jnp.concatenate([block(own_query, at_a), block(own_query, at_b)], axis=0)

    local = jnp.arange(span_len, dtype=jnp.int32)
    cosine, sine = angles_at(own_index * span_len + local, heads)
    to_end = (span_len - 1 - local).astype(jnp.float32)
    lane_decay = jnp.repeat(log_decay, HD)
    decay_rows = jnp.exp(to_end[:, None] * lane_decay[None, :])
    distance = (span_len * (groups - 1 - own_index)).astype(jnp.float32)
    carried = jnp.exp(lane_decay * distance)[None, :]
    one = jnp.exp(lane_decay)[None, :]
    new_cosine, new_sine = angles_at(jnp.full((1,), groups * span_len, jnp.int32), heads)

    messages, own_term = span_states(
        prompts,
        groups,
        decay_rows,
        own_main,
        arrived,
        own_query_rows,
        last_a,
        last_b,
        last_weights,
        last_query,
        cosine * key_scale,
        sine * key_scale,
        decay_rows,
        carried,
        one,
        new_cosine,
        new_sine,
    )
    arrived = lax.all_to_all(messages, "sp", split_axis=0, concat_axis=0, tiled=True)
    return tuple(finish(arrived, own_term, prompts, heads, HD // groups))


def solution(mesh):
    return jax.shard_map(
        body,
        mesh=mesh,
        in_specs=(
            P(None, "sp", "tp"),
            P(None, None, "tp"),
            P(None, "tp"),
            P(None, "tp"),
            P(None, "tp"),
            P("tp"),
        ),
        out_specs=(P(None, "tp", "sp", None), P(None, "tp")),
        check_vma=False,
    )
```

time: 136 us -> 141 us (1.037); the launches traced: 136 us -> 139 us
  starting transfers between devices: 6.85 us -> 79.8 us
  waiting for transfers between devices: 57.2 us -> 18.7 us
  blocking collectives: 38 us -> 13.4 us
  between operations: 14.2 us -> 1.47 us
  matrix products: 2.44 us -> 15.1 us
  Pallas kernels: 12.4 us -> 2.12 us
  other arithmetic: 1.71 us -> 4.35 us
    ppermute x0 -> x21, starting transfers between devices: none -> 79.8 us  [the longest x7 31.8 us: body(): chain_a = lax.ppermute(chain_a, 'tp', onward)]
    all_gather x1 -> x0, waiting for transfers between devices: 49.7 us -> none  [body(): gathered = lax.all_gather(tokens, 'tp', axis=0, tiled=False)]
    all_gather x1 -> x0, blocking collectives: 38 us -> none  [body(): fresh = lax.all_gather(new_token[:, 0], 'tp', axis=0, tiled=False)]
    ppermute x0 -> x21, waiting for transfers between devices: none -> 18.7 us  [the longest x7 9.55 us: body(): chain_b = lax.ppermute(chain_b, 'tp', onward)]
    all_to_all x0 -> x1, blocking collectives: none -> 13.4 us  [body(): lax.all_to_all(messages, 'sp', split_axis=0, concat_axis=0, tiled=True)]
    dot_general x1 -> x32, matrix products: 2.44 us -> 15.1 us  [the longest x8 5.43 us: project(): jnp.dot(b, block(weights, at_b), preferred_element_type=jnp.float32)]
    pallas_call x1, Pallas kernels: 11.6 us -> 1.35 us  [span_states(): pl.pallas_call(state_kernel, in_specs=[whole] * len(operands), out_specs=...]
    all_to_all x1 -> x0, waiting for transfers between devices: 6.83 us -> none  [body(): lax.all_to_all(messages, 'sp', split_axis=0, concat_axis=0, tiled=True)]
  transfers between devices with their start and end apart: 2 -> 21, of which waited for: 2 -> 10; matrix products, arithmetic and copies ran while one was open for 5% -> 14% of each run, Pallas kernels for 0% -> 0%
where the time goes in v3:
time: 141 us; the launch traced here: 139 us
  starting transfers between devices  79.8 us (57%)
  waiting for transfers between devices  18.7 us (13%)
  matrix products  15.1 us (11%)
  blocking collectives  13.4 us (10%)
  other arithmetic  4.35 us (3%)
  local copies, waits for them, and re-layouts  3.96 us (3%)
  Pallas kernels  2.12 us (2%)
  between operations  1.47 us (1%)
    ppermute x7, starting transfers between devices, body(): chain_a = lax.ppermute(chain_a, 'tp', onward)  31.8 us
    ppermute x7, starting transfers between devices, body(): chain_b = lax.ppermute(chain_b, 'tp', onward)  24.5 us
    all_to_all x1, blocking collectives, body(): lax.all_to_all(messages, 'sp', split_axis=0, concat_axis=0, tiled=True)  13.4 us
    ppermute x1, starting transfers between devices, body(): arrived = lax.ppermute(outgoing, 'tp', partner)  11 us
    ppermute x7, waiting for transfers between devices, body(): chain_b = lax.ppermute(chain_b, 'tp', onward)  9.55 us
    ppermute x3, starting transfers between devices, other(): return lax.ppermute(weights, 'tp', partner)  6.74 us
    dot_general x8, matrix products, project(): jnp.dot(b, block(weights, at_b), preferred_element_type=jnp.float32)  5.43 us
    dot_general x8, matrix products, project(): main = jnp.dot(a, block(weights, at_a), preferred_element_type=jnp.float32)  5.29 us
  transfers between devices with their start and end apart: 21, of which 10 were waited for; matrix products, arithmetic and copies ran while one was open for 14% of the time, Pallas kernels for 0%

profile of v3, /device:TPU:1, one launch (start us, length us, event | category | flops | bytes accessed | tf_op | source)
XLA Modules:
  0.0 138.9 jit_solution(18392806428477516370)
XLA Ops:
  0.7 2.8 %concatenate.41 = bf16[1552,128]{1,0:T(8,128)(2,1)S(1)} concatenate(bf16[1536,128]{1,0:T(8,128)(2,1)} %bitcast.172, bf16[3,128]{1,0:T(4,128)(2,1)} %bitcast.173, bf16[13,128]{1,0:T(8,128)(2,1)S(1)} %broadcast_in_dim.16), dimensions={0} | concatenate | bytes 794624 | tf_op jit(solution)/shard_map/concatenate | solution.py:184
  3.5 11.9 %collective-permute-start.1 = (bf16[1552,128]{1,0:T(8,128)(2,1)S(1)}, bf16[1552,128]{1,0:T(8,128)(2,1)}, u32[]{:S(2)}, u32[]{:S(2)}) collective-permute-start(bf16[1552,128]{1,0:T(8,128)(2,1)S(1)} %concatenate.41), channel_id=1, source_target_pairs={{0,2},{1,31},{2,4},{3,1},{4,6},{5,3},{6,8},{7,5},{8,10},{9,7},{10,... | collective-permute-start | bytes 1191944 | tf_op jit(solution)/shard_map/ppermute | solution.py:218
  15.4 1.9 %collective-permute-start = (bf16[1552,128]{1,0:T(8,128)(2,1)S(1)}, bf16[1552,128]{1,0:T(8,128)(2,1)}, u32[]{:S(2)}, u32[]{:S(2)}) collective-permute-start(bf16[1552,128]{1,0:T(8,128)(2,1)S(1)} %concatenate.41), channel_id=1, source_target_pairs={{0,1},{1,0},{2,3},{3,2},{4,5},{5,4},{6,7},{7,6},{8,9},{9,8},{10,11... | collective-permute-start | bytes 1191944 | tf_op jit(solution)/shard_map/ppermute | solution.py:185
  17.4 2.4 %collective-permute-start.5 = (bf16[4096,128]{1,0:T(8,128)(2,1)}, bf16[4096,128]{1,0:T(8,128)(2,1)}, u32[]{:S(2)}, u32[]{:S(2)}) collective-permute-start(bf16[4096,128]{1,0:T(8,128)(2,1)} %param.8), channel_id=1, source_target_pairs={{0,1},{1,0},{2,3},{3,2},{4,5},{5,4},{6,7},{7,6},{8,9},{9,8},{10,11... | collective-permute-start | bytes 3145736 | tf_op jit(solution)/shard_map/ppermute | solution.py:188
  19.8 1.9 %collective-permute-start.2 = (bf16[4096,128]{1,0:T(8,128)(2,1)}, bf16[4096,128]{1,0:T(8,128)(2,1)}, u32[]{:S(2)}, u32[]{:S(2)}) collective-permute-start(bf16[4096,128]{1,0:T(8,128)(2,1)} %param.9), channel_id=1, source_target_pairs={{0,1},{1,0},{2,3},{3,2},{4,5},{5,4},{6,7},{7,6},{8,9},{9,8},{10,11... | collective-permute-start | bytes 3145736 | tf_op jit(solution)/shard_map/ppermute | solution.py:188
  21.7 2.4 %collective-permute-start.3 = (bf16[4096,128]{1,0:T(8,128)(2,1)}, bf16[4096,128]{1,0:T(8,128)(2,1)}, u32[]{:S(2)}, u32[]{:S(2)}) collective-permute-start(bf16[4096,128]{1,0:T(8,128)(2,1)} %param.10), channel_id=1, source_target_pairs={{0,1},{1,0},{2,3},{3,2},{4,5},{5,4},{6,7},{7,6},{8,9},{9,8},{10,11... | collective-permute-start | bytes 3145736 | tf_op jit(solution)/shard_map/ppermute | solution.py:188
  27.0 2.6 %collective-permute-start.4 = (bf16[1552,128]{1,0:T(8,128)(2,1)}, bf16[1552,128]{1,0:T(8,128)(2,1)S(1)}, u32[]{:S(2)}, u32[]{:S(2)}) collective-permute-start(bf16[1552,128]{1,0:T(8,128)(2,1)} %collective-permute-done), channel_id=1, source_target_pairs={{0,2},{1,31},{2,4},{3,1},{4,6},{5,3},{6,8},{7,5},{8,10},{9,7},{10,... | collective-permute-start | bytes 1191944 | tf_op jit(solution)/shard_map/ppermute | solution.py:219
  29.7 3.1 %collective-permute-start.6 = (bf16[1552,128]{1,0:T(8,128)(2,1)}, bf16[1552,128]{1,0:T(8,128)(2,1)S(1)}, u32[]{:S(2)}, u32[]{:S(2)}) collective-permute-start(bf16[1552,128]{1,0:T(8,128)(2,1)} %collective-permute-done.1), channel_id=1, source_target_pairs={{0,2},{1,31},{2,4},{3,1},{4,6},{5,3},{6,8},{7,5},{8,10},{9,7},{10,... | collective-permute-start | bytes 1191944 | tf_op jit(solution)/shard_map/ppermute | solution.py:218
  33.0 3.0 %collective-permute-done.4 = bf16[1552,128]{1,0:T(8,128)(2,1)S(1)} collective-permute-done((bf16[1552,128]{1,0:T(8,128)(2,1)}, bf16[1552,128]{1,0:T(8,128)(2,1)S(1)}, u32[]{:S(2)}, u32[]{:S(2)}) %collective-permute-start.4) | collective-permute-done | bytes 397344 | tf_op jit(solution)/shard_map/ppermute | solution.py:219
  36.1 3.5 %collective-permute-start.7 = (bf16[1552,128]{1,0:T(8,128)(2,1)S(1)}, bf16[1552,128]{1,0:T(8,128)(2,1)S(1)}, u32[]{:S(2)}, u32[]{:S(2)}) collective-permute-start(bf16[1552,128]{1,0:T(8,128)(2,1)S(1)} %collective-permute-done.4), channel_id=1, source_target_pairs={{0,2},{1,31},{2,4},{3,1},{4,6},{5,3},{6,8},{7,5},{8,10},{9,7},{10,... | collective-permute-start | bytes 1191944 | tf_op jit(solution)/shard_map/ppermute | solution.py:219
  40.3 3.5 %collective-permute-start.8 = (bf16[1552,128]{1,0:T(8,128)(2,1)S(1)}, bf16[1552,128]{1,0:T(8,128)(2,1)S(1)}, u32[]{:S(2)}, u32[]{:S(2)}) collective-permute-start(bf16[1552,128]{1,0:T(8,128)(2,1)S(1)} %collective-permute-done.6), channel_id=1, source_target_pairs={{0,2},{1,31},{2,4},{3,1},{4,6},{5,3},{6,8},{7,5},{8,10},{9,7},{10,... | collective-permute-start | bytes 1191944 | tf_op jit(solution)/shard_map/ppermute | solution.py:218
  43.9 1.5 %pad_maximum_fusion.2 = bf16[4096,256]{1,0:T(8,128)(2,1)S(1)} fusion(bf16[4096,128]{1,0:T(8,128)(2,1)} %collective-permute-done.5, bf16[4096,128]{1,0:T(8,128)(2,1)S(1)} %copy-done.2), kind=kLoop, calls=%fused_computation.16 | loop fusion | flops 4194304 | bytes 4194304 | tf_op jit(solution)/shard_map/concatenate | solution.py:196
  46.2 1.8 %pad_maximum_fusion = bf16[4096,512]{1,0:T(8,128)(2,1)S(1)} fusion(bf16[4096,128]{1,0:T(8,128)(2,1)} %collective-permute-done.3, bf16[4096,128]{1,0:T(8,128)(2,1)} %collective-permute-done.2, bf16[4096,128]{1,0:T(8,128)(2,1)S(1)} %copy-done, bf16[4096,128]{1,0:T(8,128)(2,1)S(1)} %copy-done.1), kind=kLoop, calls=%fused_computation | loop fusion | flops 16777216 | bytes 8388608 | tf_op jit(solution)/shard_map/concatenate | solution.py:191
  48.0 1.6 %fusion.31 = f32[1552,512]{1,0:T(8,128)S(1)} fusion(bf16[1552,128]{1,0:T(8,128)(2,1)} %collective-permute-done.1, bf16[32,128,512]{2,1,0:T(8,128)(2,1)S(1)} %bitcast.136, s32[]{:T(128)S(6)} %select_n.128), kind=kOutput, calls=%fused_computation.56 | convolution fusion | flops 203423744 | bytes 3706884 | tf_op jit(solution)/shard_map/dot_general | solution.py:208
  50.9 2.2 %collective-permute-start.9 = (bf16[1552,128]{1,0:T(8,128)(2,1)S(1)}, bf16[1552,128]{1,0:T(8,128)(2,1)S(1)}, u32[]{:S(2)}, u32[]{:S(2)}) collective-permute-start(bf16[1552,128]{1,0:T(8,128)(2,1)S(1)} %collective-permute-done.7), channel_id=1, source_target_pairs={{0,2},{1,31},{2,4},{3,1},{4,6},{5,3},{6,8},{7,5},{8,10},{9,7},{10,... | collective-permute-start | bytes 1191944 | tf_op jit(solution)/shard_map/ppermute | solution.py:219
  53.1 2.6 %collective-permute-start.10 = (bf16[1552,128]{1,0:T(8,128)(2,1)S(1)}, bf16[1552,128]{1,0:T(8,128)(2,1)S(1)}, u32[]{:S(2)}, u32[]{:S(2)}) collective-permute-start(bf16[1552,128]{1,0:T(8,128)(2,1)S(1)} %collective-permute-done.8), channel_id=1, source_target_pairs={{0,2},{1,31},{2,4},{3,1},{4,6},{5,3},{6,8},{7,5},{8,10},{9,7},{10,... | collective-permute-start | bytes 1191944 | tf_op jit(solution)/shard_map/ppermute | solution.py:218
  57.2 2.6 %collective-permute-done.9 = bf16[1552,128]{1,0:T(8,128)(2,1)S(1)} collective-permute-done((bf16[1552,128]{1,0:T(8,128)(2,1)S(1)}, bf16[1552,128]{1,0:T(8,128)(2,1)S(1)}, u32[]{:S(2)}, u32[]{:S(2)}) %collective-permute-start.9) | collective-permute-done | bytes 397344 | tf_op jit(solution)/shard_map/ppermute | solution.py:219
  59.8 3.1 %collective-permute-start.11 = (bf16[1552,128]{1,0:T(8,128)(2,1)S(1)}, bf16[1552,128]{1,0:T(8,128)(2,1)S(1)}, u32[]{:S(2)}, u32[]{:S(2)}) collective-permute-start(bf16[1552,128]{1,0:T(8,128)(2,1)S(1)} %collective-permute-done.9), channel_id=1, source_target_pairs={{0,2},{1,31},{2,4},{3,1},{4,6},{5,3},{6,8},{7,5},{8,10},{9,7},{10,... | collective-permute-start | bytes 1191944 | tf_op jit(solution)/shard_map/ppermute | solution.py:219
  64.1 3.1 %collective-permute-start.12 = (bf16[1552,128]{1,0:T(8,128)(2,1)S(1)}, bf16[1552,128]{1,0:T(8,128)(2,1)S(1)}, u32[]{:S(2)}, u32[]{:S(2)}) collective-permute-start(bf16[1552,128]{1,0:T(8,128)(2,1)S(1)} %collective-permute-done.10), channel_id=1, source_target_pairs={{0,2},{1,31},{2,4},{3,1},{4,6},{5,3},{6,8},{7,5},{8,10},{9,7},{10,... | collective-permute-start | bytes 1191944 | tf_op jit(solution)/shard_map/ppermute | solution.py:218
  68.7 4.0 %collective-permute-start.13 = (bf16[1552,128]{1,0:T(8,128)(2,1)S(1)}, bf16[1552,128]{1,0:T(8,128)(2,1)S(1)}, u32[]{:S(2)}, u32[]{:S(2)}) collective-permute-start(bf16[1552,128]{1,0:T(8,128)(2,1)S(1)} %collective-permute-done.11), channel_id=1, source_target_pairs={{0,2},{1,31},{2,4},{3,1},{4,6},{5,3},{6,8},{7,5},{8,10},{9,7},{10,... | collective-permute-start | bytes 1191944 | tf_op jit(solution)/shard_map/ppermute | solution.py:219
  72.9 4.0 %collective-permute-start.14 = (bf16[1552,128]{1,0:T(8,128)(2,1)S(1)}, bf16[1552,128]{1,0:T(8,128)(2,1)S(1)}, u32[]{:S(2)}, u32[]{:S(2)}) collective-permute-start(bf16[1552,128]{1,0:T(8,128)(2,1)S(1)} %collective-permute-done.12), channel_id=1, source_target_pairs={{0,2},{1,31},{2,4},{3,1},{4,6},{5,3},{6,8},{7,5},{8,10},{9,7},{10,... | collective-permute-start | bytes 1191944 | tf_op jit(solution)/shard_map/ppermute | solution.py:218
  79.1 4.1 %collective-permute-start.15 = (bf16[1552,128]{1,0:T(8,128)(2,1)S(1)}, bf16[1552,128]{1,0:T(8,128)(2,1)S(1)}, u32[]{:S(2)}, u32[]{:S(2)}) collective-permute-start(bf16[1552,128]{1,0:T(8,128)(2,1)S(1)} %collective-permute-done.13), channel_id=1, source_target_pairs={{0,2},{1,31},{2,4},{3,1},{4,6},{5,3},{6,8},{7,5},{8,10},{9,7},{10,... | collective-permute-start | bytes 1191944 | tf_op jit(solution)/shard_map/ppermute | solution.py:219
  83.2 3.5 %collective-permute-start.16 = (bf16[1552,128]{1,0:T(8,128)(2,1)S(1)}, bf16[1552,128]{1,0:T(8,128)(2,1)S(1)}, u32[]{:S(2)}, u32[]{:S(2)}) collective-permute-start(bf16[1552,128]{1,0:T(8,128)(2,1)S(1)} %collective-permute-done.14), channel_id=1, source_target_pairs={{0,2},{1,31},{2,4},{3,1},{4,6},{5,3},{6,8},{7,5},{8,10},{9,7},{10,... | collective-permute-start | bytes 1191944 | tf_op jit(solution)/shard_map/ppermute | solution.py:218
  87.9 5.0 %collective-permute-start.17 = (bf16[1552,128]{1,0:T(8,128)(2,1)S(1)}, bf16[1552,128]{1,0:T(8,128)(2,1)S(1)}, u32[]{:S(2)}, u32[]{:S(2)}) collective-permute-start(bf16[1552,128]{1,0:T(8,128)(2,1)S(1)} %collective-permute-done.15), channel_id=1, source_target_pairs={{0,2},{1,31},{2,4},{3,1},{4,6},{5,3},{6,8},{7,5},{8,10},{9,7},{10,... | collective-permute-start | bytes 1191944 | tf_op jit(solution)/shard_map/ppermute | solution.py:219
  94.4 3.3 %collective-permute-done.17 = bf16[1552,128]{1,0:T(8,128)(2,1)S(1)} collective-permute-done((bf16[1552,128]{1,0:T(8,128)(2,1)S(1)}, bf16[1552,128]{1,0:T(8,128)(2,1)S(1)}, u32[]{:S(2)}, u32[]{:S(2)}) %collective-permute-start.17) | collective-permute-done | bytes 397344 | tf_op jit(solution)/shard_map/ppermute | solution.py:219
  98.7 11.0 %collective-permute-start.18 = (f32[1568,256]{1,0:T(8,128)S(1)}, f32[1568,256]{1,0:T(8,128)S(1)}, u32[]{:S(2)}, u32[]{:S(2)}) collective-permute-start(f32[1568,256]{1,0:T(8,128)S(1)} %maximum_maximum_fusion), channel_id=1, source_target_pairs={{0,1},{1,0},{2,3},{3,2},{4,5},{5,4},{6,7},{7,6},{8,9},{9,8},{10,11... | collective-permute-start | bytes 4816904 | tf_op jit(solution)/shard_map/ppermute | solution.py:230
  110.2 1.9 %collective-permute-start.19 = (bf16[1552,128]{1,0:T(8,128)(2,1)S(1)}, bf16[1552,128]{1,0:T(8,128)(2,1)S(1)}, u32[]{:S(2)}, u32[]{:S(2)}) collective-permute-start(bf16[1552,128]{1,0:T(8,128)(2,1)S(1)} %collective-permute-done.16), channel_id=1, source_target_pairs={{0,2},{1,31},{2,4},{3,1},{4,6},{5,3},{6,8},{7,5},{8,10},{9,7},{10,... | collective-permute-start | bytes 1191944 | tf_op jit(solution)/shard_map/ppermute | solution.py:224
  112.2 1.9 %collective-permute-start.20 = (bf16[1552,128]{1,0:T(8,128)(2,1)S(1)}, bf16[1552,128]{1,0:T(8,128)(2,1)S(1)}, u32[]{:S(2)}, u32[]{:S(2)}) collective-permute-start(bf16[1552,128]{1,0:T(8,128)(2,1)S(1)} %collective-permute-done.17), channel_id=1, source_target_pairs={{0,2},{1,31},{2,4},{3,1},{4,6},{5,3},{6,8},{7,5},{8,10},{9,7},{10,... | collective-permute-start | bytes 1191944 | tf_op jit(solution)/shard_map/ppermute | solution.py:225
  114.9 1.4 %slice_add_fusion.total_ref = f32[1552,256]{1,0:T(8,128)S(1)} fusion(f32[1552,512]{1,0:T(8,128)S(1)} %fusion.5, f32[1552,256]{1,0:T(8,128)S(1)} %fusion.71, bf16[1552,128]{1,0:T(8,128)(2,1)} %collective-permute-done, bf16[32,128,256]{2,1,0:T(8,128)(2,1)S(1)} %bitcast.166, s32[]{:T(128)S(6)} %select_n.126), kind=kOutput, calls=%fused_computation.18 | convolution fusion | flops 102506496 | bytes 5230596 | tf_op jit(solution)/shard_map/dot_general | solution.py:209
  116.3 2.8 %collective-permute-done.19.last_a_ref = bf16[1552,128]{1,0:T(8,128)(2,1)S(1)} collective-permute-done((bf16[1552,128]{1,0:T(8,128)(2,1)S(1)}, bf16[1552,128]{1,0:T(8,128)(2,1)S(1)}, u32[]{:S(2)}, u32[]{:S(2)}) %collective-permute-start.19) | collective-permute-done | bytes 397344 | tf_op jit(solution)/shard_map/ppermute | solution.py:224
  119.1 4.3 %collective-permute-done.20.last_b_ref = bf16[1552,128]{1,0:T(8,128)(2,1)S(1)} collective-permute-done((bf16[1552,128]{1,0:T(8,128)(2,1)S(1)}, bf16[1552,128]{1,0:T(8,128)(2,1)S(1)}, u32[]{:S(2)}, u32[]{:S(2)}) %collective-permute-start.20) | collective-permute-done | bytes 397344 | tf_op jit(solution)/shard_map/ppermute | solution.py:225
  124.7 13.4 %all_to_all.5.arrived_ref = f32[16,15,128]{2,1,0:T(8,128)S(1)} all-to-all(f32[16,15,128]{2,1,0:T(8,128)S(1)} %get-tuple-element.32), channel_id=1, replica_groups=mesh['sp'=16,'tp'=32] {'sp'}, dimensions={0} | all-to-all | bytes 245760 | tf_op jit(solution)/shard_map/all_to_all | solution.py:266
  (92 shorter events, 19.2 us)
Async XLA Ops:
  0.6 25.4 %copy-start.3 = (bf16[3,1,128]{2,0,1:T(4,128)(2,1)S(1)}, bf16[3,1,128]{2,0,1:T(4,128)(2,1)}, u32[]{:S(2)}) copy-start(bf16[3,1,128]{2,0,1:T(4,128)(2,1)} %param.7) | copy-start | bytes 2308
  0.6 32.1 %copy-start.1 = (bf16[4096,128]{1,0:T(8,128)(2,1)S(1)}, bf16[4096,128]{1,0:T(8,128)(2,1)}, u32[]{:S(2)}) copy-start(bf16[4096,128]{1,0:T(8,128)(2,1)} %param.9) | copy-start | bytes 3145732
  0.7 32.1 %copy-start = (bf16[4096,128]{1,0:T(8,128)(2,1)S(1)}, bf16[4096,128]{1,0:T(8,128)(2,1)}, u32[]{:S(2)}) copy-start(bf16[4096,128]{1,0:T(8,128)(2,1)} %param.10) | copy-start | bytes 3145732
  0.7 24.4 %copy-start.4 = (f32[2]{0:T(128)S(1)}, f32[2]{0:T(128)}, u32[]{:S(2)}) copy-start(f32[2]{0:T(128)} %param.11) | copy-start | bytes 28
  3.5 26.2 %collective-permute-start.1 = (bf16[1552,128]{1,0:T(8,128)(2,1)S(1)}, bf16[1552,128]{1,0:T(8,128)(2,1)}, u32[]{:S(2)}, u32[]{:S(2)}) collective-permute-start(bf16[1552,128]{1,0:T(8,128)(2,1)S(1)} %concatenate.41), channel_id=1, source_target_pairs={{0,2},{1,31},{2,4},{3,1},{4,6},{5,3},{6,8},{7,5},{8,10},{9,7},{10,... | collective-permute-start | bytes 1191944 | tf_op jit(solution)/shard_map/ppermute | solution.py:218
  15.4 11.6 %collective-permute-start = (bf16[1552,128]{1,0:T(8,128)(2,1)S(1)}, bf16[1552,128]{1,0:T(8,128)(2,1)}, u32[]{:S(2)}, u32[]{:S(2)}) collective-permute-start(bf16[1552,128]{1,0:T(8,128)(2,1)S(1)} %concatenate.41), channel_id=1, source_target_pairs={{0,1},{1,0},{2,3},{3,2},{4,5},{5,4},{6,7},{7,6},{8,9},{9,8},{10,11... | collective-permute-start | bytes 1191944 | tf_op jit(solution)/shard_map/ppermute | solution.py:185
  17.4 26.5 %collective-permute-start.5 = (bf16[4096,128]{1,0:T(8,128)(2,1)}, bf16[4096,128]{1,0:T(8,128)(2,1)}, u32[]{:S(2)}, u32[]{:S(2)}) collective-permute-start(bf16[4096,128]{1,0:T(8,128)(2,1)} %param.8), channel_id=1, source_target_pairs={{0,1},{1,0},{2,3},{3,2},{4,5},{5,4},{6,7},{7,6},{8,9},{9,8},{10,11... | collective-permute-start | bytes 3145736 | tf_op jit(solution)/shard_map/ppermute | solution.py:188
  19.8 26.4 %collective-permute-start.2 = (bf16[4096,128]{1,0:T(8,128)(2,1)}, bf16[4096,128]{1,0:T(8,128)(2,1)}, u32[]{:S(2)}, u32[]{:S(2)}) collective-permute-start(bf16[4096,128]{1,0:T(8,128)(2,1)} %param.9), channel_id=1, source_target_pairs={{0,1},{1,0},{2,3},{3,2},{4,5},{5,4},{6,7},{7,6},{8,9},{9,8},{10,11... | collective-permute-start | bytes 3145736 | tf_op jit(solution)/shard_map/ppermute | solution.py:188
  21.7 24.5 %collective-permute-start.3 = (bf16[4096,128]{1,0:T(8,128)(2,1)}, bf16[4096,128]{1,0:T(8,128)(2,1)}, u32[]{:S(2)}, u32[]{:S(2)}) collective-permute-start(bf16[4096,128]{1,0:T(8,128)(2,1)} %param.10), channel_id=1, source_target_pairs={{0,1},{1,0},{2,3},{3,2},{4,5},{5,4},{6,7},{7,6},{8,9},{9,8},{10,11... | collective-permute-start | bytes 3145736 | tf_op jit(solution)/shard_map/ppermute | solution.py:188
  26.0 17.9 %copy-start.2 = (bf16[4096,128]{1,0:T(8,128)(2,1)S(1)}, bf16[4096,128]{1,0:T(8,128)(2,1)}, u32[]{:S(2)}) copy-start(bf16[4096,128]{1,0:T(8,128)(2,1)} %param.8) | copy-start | bytes 3145732
  27.0 9.1 %collective-permute-start.4 = (bf16[1552,128]{1,0:T(8,128)(2,1)}, bf16[1552,128]{1,0:T(8,128)(2,1)S(1)}, u32[]{:S(2)}, u32[]{:S(2)}) collective-permute-start(bf16[1552,128]{1,0:T(8,128)(2,1)} %collective-permute-done), channel_id=1, source_target_pairs={{0,2},{1,31},{2,4},{3,1},{4,6},{5,3},{6,8},{7,5},{8,10},{9,7},{10,... | collective-permute-start | bytes 1191944 | tf_op jit(solution)/shard_map/ppermute | solution.py:219
  29.7 10.7 %collective-permute-start.6 = (bf16[1552,128]{1,0:T(8,128)(2,1)}, bf16[1552,128]{1,0:T(8,128)(2,1)S(1)}, u32[]{:S(2)}, u32[]{:S(2)}) collective-permute-start(bf16[1552,128]{1,0:T(8,128)(2,1)} %collective-permute-done.1), channel_id=1, source_target_pairs={{0,2},{1,31},{2,4},{3,1},{4,6},{5,3},{6,8},{7,5},{8,10},{9,7},{10,... | collective-permute-start | bytes 1191944 | tf_op jit(solution)/shard_map/ppermute | solution.py:218
  36.1 14.9 %collective-permute-start.7 = (bf16[1552,128]{1,0:T(8,128)(2,1)S(1)}, bf16[1552,128]{1,0:T(8,128)(2,1)S(1)}, u32[]{:S(2)}, u32[]{:S(2)}) collective-permute-start(bf16[1552,128]{1,0:T(8,128)(2,1)S(1)} %collective-permute-done.4), channel_id=1, source_target_pairs={{0,2},{1,31},{2,4},{3,1},{4,6},{5,3},{6,8},{7,5},{8,10},{9,7},{10,... | collective-permute-start | bytes 1191944 | tf_op jit(solution)/shard_map/ppermute | solution.py:219
  40.3 12.8 %collective-permute-start.8 = (bf16[1552,128]{1,0:T(8,128)(2,1)S(1)}, bf16[1552,128]{1,0:T(8,128)(2,1)S(1)}, u32[]{:S(2)}, u32[]{:S(2)}) collective-permute-start(bf16[1552,128]{1,0:T(8,128)(2,1)S(1)} %collective-permute-done.6), channel_id=1, source_target_pairs={{0,2},{1,31},{2,4},{3,1},{4,6},{5,3},{6,8},{7,5},{8,10},{9,7},{10,... | collective-permute-start | bytes 1191944 | tf_op jit(solution)/shard_map/ppermute | solution.py:218
  50.9 8.9 %collective-permute-start.9 = (bf16[1552,128]{1,0:T(8,128)(2,1)S(1)}, bf16[1552,128]{1,0:T(8,128)(2,1)S(1)}, u32[]{:S(2)}, u32[]{:S(2)}) collective-permute-start(bf16[1552,128]{1,0:T(8,128)(2,1)S(1)} %collective-permute-done.7), channel_id=1, source_target_pairs={{0,2},{1,31},{2,4},{3,1},{4,6},{5,3},{6,8},{7,5},{8,10},{9,7},{10,... | collective-permute-start | bytes 1191944 | tf_op jit(solution)/shard_map/ppermute | solution.py:219
  53.1 10.9 %collective-permute-start.10 = (bf16[1552,128]{1,0:T(8,128)(2,1)S(1)}, bf16[1552,128]{1,0:T(8,128)(2,1)S(1)}, u32[]{:S(2)}, u32[]{:S(2)}) collective-permute-start(bf16[1552,128]{1,0:T(8,128)(2,1)S(1)} %collective-permute-done.8), channel_id=1, source_target_pairs={{0,2},{1,31},{2,4},{3,1},{4,6},{5,3},{6,8},{7,5},{8,10},{9,7},{10,... | collective-permute-start | bytes 1191944 | tf_op jit(solution)/shard_map/ppermute | solution.py:218
  59.8 8.8 %collective-permute-start.11 = (bf16[1552,128]{1,0:T(8,128)(2,1)S(1)}, bf16[1552,128]{1,0:T(8,128)(2,1)S(1)}, u32[]{:S(2)}, u32[]{:S(2)}) collective-permute-start(bf16[1552,128]{1,0:T(8,128)(2,1)S(1)} %collective-permute-done.9), channel_id=1, source_target_pairs={{0,2},{1,31},{2,4},{3,1},{4,6},{5,3},{6,8},{7,5},{8,10},{9,7},{10,... | collective-permute-start | bytes 1191944 | tf_op jit(solution)/shard_map/ppermute | solution.py:219
  64.1 8.8 %collective-permute-start.12 = (bf16[1552,128]{1,0:T(8,128)(2,1)S(1)}, bf16[1552,128]{1,0:T(8,128)(2,1)S(1)}, u32[]{:S(2)}, u32[]{:S(2)}) collective-permute-start(bf16[1552,128]{1,0:T(8,128)(2,1)S(1)} %collective-permute-done.10), channel_id=1, source_target_pairs={{0,2},{1,31},{2,4},{3,1},{4,6},{5,3},{6,8},{7,5},{8,10},{9,7},{10,... | collective-permute-start | bytes 1191944 | tf_op jit(solution)/shard_map/ppermute | solution.py:218
  68.7 9.7 %collective-permute-start.13 = (bf16[1552,128]{1,0:T(8,128)(2,1)S(1)}, bf16[1552,128]{1,0:T(8,128)(2,1)S(1)}, u32[]{:S(2)}, u32[]{:S(2)}) collective-permute-start(bf16[1552,128]{1,0:T(8,128)(2,1)S(1)} %collective-permute-done.11), channel_id=1, source_target_pairs={{0,2},{1,31},{2,4},{3,1},{4,6},{5,3},{6,8},{7,5},{8,10},{9,7},{10,... | collective-permute-start | bytes 1191944 | tf_op jit(solution)/shard_map/ppermute | solution.py:219
  72.9 10.2 %collective-permute-start.14 = (bf16[1552,128]{1,0:T(8,128)(2,1)S(1)}, bf16[1552,128]{1,0:T(8,128)(2,1)S(1)}, u32[]{:S(2)}, u32[]{:S(2)}) collective-permute-start(bf16[1552,128]{1,0:T(8,128)(2,1)S(1)} %collective-permute-done.12), channel_id=1, source_target_pairs={{0,2},{1,31},{2,4},{3,1},{4,6},{5,3},{6,8},{7,5},{8,10},{9,7},{10,... | collective-permute-start | bytes 1191944 | tf_op jit(solution)/shard_map/ppermute | solution.py:218
  79.1 8.9 %collective-permute-start.15 = (bf16[1552,128]{1,0:T(8,128)(2,1)S(1)}, bf16[1552,128]{1,0:T(8,128)(2,1)S(1)}, u32[]{:S(2)}, u32[]{:S(2)}) collective-permute-start(bf16[1552,128]{1,0:T(8,128)(2,1)S(1)} %collective-permute-done.13), channel_id=1, source_target_pairs={{0,2},{1,31},{2,4},{3,1},{4,6},{5,3},{6,8},{7,5},{8,10},{9,7},{10,... | collective-permute-start | bytes 1191944 | tf_op jit(solution)/shard_map/ppermute | solution.py:219
  83.2 10.5 %collective-permute-start.16 = (bf16[1552,128]{1,0:T(8,128)(2,1)S(1)}, bf16[1552,128]{1,0:T(8,128)(2,1)S(1)}, u32[]{:S(2)}, u32[]{:S(2)}) collective-permute-start(bf16[1552,128]{1,0:T(8,128)(2,1)S(1)} %collective-permute-done.14), channel_id=1, source_target_pairs={{0,2},{1,31},{2,4},{3,1},{4,6},{5,3},{6,8},{7,5},{8,10},{9,7},{10,... | collective-permute-start | bytes 1191944 | tf_op jit(solution)/shard_map/ppermute | solution.py:218
  87.9 9.7 %collective-permute-start.17 = (bf16[1552,128]{1,0:T(8,128)(2,1)S(1)}, bf16[1552,128]{1,0:T(8,128)(2,1)S(1)}, u32[]{:S(2)}, u32[]{:S(2)}) collective-permute-start(bf16[1552,128]{1,0:T(8,128)(2,1)S(1)} %collective-permute-done.15), channel_id=1, source_target_pairs={{0,2},{1,31},{2,4},{3,1},{4,6},{5,3},{6,8},{7,5},{8,10},{9,7},{10,... | collective-permute-start | bytes 1191944 | tf_op jit(solution)/shard_map/ppermute | solution.py:219
  98.7 24.7 %collective-permute-start.18 = (f32[1568,256]{1,0:T(8,128)S(1)}, f32[1568,256]{1,0:T(8,128)S(1)}, u32[]{:S(2)}, u32[]{:S(2)}) collective-permute-start(f32[1568,256]{1,0:T(8,128)S(1)} %maximum_maximum_fusion), channel_id=1, source_target_pairs={{0,1},{1,0},{2,3},{3,2},{4,5},{5,4},{6,7},{7,6},{8,9},{9,8},{10,11... | collective-permute-start | bytes 4816904 | tf_op jit(solution)/shard_map/ppermute | solution.py:230
  110.2 8.9 %collective-permute-start.19 = (bf16[1552,128]{1,0:T(8,128)(2,1)S(1)}, bf16[1552,128]{1,0:T(8,128)(2,1)S(1)}, u32[]{:S(2)}, u32[]{:S(2)}) collective-permute-start(bf16[1552,128]{1,0:T(8,128)(2,1)S(1)} %collective-permute-done.16), channel_id=1, source_target_pairs={{0,2},{1,31},{2,4},{3,1},{4,6},{5,3},{6,8},{7,5},{8,10},{9,7},{10,... | collective-permute-start | bytes 1191944 | tf_op jit(solution)/shard_map/ppermute | solution.py:224
  112.2 11.2 %collective-permute-start.20 = (bf16[1552,128]{1,0:T(8,128)(2,1)S(1)}, bf16[1552,128]{1,0:T(8,128)(2,1)S(1)}, u32[]{:S(2)}, u32[]{:S(2)}) collective-permute-start(bf16[1552,128]{1,0:T(8,128)(2,1)S(1)} %collective-permute-done.17), channel_id=1, source_target_pairs={{0,2},{1,31},{2,4},{3,1},{4,6},{5,3},{6,8},{7,5},{8,10},{9,7},{10,... | collective-permute-start | bytes 1191944 | tf_op jit(solution)/shard_map/ppermute | solution.py:225

commit v4 on v3

--- a/solution.py
+++ b/solution.py
@@ -21,8 +21,9 @@
 
 def state_kernel(
     total_ref,
+    new_ref,
+    query_ref,
     arrived_ref,
-    query_ref,
     last_a_ref,
     last_b_ref,
     weight_ref,
@@ -38,21 +39,18 @@
     own_ref,
 ):
     span_len, inner = decay_ref.shape
-    rows = last_a_ref.shape[0] - EXTRA
+    rows = last_a_ref.shape[0]
     prompts = rows // span_len
     groups = out_ref.shape[0]
     keep = HD // groups
     key_scale = HD ** (-0.5)
     lane = lax.broadcasted_iota(jnp.int32, (HD, inner), 1)
 
-    def projected(start, count):
-        at = pl.ds(start, count)
-        last = jnp.concatenate([last_a_ref[at, :], last_b_ref[at, :]], axis=1)
-        part = jnp.dot(last, weight_ref[...], preferred_element_type=jnp.float32)
-        return total_ref[at, :] + arrived_ref[at, :] + part
-
-    fresh = projected(rows, EXTRA)
-    last = jnp.concatenate([last_a_ref[rows:, :], last_b_ref[rows:, :]], axis=1)
+    last = jnp.concatenate(
+        [last_b_ref[rows + EXTRA : rows + 2 * EXTRA, :], last_b_ref[rows : rows + EXTRA, :]], axis=1
+    )
+    fresh = new_ref[...] + arrived_ref[rows : rows + EXTRA, :]
+    fresh += jnp.dot(last, weight_ref[...], preferred_element_type=jnp.float32)
     query = query_ref[...] + arrived_ref[rows + EXTRA :, :inner]
     query += jnp.dot(last, query_weight_ref[...], preferred_element_type=jnp.float32)
     query = query * new_cos_ref[...] + swap_halves(query) * new_sin_ref[...]
@@ -73,7 +71,10 @@
     columns = jnp.transpose(query)
 
     for s in range(prompts):
-        total = projected(s * span_len, span_len)
+        at = pl.ds(s * span_len, span_len)
+        last = jnp.concatenate([last_a_ref[at, :], last_b_ref[at, :]], axis=1)
+        total = total_ref[at, :] + arrived_ref[at, :]
+        total += jnp.dot(last, weight_ref[...], preferred_element_type=jnp.float32)
         keys = total[:, :inner]
         values = total[:, inner:].astype(jnp.bfloat16)
         keys = (keys * cos_ref[...] + swap_halves(keys) * sin_ref[...]).astype(jnp.bfloat16)
@@ -178,22 +179,25 @@
         for c in range(2)
     ]
 
-    fresh = jnp.concatenate(
+    def sent(value, pairs):
+        return lax.ppermute(value, "tp", pairs)
+
+    chain_a = tokens.reshape(rows, width)
+    new_rows = jnp.concatenate(
         [new_token[:, 0], jnp.zeros((EXTRA - prompts, width), new_token.dtype)], axis=0
     )
-    chain_a = jnp.concatenate([tokens.reshape(rows, width), fresh], axis=0)
-    chain_b = lax.ppermute(chain_a, "tp", partner)
-
-    def other(weights):
-        return lax.ppermute(weights, "tp", partner)
+    other_tokens = sent(chain_a, partner)
+    other_rows = sent(new_rows, partner)
+    chain_b = jnp.concatenate([other_tokens, other_rows, new_rows], axis=0)
 
     main_weights = jnp.concatenate([key_weight, value_weight], axis=1)
     all_weights = jnp.concatenate(
-        [main_weights, other(key_weight), other(value_weight)], axis=1
+        [main_weights, sent(key_weight, partner), sent(value_weight, partner)],
+        axis=1,
     ).reshape(2 * planes, width, 4 * inner)
     main_weights = main_weights.reshape(2 * planes, width, 2 * inner)
     own_query = query_weight.reshape(2 * planes, width, inner)
-    all_query = jnp.concatenate([query_weight, other(query_weight)], axis=1)
+    all_query = jnp.concatenate([query_weight, sent(query_weight, partner)], axis=1)
     all_query = all_query.reshape(2 * planes, width, 2 * inner)
 
     def places(offset):
@@ -205,31 +209,45 @@
 
     def project(a, b, offset, weights, queries):
         at_a, at_b = places(offset)
-        main = jnp.dot(a, block(weights, at_a), preferred_element_type=jnp.float32)
-        main = main + jnp.dot(b, block(weights, at_b), preferred_element_type=jnp.float32)
-        query = jnp.dot(a[rows:], block(queries, at_a), preferred_element_type=jnp.float32)
-        query = query + jnp.dot(b[rows:], block(queries, at_b), preferred_element_type=jnp.float32)
-        return main, query
-
-    own_main, own_query_rows = project(chain_a, chain_b, 0, main_weights, own_query)
+
+        def both(left, right, table):
+            part = jnp.dot(left, block(table, at_a), preferred_element_type=jnp.float32)
+            return part + jnp.dot(right, block(table, at_b), preferred_element_type=jnp.float32)
+
+        new_b = b[rows : rows + EXTRA]
+        new_a = b[rows + EXTRA :]
+        return (
+            both(a, b[:rows], weights),
+            both(new_a, new_b, weights),
+            both(new_a, new_b, queries),
+        )
+
+    def added(left, right):
+        return tuple(x + y for x, y in zip(left, right))
+
+    own = project(chain_a, chain_b, 0, main_weights, own_query)
     reach = planes // 2
-    main = query = None
+    sums = None
     for step in range(1, reach):
-        chain_a = lax.ppermute(chain_a, "tp", onward)
-        chain_b = lax.ppermute(chain_b, "tp", onward)
-        more, more_query = project(chain_a, chain_b, step, all_weights, all_query)
-        main = more if main is None else main + more
-        query = more_query if query is None else query + more_query
-        main, query = lax.optimization_barrier((main, query))
-    last_a = lax.ppermute(chain_a, "tp", onward)
-    last_b = lax.ppermute(chain_b, "tp", onward)
-
+        chain_a = sent(chain_a, onward)
+        chain_b = sent(chain_b, onward)
+        more = project(chain_a, chain_b, step, all_weights, all_query)
+        sums = more if sums is None else added(sums, more)
+        sums = lax.optimization_barrier(sums)
+    last_a = sent(chain_a, onward)
+    last_b = sent(chain_b, onward)
+
+    main, new_main, query = sums
     outgoing = jnp.concatenate(
-        [main[:, 2 * inner :], jnp.concatenate([query[:, inner:]] * 2, axis=1)], axis=0
-    )
-    arrived = lax.ppermute(outgoing, "tp", partner)
-    own_main = own_main + main[:, : 2 * inner]
-    own_query_rows = own_query_rows + query[:, :inner]
+        [
+            main[:, 2 * inner :],
+            new_main[:, 2 * inner :],
+            jnp.concatenate([query[:, inner:]] * 2, axis=1),
+        ],
+        axis=0,
+    )
+    arrived = sent(outgoing, partner)
+    own = added(own, (main[:, : 2 * inner], new_main[:, : 2 * inner], query[:, :inner]))
     at_a, at_b = places(reach)
     last_weights = jnp.concatenate([block(main_weights, at_a), block(main_weights, at_b)], axis=0)
     last_query = jnp.concatenate([block(own_query, at_a), block(own_query, at_b)], axis=0)
@@ -248,9 +266,8 @@
         prompts,
         groups,
         decay_rows,
-        own_main,
+        *own,
         arrived,
-        own_query_rows,
         last_a,
         last_b,
         last_weights,

time: 141 us -> 163 us (1.16)
  matrix products: 15.1 us -> 23.4 us
  waiting for transfers between devices: 18.7 us -> 22.3 us
  local copies, waits for them, and re-layouts: 3.96 us -> 7.31 us
  other arithmetic: 4.35 us -> 7.69 us
  starting transfers between devices: 79.8 us -> 82.9 us
    dot_general x32 -> x48, matrix products: 15.1 us -> 23.4 us  [the longest x24 12.2 us: both(): part = jnp.dot(left, block(table, at_a), preferred_element_type=jnp.float32)]
    ppermute x21 -> x22, waiting for transfers between devices: 18.7 us -> 22.3 us  [sent(): return lax.ppermute(value, 'tp', pairs)]
    ppermute x21 -> x22, starting transfers between devices: 79.8 us -> 82.9 us  [sent(): return lax.ppermute(value, 'tp', pairs)]
    concatenate x1, other arithmetic: 0.23 us -> 3.27 us  [body(): main_weights = jnp.concatenate([key_weight, value_weight], axis=1)]
    concatenate x1 -> x2, local copies, waits for them, and re-layouts: 2.79 us -> 4.5 us  [the longest x1 3.82 us: body(): chain_b = jnp.concatenate([other_tokens, other_rows, new_rows], axis=0)]
    squeeze x2, local copies, waits for them, and re-layouts: 0.03 us -> 1.68 us  [block(): return lax.dynamic_index_in_dim(weights, at, 0, keepdims=False)]
  transfers between devices with their start and end apart: 21 -> 22, of which waited for: 10 -> 8; matrix products, arithmetic and copies ran while one was open for 14% -> 23% of each run, Pallas kernels for 0% -> 0%
where the time goes in v4:
time: 163 us; the launch traced here: 161 us
  starting transfers between devices  82.9 us (51%)
  matrix products  23.4 us (14%)
  waiting for transfers between devices  22.3 us (14%)
  blocking collectives  13.4 us (8%)
  other arithmetic  7.69 us (5%)
  local copies, waits for them, and re-layouts  7.31 us (4%)
  Pallas kernels  2.11 us (1%)
    ppermute x22, starting transfers between devices, sent(): return lax.ppermute(value, 'tp', pairs)  82.9 us
    ppermute x22, waiting for transfers between devices, sent(): return lax.ppermute(value, 'tp', pairs)  22.3 us
    all_to_all x1, blocking collectives, body(): lax.all_to_all(messages, 'sp', split_axis=0, concat_axis=0, tiled=True)  13.4 us
    dot_general x24, matrix products, both(): part = jnp.dot(left, block(table, at_a), preferred_element_type=jnp.float32)  12.2 us
    dot_general x24, matrix products, both(): jnp.dot(right, block(table, at_b), preferred_element_type=jnp.float32)  11.2 us
    concatenate x1, local copies, waits for them, and re-layouts, body(): chain_b = jnp.concatenate([other_tokens, other_rows, new_rows], axis=0)  3.82 us
    concatenate x1, other arithmetic, body(): main_weights = jnp.concatenate([key_weight, value_weight], axis=1)  3.27 us
  transfers between devices with their start and end apart: 22, of which 8 were waited for; matrix products, arithmetic and copies ran while one was open for 23% of the time, Pallas kernels for 0%

profile of v4, /device:TPU:1, one launch (start us, length us, event | category | flops | bytes accessed | tf_op | source)
XLA Modules:
  0.0 160.5 jit_solution(16229251146148469540)
XLA Ops:
  0.6 8.9 %collective-permute-start = (bf16[1536,128]{1,0:T(8,128)(2,1)}, bf16[1536,128]{1,0:T(8,128)(2,1)S(1)}, u32[]{:S(2)}, u32[]{:S(2)}) collective-permute-start(bf16[1536,128]{1,0:T(8,128)(2,1)} %bitcast.258), channel_id=1, source_target_pairs={{0,1},{1,0},{2,3},{3,2},{4,5},{5,4},{6,7},{7,6},{8,9},{9,8},{10,11... | collective-permute-start | bytes 1179656 | tf_op jit(solution)/shard_map/ppermute | solution.py:183
  9.5 5.8 %collective-permute-start.3 = (bf16[1536,128]{1,0:T(8,128)(2,1)}, bf16[1536,128]{1,0:T(8,128)(2,1)}, u32[]{:S(2)}, u32[]{:S(2)}) collective-permute-start(bf16[1536,128]{1,0:T(8,128)(2,1)} %bitcast.259), channel_id=1, source_target_pairs={{0,2},{1,31},{2,4},{3,1},{4,6},{5,3},{6,8},{7,5},{8,10},{9,7},{10,... | collective-permute-start | bytes 1179656 | tf_op jit(solution)/shard_map/ppermute | solution.py:183
  16.0 1.9 %collective-permute-start.4 = (bf16[16,128]{1,0:T(8,128)(2,1)S(1)}, bf16[16,128]{1,0:T(8,128)(2,1)S(1)}, u32[]{:S(2)}, u32[]{:S(2)}) collective-permute-start(bf16[16,128]{1,0:T(8,128)(2,1)S(1)} %concatenate.43), channel_id=1, source_target_pairs={{0,1},{1,0},{2,3},{3,2},{4,5},{5,4},{6,7},{7,6},{8,9},{9,8},{10,11... | collective-permute-start | bytes 12296 | tf_op jit(solution)/shard_map/ppermute | solution.py:183
  17.9 2.4 %collective-permute-start.1 = (bf16[4096,128]{1,0:T(8,128)(2,1)}, bf16[4096,128]{1,0:T(8,128)(2,1)}, u32[]{:S(2)}, u32[]{:S(2)}) collective-permute-start(bf16[4096,128]{1,0:T(8,128)(2,1)} %param.9), channel_id=1, source_target_pairs={{0,1},{1,0},{2,3},{3,2},{4,5},{5,4},{6,7},{7,6},{8,9},{9,8},{10,11... | collective-permute-start | bytes 3145736 | tf_op jit(solution)/shard_map/ppermute | solution.py:183
  20.3 1.9 %collective-permute-start.2 = (bf16[4096,128]{1,0:T(8,128)(2,1)}, bf16[4096,128]{1,0:T(8,128)(2,1)}, u32[]{:S(2)}, u32[]{:S(2)}) collective-permute-start(bf16[4096,128]{1,0:T(8,128)(2,1)} %param.10), channel_id=1, source_target_pairs={{0,1},{1,0},{2,3},{3,2},{4,5},{5,4},{6,7},{7,6},{8,9},{9,8},{10,11... | collective-permute-start | bytes 3145736 | tf_op jit(solution)/shard_map/ppermute | solution.py:183
  22.3 3.3 %pad_maximum_fusion.1 = bf16[4096,256]{1,0:T(8,128)(2,1)} fusion(bf16[4096,128]{1,0:T(8,128)(2,1)} %param.10, bf16[4096,128]{1,0:T(8,128)(2,1)} %param.9), kind=kLoop, calls=%fused_computation.23 | loop fusion | flops 4194304 | bytes 4194304 | tf_op jit(solution)/shard_map/concatenate | solution.py:193
  26.1 2.4 %collective-permute-start.6 = (bf16[4096,128]{1,0:T(8,128)(2,1)}, bf16[4096,128]{1,0:T(8,128)(2,1)}, u32[]{:S(2)}, u32[]{:S(2)}) collective-permute-start(bf16[4096,128]{1,0:T(8,128)(2,1)} %param.8), channel_id=1, source_target_pairs={{0,1},{1,0},{2,3},{3,2},{4,5},{5,4},{6,7},{7,6},{8,9},{9,8},{10,11... | collective-permute-start | bytes 3145736 | tf_op jit(solution)/shard_map/ppermute | solution.py:183
  28.5 3.8 %concatenate.44 = bf16[1568,128]{1,0:T(8,128)(2,1)} concatenate(bf16[1536,128]{1,0:T(8,128)(2,1)S(1)} %collective-permute-done, bf16[16,128]{1,0:T(8,128)(2,1)S(1)} %collective-permute-done.4, bf16[3,128]{1,0:T(4,128)(2,1)S(1)} %bitcast.262, bf16[13,128]{1,0:T(8,128)(2,1)S(1)} %broadcast_in_dim.16), dimensions={0} | concatenate | bytes 802816 | tf_op jit(solution)/shard_map/concatenate | solution.py:191
  32.4 2.6 %collective-permute-start.5 = (bf16[1568,128]{1,0:T(8,128)(2,1)}, bf16[1568,128]{1,0:T(8,128)(2,1)}, u32[]{:S(2)}, u32[]{:S(2)}) collective-permute-start(bf16[1568,128]{1,0:T(8,128)(2,1)} %concatenate.44), channel_id=1, source_target_pairs={{0,2},{1,31},{2,4},{3,1},{4,6},{5,3},{6,8},{7,5},{8,10},{9,7},{10,... | collective-permute-start | bytes 1204232 | tf_op jit(solution)/shard_map/ppermute | solution.py:183
  35.0 2.6 %collective-permute-start.7 = (bf16[1536,128]{1,0:T(8,128)(2,1)}, bf16[1536,128]{1,0:T(8,128)(2,1)}, u32[]{:S(2)}, u32[]{:S(2)}) collective-permute-start(bf16[1536,128]{1,0:T(8,128)(2,1)} %collective-permute-done.3), channel_id=1, source_target_pairs={{0,2},{1,31},{2,4},{3,1},{4,6},{5,3},{6,8},{7,5},{8,10},{9,7},{10,... | collective-permute-start | bytes 1179656 | tf_op jit(solution)/shard_map/ppermute | solution.py:183
  40.8 5.0 %collective-permute-done.7 = bf16[1536,128]{1,0:T(8,128)(2,1)} collective-permute-done((bf16[1536,128]{1,0:T(8,128)(2,1)}, bf16[1536,128]{1,0:T(8,128)(2,1)}, u32[]{:S(2)}, u32[]{:S(2)}) %collective-permute-start.7) | collective-permute-done | bytes 393248 | tf_op jit(solution)/shard_map/ppermute | solution.py:183
  45.8 3.5 %collective-permute-start.9 = (bf16[1536,128]{1,0:T(8,128)(2,1)}, bf16[1536,128]{1,0:T(8,128)(2,1)S(1)}, u32[]{:S(2)}, u32[]{:S(2)}) collective-permute-start(bf16[1536,128]{1,0:T(8,128)(2,1)} %collective-permute-done.7), channel_id=1, source_target_pairs={{0,2},{1,31},{2,4},{3,1},{4,6},{5,3},{6,8},{7,5},{8,10},{9,7},{10,... | collective-permute-start | bytes 1179656 | tf_op jit(solution)/shard_map/ppermute | solution.py:183
  49.3 1.9 %collective-permute-start.8 = (bf16[1568,128]{1,0:T(8,128)(2,1)}, bf16[1568,128]{1,0:T(8,128)(2,1)S(1)}, u32[]{:S(2)}, u32[]{:S(2)}) collective-permute-start(bf16[1568,128]{1,0:T(8,128)(2,1)} %collective-permute-done.5), channel_id=1, source_target_pairs={{0,2},{1,31},{2,4},{3,1},{4,6},{5,3},{6,8},{7,5},{8,10},{9,7},{10,... | collective-permute-start | bytes 1204232 | tf_op jit(solution)/shard_map/ppermute | solution.py:183
  51.3 1.8 %pad_maximum_fusion = bf16[4096,512]{1,0:T(8,128)(2,1)S(1)} fusion(bf16[4096,128]{1,0:T(8,128)(2,1)} %collective-permute-done.2, bf16[4096,128]{1,0:T(8,128)(2,1)} %collective-permute-done.1, bf16[4096,128]{1,0:T(8,128)(2,1)S(1)} %copy-done, bf16[4096,128]{1,0:T(8,128)(2,1)S(1)} %copy-done.1), kind=kLoop, calls=%fused_computation | loop fusion | flops 16777216 | bytes 8388608 | tf_op jit(solution)/shard_map/concatenate | solution.py:194
  55.5 1.8 %pad_maximum_fusion.2 = bf16[4096,256]{1,0:T(8,128)(2,1)S(1)} fusion(bf16[4096,128]{1,0:T(8,128)(2,1)} %collective-permute-done.6, bf16[4096,128]{1,0:T(8,128)(2,1)} %param.8), kind=kLoop, calls=%fused_computation.24 | loop fusion | flops 4194304 | bytes 4194304 | tf_op jit(solution)/shard_map/concatenate | solution.py:200
  61.2 2.4 %collective-permute-start.11 = (bf16[1536,128]{1,0:T(8,128)(2,1)S(1)}, bf16[1536,128]{1,0:T(8,128)(2,1)S(1)}, u32[]{:S(2)}, u32[]{:S(2)}) collective-permute-start(bf16[1536,128]{1,0:T(8,128)(2,1)S(1)} %collective-permute-done.9), channel_id=1, source_target_pairs={{0,2},{1,31},{2,4},{3,1},{4,6},{5,3},{6,8},{7,5},{8,10},{9,7},{10,... | collective-permute-start | bytes 1179656 | tf_op jit(solution)/shard_map/ppermute | solution.py:183
  64.5 3.9 %collective-permute-start.10 = (bf16[1568,128]{1,0:T(8,128)(2,1)S(1)}, bf16[1568,128]{1,0:T(8,128)(2,1)S(1)}, u32[]{:S(2)}, u32[]{:S(2)}) collective-permute-start(bf16[1568,128]{1,0:T(8,128)(2,1)S(1)} %collective-permute-done.8), channel_id=1, source_target_pairs={{0,2},{1,31},{2,4},{3,1},{4,6},{5,3},{6,8},{7,5},{8,10},{9,7},{10,... | collective-permute-start | bytes 1204232 | tf_op jit(solution)/shard_map/ppermute | solution.py:183
  70.2 3.6 %collective-permute-start.13 = (bf16[1536,128]{1,0:T(8,128)(2,1)S(1)}, bf16[1536,128]{1,0:T(8,128)(2,1)S(1)}, u32[]{:S(2)}, u32[]{:S(2)}) collective-permute-start(bf16[1536,128]{1,0:T(8,128)(2,1)S(1)} %collective-permute-done.11), channel_id=1, source_target_pairs={{0,2},{1,31},{2,4},{3,1},{4,6},{5,3},{6,8},{7,5},{8,10},{9,7},{10,... | collective-permute-start | bytes 1179656 | tf_op jit(solution)/shard_map/ppermute | solution.py:183
  75.1 3.8 %collective-permute-start.12 = (bf16[1568,128]{1,0:T(8,128)(2,1)S(1)}, bf16[1568,128]{1,0:T(8,128)(2,1)S(1)}, u32[]{:S(2)}, u32[]{:S(2)}) collective-permute-start(bf16[1568,128]{1,0:T(8,128)(2,1)S(1)} %collective-permute-done.10), channel_id=1, source_target_pairs={{0,2},{1,31},{2,4},{3,1},{4,6},{5,3},{6,8},{7,5},{8,10},{9,7},{10,... | collective-permute-start | bytes 1204232 | tf_op jit(solution)/shard_map/ppermute | solution.py:183
  79.8 3.6 %collective-permute-start.15 = (bf16[1536,128]{1,0:T(8,128)(2,1)S(1)}, bf16[1536,128]{1,0:T(8,128)(2,1)S(1)}, u32[]{:S(2)}, u32[]{:S(2)}) collective-permute-start(bf16[1536,128]{1,0:T(8,128)(2,1)S(1)} %collective-permute-done.13), channel_id=1, source_target_pairs={{0,2},{1,31},{2,4},{3,1},{4,6},{5,3},{6,8},{7,5},{8,10},{9,7},{10,... | collective-permute-start | bytes 1179656 | tf_op jit(solution)/shard_map/ppermute | solution.py:183
  84.9 4.7 %collective-permute-start.14 = (bf16[1568,128]{1,0:T(8,128)(2,1)S(1)}, bf16[1568,128]{1,0:T(8,128)(2,1)S(1)}, u32[]{:S(2)}, u32[]{:S(2)}) collective-permute-start(bf16[1568,128]{1,0:T(8,128)(2,1)S(1)} %collective-permute-done.12), channel_id=1, source_target_pairs={{0,2},{1,31},{2,4},{3,1},{4,6},{5,3},{6,8},{7,5},{8,10},{9,7},{10,... | collective-permute-start | bytes 1204232 | tf_op jit(solution)/shard_map/ppermute | solution.py:183
  90.5 2.7 %collective-permute-start.17 = (bf16[1536,128]{1,0:T(8,128)(2,1)S(1)}, bf16[1536,128]{1,0:T(8,128)(2,1)S(1)}, u32[]{:S(2)}, u32[]{:S(2)}) collective-permute-start(bf16[1536,128]{1,0:T(8,128)(2,1)S(1)} %collective-permute-done.15), channel_id=1, source_target_pairs={{0,2},{1,31},{2,4},{3,1},{4,6},{5,3},{6,8},{7,5},{8,10},{9,7},{10,... | collective-permute-start | bytes 1179656 | tf_op jit(solution)/shard_map/ppermute | solution.py:183
  95.2 5.0 %collective-permute-start.16 = (bf16[1568,128]{1,0:T(8,128)(2,1)S(1)}, bf16[1568,128]{1,0:T(8,128)(2,1)S(1)}, u32[]{:S(2)}, u32[]{:S(2)}) collective-permute-start(bf16[1568,128]{1,0:T(8,128)(2,1)S(1)} %collective-permute-done.14), channel_id=1, source_target_pairs={{0,2},{1,31},{2,4},{3,1},{4,6},{5,3},{6,8},{7,5},{8,10},{9,7},{10,... | collective-permute-start | bytes 1204232 | tf_op jit(solution)/shard_map/ppermute | solution.py:183
  101.1 3.9 %collective-permute-done.16 = bf16[1568,128]{1,0:T(8,128)(2,1)S(1)} collective-permute-done((bf16[1568,128]{1,0:T(8,128)(2,1)S(1)}, bf16[1568,128]{1,0:T(8,128)(2,1)S(1)}, u32[]{:S(2)}, u32[]{:S(2)}) %collective-permute-start.16) | collective-permute-done | bytes 401440 | tf_op jit(solution)/shard_map/ppermute | solution.py:183
  105.9 5.0 %collective-permute-start.18 = (bf16[1568,128]{1,0:T(8,128)(2,1)S(1)}, bf16[1568,128]{1,0:T(8,128)(2,1)S(1)}, u32[]{:S(2)}, u32[]{:S(2)}) collective-permute-start(bf16[1568,128]{1,0:T(8,128)(2,1)S(1)} %collective-permute-done.16), channel_id=1, source_target_pairs={{0,2},{1,31},{2,4},{3,1},{4,6},{5,3},{6,8},{7,5},{8,10},{9,7},{10,... | collective-permute-start | bytes 1204232 | tf_op jit(solution)/shard_map/ppermute | solution.py:183
  111.7 3.9 %collective-permute-done.18 = bf16[1568,128]{1,0:T(8,128)(2,1)S(1)} collective-permute-done((bf16[1568,128]{1,0:T(8,128)(2,1)S(1)}, bf16[1568,128]{1,0:T(8,128)(2,1)S(1)}, u32[]{:S(2)}, u32[]{:S(2)}) %collective-permute-start.18) | collective-permute-done | bytes 401440 | tf_op jit(solution)/shard_map/ppermute | solution.py:183
  118.6 10.2 %collective-permute-start.19 = (f32[1568,256]{1,0:T(8,128)S(1)}, f32[1568,256]{1,0:T(8,128)S(1)}, u32[]{:S(2)}, u32[]{:S(2)}) collective-permute-start(f32[1568,256]{1,0:T(8,128)S(1)} %maximum_maximum_fusion), channel_id=1, source_target_pairs={{0,1},{1,0},{2,3},{3,2},{4,5},{5,4},{6,7},{7,6},{8,9},{9,8},{10,11... | collective-permute-start | bytes 4816904 | tf_op jit(solution)/shard_map/ppermute | solution.py:183
  131.9 1.9 %collective-permute-start.20 = (bf16[1536,128]{1,0:T(8,128)(2,1)S(1)}, bf16[1536,128]{1,0:T(8,128)(2,1)S(1)}, u32[]{:S(2)}, u32[]{:S(2)}) collective-permute-start(bf16[1536,128]{1,0:T(8,128)(2,1)S(1)} %collective-permute-done.17), channel_id=1, source_target_pairs={{0,2},{1,31},{2,4},{3,1},{4,6},{5,3},{6,8},{7,5},{8,10},{9,7},{10,... | collective-permute-start | bytes 1179656 | tf_op jit(solution)/shard_map/ppermute | solution.py:183
  133.8 1.9 %collective-permute-start.21 = (bf16[1568,128]{1,0:T(8,128)(2,1)S(1)}, bf16[1568,128]{1,0:T(8,128)(2,1)S(1)}, u32[]{:S(2)}, u32[]{:S(2)}) collective-permute-start(bf16[1568,128]{1,0:T(8,128)(2,1)S(1)} %collective-permute-done.18), channel_id=1, source_target_pairs={{0,2},{1,31},{2,4},{3,1},{4,6},{5,3},{6,8},{7,5},{8,10},{9,7},{10,... | collective-permute-start | bytes 1204232 | tf_op jit(solution)/shard_map/ppermute | solution.py:183
  137.9 2.7 %collective-permute-done.20.last_a_ref = bf16[1536,128]{1,0:T(8,128)(2,1)S(1)} collective-permute-done((bf16[1536,128]{1,0:T(8,128)(2,1)S(1)}, bf16[1536,128]{1,0:T(8,128)(2,1)S(1)}, u32[]{:S(2)}, u32[]{:S(2)}) %collective-permute-start.20) | collective-permute-done | bytes 393248 | tf_op jit(solution)/shard_map/ppermute | solution.py:183
  140.7 4.3 %collective-permute-done.21.last_b_ref = bf16[1568,128]{1,0:T(8,128)(2,1)S(1)} collective-permute-done((bf16[1568,128]{1,0:T(8,128)(2,1)S(1)}, bf16[1568,128]{1,0:T(8,128)(2,1)S(1)}, u32[]{:S(2)}, u32[]{:S(2)}) %collective-permute-start.21) | collective-permute-done | bytes 401440 | tf_op jit(solution)/shard_map/ppermute | solution.py:183
  146.3 13.4 %all_to_all.5.arrived_ref = f32[16,15,128]{2,1,0:T(8,128)S(1)} all-to-all(f32[16,15,128]{2,1,0:T(8,128)S(1)} %get-tuple-element.46), channel_id=1, replica_groups=mesh['sp'=16,'tp'=32] {'sp'}, dimensions={0} | all-to-all | bytes 245760 | tf_op jit(solution)/shard_map/all_to_all | solution.py:283
  (111 shorter events, 32.3 us)
Async XLA Ops:
  0.6 27.9 %copy-start.3 = (bf16[3,1,128]{2,0,1:T(4,128)(2,1)S(1)}, bf16[3,1,128]{2,0,1:T(4,128)(2,1)}, u32[]{:S(2)}) copy-start(bf16[3,1,128]{2,0,1:T(4,128)(2,1)} %param.7) | copy-start | bytes 2308
  0.6 25.4 %copy-start.4 = (f32[2]{0:T(128)S(1)}, f32[2]{0:T(128)}, u32[]{:S(2)}) copy-start(f32[2]{0:T(128)} %param.11) | copy-start | bytes 28
  0.6 27.9 %collective-permute-start = (bf16[1536,128]{1,0:T(8,128)(2,1)}, bf16[1536,128]{1,0:T(8,128)(2,1)S(1)}, u32[]{:S(2)}, u32[]{:S(2)}) collective-permute-start(bf16[1536,128]{1,0:T(8,128)(2,1)} %bitcast.258), channel_id=1, source_target_pairs={{0,1},{1,0},{2,3},{3,2},{4,5},{5,4},{6,7},{7,6},{8,9},{9,8},{10,11... | collective-permute-start | bytes 1179656 | tf_op jit(solution)/shard_map/ppermute | solution.py:183
  9.5 25.5 %collective-permute-start.3 = (bf16[1536,128]{1,0:T(8,128)(2,1)}, bf16[1536,128]{1,0:T(8,128)(2,1)}, u32[]{:S(2)}, u32[]{:S(2)}) collective-permute-start(bf16[1536,128]{1,0:T(8,128)(2,1)} %bitcast.259), channel_id=1, source_target_pairs={{0,2},{1,31},{2,4},{3,1},{4,6},{5,3},{6,8},{7,5},{8,10},{9,7},{10,... | collective-permute-start | bytes 1179656 | tf_op jit(solution)/shard_map/ppermute | solution.py:183
  16.0 10.1 %collective-permute-start.4 = (bf16[16,128]{1,0:T(8,128)(2,1)S(1)}, bf16[16,128]{1,0:T(8,128)(2,1)S(1)}, u32[]{:S(2)}, u32[]{:S(2)}) collective-permute-start(bf16[16,128]{1,0:T(8,128)(2,1)S(1)} %concatenate.43), channel_id=1, source_target_pairs={{0,1},{1,0},{2,3},{3,2},{4,5},{5,4},{6,7},{7,6},{8,9},{9,8},{10,11... | collective-permute-start | bytes 12296 | tf_op jit(solution)/shard_map/ppermute | solution.py:183
  17.9 33.3 %collective-permute-start.1 = (bf16[4096,128]{1,0:T(8,128)(2,1)}, bf16[4096,128]{1,0:T(8,128)(2,1)}, u32[]{:S(2)}, u32[]{:S(2)}) collective-permute-start(bf16[4096,128]{1,0:T(8,128)(2,1)} %param.9), channel_id=1, source_target_pairs={{0,1},{1,0},{2,3},{3,2},{4,5},{5,4},{6,7},{7,6},{8,9},{9,8},{10,11... | collective-permute-start | bytes 3145736 | tf_op jit(solution)/shard_map/ppermute | solution.py:183
  20.3 30.9 %collective-permute-start.2 = (bf16[4096,128]{1,0:T(8,128)(2,1)}, bf16[4096,128]{1,0:T(8,128)(2,1)}, u32[]{:S(2)}, u32[]{:S(2)}) collective-permute-start(bf16[4096,128]{1,0:T(8,128)(2,1)} %param.10), channel_id=1, source_target_pairs={{0,1},{1,0},{2,3},{3,2},{4,5},{5,4},{6,7},{7,6},{8,9},{9,8},{10,11... | collective-permute-start | bytes 3145736 | tf_op jit(solution)/shard_map/ppermute | solution.py:183
  22.3 29.0 %copy-start = (bf16[4096,128]{1,0:T(8,128)(2,1)S(1)}, bf16[4096,128]{1,0:T(8,128)(2,1)}, u32[]{:S(2)}) copy-start(bf16[4096,128]{1,0:T(8,128)(2,1)} %param.10) | copy-start | bytes 3145732
  22.3 29.0 %copy-start.1 = (bf16[4096,128]{1,0:T(8,128)(2,1)S(1)}, bf16[4096,128]{1,0:T(8,128)(2,1)}, u32[]{:S(2)}) copy-start(bf16[4096,128]{1,0:T(8,128)(2,1)} %param.9) | copy-start | bytes 3145732
  26.1 29.4 %collective-permute-start.6 = (bf16[4096,128]{1,0:T(8,128)(2,1)}, bf16[4096,128]{1,0:T(8,128)(2,1)}, u32[]{:S(2)}, u32[]{:S(2)}) collective-permute-start(bf16[4096,128]{1,0:T(8,128)(2,1)} %param.8), channel_id=1, source_target_pairs={{0,1},{1,0},{2,3},{3,2},{4,5},{5,4},{6,7},{7,6},{8,9},{9,8},{10,11... | collective-permute-start | bytes 3145736 | tf_op jit(solution)/shard_map/ppermute | solution.py:183
  32.4 17.0 %collective-permute-start.5 = (bf16[1568,128]{1,0:T(8,128)(2,1)}, bf16[1568,128]{1,0:T(8,128)(2,1)}, u32[]{:S(2)}, u32[]{:S(2)}) collective-permute-start(bf16[1568,128]{1,0:T(8,128)(2,1)} %concatenate.44), channel_id=1, source_target_pairs={{0,2},{1,31},{2,4},{3,1},{4,6},{5,3},{6,8},{7,5},{8,10},{9,7},{10,... | collective-permute-start | bytes 1204232 | tf_op jit(solution)/shard_map/ppermute | solution.py:183
  35.0 10.8 %collective-permute-start.7 = (bf16[1536,128]{1,0:T(8,128)(2,1)}, bf16[1536,128]{1,0:T(8,128)(2,1)}, u32[]{:S(2)}, u32[]{:S(2)}) collective-permute-start(bf16[1536,128]{1,0:T(8,128)(2,1)} %collective-permute-done.3), channel_id=1, source_target_pairs={{0,2},{1,31},{2,4},{3,1},{4,6},{5,3},{6,8},{7,5},{8,10},{9,7},{10,... | collective-permute-start | bytes 1179656 | tf_op jit(solution)/shard_map/ppermute | solution.py:183
  45.8 15.4 %collective-permute-start.9 = (bf16[1536,128]{1,0:T(8,128)(2,1)}, bf16[1536,128]{1,0:T(8,128)(2,1)S(1)}, u32[]{:S(2)}, u32[]{:S(2)}) collective-permute-start(bf16[1536,128]{1,0:T(8,128)(2,1)} %collective-permute-done.7), channel_id=1, source_target_pairs={{0,2},{1,31},{2,4},{3,1},{4,6},{5,3},{6,8},{7,5},{8,10},{9,7},{10,... | collective-permute-start | bytes 1179656 | tf_op jit(solution)/shard_map/ppermute | solution.py:183
  49.3 14.3 %collective-permute-start.8 = (bf16[1568,128]{1,0:T(8,128)(2,1)}, bf16[1568,128]{1,0:T(8,128)(2,1)S(1)}, u32[]{:S(2)}, u32[]{:S(2)}) collective-permute-start(bf16[1568,128]{1,0:T(8,128)(2,1)} %collective-permute-done.5), channel_id=1, source_target_pairs={{0,2},{1,31},{2,4},{3,1},{4,6},{5,3},{6,8},{7,5},{8,10},{9,7},{10,... | collective-permute-start | bytes 1204232 | tf_op jit(solution)/shard_map/ppermute | solution.py:183
  61.2 9.0 %collective-permute-start.11 = (bf16[1536,128]{1,0:T(8,128)(2,1)S(1)}, bf16[1536,128]{1,0:T(8,128)(2,1)S(1)}, u32[]{:S(2)}, u32[]{:S(2)}) collective-permute-start(bf16[1536,128]{1,0:T(8,128)(2,1)S(1)} %collective-permute-done.9), channel_id=1, source_target_pairs={{0,2},{1,31},{2,4},{3,1},{4,6},{5,3},{6,8},{7,5},{8,10},{9,7},{10,... | collective-permute-start | bytes 1179656 | tf_op jit(solution)/shard_map/ppermute | solution.py:183
  64.5 9.8 %collective-permute-start.10 = (bf16[1568,128]{1,0:T(8,128)(2,1)S(1)}, bf16[1568,128]{1,0:T(8,128)(2,1)S(1)}, u32[]{:S(2)}, u32[]{:S(2)}) collective-permute-start(bf16[1568,128]{1,0:T(8,128)(2,1)S(1)} %collective-permute-done.8), channel_id=1, source_target_pairs={{0,2},{1,31},{2,4},{3,1},{4,6},{5,3},{6,8},{7,5},{8,10},{9,7},{10,... | collective-permute-start | bytes 1204232 | tf_op jit(solution)/shard_map/ppermute | solution.py:183
  70.2 9.6 %collective-permute-start.13 = (bf16[1536,128]{1,0:T(8,128)(2,1)S(1)}, bf16[1536,128]{1,0:T(8,128)(2,1)S(1)}, u32[]{:S(2)}, u32[]{:S(2)}) collective-permute-start(bf16[1536,128]{1,0:T(8,128)(2,1)S(1)} %collective-permute-done.11), channel_id=1, source_target_pairs={{0,2},{1,31},{2,4},{3,1},{4,6},{5,3},{6,8},{7,5},{8,10},{9,7},{10,... | collective-permute-start | bytes 1179656 | tf_op jit(solution)/shard_map/ppermute | solution.py:183
  75.1 8.9 %collective-permute-start.12 = (bf16[1568,128]{1,0:T(8,128)(2,1)S(1)}, bf16[1568,128]{1,0:T(8,128)(2,1)S(1)}, u32[]{:S(2)}, u32[]{:S(2)}) collective-permute-start(bf16[1568,128]{1,0:T(8,128)(2,1)S(1)} %collective-permute-done.10), channel_id=1, source_target_pairs={{0,2},{1,31},{2,4},{3,1},{4,6},{5,3},{6,8},{7,5},{8,10},{9,7},{10,... | collective-permute-start | bytes 1204232 | tf_op jit(solution)/shard_map/ppermute | solution.py:183
  79.8 10.6 %collective-permute-start.15 = (bf16[1536,128]{1,0:T(8,128)(2,1)S(1)}, bf16[1536,128]{1,0:T(8,128)(2,1)S(1)}, u32[]{:S(2)}, u32[]{:S(2)}) collective-permute-start(bf16[1536,128]{1,0:T(8,128)(2,1)S(1)} %collective-permute-done.13), channel_id=1, source_target_pairs={{0,2},{1,31},{2,4},{3,1},{4,6},{5,3},{6,8},{7,5},{8,10},{9,7},{10,... | collective-permute-start | bytes 1179656 | tf_op jit(solution)/shard_map/ppermute | solution.py:183
  84.9 9.5 %collective-permute-start.14 = (bf16[1568,128]{1,0:T(8,128)(2,1)S(1)}, bf16[1568,128]{1,0:T(8,128)(2,1)S(1)}, u32[]{:S(2)}, u32[]{:S(2)}) collective-permute-start(bf16[1568,128]{1,0:T(8,128)(2,1)S(1)} %collective-permute-done.12), channel_id=1, source_target_pairs={{0,2},{1,31},{2,4},{3,1},{4,6},{5,3},{6,8},{7,5},{8,10},{9,7},{10,... | collective-permute-start | bytes 1204232 | tf_op jit(solution)/shard_map/ppermute | solution.py:183
  90.5 26.3 %collective-permute-start.17 = (bf16[1536,128]{1,0:T(8,128)(2,1)S(1)}, bf16[1536,128]{1,0:T(8,128)(2,1)S(1)}, u32[]{:S(2)}, u32[]{:S(2)}) collective-permute-start(bf16[1536,128]{1,0:T(8,128)(2,1)S(1)} %collective-permute-done.15), channel_id=1, source_target_pairs={{0,2},{1,31},{2,4},{3,1},{4,6},{5,3},{6,8},{7,5},{8,10},{9,7},{10,... | collective-permute-start | bytes 1179656 | tf_op jit(solution)/shard_map/ppermute | solution.py:183
  95.2 9.8 %collective-permute-start.16 = (bf16[1568,128]{1,0:T(8,128)(2,1)S(1)}, bf16[1568,128]{1,0:T(8,128)(2,1)S(1)}, u32[]{:S(2)}, u32[]{:S(2)}) collective-permute-start(bf16[1568,128]{1,0:T(8,128)(2,1)S(1)} %collective-permute-done.14), channel_id=1, source_target_pairs={{0,2},{1,31},{2,4},{3,1},{4,6},{5,3},{6,8},{7,5},{8,10},{9,7},{10,... | collective-permute-start | bytes 1204232 | tf_op jit(solution)/shard_map/ppermute | solution.py:183
  105.9 9.8 %collective-permute-start.18 = (bf16[1568,128]{1,0:T(8,128)(2,1)S(1)}, bf16[1568,128]{1,0:T(8,128)(2,1)S(1)}, u32[]{:S(2)}, u32[]{:S(2)}) collective-permute-start(bf16[1568,128]{1,0:T(8,128)(2,1)S(1)} %collective-permute-done.16), channel_id=1, source_target_pairs={{0,2},{1,31},{2,4},{3,1},{4,6},{5,3},{6,8},{7,5},{8,10},{9,7},{10,... | collective-permute-start | bytes 1204232 | tf_op jit(solution)/shard_map/ppermute | solution.py:183
  117.4 13.3 %copy-start.2 = (bf16[3,512,128]{2,1,0:T(8,128)(2,1)S(1)}, bf16[3,512,128]{2,1,0:T(8,128)(2,1)}, u32[]{:S(2)}) copy-start(bf16[3,512,128]{2,1,0:T(8,128)(2,1)} %param.6) | copy-start | bytes 1179652
  118.6 26.4 %collective-permute-start.19 = (f32[1568,256]{1,0:T(8,128)S(1)}, f32[1568,256]{1,0:T(8,128)S(1)}, u32[]{:S(2)}, u32[]{:S(2)}) collective-permute-start(f32[1568,256]{1,0:T(8,128)S(1)} %maximum_maximum_fusion), channel_id=1, source_target_pairs={{0,1},{1,0},{2,3},{3,2},{4,5},{5,4},{6,7},{7,6},{8,9},{9,8},{10,11... | collective-permute-start | bytes 4816904 | tf_op jit(solution)/shard_map/ppermute | solution.py:183
  131.9 8.8 %collective-permute-start.20 = (bf16[1536,128]{1,0:T(8,128)(2,1)S(1)}, bf16[1536,128]{1,0:T(8,128)(2,1)S(1)}, u32[]{:S(2)}, u32[]{:S(2)}) collective-permute-start(bf16[1536,128]{1,0:T(8,128)(2,1)S(1)} %collective-permute-done.17), channel_id=1, source_target_pairs={{0,2},{1,31},{2,4},{3,1},{4,6},{5,3},{6,8},{7,5},{8,10},{9,7},{10,... | collective-permute-start | bytes 1179656 | tf_op jit(solution)/shard_map/ppermute | solution.py:183
  133.8 11.2 %collective-permute-start.21 = (bf16[1568,128]{1,0:T(8,128)(2,1)S(1)}, bf16[1568,128]{1,0:T(8,128)(2,1)S(1)}, u32[]{:S(2)}, u32[]{:S(2)}) collective-permute-start(bf16[1568,128]{1,0:T(8,128)(2,1)S(1)} %collective-permute-done.18), channel_id=1, source_target_pairs={{0,2},{1,31},{2,4},{3,1},{4,6},{5,3},{6,8},{7,5},{8,10},{9,7},{10,... | collective-permute-start | bytes 1204232 | tf_op jit(solution)/shard_map/ppermute | solution.py:183

commit v5 on v4

v5 whole, which is shorter than its diff:
```python
import functools

import jax
import jax.numpy as jnp
from jax import lax
from jax.experimental import pallas as pl
from jax.experimental.pallas import tpu as pltpu
from jax.sharding import PartitionSpec as P

HD = 64
EPS = 1e-05
EXTRA = 16


def swap_halves(values):
    lanes = values.shape[-1]
    lane = lax.broadcasted_iota(jnp.int32, values.shape, len(values.shape) - 1)
    quarter = HD // 2
    back = pltpu.roll(values, lanes - quarter, len(values.shape) - 1)
    ahead = pltpu.roll(values, quarter, len(values.shape) - 1)
    return jnp.where(lane % HD < quarter, back, ahead)


def row_block(place_ref, offset):
    planes = place_ref[3]
    toward = 1 - 2 * place_ref[1]
    return lax.rem(place_ref[0] - offset * toward + planes, planes)


def at_rows(block, width):
    return pl.ds(pl.multiple_of(block * width, width), width)


def stacked(place_ref, weight_ref, offsets, width):
    core = place_ref[1]
    blocks = []
    for offset in offsets:
        plane = row_block(place_ref, offset)
        blocks.append(weight_ref[at_rows(2 * plane + core, width), :])
        blocks.append(weight_ref[at_rows(2 * plane + 1 - core, width), :])
    return jnp.concatenate(blocks, axis=0)


def sums_kernel(offsets, span_len, place_ref, own_w_ref, other_w_ref, *refs):
    count = len(offsets)
    a_refs, b_refs, rest = refs[:count], refs[count : 2 * count], refs[2 * count :]
    own_ref, other_ref = rest[-2:]
    before = rest[:-2]
    rows, width = a_refs[0].shape
    inner = own_ref.shape[1]
    hops = [i for i in range(count) if offsets[i] > 0]
    own_plane = [i for i in range(count) if offsets[i] == 0]

    def step(s, carry):
        at = pl.ds(pl.multiple_of(s * span_len, span_len), span_len)

        def gathered(which):
            pieces = []
            for i in which:
                pieces += [a_refs[i][at, :], b_refs[i][at, :]]
            return jnp.concatenate(pieces, axis=1)

        weights = jnp.concatenate(
            [
                stacked(place_ref, own_w_ref, [offsets[i] for i in hops], width),
                stacked(place_ref, other_w_ref, [offsets[i] for i in hops], width),
            ],
            axis=1,
        )
        part = jnp.dot(gathered(hops), weights, preferred_element_type=jnp.float32)
        own, other = part[:, :inner], part[:, inner:]
        if own_plane:
            here = stacked(place_ref, own_w_ref, [0], width)
            own += jnp.dot(gathered(own_plane), here, preferred_element_type=jnp.float32)
        if before:
            own += before[0][at, :]
            other += before[1][at, :]
        own_ref[at, :] = own
        other_ref[at, :] = other
        return carry

    lax.fori_loop(0, rows // span_len, step, 0)


def ring_sums(offsets, span_len, place, own_weights, other_weights, a_list, b_list, before):
    rows, width = a_list[0].shape
    inner = own_weights.shape[1]
    whole = pl.BlockSpec(memory_space=pltpu.VMEM)
    operands = [own_weights, other_weights, *a_list, *b_list, *before]
    flops = 2 * rows * 2 * inner * 2 * width * len(offsets)
    return pl.pallas_call(
        functools.partial(sums_kernel, offsets, span_len),
        in_specs=[pl.BlockSpec(memory_space=pltpu.SMEM)] + [whole] * len(operands),
        out_specs=[whole, whole],
        out_shape=[jax.ShapeDtypeStruct((rows, inner), jnp.float32)] * 2,
        compiler_params=pltpu.CompilerParams(vmem_limit_bytes=16 * 1024 * 1024),
        cost_estimate=pl.CostEstimate(flops=flops, bytes_accessed=0, transcendentals=0),
        name="ring_sums",
    )(place, *operands)


def state_kernel(
    place_ref,
    total_ref,
    arrived_ref,
    here_new_ref,
    mine_new_ref,
    theirs_new_ref,
    last_a_ref,
    last_b_ref,
    main_ref,
    query_w_ref,
    cos_ref,
    sin_ref,
    lane_ref,
    out_ref,
    own_ref,
):
    rows, width = last_a_ref.shape
    inner = query_w_ref.shape[1]
    groups, out_rows, _ = out_ref.shape
    keep = HD // groups
    prompts = out_rows // (keep + 1)
    span_len = rows // prompts
    reach = mine_new_ref.shape[0] // (2 * EXTRA) + 1
    lane = lax.broadcasted_iota(jnp.int32, (HD, inner), 1)
    lane_decay = lane_ref[...]
    distance = ((groups - 1 - place_ref[2]) * span_len).astype(jnp.float32)
    carried = jnp.exp(lane_decay * distance)
    one = jnp.exp(lane_decay)
    to_end = lax.broadcasted_iota(jnp.int32, (span_len, inner), 0)
    decay = jnp.exp((span_len - 1 - to_end).astype(jnp.float32) * lane_decay)

    def pair(ref, start):
        return [ref[start : start + EXTRA, :], ref[start + EXTRA : start + 2 * EXTRA, :]]

    pieces = pair(here_new_ref, 0)
    order = [0]
    for k in range(1, reach):
        pieces += pair(mine_new_ref, (k - 1) * 2 * EXTRA)
        pieces += pair(theirs_new_ref, (k - 1) * 2 * EXTRA)
        order += [k, -k]
    pieces += pair(last_b_ref, rows)
    order.append(reach)
    entries = jnp.concatenate(pieces, axis=1)
    plane_rows = [at_rows(row_block(place_ref, k), 2 * width) for k in order]
    weights = jnp.concatenate(
        [jnp.concatenate([main_ref[at, :], query_w_ref[at, :]], axis=1) for at in plane_rows], axis=0
    )
    fresh = jnp.dot(entries, weights, preferred_element_type=jnp.float32)
    new_cos = cos_ref[span_len : span_len + 1, :]
    new_sin = sin_ref[span_len : span_len + 1, :]
    new_key = fresh[:, :inner]
    new_key = new_key * new_cos + swap_halves(new_key) * new_sin
    new_key = new_key.astype(jnp.bfloat16).astype(jnp.float32)
    new_value = fresh[:, inner : 2 * inner].astype(jnp.bfloat16).astype(jnp.float32)
    query = fresh[:, 2 * inner :]
    query = (query * new_cos + swap_halves(query) * new_sin) * (HD**0.5)
    query = query.astype(jnp.bfloat16).astype(jnp.float32)
    products = query * new_key
    new_lane = lax.broadcasted_iota(jnp.int32, products.shape, 1)
    score = jnp.zeros_like(products)
    for h in range(inner // HD):
        here = new_lane // HD == h
        score = jnp.where(
            here, jnp.sum(jnp.where(here, products, 0.0), axis=1, keepdims=True), score
        )
    own_ref[...] = score * new_value
    columns = jnp.transpose(query)

    last_weights = stacked(place_ref, main_ref, [reach], width)
    cosine = cos_ref[:span_len, :]
    sine = sin_ref[:span_len, :]
    for s in range(prompts):
        at = pl.ds(s * span_len, span_len)
        last = jnp.concatenate([last_a_ref[at, :], last_b_ref[at, :]], axis=1)
        total = total_ref[at, :] + arrived_ref[at, :]
        total += jnp.dot(last, last_weights, preferred_element_type=jnp.float32)
        keys = total[:, :inner]
        values = total[:, inner:].astype(jnp.bfloat16)
        keys = (keys * cosine + swap_halves(keys) * sine).astype(jnp.bfloat16)
        weighted = (keys.astype(jnp.float32) * decay).astype(jnp.bfloat16)
        full = lax.dot_general(
            weighted, values, (((0,), (0,)), ((), ())), preferred_element_type=jnp.float32
        )
        state = jnp.where(lane < HD, full[:HD], full[HD:]) * carried
        column = jnp.where(lane < HD, columns[:HD, s : s + 1], columns[HD:, s : s + 1])
        read = jnp.sum(state * column, axis=0, keepdims=True) * one
        for g in range(groups):
            out_ref[g, s * keep : (s + 1) * keep, :] = state[g * keep : (g + 1) * keep]
            out_ref[g, prompts * keep + s : prompts * keep + s + 1, :] = read


def span_states(prompts, groups, inner, place, *operands):
    keep = HD // groups
    whole = pl.BlockSpec(memory_space=pltpu.VMEM)
    return pl.pallas_call(
        state_kernel,
        in_specs=[pl.BlockSpec(memory_space=pltpu.SMEM)] + [whole] * len(operands),
        out_specs=[whole, whole],
        out_shape=[
            jax.ShapeDtypeStruct((groups, prompts * (keep + 1), inner), jnp.float32),
            jax.ShapeDtypeStruct((EXTRA, inner), jnp.float32),
        ],
        compiler_params=pltpu.CompilerParams(vmem_limit_bytes=24 * 1024 * 1024),
        name="span_states",
    )(place, *operands)


def finish_kernel(arrived_ref, own_ref, state_ref, read_ref):
    total = jnp.sum(arrived_ref[...], axis=0)
    prompts, heads, keep, _ = state_ref.shape
    for s in range(prompts):
        for h in range(heads):
            state_ref[s, h] = total[s * keep : (s + 1) * keep, h * HD : (h + 1) * HD].astype(
                jnp.bfloat16
            )
    raw = total[prompts * keep :] + own_ref[:prompts, :]
    lane = lax.broadcasted_iota(jnp.int32, raw.shape, 1)

    def per_head(values):
        result = jnp.zeros_like(values)
        for h in range(heads):
            here = lane // HD == h
            mean = jnp.sum(jnp.where(here, values, 0.0), axis=1, keepdims=True) / HD
            result = jnp.where(here, mean, result)
        return result

    centered = raw - per_head(raw)
    spread = per_head(centered * centered)
    read_ref[...] = (centered * lax.rsqrt(spread + EPS)).astype(jnp.bfloat16)


def finish(arrived, own_term, prompts, heads, keep):
    inner = own_term.shape[1]
    whole = pl.BlockSpec(memory_space=pltpu.VMEM)
    return pl.pallas_call(
        finish_kernel,
        in_specs=[whole, whole],
        out_specs=[whole, whole],
        out_shape=[
            jax.ShapeDtypeStruct((prompts, heads, keep, HD), jnp.bfloat16),
            jax.ShapeDtypeStruct((prompts, inner), jnp.bfloat16),
        ],
        compiler_params=pltpu.CompilerParams(vmem_limit_bytes=4 * 1024 * 1024),
        name="finish",
    )(arrived, own_term)


def tables(first_position, span_len, new_position, heads):
    quarter = HD // 2
    lane = jnp.arange(heads * HD, dtype=jnp.int32)
    inverse = 10000.0 ** (-(lane % quarter).astype(jnp.float32) / quarter)
    row = jnp.arange(span_len + 8, dtype=jnp.int32)
    position = jnp.where(row < span_len, first_position + row, new_position).astype(jnp.float32)
    angles = position[:, None] * inverse[None, :]
    key_scale = HD ** (-0.5)
    sign = jnp.where(lane % HD < quarter, -key_scale, key_scale)
    return jnp.cos(angles) * key_scale, jnp.sin(angles) * sign[None, :]


def body(tokens, new_token, query_weight, key_weight, value_weight, log_decay):
    prompts, span_len, width = tokens.shape
    heads = log_decay.shape[0]
    inner = heads * HD
    groups = lax.axis_size("sp")
    own_index = lax.axis_index("sp")
    tp_index = lax.axis_index("tp")
    planes = lax.axis_size("tp") // 2
    reach = planes // 2
    plane = tp_index // 2
    core = tp_index % 2
    rows = prompts * span_len
    place = jnp.stack([plane, core, own_index, jnp.int32(planes)]).astype(jnp.int32)

    partner = [(i, i ^ 1) for i in range(2 * planes)]
    onward = [
        (2 * z + c, 2 * ((z + (1 if c == 0 else -1)) % planes) + c)
        for z in range(planes)
        for c in range(2)
    ]

    def sent(value, pairs):
        return lax.ppermute(value, "tp", pairs)

    chain_a = tokens.reshape(rows, width)
    new_rows = jnp.concatenate(
        [new_token[:, 0], jnp.zeros((EXTRA - prompts, width), new_token.dtype)], axis=0
    )
    other_tokens = sent(chain_a, partner)
    other_rows = sent(new_rows, partner)
    new_pair = jnp.concatenate(
        [
            jnp.where(core == 0, new_rows, other_rows),
            jnp.where(core == 0, other_rows, new_rows),
        ],
        axis=0,
    )
    chain_b = jnp.concatenate([other_tokens, new_pair], axis=0)
    main_weights = jnp.concatenate([key_weight, value_weight], axis=1)
    other_weights = sent(main_weights, partner)
    cosine, sine = tables(own_index * span_len, span_len, groups * span_len, heads)
    lane_decay = jnp.repeat(log_decay, HD)[None, :]

    a_list, b_list = [chain_a], [other_tokens]
    new_list = []
    for step in range(1, reach + 1):
        chain_a = sent(chain_a, onward)
        chain_b = sent(chain_b, onward)
        if step == 1:
            chain_a, cosine, sine, lane_decay = lax.optimization_barrier(
                (chain_a, cosine, sine, lane_decay)
            )
        a_list.append(chain_a)
        b_list.append(chain_b)
        new_list.append(chain_b[rows:])
    sums = ()
    for low, high in ((0, 4), (4, 7), (7, 8)):
        sums = ring_sums(
            tuple(range(low, high)),
            span_len,
            place,
            main_weights,
            other_weights,
            a_list[low:high],
            b_list[low:high],
            sums,
        )
    own, other = sums

    arrived = sent(other, partner)
    mine_new = jnp.concatenate(new_list[:-1], axis=0)
    theirs_new = sent(mine_new, partner)

    messages, own_term = span_states(
        prompts,
        groups,
        inner,
        place,
        own,
        arrived,
        new_pair,
        mine_new,
        theirs_new,
        a_list[-1],
        b_list[-1],
        main_weights,
        query_weight,
        cosine,
        sine,
        lane_decay,
    )
    arrived = lax.all_to_all(messages, "sp", split_axis=0, concat_axis=0, tiled=True)
    return tuple(finish(arrived, own_term, prompts, heads, HD // groups))


def solution(mesh):
    return jax.shard_map(
        body,
        mesh=mesh,
        in_specs=(
            P(None, "sp", "tp"),
            P(None, None, "tp"),
            P(None, "tp"),
            P(None, "tp"),
            P(None, "tp"),
            P("tp"),
        ),
        out_specs=(P(None, "tp", "sp", None), P(None, "tp")),
        check_vma=False,
    )
```

time: 163 us -> 141 us (0.87)
  matrix products: 23.4 us -> 0 us
  waiting for transfers between devices: 22.3 us -> 9.68 us
  Pallas kernels: 2.11 us -> 13.3 us
  local copies, waits for them, and re-layouts: 7.31 us -> 15.1 us
  other arithmetic: 7.69 us -> 1.15 us
  starting transfers between devices: 82.9 us -> 86.1 us
    dot_general x48 -> x0, matrix products: 23.4 us -> none  [the longest x24 12.2 us: both(): part = jnp.dot(left, block(table, at_a), preferred_element_type=jnp.float32)]
    ppermute x22 -> x21, waiting for transfers between devices: 22.3 us -> 9.68 us  [sent(): return lax.ppermute(value, 'tp', pairs)]
    unnamed x10 -> x43, local copies, waits for them, and re-layouts: 0.03 us -> 12.1 us
    pallas_call x1 -> x4, Pallas kernels: 1.34 us -> 12.5 us  [the longest x3 10.3 us: ring_sums(): pl.pallas_call(functools.partial(sums_kernel, offsets, span_len), in_spec...]
    concatenate x6 -> x2, other arithmetic: 6.93 us -> 0.03 us  [the longest x1 0.03 us: body(): chain_b = jnp.concatenate([other_tokens, new_pair], axis=0)]
    ppermute x22 -> x21, starting transfers between devices: 82.9 us -> 86.1 us  [sent(): return lax.ppermute(value, 'tp', pairs)]
    squeeze x2 -> x0, local copies, waits for them, and re-layouts: 1.68 us -> none  [block(): return lax.dynamic_index_in_dim(weights, at, 0, keepdims=False)]
    concatenate x1 -> x2, local copies, waits for them, and re-layouts: 3.82 us -> 2.18 us  [the longest x1 1.47 us: body(): main_weights = jnp.concatenate([key_weight, value_weight], axis=1)]
  transfers between devices with their start and end apart: 22 -> 21, of which waited for: 8 -> 6; matrix products, arithmetic and copies ran while one was open for 23% -> 5% of each run, Pallas kernels for 0% -> 5%
where the time goes in v5:
time: 141 us; the launch traced here: 140 us
  starting transfers between devices  86.1 us (61%)
  local copies, waits for them, and re-layouts  15.1 us (11%)
  blocking collectives  13.4 us (10%)
  Pallas kernels  13.3 us (9%)
  waiting for transfers between devices  9.68 us (7%)
    ppermute x21, starting transfers between devices, sent(): return lax.ppermute(value, 'tp', pairs)  86.1 us
    all_to_all x1, blocking collectives, body(): lax.all_to_all(messages, 'sp', split_axis=0, concat_axis=0, tiled=True)  13.4 us
    unnamed x43, local copies, waits for them, and re-layouts  12.1 us
    pallas_call x3, Pallas kernels, ring_sums(): pl.pallas_call(functools.partial(sums_kernel, offsets, span_len), in_spec...  10.3 us
    ppermute x21, waiting for transfers between devices, sent(): return lax.ppermute(value, 'tp', pairs)  9.68 us
  transfers between devices with their start and end apart: 21, of which 6 were waited for; matrix products, arithmetic and copies ran while one was open for 5% of the time, Pallas kernels for 5%

profile of v5, /device:TPU:1, one launch (start us, length us, event | category | flops | bytes accessed | tf_op | source)
XLA Modules:
  0.0 139.8 jit_solution(6287087054624742168)
XLA Ops:
  0.6 8.7 %collective-permute-start.8 = (bf16[1536,128]{1,0:T(8,128)(2,1)}, bf16[1536,128]{1,0:T(8,128)(2,1)S(1)}, u32[]{:S(2)}, u32[]{:S(2)}) collective-permute-start(bf16[1536,128]{1,0:T(8,128)(2,1)} %bitcast.5), channel_id=1, source_target_pairs={{0,1},{1,0},{2,3},{3,2},{4,5},{5,4},{6,7},{7,6},{8,9},{9,8},{10,11... | collective-permute-start | bytes 1179656 | tf_op jit(solution)/shard_map/ppermute | solution.py:284
  9.4 5.8 %collective-permute-start.1 = (bf16[1536,128]{1,0:T(8,128)(2,1)}, bf16[1536,128]{1,0:T(8,128)(2,1)}, u32[]{:S(2)}, u32[]{:S(2)}) collective-permute-start(bf16[1536,128]{1,0:T(8,128)(2,1)} %bitcast.6), channel_id=1, source_target_pairs={{0,2},{1,31},{2,4},{3,1},{4,6},{5,3},{6,8},{7,5},{8,10},{9,7},{10,... | collective-permute-start | bytes 1179656 | tf_op jit(solution)/shard_map/ppermute | solution.py:284
  15.9 1.9 %collective-permute-start.9 = (bf16[16,128]{1,0:T(8,128)(2,1)S(1)}, bf16[16,128]{1,0:T(8,128)(2,1)S(1)}, u32[]{:S(2)}, u32[]{:S(2)}) collective-permute-start(bf16[16,128]{1,0:T(8,128)(2,1)S(1)} %concatenate.17), channel_id=1, source_target_pairs={{0,1},{1,0},{2,3},{3,2},{4,5},{5,4},{6,7},{7,6},{8,9},{9,8},{10,11... | collective-permute-start | bytes 12296 | tf_op jit(solution)/shard_map/ppermute | solution.py:284
  17.8 1.4 %constant_dynamic-update-slice_fusion.1 = bf16[4096,256]{1,0:T(8,128)(2,1)S(1)} fusion(bf16[4096,128]{1,0:T(8,128)(2,1)} %param.9), kind=kLoop, calls=%fused_computation.6 | loop fusion | bytes 2097152
  19.3 2.6 %collective-permute-start.10 = (bf16[1568,128]{1,0:T(8,128)(2,1)S(1)}, bf16[1568,128]{1,0:T(8,128)(2,1)S(1)}, u32[]{:S(2)}, u32[]{:S(2)}) collective-permute-start(bf16[1568,128]{1,0:T(8,128)(2,1)S(1)} %pad_maximum_fusion), channel_id=1, source_target_pairs={{0,2},{1,31},{2,4},{3,1},{4,6},{5,3},{6,8},{7,5},{8,10},{9,7},{10,... | collective-permute-start | bytes 1204232 | tf_op jit(solution)/shard_map/ppermute | solution.py:284
  22.0 1.5 %constant_dynamic-update-slice_fusion.own_w_ref.main_ref = bf16[4096,256]{1,0:T(8,128)(2,1)S(1)} fusion(bf16[4096,256]{1,0:T(8,128)(2,1)S(1)} %constant_dynamic-update-slice_fusion.1, bf16[4096,128]{1,0:T(8,128)(2,1)} %param.10), kind=kLoop, calls=%fused_computation.5 | loop fusion | bytes 2097152 | tf_op jit(solution)/shard_map/concatenate | solution.py:300
  23.4 1.9 %collective-permute-start = (bf16[4096,256]{1,0:T(8,128)(2,1)S(1)}, bf16[4096,256]{1,0:T(8,128)(2,1)}, u32[]{:S(2)}, u32[]{:S(2)}) collective-permute-start(bf16[4096,256]{1,0:T(8,128)(2,1)S(1)} %constant_dynamic-update-slice_fusion.own_w_ref.main_ref), channel_id=1, source_target_pairs={{0,1},{1,0},{2,3},{3,2},{4,5},{5,4},{6,7},{7,6},{8,9},{9,8},{10,11... | collective-permute-start | bytes 6291464 | tf_op jit(solution)/shard_map/ppermute | solution.py:284
  25.4 2.8 %collective-permute-done.10.refs_5_ = bf16[1568,128]{1,0:T(8,128)(2,1)S(1)} collective-permute-done((bf16[1568,128]{1,0:T(8,128)(2,1)S(1)}, bf16[1568,128]{1,0:T(8,128)(2,1)S(1)}, u32[]{:S(2)}, u32[]{:S(2)}) %collective-permute-start.10) | collective-permute-done | bytes 401440 | tf_op jit(solution)/shard_map/ppermute | solution.py:284
  28.2 3.5 %collective-permute-start.11 = (bf16[1568,128]{1,0:T(8,128)(2,1)S(1)}, bf16[1568,128]{1,0:T(8,128)(2,1)}, u32[]{:S(2)}, u32[]{:S(2)}) collective-permute-start(bf16[1568,128]{1,0:T(8,128)(2,1)S(1)} %collective-permute-done.10.refs_5_), channel_id=1, source_target_pairs={{0,2},{1,31},{2,4},{3,1},{4,6},{5,3},{6,8},{7,5},{8,10},{9,7},{10,... | collective-permute-start | bytes 1204232 | tf_op jit(solution)/shard_map/ppermute | solution.py:284
  33.0 2.0 %collective-permute-start.2 = (bf16[1536,128]{1,0:T(8,128)(2,1)}, bf16[1536,128]{1,0:T(8,128)(2,1)S(1)}, u32[]{:S(2)}, u32[]{:S(2)}) collective-permute-start(bf16[1536,128]{1,0:T(8,128)(2,1)} %collective-permute-done.1.refs_1_), channel_id=1, source_target_pairs={{0,2},{1,31},{2,4},{3,1},{4,6},{5,3},{6,8},{7,5},{8,10},{9,7},{10,... | collective-permute-start | bytes 1179656 | tf_op jit(solution)/shard_map/ppermute | solution.py:284
  35.0 2.3 %collective-permute-done.11.refs_6_ = bf16[1568,128]{1,0:T(8,128)(2,1)} collective-permute-done((bf16[1568,128]{1,0:T(8,128)(2,1)S(1)}, bf16[1568,128]{1,0:T(8,128)(2,1)}, u32[]{:S(2)}, u32[]{:S(2)}) %collective-permute-start.11) | collective-permute-done | bytes 401440 | tf_op jit(solution)/shard_map/ppermute | solution.py:284
  37.2 4.5 %collective-permute-start.12 = (bf16[1568,128]{1,0:T(8,128)(2,1)}, bf16[1568,128]{1,0:T(8,128)(2,1)S(1)}, u32[]{:S(2)}, u32[]{:S(2)}) collective-permute-start(bf16[1568,128]{1,0:T(8,128)(2,1)} %collective-permute-done.11.refs_6_), channel_id=1, source_target_pairs={{0,2},{1,31},{2,4},{3,1},{4,6},{5,3},{6,8},{7,5},{8,10},{9,7},{10,... | collective-permute-start | bytes 1204232 | tf_op jit(solution)/shard_map/ppermute | solution.py:284
  42.0 3.8 %collective-permute-start.3 = (bf16[1536,128]{1,0:T(8,128)(2,1)S(1)}, bf16[1536,128]{1,0:T(8,128)(2,1)S(1)}, u32[]{:S(2)}, u32[]{:S(2)}) collective-permute-start(bf16[1536,128]{1,0:T(8,128)(2,1)S(1)} %collective-permute-done.2.refs_2_), channel_id=1, source_target_pairs={{0,2},{1,31},{2,4},{3,1},{4,6},{5,3},{6,8},{7,5},{8,10},{9,7},{10,... | collective-permute-start | bytes 1179656 | tf_op jit(solution)/shard_map/ppermute | solution.py:284
  46.8 4.9 %collective-permute-start.13 = (bf16[1568,128]{1,0:T(8,128)(2,1)S(1)}, bf16[1568,128]{1,0:T(8,128)(2,1)S(1)}, u32[]{:S(2)}, u32[]{:S(2)}) collective-permute-start(bf16[1568,128]{1,0:T(8,128)(2,1)S(1)} %collective-permute-done.12.refs_7_), channel_id=1, source_target_pairs={{0,2},{1,31},{2,4},{3,1},{4,6},{5,3},{6,8},{7,5},{8,10},{9,7},{10,... | collective-permute-start | bytes 1204232 | tf_op jit(solution)/shard_map/ppermute | solution.py:284
  52.5 3.4 %collective-permute-start.4 = (bf16[1536,128]{1,0:T(8,128)(2,1)S(1)}, bf16[1536,128]{1,0:T(8,128)(2,1)S(1)}, u32[]{:S(2)}, u32[]{:S(2)}) collective-permute-start(bf16[1536,128]{1,0:T(8,128)(2,1)S(1)} %collective-permute-done.3.refs_3_), channel_id=1, source_target_pairs={{0,2},{1,31},{2,4},{3,1},{4,6},{5,3},{6,8},{7,5},{8,10},{9,7},{10,... | collective-permute-start | bytes 1179656 | tf_op jit(solution)/shard_map/ppermute | solution.py:284
  56.7 4.8 %collective-permute-start.14 = (bf16[1568,128]{1,0:T(8,128)(2,1)S(1)}, bf16[1568,128]{1,0:T(8,128)(2,1)S(1)}, u32[]{:S(2)}, u32[]{:S(2)}) collective-permute-start(bf16[1568,128]{1,0:T(8,128)(2,1)S(1)} %collective-permute-done.13.refs_3_), channel_id=1, source_target_pairs={{0,2},{1,31},{2,4},{3,1},{4,6},{5,3},{6,8},{7,5},{8,10},{9,7},{10,... | collective-permute-start | bytes 1204232 | tf_op jit(solution)/shard_map/ppermute | solution.py:284
  62.2 3.5 %collective-permute-start.5 = (bf16[1536,128]{1,0:T(8,128)(2,1)S(1)}, bf16[1536,128]{1,0:T(8,128)(2,1)S(1)}, u32[]{:S(2)}, u32[]{:S(2)}) collective-permute-start(bf16[1536,128]{1,0:T(8,128)(2,1)S(1)} %collective-permute-done.4.refs_0_), channel_id=1, source_target_pairs={{0,2},{1,31},{2,4},{3,1},{4,6},{5,3},{6,8},{7,5},{8,10},{9,7},{10,... | collective-permute-start | bytes 1179656 | tf_op jit(solution)/shard_map/ppermute | solution.py:284
  66.5 4.8 %collective-permute-start.15 = (bf16[1568,128]{1,0:T(8,128)(2,1)S(1)}, bf16[1568,128]{1,0:T(8,128)(2,1)}, u32[]{:S(2)}, u32[]{:S(2)}) collective-permute-start(bf16[1568,128]{1,0:T(8,128)(2,1)S(1)} %collective-permute-done.14.refs_4_), channel_id=1, source_target_pairs={{0,2},{1,31},{2,4},{3,1},{4,6},{5,3},{6,8},{7,5},{8,10},{9,7},{10,... | collective-permute-start | bytes 1204232 | tf_op jit(solution)/shard_map/ppermute | solution.py:284
  72.1 3.4 %collective-permute-start.6 = (bf16[1536,128]{1,0:T(8,128)(2,1)S(1)}, bf16[1536,128]{1,0:T(8,128)(2,1)}, u32[]{:S(2)}, u32[]{:S(2)}) collective-permute-start(bf16[1536,128]{1,0:T(8,128)(2,1)S(1)} %collective-permute-done.5.refs_1_), channel_id=1, source_target_pairs={{0,2},{1,31},{2,4},{3,1},{4,6},{5,3},{6,8},{7,5},{8,10},{9,7},{10,... | collective-permute-start | bytes 1179656 | tf_op jit(solution)/shard_map/ppermute | solution.py:284
  76.3 4.9 %collective-permute-start.16 = (bf16[1568,128]{1,0:T(8,128)(2,1)}, bf16[1568,128]{1,0:T(8,128)(2,1)}, u32[]{:S(2)}, u32[]{:S(2)}) collective-permute-start(bf16[1568,128]{1,0:T(8,128)(2,1)} %collective-permute-done.15.refs_5_), channel_id=1, source_target_pairs={{0,2},{1,31},{2,4},{3,1},{4,6},{5,3},{6,8},{7,5},{8,10},{9,7},{10,... | collective-permute-start | bytes 1204232 | tf_op jit(solution)/shard_map/ppermute | solution.py:284
  81.2 4.2 %collective-permute-start.7 = (bf16[1536,128]{1,0:T(8,128)(2,1)}, bf16[1536,128]{1,0:T(8,128)(2,1)}, u32[]{:S(2)}, u32[]{:S(2)}) collective-permute-start(bf16[1536,128]{1,0:T(8,128)(2,1)} %collective-permute-done.6.refs_2_), channel_id=1, source_target_pairs={{0,2},{1,31},{2,4},{3,1},{4,6},{5,3},{6,8},{7,5},{8,10},{9,7},{10,... | collective-permute-start | bytes 1179656 | tf_op jit(solution)/shard_map/ppermute | solution.py:284
  89.5 3.9 %ring_sums.3 = (f32[1536,256]{1,0:T(8,128)S(1)}, f32[1536,256]{1,0:T(8,128)S(1)}) custom-call(s32[4]{0:T(128)S(1)} %pad_add_fusion.place_ref, bf16[4096,256]{1,0:T(8,128)(2,1)S(1)} %constant_dynamic-update-slice_fusion.own_w_ref.main_ref, bf16[4096,256]{1,0:T(8,128)(2,1)} %collective-permute-done.other_w_ref, bf16[1536,128]{1,0:T(8,128)(2,1)S(1)} %bitcast.7, ...), custom_call_target="tpu_custom_call" | custom-call | flops 1610612736 | tf_op jit(solution)/shard_map/ring_sums/pallas_call | solution.py:91
  93.4 3.6 %ring_sums.4 = (f32[1536,256]{1,0:T(8,128)S(1)}, f32[1536,256]{1,0:T(8,128)S(1)}) custom-call(s32[4]{0:T(128)S(1)} %pad_add_fusion.place_ref, bf16[4096,256]{1,0:T(8,128)(2,1)S(1)} %constant_dynamic-update-slice_fusion.own_w_ref.main_ref, bf16[4096,256]{1,0:T(8,128)(2,1)} %collective-permute-done.other_w_ref, bf16[1536,128]{1,0:T(8,128)(2,1)S(1)} %copy-done.13, ...), custom_call_target="tpu_custom_call" | custom-call | flops 1207959552 | tf_op jit(solution)/shard_map/ring_sums/pallas_call | solution.py:91
  97.1 2.8 %ring_sums.5 = (f32[1536,256]{1,0:T(8,128)S(1)}, f32[1536,256]{1,0:T(8,128)S(1)}) custom-call(s32[4]{0:T(128)S(1)} %pad_add_fusion.place_ref, bf16[4096,256]{1,0:T(8,128)(2,1)S(1)} %constant_dynamic-update-slice_fusion.own_w_ref.main_ref, bf16[4096,256]{1,0:T(8,128)(2,1)} %collective-permute-done.other_w_ref, ...), custom_call_target="tpu_custom_call" | custom-call | flops 402653184 | tf_op jit(solution)/shard_map/ring_sums/pallas_call | solution.py:91
  99.9 8.6 %collective-permute-start.17 = (f32[1536,256]{1,0:T(8,128)S(1)}, f32[1536,256]{1,0:T(8,128)S(1)}, u32[]{:S(2)}, u32[]{:S(2)}) collective-permute-start(f32[1536,256]{1,0:T(8,128)S(1)} %get-tuple-element.20), channel_id=1, source_target_pairs={{0,1},{1,0},{2,3},{3,2},{4,5},{5,4},{6,7},{7,6},{8,9},{9,8},{10,11... | collective-permute-start | bytes 4718600 | tf_op jit(solution)/shard_map/ppermute | solution.py:284
  109.2 4.8 %collective-permute-start.19 = (bf16[1536,128]{1,0:T(8,128)(2,1)}, bf16[1536,128]{1,0:T(8,128)(2,1)S(1)}, u32[]{:S(2)}, u32[]{:S(2)}) collective-permute-start(bf16[1536,128]{1,0:T(8,128)(2,1)} %collective-permute-done.7.refs_0_), channel_id=1, source_target_pairs={{0,2},{1,31},{2,4},{3,1},{4,6},{5,3},{6,8},{7,5},{8,10},{9,7},{10,... | collective-permute-start | bytes 1179656 | tf_op jit(solution)/shard_map/ppermute | solution.py:284
  114.1 1.9 %collective-permute-start.20 = (bf16[1568,128]{1,0:T(8,128)(2,1)}, bf16[1568,128]{1,0:T(8,128)(2,1)S(1)}, u32[]{:S(2)}, u32[]{:S(2)}) collective-permute-start(bf16[1568,128]{1,0:T(8,128)(2,1)} %collective-permute-done.16.refs_1_), channel_id=1, source_target_pairs={{0,2},{1,31},{2,4},{3,1},{4,6},{5,3},{6,8},{7,5},{8,10},{9,7},{10,... | collective-permute-start | bytes 1204232 | tf_op jit(solution)/shard_map/ppermute | solution.py:284
  117.4 1.9 %collective-permute-start.18 = (bf16[224,128]{1,0:T(8,128)(2,1)S(1)}, bf16[224,128]{1,0:T(8,128)(2,1)S(1)}, u32[]{:S(2)}, u32[]{:S(2)}) collective-permute-start(bf16[224,128]{1,0:T(8,128)(2,1)S(1)} %constant_dynamic-update-slice_fusion.2.mine_new_ref), channel_id=1, source_target_pairs={{0,1},{1,0},{2,3},{3,2},{4,5},{5,4},{6,7},{7,6},{8,9},{9,8},{10,11... | collective-permute-start | bytes 172040 | tf_op jit(solution)/shard_map/ppermute | solution.py:284
  119.3 1.2 collective-permute-done.18.theirs_new_ref
  120.5 2.9 %collective-permute-done.20.last_b_ref = bf16[1568,128]{1,0:T(8,128)(2,1)S(1)} collective-permute-done((bf16[1568,128]{1,0:T(8,128)(2,1)}, bf16[1568,128]{1,0:T(8,128)(2,1)S(1)}, u32[]{:S(2)}, u32[]{:S(2)}) %collective-permute-start.20) | collective-permute-done | bytes 401440 | tf_op jit(solution)/shard_map/ppermute | solution.py:284
  123.4 2.2 %span_states.1 = (f32[16,15,128]{2,1,0:T(8,128)S(1)}, f32[16,128]{1,0:T(8,128)S(1)}) custom-call(s32[4]{0:T(128)S(1)} %pad_add_fusion.place_ref, f32[1536,256]{1,0:T(8,128)S(1)} %get-tuple-element.19.total_ref, f32[1536,256]{1,0:T(8,128)S(1)} %collective-permute-done.17.arrived_ref, bf16[32,128]{1,0:T(8,128)(2,1)S(1)} %pad_maximum_fusion.1.here_new_ref, ...), custom_call_target="tpu_custom_call" | custom-call | tf_op jit(solution)/shard_map/span_states/pallas_call | solution.py:197
  125.6 13.4 %all_to_all.5.arrived_ref = f32[16,15,128]{2,1,0:T(8,128)S(1)} all-to-all(f32[16,15,128]{2,1,0:T(8,128)S(1)} %get-tuple-element.24), channel_id=1, replica_groups=mesh['sp'=16,'tp'=32] {'sp'}, dimensions={0} | all-to-all | bytes 245760 | tf_op jit(solution)/shard_map/all_to_all | solution.py:353
  (71 shorter events, 14.7 us)
Async XLA Ops:
  0.6 18.6 %copy-start.16 = (bf16[3,1,128]{2,0,1:T(4,128)(2,1)S(1)}, bf16[3,1,128]{2,0,1:T(4,128)(2,1)}, u32[]{:S(2)}) copy-start(bf16[3,1,128]{2,0,1:T(4,128)(2,1)} %param.7) | copy-start | bytes 2308
  0.6 18.6 %collective-permute-start.8 = (bf16[1536,128]{1,0:T(8,128)(2,1)}, bf16[1536,128]{1,0:T(8,128)(2,1)S(1)}, u32[]{:S(2)}, u32[]{:S(2)}) collective-permute-start(bf16[1536,128]{1,0:T(8,128)(2,1)} %bitcast.5), channel_id=1, source_target_pairs={{0,1},{1,0},{2,3},{3,2},{4,5},{5,4},{6,7},{7,6},{8,9},{9,8},{10,11... | collective-permute-start | bytes 1179656 | tf_op jit(solution)/shard_map/ppermute | solution.py:284
  9.4 23.6 %collective-permute-start.1 = (bf16[1536,128]{1,0:T(8,128)(2,1)}, bf16[1536,128]{1,0:T(8,128)(2,1)}, u32[]{:S(2)}, u32[]{:S(2)}) collective-permute-start(bf16[1536,128]{1,0:T(8,128)(2,1)} %bitcast.6), channel_id=1, source_target_pairs={{0,2},{1,31},{2,4},{3,1},{4,6},{5,3},{6,8},{7,5},{8,10},{9,7},{10,... | collective-permute-start | bytes 1179656 | tf_op jit(solution)/shard_map/ppermute | solution.py:284
  15.9 3.4 %collective-permute-start.9 = (bf16[16,128]{1,0:T(8,128)(2,1)S(1)}, bf16[16,128]{1,0:T(8,128)(2,1)S(1)}, u32[]{:S(2)}, u32[]{:S(2)}) collective-permute-start(bf16[16,128]{1,0:T(8,128)(2,1)S(1)} %concatenate.17), channel_id=1, source_target_pairs={{0,1},{1,0},{2,3},{3,2},{4,5},{5,4},{6,7},{7,6},{8,9},{9,8},{10,11... | collective-permute-start | bytes 12296 | tf_op jit(solution)/shard_map/ppermute | solution.py:284
  19.2 13.6 %copy-start.17 = (f32[2]{0:T(128)S(1)}, f32[2]{0:T(128)}, u32[]{:S(2)}) copy-start(f32[2]{0:T(128)} %param.11) | copy-start | bytes 28
  19.3 8.9 %collective-permute-start.10 = (bf16[1568,128]{1,0:T(8,128)(2,1)S(1)}, bf16[1568,128]{1,0:T(8,128)(2,1)S(1)}, u32[]{:S(2)}, u32[]{:S(2)}) collective-permute-start(bf16[1568,128]{1,0:T(8,128)(2,1)S(1)} %pad_maximum_fusion), channel_id=1, source_target_pairs={{0,2},{1,31},{2,4},{3,1},{4,6},{5,3},{6,8},{7,5},{8,10},{9,7},{10,... | collective-permute-start | bytes 1204232 | tf_op jit(solution)/shard_map/ppermute | solution.py:284
  23.4 62.1 %collective-permute-start = (bf16[4096,256]{1,0:T(8,128)(2,1)S(1)}, bf16[4096,256]{1,0:T(8,128)(2,1)}, u32[]{:S(2)}, u32[]{:S(2)}) collective-permute-start(bf16[4096,256]{1,0:T(8,128)(2,1)S(1)} %constant_dynamic-update-slice_fusion.own_w_ref.main_ref), channel_id=1, source_target_pairs={{0,1},{1,0},{2,3},{3,2},{4,5},{5,4},{6,7},{7,6},{8,9},{9,8},{10,11... | collective-permute-start | bytes 6291464 | tf_op jit(solution)/shard_map/ppermute | solution.py:284
  28.2 9.0 %collective-permute-start.11 = (bf16[1568,128]{1,0:T(8,128)(2,1)S(1)}, bf16[1568,128]{1,0:T(8,128)(2,1)}, u32[]{:S(2)}, u32[]{:S(2)}) collective-permute-start(bf16[1568,128]{1,0:T(8,128)(2,1)S(1)} %collective-permute-done.10.refs_5_), channel_id=1, source_target_pairs={{0,2},{1,31},{2,4},{3,1},{4,6},{5,3},{6,8},{7,5},{8,10},{9,7},{10,... | collective-permute-start | bytes 1204232 | tf_op jit(solution)/shard_map/ppermute | solution.py:284
  33.0 9.0 %collective-permute-start.2 = (bf16[1536,128]{1,0:T(8,128)(2,1)}, bf16[1536,128]{1,0:T(8,128)(2,1)S(1)}, u32[]{:S(2)}, u32[]{:S(2)}) collective-permute-start(bf16[1536,128]{1,0:T(8,128)(2,1)} %collective-permute-done.1.refs_1_), channel_id=1, source_target_pairs={{0,2},{1,31},{2,4},{3,1},{4,6},{5,3},{6,8},{7,5},{8,10},{9,7},{10,... | collective-permute-start | bytes 1179656 | tf_op jit(solution)/shard_map/ppermute | solution.py:284
  37.2 9.6 %collective-permute-start.12 = (bf16[1568,128]{1,0:T(8,128)(2,1)}, bf16[1568,128]{1,0:T(8,128)(2,1)S(1)}, u32[]{:S(2)}, u32[]{:S(2)}) collective-permute-start(bf16[1568,128]{1,0:T(8,128)(2,1)} %collective-permute-done.11.refs_6_), channel_id=1, source_target_pairs={{0,2},{1,31},{2,4},{3,1},{4,6},{5,3},{6,8},{7,5},{8,10},{9,7},{10,... | collective-permute-start | bytes 1204232 | tf_op jit(solution)/shard_map/ppermute | solution.py:284
  42.0 10.5 %collective-permute-start.3 = (bf16[1536,128]{1,0:T(8,128)(2,1)S(1)}, bf16[1536,128]{1,0:T(8,128)(2,1)S(1)}, u32[]{:S(2)}, u32[]{:S(2)}) collective-permute-start(bf16[1536,128]{1,0:T(8,128)(2,1)S(1)} %collective-permute-done.2.refs_2_), channel_id=1, source_target_pairs={{0,2},{1,31},{2,4},{3,1},{4,6},{5,3},{6,8},{7,5},{8,10},{9,7},{10,... | collective-permute-start | bytes 1179656 | tf_op jit(solution)/shard_map/ppermute | solution.py:284
  46.8 9.9 %collective-permute-start.13 = (bf16[1568,128]{1,0:T(8,128)(2,1)S(1)}, bf16[1568,128]{1,0:T(8,128)(2,1)S(1)}, u32[]{:S(2)}, u32[]{:S(2)}) collective-permute-start(bf16[1568,128]{1,0:T(8,128)(2,1)S(1)} %collective-permute-done.12.refs_7_), channel_id=1, source_target_pairs={{0,2},{1,31},{2,4},{3,1},{4,6},{5,3},{6,8},{7,5},{8,10},{9,7},{10,... | collective-permute-start | bytes 1204232 | tf_op jit(solution)/shard_map/ppermute | solution.py:284
  52.5 9.8 %collective-permute-start.4 = (bf16[1536,128]{1,0:T(8,128)(2,1)S(1)}, bf16[1536,128]{1,0:T(8,128)(2,1)S(1)}, u32[]{:S(2)}, u32[]{:S(2)}) collective-permute-start(bf16[1536,128]{1,0:T(8,128)(2,1)S(1)} %collective-permute-done.3.refs_3_), channel_id=1, source_target_pairs={{0,2},{1,31},{2,4},{3,1},{4,6},{5,3},{6,8},{7,5},{8,10},{9,7},{10,... | collective-permute-start | bytes 1179656 | tf_op jit(solution)/shard_map/ppermute | solution.py:284
  56.7 9.8 %collective-permute-start.14 = (bf16[1568,128]{1,0:T(8,128)(2,1)S(1)}, bf16[1568,128]{1,0:T(8,128)(2,1)S(1)}, u32[]{:S(2)}, u32[]{:S(2)}) collective-permute-start(bf16[1568,128]{1,0:T(8,128)(2,1)S(1)} %collective-permute-done.13.refs_3_), channel_id=1, source_target_pairs={{0,2},{1,31},{2,4},{3,1},{4,6},{5,3},{6,8},{7,5},{8,10},{9,7},{10,... | collective-permute-start | bytes 1204232 | tf_op jit(solution)/shard_map/ppermute | solution.py:284
  62.2 9.8 %collective-permute-start.5 = (bf16[1536,128]{1,0:T(8,128)(2,1)S(1)}, bf16[1536,128]{1,0:T(8,128)(2,1)S(1)}, u32[]{:S(2)}, u32[]{:S(2)}) collective-permute-start(bf16[1536,128]{1,0:T(8,128)(2,1)S(1)} %collective-permute-done.4.refs_0_), channel_id=1, source_target_pairs={{0,2},{1,31},{2,4},{3,1},{4,6},{5,3},{6,8},{7,5},{8,10},{9,7},{10,... | collective-permute-start | bytes 1179656 | tf_op jit(solution)/shard_map/ppermute | solution.py:284
  66.5 9.8 %collective-permute-start.15 = (bf16[1568,128]{1,0:T(8,128)(2,1)S(1)}, bf16[1568,128]{1,0:T(8,128)(2,1)}, u32[]{:S(2)}, u32[]{:S(2)}) collective-permute-start(bf16[1568,128]{1,0:T(8,128)(2,1)S(1)} %collective-permute-done.14.refs_4_), channel_id=1, source_target_pairs={{0,2},{1,31},{2,4},{3,1},{4,6},{5,3},{6,8},{7,5},{8,10},{9,7},{10,... | collective-permute-start | bytes 1204232 | tf_op jit(solution)/shard_map/ppermute | solution.py:284
  72.1 9.1 %collective-permute-start.6 = (bf16[1536,128]{1,0:T(8,128)(2,1)S(1)}, bf16[1536,128]{1,0:T(8,128)(2,1)}, u32[]{:S(2)}, u32[]{:S(2)}) collective-permute-start(bf16[1536,128]{1,0:T(8,128)(2,1)S(1)} %collective-permute-done.5.refs_1_), channel_id=1, source_target_pairs={{0,2},{1,31},{2,4},{3,1},{4,6},{5,3},{6,8},{7,5},{8,10},{9,7},{10,... | collective-permute-start | bytes 1179656 | tf_op jit(solution)/shard_map/ppermute | solution.py:284
  76.3 20.8 %collective-permute-start.16 = (bf16[1568,128]{1,0:T(8,128)(2,1)}, bf16[1568,128]{1,0:T(8,128)(2,1)}, u32[]{:S(2)}, u32[]{:S(2)}) collective-permute-start(bf16[1568,128]{1,0:T(8,128)(2,1)} %collective-permute-done.15.refs_5_), channel_id=1, source_target_pairs={{0,2},{1,31},{2,4},{3,1},{4,6},{5,3},{6,8},{7,5},{8,10},{9,7},{10,... | collective-permute-start | bytes 1204232 | tf_op jit(solution)/shard_map/ppermute | solution.py:284
  81.2 15.8 %collective-permute-start.7 = (bf16[1536,128]{1,0:T(8,128)(2,1)}, bf16[1536,128]{1,0:T(8,128)(2,1)}, u32[]{:S(2)}, u32[]{:S(2)}) collective-permute-start(bf16[1536,128]{1,0:T(8,128)(2,1)} %collective-permute-done.6.refs_2_), channel_id=1, source_target_pairs={{0,2},{1,31},{2,4},{3,1},{4,6},{5,3},{6,8},{7,5},{8,10},{9,7},{10,... | collective-permute-start | bytes 1179656 | tf_op jit(solution)/shard_map/ppermute | solution.py:284
  85.5 1.0 copy-start.2
  86.5 1.0 copy-start.7
  87.5 1.0 copy-start.9
  88.5 1.0 copy-start.11
  89.5 3.9 %copy-start.4 = (bf16[1568,128]{1,0:T(8,128)(2,1)S(1)}, bf16[1568,128]{1,0:T(8,128)(2,1)}, u32[]{:S(2)}) copy-start(bf16[1568,128]{1,0:T(8,128)(2,1)} %copy-done.3) | copy-start | bytes 1204228
  89.5 3.9 %copy-start.6 = (bf16[1568,128]{1,0:T(8,128)(2,1)S(1)}, bf16[1568,128]{1,0:T(8,128)(2,1)}, u32[]{:S(2)}) copy-start(bf16[1568,128]{1,0:T(8,128)(2,1)} %copy-done.5) | copy-start | bytes 1204228
  89.5 3.9 %copy-start.13 = (bf16[1536,128]{1,0:T(8,128)(2,1)S(1)}, bf16[1536,128]{1,0:T(8,128)(2,1)}, u32[]{:S(2)}) copy-start(bf16[1536,128]{1,0:T(8,128)(2,1)} %copy-done.12) | copy-start | bytes 1179652
  89.5 3.9 %copy-start.15 = (bf16[1536,128]{1,0:T(8,128)(2,1)S(1)}, bf16[1536,128]{1,0:T(8,128)(2,1)}, u32[]{:S(2)}) copy-start(bf16[1536,128]{1,0:T(8,128)(2,1)} %copy-done.14) | copy-start | bytes 1179652
  97.1 26.3 %copy-start = (bf16[4096,128]{1,0:T(8,128)(2,1)S(1)}, bf16[4096,128]{1,0:T(8,128)(2,1)}, u32[]{:S(2)}) copy-start(bf16[4096,128]{1,0:T(8,128)(2,1)} %query_w_ref.1) | copy-start | bytes 3145732
  99.9 23.5 %collective-permute-start.17 = (f32[1536,256]{1,0:T(8,128)S(1)}, f32[1536,256]{1,0:T(8,128)S(1)}, u32[]{:S(2)}, u32[]{:S(2)}) collective-permute-start(f32[1536,256]{1,0:T(8,128)S(1)} %get-tuple-element.20), channel_id=1, source_target_pairs={{0,1},{1,0},{2,3},{3,2},{4,5},{5,4},{6,7},{7,6},{8,9},{9,8},{10,11... | collective-permute-start | bytes 4718600 | tf_op jit(solution)/shard_map/ppermute | solution.py:284
  109.2 10.1 %collective-permute-start.19 = (bf16[1536,128]{1,0:T(8,128)(2,1)}, bf16[1536,128]{1,0:T(8,128)(2,1)S(1)}, u32[]{:S(2)}, u32[]{:S(2)}) collective-permute-start(bf16[1536,128]{1,0:T(8,128)(2,1)} %collective-permute-done.7.refs_0_), channel_id=1, source_target_pairs={{0,2},{1,31},{2,4},{3,1},{4,6},{5,3},{6,8},{7,5},{8,10},{9,7},{10,... | collective-permute-start | bytes 1179656 | tf_op jit(solution)/shard_map/ppermute | solution.py:284
  114.1 9.3 %collective-permute-start.20 = (bf16[1568,128]{1,0:T(8,128)(2,1)}, bf16[1568,128]{1,0:T(8,128)(2,1)S(1)}, u32[]{:S(2)}, u32[]{:S(2)}) collective-permute-start(bf16[1568,128]{1,0:T(8,128)(2,1)} %collective-permute-done.16.refs_1_), channel_id=1, source_target_pairs={{0,2},{1,31},{2,4},{3,1},{4,6},{5,3},{6,8},{7,5},{8,10},{9,7},{10,... | collective-permute-start | bytes 1204232 | tf_op jit(solution)/shard_map/ppermute | solution.py:284
  117.4 3.1 %collective-permute-start.18 = (bf16[224,128]{1,0:T(8,128)(2,1)S(1)}, bf16[224,128]{1,0:T(8,128)(2,1)S(1)}, u32[]{:S(2)}, u32[]{:S(2)}) collective-permute-start(bf16[224,128]{1,0:T(8,128)(2,1)S(1)} %constant_dynamic-update-slice_fusion.2.mine_new_ref), channel_id=1, source_target_pairs={{0,1},{1,0},{2,3},{3,2},{4,5},{5,4},{6,7},{7,6},{8,9},{9,8},{10,11... | collective-permute-start | bytes 172040 | tf_op jit(solution)/shard_map/ppermute | solution.py:284
  (7 other events, 5.3 us)

commit v6 on v5

--- a/solution.py
+++ b/solution.py
@@ -41,62 +41,81 @@
     return jnp.concatenate(blocks, axis=0)
 
 
-def sums_kernel(offsets, span_len, place_ref, own_w_ref, other_w_ref, *refs):
+def sums_kernel(offsets, span_len, has_before, place_ref, own_w_ref, other_w_ref, *refs):
     count = len(offsets)
     a_refs, b_refs, rest = refs[:count], refs[count : 2 * count], refs[2 * count :]
-    own_ref, other_ref = rest[-2:]
-    before = rest[:-2]
+    before = rest[:2] if has_before else ()
+    own_ref, other_ref, held, landed = rest[len(before) :]
     rows, width = a_refs[0].shape
-    inner = own_ref.shape[1]
+    core = place_ref[1]
     hops = [i for i in range(count) if offsets[i] > 0]
-    own_plane = [i for i in range(count) if offsets[i] == 0]
-
-    def step(s, carry):
-        at = pl.ds(pl.multiple_of(s * span_len, span_len), span_len)
-
-        def gathered(which):
+
+    copies = []
+    for j, i in enumerate(hops):
+        plane = row_block(place_ref, offsets[i])
+        for side, block in enumerate((2 * plane + core, 2 * plane + 1 - core)):
+            slot = 2 * j + side
+            copies.append(
+                pltpu.make_async_copy(
+                    other_w_ref.at[at_rows(block, width), :],
+                    held.at[pl.ds(slot * width, width), :],
+                    landed.at[slot],
+                )
+            )
+    for copy in copies:
+        copy.start()
+
+    def summed(out_ref, earlier, which, weights_of):
+        def step(s, carry):
+            at = pl.ds(pl.multiple_of(s * span_len, span_len), span_len)
             pieces = []
             for i in which:
                 pieces += [a_refs[i][at, :], b_refs[i][at, :]]
-            return jnp.concatenate(pieces, axis=1)
-
-        weights = jnp.concatenate(
-            [
-                stacked(place_ref, own_w_ref, [offsets[i] for i in hops], width),
-                stacked(place_ref, other_w_ref, [offsets[i] for i in hops], width),
-            ],
-            axis=1,
-        )
-        part = jnp.dot(gathered(hops), weights, preferred_element_type=jnp.float32)
-        own, other = part[:, :inner], part[:, inner:]
-        if own_plane:
-            here = stacked(place_ref, own_w_ref, [0], width)
-            own += jnp.dot(gathered(own_plane), here, preferred_element_type=jnp.float32)
-        if before:
-            own += before[0][at, :]
-            other += before[1][at, :]
-        own_ref[at, :] = own
-        other_ref[at, :] = other
-        return carry
-
-    lax.fori_loop(0, rows // span_len, step, 0)
+            both = jnp.concatenate(pieces, axis=1)
+            part = jnp.dot(both, weights_of(), preferred_element_type=jnp.float32)
+            if earlier is not None:
+                part += earlier[at, :]
+            out_ref[at, :] = part
+            return carry
+
+        lax.fori_loop(0, rows // span_len, step, 0)
+
+    summed(
+        own_ref,
+        before[0] if before else None,
+        list(range(count)),
+        lambda: stacked(place_ref, own_w_ref, offsets, width),
+    )
+    for copy in copies:
+        copy.wait()
+    summed(other_ref, before[1] if before else None, hops, lambda: held[...])
 
 
 def ring_sums(offsets, span_len, place, own_weights, other_weights, a_list, b_list, before):
     rows, width = a_list[0].shape
     inner = own_weights.shape[1]
     whole = pl.BlockSpec(memory_space=pltpu.VMEM)
-    operands = [own_weights, other_weights, *a_list, *b_list, *before]
+    operands = [*a_list, *b_list, *before]
+    blocks = 2 * sum(1 for offset in offsets if offset > 0)
     flops = 2 * rows * 2 * inner * 2 * width * len(offsets)
     return pl.pallas_call(
-        functools.partial(sums_kernel, offsets, span_len),
-        in_specs=[pl.BlockSpec(memory_space=pltpu.SMEM)] + [whole] * len(operands),
+        functools.partial(sums_kernel, offsets, span_len, bool(before)),
+        in_specs=[
+            pl.BlockSpec(memory_space=pltpu.SMEM),
+            whole,
+            pl.BlockSpec(memory_space=pltpu.HBM),
+        ]
+        + [whole] * len(operands),
         out_specs=[whole, whole],
         out_shape=[jax.ShapeDtypeStruct((rows, inner), jnp.float32)] * 2,
+        scratch_shapes=[
+            pltpu.VMEM((blocks * width, inner), own_weights.dtype),
+            pltpu.SemaphoreType.DMA((blocks,)),
+        ],
         compiler_params=pltpu.CompilerParams(vmem_limit_bytes=16 * 1024 * 1024),
         cost_estimate=pl.CostEstimate(flops=flops, bytes_accessed=0, transcendentals=0),
         name="ring_sums",
-    )(place, *operands)
+    )(place, own_weights, other_weights, *operands)
 
 
 def state_kernel(
@@ -280,50 +299,59 @@
         for c in range(2)
     ]
 
+    across = [
+        (2 * z + 1 - c, 2 * ((z + (1 if c == 0 else -1)) % planes) + c)
+        for z in range(planes)
+        for c in range(2)
+    ]
+
     def sent(value, pairs):
         return lax.ppermute(value, "tp", pairs)
 
-    chain_a = tokens.reshape(rows, width)
-    new_rows = jnp.concatenate(
-        [new_token[:, 0], jnp.zeros((EXTRA - prompts, width), new_token.dtype)], axis=0
-    )
-    other_tokens = sent(chain_a, partner)
-    other_rows = sent(new_rows, partner)
+    tokens = tokens.reshape(rows, width)
+    chain_a = sent(tokens, onward)
+    chain_b = sent(tokens, across)
+    fresh = new_token[:, 0]
+    other_fresh = sent(new_token, partner)[:, 0]
+    padding = jnp.zeros((EXTRA - prompts, width), new_token.dtype)
     new_pair = jnp.concatenate(
         [
-            jnp.where(core == 0, new_rows, other_rows),
-            jnp.where(core == 0, other_rows, new_rows),
+            jnp.where(core == 0, fresh, other_fresh),
+            padding,
+            jnp.where(core == 0, other_fresh, fresh),
+            padding,
         ],
         axis=0,
     )
-    chain_b = jnp.concatenate([other_tokens, new_pair], axis=0)
+    new_first = sent(new_pair, onward)
     main_weights = jnp.concatenate([key_weight, value_weight], axis=1)
     other_weights = sent(main_weights, partner)
+    other_tokens = sent(tokens, partner)
     cosine, sine = tables(own_index * span_len, span_len, groups * span_len, heads)
     lane_decay = jnp.repeat(log_decay, HD)[None, :]
-
-    a_list, b_list = [chain_a], [other_tokens]
-    new_list = []
-    for step in range(1, reach + 1):
+    chain_a, cosine, sine, lane_decay = lax.optimization_barrier(
+        (chain_a, cosine, sine, lane_decay)
+    )
+
+    a_list, b_list = [tokens, chain_a], [other_tokens, chain_b]
+    new_list = [new_first]
+    chain_b = jnp.concatenate([chain_b, new_first], axis=0)
+    for _ in range(2, reach + 1):
         chain_a = sent(chain_a, onward)
         chain_b = sent(chain_b, onward)
-        if step == 1:
-            chain_a, cosine, sine, lane_decay = lax.optimization_barrier(
-                (chain_a, cosine, sine, lane_decay)
-            )
         a_list.append(chain_a)
         b_list.append(chain_b)
         new_list.append(chain_b[rows:])
     sums = ()
-    for low, high in ((0, 4), (4, 7), (7, 8)):
+    for offsets in ((1, 2), (0, 3, 4), (5, 6), (7,)):
         sums = ring_sums(
-            tuple(range(low, high)),
+            offsets,
             span_len,
             place,
             main_weights,
             other_weights,
-            a_list[low:high],
-            b_list[low:high],
+            [a_list[k] for k in offsets],
+            [b_list[k] for k in offsets],
             sums,
         )
     own, other = sums

time: 141 us -> 137 us (0.972)
  local copies, waits for them, and re-layouts: 15.1 us -> 9.57 us
  waiting for transfers between devices: 9.68 us -> 7.07 us
  starting transfers between devices: 86.1 us -> 88.6 us
  Pallas kernels: 13.3 us -> 15.1 us
    unnamed x43 -> x41, local copies, waits for them, and re-layouts: 12.1 us -> 8.46 us
    ppermute x21 -> x22, waiting for transfers between devices: 9.68 us -> 7.07 us  [sent(): return lax.ppermute(value, 'tp', pairs)]
    ppermute x21 -> x22, starting transfers between devices: 86.1 us -> 88.6 us  [sent(): return lax.ppermute(value, 'tp', pairs)]
    pallas_call x3 -> x4, Pallas kernels: 10.3 us -> 12.1 us  [ring_sums(): pl.pallas_call(functools.partial(sums_kernel, offsets, span_len, bool(bef...]
  transfers between devices with their start and end apart: 21 -> 22, of which waited for: 6 -> 6; matrix products, arithmetic and copies ran while one was open for 5% -> 4% of each run, Pallas kernels for 5% -> 7%
where the time goes in v6:
time: 137 us; the launch traced here: 136 us
  starting transfers between devices  88.6 us (65%)
  Pallas kernels  15.1 us (11%)
  blocking collectives  13.4 us (10%)
  local copies, waits for them, and re-layouts  9.57 us (7%)
  waiting for transfers between devices  7.07 us (5%)
    ppermute x22, starting transfers between devices, sent(): return lax.ppermute(value, 'tp', pairs)  88.6 us
    all_to_all x1, blocking collectives, body(): lax.all_to_all(messages, 'sp', split_axis=0, concat_axis=0, tiled=True)  13.4 us
    pallas_call x4, Pallas kernels, ring_sums(): pl.pallas_call(functools.partial(sums_kernel, offsets, span_len, bool(bef...  12.1 us
    unnamed x41, local copies, waits for them, and re-layouts  8.46 us
    ppermute x22, waiting for transfers between devices, sent(): return lax.ppermute(value, 'tp', pairs)  7.07 us
  transfers between devices with their start and end apart: 22, of which 6 were waited for; matrix products, arithmetic and copies ran while one was open for 4% of the time, Pallas kernels for 7%

profile of v6, /device:TPU:1, one launch (start us, length us, event | category | flops | bytes accessed | tf_op | source)
XLA Modules:
  0.0 136.1 jit_solution(7232385155629909195)
XLA Ops:
  0.6 5.1 %collective-permute-start.8 = (bf16[1536,128]{1,0:T(8,128)(2,1)}, bf16[1536,128]{1,0:T(8,128)(2,1)S(1)}, u32[]{:S(2)}, u32[]{:S(2)}) collective-permute-start(bf16[1536,128]{1,0:T(8,128)(2,1)} %bitcast.8), channel_id=1, source_target_pairs={{1,2},{0,31},{3,4},{2,1},{5,6},{4,3},{7,8},{6,5},{9,10},{8,7},{11,... | collective-permute-start | bytes 1179656 | tf_op jit(solution)/shard_map/ppermute | solution.py:309
  5.7 8.9 %collective-permute-start.1 = (bf16[1536,128]{1,0:T(8,128)(2,1)}, bf16[1536,128]{1,0:T(8,128)(2,1)}, u32[]{:S(2)}, u32[]{:S(2)}) collective-permute-start(bf16[1536,128]{1,0:T(8,128)(2,1)} %bitcast.9), channel_id=1, source_target_pairs={{0,2},{1,31},{2,4},{3,1},{4,6},{5,3},{6,8},{7,5},{8,10},{9,7},{10,... | collective-permute-start | bytes 1179656 | tf_op jit(solution)/shard_map/ppermute | solution.py:309
  14.7 2.3 %collective-permute-start.9 = (bf16[3,1,128]{2,0,1:T(4,128)(2,1)}, bf16[3,1,128]{2,0,1:T(4,128)(2,1)S(1)}, u32[]{:S(2)}, u32[]{:S(2)}) collective-permute-start(bf16[3,1,128]{2,0,1:T(4,128)(2,1)} %param.7), channel_id=1, source_target_pairs={{0,1},{1,0},{2,3},{3,2},{4,5},{5,4},{6,7},{7,6},{8,9},{9,8},{10,11... | collective-permute-start | bytes 2312 | tf_op jit(solution)/shard_map/ppermute | solution.py:309
  17.0 1.4 %constant_dynamic-update-slice_fusion.1 = bf16[4096,256]{1,0:T(8,128)(2,1)S(1)} fusion(bf16[4096,128]{1,0:T(8,128)(2,1)} %param.9), kind=kLoop, calls=%fused_computation.6 | loop fusion | bytes 2097152
  18.7 2.0 %collective-permute-start = (bf16[4096,256]{1,0:T(8,128)(2,1)S(1)}, bf16[4096,256]{1,0:T(8,128)(2,1)}, u32[]{:S(2)}, u32[]{:S(2)}) collective-permute-start(bf16[4096,256]{1,0:T(8,128)(2,1)S(1)} %constant_dynamic-update-slice_fusion.own_w_ref.main_ref), channel_id=1, source_target_pairs={{0,1},{1,0},{2,3},{3,2},{4,5},{5,4},{6,7},{7,6},{8,9},{9,8},{10,11... | collective-permute-start | bytes 6291464 | tf_op jit(solution)/shard_map/ppermute | solution.py:309
  20.8 4.7 %collective-permute-start.10 = (bf16[32,128]{1,0:T(8,128)(2,1)S(1)}, bf16[32,128]{1,0:T(8,128)(2,1)S(1)}, u32[]{:S(2)}, u32[]{:S(2)}) collective-permute-start(bf16[32,128]{1,0:T(8,128)(2,1)S(1)} %pad_maximum_fusion.1.here_new_ref), channel_id=1, source_target_pairs={{0,2},{1,31},{2,4},{3,1},{4,6},{5,3},{6,8},{7,5},{8,10},{9,7},{10,... | collective-permute-start | bytes 24584 | tf_op jit(solution)/shard_map/ppermute | solution.py:309
  26.4 4.8 %collective-permute-start.11 = (bf16[1568,128]{1,0:T(8,128)(2,1)S(1)}, bf16[1568,128]{1,0:T(8,128)(2,1)}, u32[]{:S(2)}, u32[]{:S(2)}) collective-permute-start(bf16[1568,128]{1,0:T(8,128)(2,1)S(1)} %pad_maximum_fusion), channel_id=1, source_target_pairs={{0,2},{1,31},{2,4},{3,1},{4,6},{5,3},{6,8},{7,5},{8,10},{9,7},{10,... | collective-permute-start | bytes 1204232 | tf_op jit(solution)/shard_map/ppermute | solution.py:309
  32.4 1.9 %collective-permute-start.2 = (bf16[1536,128]{1,0:T(8,128)(2,1)}, bf16[1536,128]{1,0:T(8,128)(2,1)S(1)}, u32[]{:S(2)}, u32[]{:S(2)}) collective-permute-start(bf16[1536,128]{1,0:T(8,128)(2,1)} %collective-permute-done.1.refs_0_), channel_id=1, source_target_pairs={{0,2},{1,31},{2,4},{3,1},{4,6},{5,3},{6,8},{7,5},{8,10},{9,7},{10,... | collective-permute-start | bytes 1179656 | tf_op jit(solution)/shard_map/ppermute | solution.py:309
  34.3 1.7 %collective-permute-done.11.refs_3_ = bf16[1568,128]{1,0:T(8,128)(2,1)} collective-permute-done((bf16[1568,128]{1,0:T(8,128)(2,1)S(1)}, bf16[1568,128]{1,0:T(8,128)(2,1)}, u32[]{:S(2)}, u32[]{:S(2)}) %collective-permute-start.11) | collective-permute-done | bytes 401440 | tf_op jit(solution)/shard_map/ppermute | solution.py:309
  36.0 5.1 %collective-permute-start.12 = (bf16[1568,128]{1,0:T(8,128)(2,1)}, bf16[1568,128]{1,0:T(8,128)(2,1)S(1)}, u32[]{:S(2)}, u32[]{:S(2)}) collective-permute-start(bf16[1568,128]{1,0:T(8,128)(2,1)} %collective-permute-done.11.refs_3_), channel_id=1, source_target_pairs={{0,2},{1,31},{2,4},{3,1},{4,6},{5,3},{6,8},{7,5},{8,10},{9,7},{10,... | collective-permute-start | bytes 1204232 | tf_op jit(solution)/shard_map/ppermute | solution.py:309
  41.4 3.8 %collective-permute-start.3 = (bf16[1536,128]{1,0:T(8,128)(2,1)S(1)}, bf16[1536,128]{1,0:T(8,128)(2,1)S(1)}, u32[]{:S(2)}, u32[]{:S(2)}) collective-permute-start(bf16[1536,128]{1,0:T(8,128)(2,1)S(1)} %collective-permute-done.2.refs_1_), channel_id=1, source_target_pairs={{0,2},{1,31},{2,4},{3,1},{4,6},{5,3},{6,8},{7,5},{8,10},{9,7},{10,... | collective-permute-start | bytes 1179656 | tf_op jit(solution)/shard_map/ppermute | solution.py:309
  46.2 4.9 %collective-permute-start.13 = (bf16[1568,128]{1,0:T(8,128)(2,1)S(1)}, bf16[1568,128]{1,0:T(8,128)(2,1)S(1)}, u32[]{:S(2)}, u32[]{:S(2)}) collective-permute-start(bf16[1568,128]{1,0:T(8,128)(2,1)S(1)} %collective-permute-done.12.refs_4_), channel_id=1, source_target_pairs={{0,2},{1,31},{2,4},{3,1},{4,6},{5,3},{6,8},{7,5},{8,10},{9,7},{10,... | collective-permute-start | bytes 1204232 | tf_op jit(solution)/shard_map/ppermute | solution.py:309
  51.1 4.2 %collective-permute-start.4 = (bf16[1536,128]{1,0:T(8,128)(2,1)S(1)}, bf16[1536,128]{1,0:T(8,128)(2,1)S(1)}, u32[]{:S(2)}, u32[]{:S(2)}) collective-permute-start(bf16[1536,128]{1,0:T(8,128)(2,1)S(1)} %collective-permute-done.3.refs_1_), channel_id=1, source_target_pairs={{0,2},{1,31},{2,4},{3,1},{4,6},{5,3},{6,8},{7,5},{8,10},{9,7},{10,... | collective-permute-start | bytes 1179656 | tf_op jit(solution)/shard_map/ppermute | solution.py:309
  56.1 4.8 %collective-permute-start.14 = (bf16[1568,128]{1,0:T(8,128)(2,1)S(1)}, bf16[1568,128]{1,0:T(8,128)(2,1)S(1)}, u32[]{:S(2)}, u32[]{:S(2)}) collective-permute-start(bf16[1568,128]{1,0:T(8,128)(2,1)S(1)} %collective-permute-done.13.refs_5_), channel_id=1, source_target_pairs={{0,2},{1,31},{2,4},{3,1},{4,6},{5,3},{6,8},{7,5},{8,10},{9,7},{10,... | collective-permute-start | bytes 1204232 | tf_op jit(solution)/shard_map/ppermute | solution.py:309
  61.7 3.4 %collective-permute-start.5 = (bf16[1536,128]{1,0:T(8,128)(2,1)S(1)}, bf16[1536,128]{1,0:T(8,128)(2,1)S(1)}, u32[]{:S(2)}, u32[]{:S(2)}) collective-permute-start(bf16[1536,128]{1,0:T(8,128)(2,1)S(1)} %collective-permute-done.4.refs_2_), channel_id=1, source_target_pairs={{0,2},{1,31},{2,4},{3,1},{4,6},{5,3},{6,8},{7,5},{8,10},{9,7},{10,... | collective-permute-start | bytes 1179656 | tf_op jit(solution)/shard_map/ppermute | solution.py:309
  65.9 4.8 %collective-permute-start.15 = (bf16[1568,128]{1,0:T(8,128)(2,1)S(1)}, bf16[1568,128]{1,0:T(8,128)(2,1)}, u32[]{:S(2)}, u32[]{:S(2)}) collective-permute-start(bf16[1568,128]{1,0:T(8,128)(2,1)S(1)} %collective-permute-done.14.refs_2_), channel_id=1, source_target_pairs={{0,2},{1,31},{2,4},{3,1},{4,6},{5,3},{6,8},{7,5},{8,10},{9,7},{10,... | collective-permute-start | bytes 1204232 | tf_op jit(solution)/shard_map/ppermute | solution.py:309
  71.5 3.5 %collective-permute-start.6 = (bf16[1536,128]{1,0:T(8,128)(2,1)S(1)}, bf16[1536,128]{1,0:T(8,128)(2,1)}, u32[]{:S(2)}, u32[]{:S(2)}) collective-permute-start(bf16[1536,128]{1,0:T(8,128)(2,1)S(1)} %collective-permute-done.5.refs_0_), channel_id=1, source_target_pairs={{0,2},{1,31},{2,4},{3,1},{4,6},{5,3},{6,8},{7,5},{8,10},{9,7},{10,... | collective-permute-start | bytes 1179656 | tf_op jit(solution)/shard_map/ppermute | solution.py:309
  75.7 5.2 %collective-permute-start.17 = (bf16[1536,128]{1,0:T(8,128)(2,1)}, bf16[1536,128]{1,0:T(8,128)(2,1)}, u32[]{:S(2)}, u32[]{:S(2)}) collective-permute-start(bf16[1536,128]{1,0:T(8,128)(2,1)} %bitcast.10), channel_id=1, source_target_pairs={{0,1},{1,0},{2,3},{3,2},{4,5},{5,4},{6,7},{7,6},{8,9},{9,8},{10,11... | collective-permute-start | bytes 1179656 | tf_op jit(solution)/shard_map/ppermute | solution.py:309
  80.9 4.9 %collective-permute-start.16 = (bf16[1568,128]{1,0:T(8,128)(2,1)}, bf16[1568,128]{1,0:T(8,128)(2,1)}, u32[]{:S(2)}, u32[]{:S(2)}) collective-permute-start(bf16[1568,128]{1,0:T(8,128)(2,1)} %collective-permute-done.15.refs_3_), channel_id=1, source_target_pairs={{0,2},{1,31},{2,4},{3,1},{4,6},{5,3},{6,8},{7,5},{8,10},{9,7},{10,... | collective-permute-start | bytes 1204232 | tf_op jit(solution)/shard_map/ppermute | solution.py:309
  85.8 2.1 %collective-permute-start.7 = (bf16[1536,128]{1,0:T(8,128)(2,1)}, bf16[1536,128]{1,0:T(8,128)(2,1)}, u32[]{:S(2)}, u32[]{:S(2)}) collective-permute-start(bf16[1536,128]{1,0:T(8,128)(2,1)} %collective-permute-done.6.refs_1_), channel_id=1, source_target_pairs={{0,2},{1,31},{2,4},{3,1},{4,6},{5,3},{6,8},{7,5},{8,10},{9,7},{10,... | collective-permute-start | bytes 1179656 | tf_op jit(solution)/shard_map/ppermute | solution.py:309
  89.1 3.0 %ring_sums.4 = (f32[1536,256]{1,0:T(8,128)S(1)}, f32[1536,256]{1,0:T(8,128)S(1)}) custom-call(s32[4]{0:T(128)S(1)} %pad_add_fusion.place_ref, bf16[4096,256]{1,0:T(8,128)(2,1)S(1)} %constant_dynamic-update-slice_fusion.own_w_ref.main_ref, bf16[4096,256]{1,0:T(8,128)(2,1)} %collective-permute-done.other_w_ref, ...), custom_call_target="tpu_custom_call" | custom-call | flops 805306368 | tf_op jit(solution)/shard_map/ring_sums/pallas_call | solution.py:101
  92.3 3.2 %ring_sums.5 = (f32[1536,256]{1,0:T(8,128)S(1)}, f32[1536,256]{1,0:T(8,128)S(1)}) custom-call(s32[4]{0:T(128)S(1)} %pad_add_fusion.place_ref, bf16[4096,256]{1,0:T(8,128)(2,1)S(1)} %constant_dynamic-update-slice_fusion.own_w_ref.main_ref, bf16[4096,256]{1,0:T(8,128)(2,1)} %collective-permute-done.other_w_ref, bf16[1536,128]{1,0:T(8,128)(2,1)S(1)} %bitcast.11, ...), custom_call_target="tpu_custom_call" | custom-call | flops 1207959552 | tf_op jit(solution)/shard_map/ring_sums/pallas_call | solution.py:101
  95.5 3.0 %ring_sums.6 = (f32[1536,256]{1,0:T(8,128)S(1)}, f32[1536,256]{1,0:T(8,128)S(1)}) custom-call(s32[4]{0:T(128)S(1)} %pad_add_fusion.place_ref, bf16[4096,256]{1,0:T(8,128)(2,1)S(1)} %constant_dynamic-update-slice_fusion.own_w_ref.main_ref, bf16[4096,256]{1,0:T(8,128)(2,1)} %collective-permute-done.other_w_ref, bf16[1536,128]{1,0:T(8,128)(2,1)S(1)} %copy-done.11, ...), custom_call_target="tpu_custom_call" | custom-call | flops 805306368 | tf_op jit(solution)/shard_map/ring_sums/pallas_call | solution.py:101
  98.6 2.8 %ring_sums.7 = (f32[1536,256]{1,0:T(8,128)S(1)}, f32[1536,256]{1,0:T(8,128)S(1)}) custom-call(s32[4]{0:T(128)S(1)} %pad_add_fusion.place_ref, bf16[4096,256]{1,0:T(8,128)(2,1)S(1)} %constant_dynamic-update-slice_fusion.own_w_ref.main_ref, bf16[4096,256]{1,0:T(8,128)(2,1)} %collective-permute-done.other_w_ref, ...), custom_call_target="tpu_custom_call" | custom-call | flops 402653184 | tf_op jit(solution)/shard_map/ring_sums/pallas_call | solution.py:101
  101.4 3.3 %collective-permute-start.18 = (f32[1536,256]{1,0:T(8,128)S(1)}, f32[1536,256]{1,0:T(8,128)S(1)}, u32[]{:S(2)}, u32[]{:S(2)}) collective-permute-start(f32[1536,256]{1,0:T(8,128)S(1)} %get-tuple-element.24), channel_id=1, source_target_pairs={{0,1},{1,0},{2,3},{3,2},{4,5},{5,4},{6,7},{7,6},{8,9},{9,8},{10,11... | collective-permute-start | bytes 4718600 | tf_op jit(solution)/shard_map/ppermute | solution.py:309
  105.5 4.9 %collective-permute-start.20 = (bf16[1536,128]{1,0:T(8,128)(2,1)}, bf16[1536,128]{1,0:T(8,128)(2,1)S(1)}, u32[]{:S(2)}, u32[]{:S(2)}) collective-permute-start(bf16[1536,128]{1,0:T(8,128)(2,1)} %collective-permute-done.7.refs_0_), channel_id=1, source_target_pairs={{0,2},{1,31},{2,4},{3,1},{4,6},{5,3},{6,8},{7,5},{8,10},{9,7},{10,... | collective-permute-start | bytes 1179656 | tf_op jit(solution)/shard_map/ppermute | solution.py:309
  110.3 1.9 %collective-permute-start.21 = (bf16[1568,128]{1,0:T(8,128)(2,1)}, bf16[1568,128]{1,0:T(8,128)(2,1)S(1)}, u32[]{:S(2)}, u32[]{:S(2)}) collective-permute-start(bf16[1568,128]{1,0:T(8,128)(2,1)} %collective-permute-done.16.refs_1_), channel_id=1, source_target_pairs={{0,2},{1,31},{2,4},{3,1},{4,6},{5,3},{6,8},{7,5},{8,10},{9,7},{10,... | collective-permute-start | bytes 1204232 | tf_op jit(solution)/shard_map/ppermute | solution.py:309
  113.7 1.9 %collective-permute-start.19 = (bf16[224,128]{1,0:T(8,128)(2,1)S(1)}, bf16[224,128]{1,0:T(8,128)(2,1)S(1)}, u32[]{:S(2)}, u32[]{:S(2)}) collective-permute-start(bf16[224,128]{1,0:T(8,128)(2,1)S(1)} %constant_dynamic-update-slice_fusion.2.mine_new_ref), channel_id=1, source_target_pairs={{0,1},{1,0},{2,3},{3,2},{4,5},{5,4},{6,7},{7,6},{8,9},{9,8},{10,11... | collective-permute-start | bytes 172040 | tf_op jit(solution)/shard_map/ppermute | solution.py:309
  115.6 1.2 collective-permute-done.19.theirs_new_ref
  116.8 2.9 %collective-permute-done.21.last_b_ref = bf16[1568,128]{1,0:T(8,128)(2,1)S(1)} collective-permute-done((bf16[1568,128]{1,0:T(8,128)(2,1)}, bf16[1568,128]{1,0:T(8,128)(2,1)S(1)}, u32[]{:S(2)}, u32[]{:S(2)}) %collective-permute-start.21) | collective-permute-done | bytes 401440 | tf_op jit(solution)/shard_map/ppermute | solution.py:309
  119.6 2.3 %span_states.1 = (f32[16,15,128]{2,1,0:T(8,128)S(1)}, f32[16,128]{1,0:T(8,128)S(1)}) custom-call(s32[4]{0:T(128)S(1)} %pad_add_fusion.place_ref, f32[1536,256]{1,0:T(8,128)S(1)} %get-tuple-element.23.total_ref, f32[1536,256]{1,0:T(8,128)S(1)} %collective-permute-done.18.arrived_ref, bf16[32,128]{1,0:T(8,128)(2,1)S(1)} %pad_maximum_fusion.1.here_new_ref, ...), custom_call_target="tpu_custom_call" | custom-call | tf_op jit(solution)/shard_map/span_states/pallas_call | solution.py:216
  121.9 13.4 %all_to_all.5.arrived_ref = f32[16,15,128]{2,1,0:T(8,128)S(1)} all-to-all(f32[16,15,128]{2,1,0:T(8,128)S(1)} %get-tuple-element.28), channel_id=1, replica_groups=mesh['sp'=16,'tp'=32] {'sp'}, dimensions={0} | all-to-all | bytes 245760 | tf_op jit(solution)/shard_map/all_to_all | solution.py:381
  (72 shorter events, 11.4 us)
Async XLA Ops:
  0.6 17.7 %copy-start.14 = (bf16[4096,128]{1,0:T(8,128)(2,1)S(1)}, bf16[4096,128]{1,0:T(8,128)(2,1)}, u32[]{:S(2)}) copy-start(bf16[4096,128]{1,0:T(8,128)(2,1)} %param.10) | copy-start | bytes 3145732
  0.6 25.7 %collective-permute-start.8 = (bf16[1536,128]{1,0:T(8,128)(2,1)}, bf16[1536,128]{1,0:T(8,128)(2,1)S(1)}, u32[]{:S(2)}, u32[]{:S(2)}) collective-permute-start(bf16[1536,128]{1,0:T(8,128)(2,1)} %bitcast.8), channel_id=1, source_target_pairs={{1,2},{0,31},{3,4},{2,1},{5,6},{4,3},{7,8},{6,5},{9,10},{8,7},{11,... | collective-permute-start | bytes 1179656 | tf_op jit(solution)/shard_map/ppermute | solution.py:309
  5.7 26.7 %collective-permute-start.1 = (bf16[1536,128]{1,0:T(8,128)(2,1)}, bf16[1536,128]{1,0:T(8,128)(2,1)}, u32[]{:S(2)}, u32[]{:S(2)}) collective-permute-start(bf16[1536,128]{1,0:T(8,128)(2,1)} %bitcast.9), channel_id=1, source_target_pairs={{0,2},{1,31},{2,4},{3,1},{4,6},{5,3},{6,8},{7,5},{8,10},{9,7},{10,... | collective-permute-start | bytes 1179656 | tf_op jit(solution)/shard_map/ppermute | solution.py:309
  14.7 6.1 %collective-permute-start.9 = (bf16[3,1,128]{2,0,1:T(4,128)(2,1)}, bf16[3,1,128]{2,0,1:T(4,128)(2,1)S(1)}, u32[]{:S(2)}, u32[]{:S(2)}) collective-permute-start(bf16[3,1,128]{2,0,1:T(4,128)(2,1)} %param.7), channel_id=1, source_target_pairs={{0,1},{1,0},{2,3},{3,2},{4,5},{5,4},{6,7},{7,6},{8,9},{9,8},{10,11... | collective-permute-start | bytes 2312 | tf_op jit(solution)/shard_map/ppermute | solution.py:309
  18.4 2.4 %copy-start.15 = (bf16[3,1,128]{2,0,1:T(4,128)(2,1)S(1)}, bf16[3,1,128]{2,0,1:T(4,128)(2,1)}, u32[]{:S(2)}) copy-start(bf16[3,1,128]{2,0,1:T(4,128)(2,1)} %param.7) | copy-start | bytes 2308
  18.4 13.8 %copy-start.16 = (f32[2]{0:T(128)S(1)}, f32[2]{0:T(128)}, u32[]{:S(2)}) copy-start(f32[2]{0:T(128)} %param.11) | copy-start | bytes 28
  18.7 69.4 %collective-permute-start = (bf16[4096,256]{1,0:T(8,128)(2,1)S(1)}, bf16[4096,256]{1,0:T(8,128)(2,1)}, u32[]{:S(2)}, u32[]{:S(2)}) collective-permute-start(bf16[4096,256]{1,0:T(8,128)(2,1)S(1)} %constant_dynamic-update-slice_fusion.own_w_ref.main_ref), channel_id=1, source_target_pairs={{0,1},{1,0},{2,3},{3,2},{4,5},{5,4},{6,7},{7,6},{8,9},{9,8},{10,11... | collective-permute-start | bytes 6291464 | tf_op jit(solution)/shard_map/ppermute | solution.py:309
  20.8 5.5 %collective-permute-start.10 = (bf16[32,128]{1,0:T(8,128)(2,1)S(1)}, bf16[32,128]{1,0:T(8,128)(2,1)S(1)}, u32[]{:S(2)}, u32[]{:S(2)}) collective-permute-start(bf16[32,128]{1,0:T(8,128)(2,1)S(1)} %pad_maximum_fusion.1.here_new_ref), channel_id=1, source_target_pairs={{0,2},{1,31},{2,4},{3,1},{4,6},{5,3},{6,8},{7,5},{8,10},{9,7},{10,... | collective-permute-start | bytes 24584 | tf_op jit(solution)/shard_map/ppermute | solution.py:309
  26.4 9.6 %collective-permute-start.11 = (bf16[1568,128]{1,0:T(8,128)(2,1)S(1)}, bf16[1568,128]{1,0:T(8,128)(2,1)}, u32[]{:S(2)}, u32[]{:S(2)}) collective-permute-start(bf16[1568,128]{1,0:T(8,128)(2,1)S(1)} %pad_maximum_fusion), channel_id=1, source_target_pairs={{0,2},{1,31},{2,4},{3,1},{4,6},{5,3},{6,8},{7,5},{8,10},{9,7},{10,... | collective-permute-start | bytes 1204232 | tf_op jit(solution)/shard_map/ppermute | solution.py:309
  32.4 9.0 %collective-permute-start.2 = (bf16[1536,128]{1,0:T(8,128)(2,1)}, bf16[1536,128]{1,0:T(8,128)(2,1)S(1)}, u32[]{:S(2)}, u32[]{:S(2)}) collective-permute-start(bf16[1536,128]{1,0:T(8,128)(2,1)} %collective-permute-done.1.refs_0_), channel_id=1, source_target_pairs={{0,2},{1,31},{2,4},{3,1},{4,6},{5,3},{6,8},{7,5},{8,10},{9,7},{10,... | collective-permute-start | bytes 1179656 | tf_op jit(solution)/shard_map/ppermute | solution.py:309
  36.0 10.2 %collective-permute-start.12 = (bf16[1568,128]{1,0:T(8,128)(2,1)}, bf16[1568,128]{1,0:T(8,128)(2,1)S(1)}, u32[]{:S(2)}, u32[]{:S(2)}) collective-permute-start(bf16[1568,128]{1,0:T(8,128)(2,1)} %collective-permute-done.11.refs_3_), channel_id=1, source_target_pairs={{0,2},{1,31},{2,4},{3,1},{4,6},{5,3},{6,8},{7,5},{8,10},{9,7},{10,... | collective-permute-start | bytes 1204232 | tf_op jit(solution)/shard_map/ppermute | solution.py:309
  41.4 9.7 %collective-permute-start.3 = (bf16[1536,128]{1,0:T(8,128)(2,1)S(1)}, bf16[1536,128]{1,0:T(8,128)(2,1)S(1)}, u32[]{:S(2)}, u32[]{:S(2)}) collective-permute-start(bf16[1536,128]{1,0:T(8,128)(2,1)S(1)} %collective-permute-done.2.refs_1_), channel_id=1, source_target_pairs={{0,2},{1,31},{2,4},{3,1},{4,6},{5,3},{6,8},{7,5},{8,10},{9,7},{10,... | collective-permute-start | bytes 1179656 | tf_op jit(solution)/shard_map/ppermute | solution.py:309
  46.2 9.9 %collective-permute-start.13 = (bf16[1568,128]{1,0:T(8,128)(2,1)S(1)}, bf16[1568,128]{1,0:T(8,128)(2,1)S(1)}, u32[]{:S(2)}, u32[]{:S(2)}) collective-permute-start(bf16[1568,128]{1,0:T(8,128)(2,1)S(1)} %collective-permute-done.12.refs_4_), channel_id=1, source_target_pairs={{0,2},{1,31},{2,4},{3,1},{4,6},{5,3},{6,8},{7,5},{8,10},{9,7},{10,... | collective-permute-start | bytes 1204232 | tf_op jit(solution)/shard_map/ppermute | solution.py:309
  51.1 10.6 %collective-permute-start.4 = (bf16[1536,128]{1,0:T(8,128)(2,1)S(1)}, bf16[1536,128]{1,0:T(8,128)(2,1)S(1)}, u32[]{:S(2)}, u32[]{:S(2)}) collective-permute-start(bf16[1536,128]{1,0:T(8,128)(2,1)S(1)} %collective-permute-done.3.refs_1_), channel_id=1, source_target_pairs={{0,2},{1,31},{2,4},{3,1},{4,6},{5,3},{6,8},{7,5},{8,10},{9,7},{10,... | collective-permute-start | bytes 1179656 | tf_op jit(solution)/shard_map/ppermute | solution.py:309
  56.1 9.8 %collective-permute-start.14 = (bf16[1568,128]{1,0:T(8,128)(2,1)S(1)}, bf16[1568,128]{1,0:T(8,128)(2,1)S(1)}, u32[]{:S(2)}, u32[]{:S(2)}) collective-permute-start(bf16[1568,128]{1,0:T(8,128)(2,1)S(1)} %collective-permute-done.13.refs_5_), channel_id=1, source_target_pairs={{0,2},{1,31},{2,4},{3,1},{4,6},{5,3},{6,8},{7,5},{8,10},{9,7},{10,... | collective-permute-start | bytes 1204232 | tf_op jit(solution)/shard_map/ppermute | solution.py:309
  61.7 9.8 %collective-permute-start.5 = (bf16[1536,128]{1,0:T(8,128)(2,1)S(1)}, bf16[1536,128]{1,0:T(8,128)(2,1)S(1)}, u32[]{:S(2)}, u32[]{:S(2)}) collective-permute-start(bf16[1536,128]{1,0:T(8,128)(2,1)S(1)} %collective-permute-done.4.refs_2_), channel_id=1, source_target_pairs={{0,2},{1,31},{2,4},{3,1},{4,6},{5,3},{6,8},{7,5},{8,10},{9,7},{10,... | collective-permute-start | bytes 1179656 | tf_op jit(solution)/shard_map/ppermute | solution.py:309
  65.9 15.0 %collective-permute-start.15 = (bf16[1568,128]{1,0:T(8,128)(2,1)S(1)}, bf16[1568,128]{1,0:T(8,128)(2,1)}, u32[]{:S(2)}, u32[]{:S(2)}) collective-permute-start(bf16[1568,128]{1,0:T(8,128)(2,1)S(1)} %collective-permute-done.14.refs_2_), channel_id=1, source_target_pairs={{0,2},{1,31},{2,4},{3,1},{4,6},{5,3},{6,8},{7,5},{8,10},{9,7},{10,... | collective-permute-start | bytes 1204232 | tf_op jit(solution)/shard_map/ppermute | solution.py:309
  71.5 14.3 %collective-permute-start.6 = (bf16[1536,128]{1,0:T(8,128)(2,1)S(1)}, bf16[1536,128]{1,0:T(8,128)(2,1)}, u32[]{:S(2)}, u32[]{:S(2)}) collective-permute-start(bf16[1536,128]{1,0:T(8,128)(2,1)S(1)} %collective-permute-done.5.refs_0_), channel_id=1, source_target_pairs={{0,2},{1,31},{2,4},{3,1},{4,6},{5,3},{6,8},{7,5},{8,10},{9,7},{10,... | collective-permute-start | bytes 1179656 | tf_op jit(solution)/shard_map/ppermute | solution.py:309
  75.7 16.5 %collective-permute-start.17 = (bf16[1536,128]{1,0:T(8,128)(2,1)}, bf16[1536,128]{1,0:T(8,128)(2,1)}, u32[]{:S(2)}, u32[]{:S(2)}) collective-permute-start(bf16[1536,128]{1,0:T(8,128)(2,1)} %bitcast.10), channel_id=1, source_target_pairs={{0,1},{1,0},{2,3},{3,2},{4,5},{5,4},{6,7},{7,6},{8,9},{9,8},{10,11... | collective-permute-start | bytes 1179656 | tf_op jit(solution)/shard_map/ppermute | solution.py:309
  80.9 17.6 %collective-permute-start.16 = (bf16[1568,128]{1,0:T(8,128)(2,1)}, bf16[1568,128]{1,0:T(8,128)(2,1)}, u32[]{:S(2)}, u32[]{:S(2)}) collective-permute-start(bf16[1568,128]{1,0:T(8,128)(2,1)} %collective-permute-done.15.refs_3_), channel_id=1, source_target_pairs={{0,2},{1,31},{2,4},{3,1},{4,6},{5,3},{6,8},{7,5},{8,10},{9,7},{10,... | collective-permute-start | bytes 1204232 | tf_op jit(solution)/shard_map/ppermute | solution.py:309
  85.8 12.7 %collective-permute-start.7 = (bf16[1536,128]{1,0:T(8,128)(2,1)}, bf16[1536,128]{1,0:T(8,128)(2,1)}, u32[]{:S(2)}, u32[]{:S(2)}) collective-permute-start(bf16[1536,128]{1,0:T(8,128)(2,1)} %collective-permute-done.6.refs_1_), channel_id=1, source_target_pairs={{0,2},{1,31},{2,4},{3,1},{4,6},{5,3},{6,8},{7,5},{8,10},{9,7},{10,... | collective-permute-start | bytes 1179656 | tf_op jit(solution)/shard_map/ppermute | solution.py:309
  88.0 4.2 %copy-start.2 = (bf16[1568,128]{1,0:T(8,128)(2,1)S(1)}, bf16[1568,128]{1,0:T(8,128)(2,1)}, u32[]{:S(2)}) copy-start(bf16[1568,128]{1,0:T(8,128)(2,1)} %copy-done.1) | copy-start | bytes 1204228
  88.0 4.2 %copy-start.5 = (bf16[3,512,128]{2,1,0:T(8,128)(2,1)S(1)}, bf16[3,512,128]{2,1,0:T(8,128)(2,1)}, u32[]{:S(2)}) copy-start(bf16[3,512,128]{2,1,0:T(8,128)(2,1)} %param.6) | copy-start | bytes 1179652
  88.0 4.2 %copy-start.7 = (bf16[1536,128]{1,0:T(8,128)(2,1)S(1)}, bf16[1536,128]{1,0:T(8,128)(2,1)}, u32[]{:S(2)}) copy-start(bf16[1536,128]{1,0:T(8,128)(2,1)} %copy-done.6) | copy-start | bytes 1179652
  88.0 4.2 %copy-start.9 = (bf16[1536,128]{1,0:T(8,128)(2,1)S(1)}, bf16[1536,128]{1,0:T(8,128)(2,1)}, u32[]{:S(2)}) copy-start(bf16[1536,128]{1,0:T(8,128)(2,1)} %copy-done.8) | copy-start | bytes 1179652
  92.2 3.3 %copy-start.4 = (bf16[1568,128]{1,0:T(8,128)(2,1)S(1)}, bf16[1568,128]{1,0:T(8,128)(2,1)}, u32[]{:S(2)}) copy-start(bf16[1568,128]{1,0:T(8,128)(2,1)} %copy-done.3) | copy-start | bytes 1204228
  92.2 3.3 %copy-start.11 = (bf16[1536,128]{1,0:T(8,128)(2,1)S(1)}, bf16[1536,128]{1,0:T(8,128)(2,1)}, u32[]{:S(2)}) copy-start(bf16[1536,128]{1,0:T(8,128)(2,1)} %copy-done.10) | copy-start | bytes 1179652
  98.6 21.1 %copy-start = (bf16[4096,128]{1,0:T(8,128)(2,1)S(1)}, bf16[4096,128]{1,0:T(8,128)(2,1)}, u32[]{:S(2)}) copy-start(bf16[4096,128]{1,0:T(8,128)(2,1)} %query_w_ref.1) | copy-start | bytes 3145732
  101.4 18.3 %collective-permute-start.18 = (f32[1536,256]{1,0:T(8,128)S(1)}, f32[1536,256]{1,0:T(8,128)S(1)}, u32[]{:S(2)}, u32[]{:S(2)}) collective-permute-start(f32[1536,256]{1,0:T(8,128)S(1)} %get-tuple-element.24), channel_id=1, source_target_pairs={{0,1},{1,0},{2,3},{3,2},{4,5},{5,4},{6,7},{7,6},{8,9},{9,8},{10,11... | collective-permute-start | bytes 4718600 | tf_op jit(solution)/shard_map/ppermute | solution.py:309
  105.5 11.3 %collective-permute-start.20 = (bf16[1536,128]{1,0:T(8,128)(2,1)}, bf16[1536,128]{1,0:T(8,128)(2,1)S(1)}, u32[]{:S(2)}, u32[]{:S(2)}) collective-permute-start(bf16[1536,128]{1,0:T(8,128)(2,1)} %collective-permute-done.7.refs_0_), channel_id=1, source_target_pairs={{0,2},{1,31},{2,4},{3,1},{4,6},{5,3},{6,8},{7,5},{8,10},{9,7},{10,... | collective-permute-start | bytes 1179656 | tf_op jit(solution)/shard_map/ppermute | solution.py:309
  110.3 9.3 %collective-permute-start.21 = (bf16[1568,128]{1,0:T(8,128)(2,1)}, bf16[1568,128]{1,0:T(8,128)(2,1)S(1)}, u32[]{:S(2)}, u32[]{:S(2)}) collective-permute-start(bf16[1568,128]{1,0:T(8,128)(2,1)} %collective-permute-done.16.refs_1_), channel_id=1, source_target_pairs={{0,2},{1,31},{2,4},{3,1},{4,6},{5,3},{6,8},{7,5},{8,10},{9,7},{10,... | collective-permute-start | bytes 1204232 | tf_op jit(solution)/shard_map/ppermute | solution.py:309
  113.7 3.1 %collective-permute-start.19 = (bf16[224,128]{1,0:T(8,128)(2,1)S(1)}, bf16[224,128]{1,0:T(8,128)(2,1)S(1)}, u32[]{:S(2)}, u32[]{:S(2)}) collective-permute-start(bf16[224,128]{1,0:T(8,128)(2,1)S(1)} %constant_dynamic-update-slice_fusion.2.mine_new_ref), channel_id=1, source_target_pairs={{0,1},{1,0},{2,3},{3,2},{4,5},{5,4},{6,7},{7,6},{8,9},{9,8},{10,11... | collective-permute-start | bytes 172040 | tf_op jit(solution)/shard_map/ppermute | solution.py:309
  (7 other events, 5.6 us)

commit v7 on v6

--- a/solution.py
+++ b/solution.py
@@ -19,6 +19,26 @@
     back = pltpu.roll(values, lanes - quarter, len(values.shape) - 1)
     ahead = pltpu.roll(values, quarter, len(values.shape) - 1)
     return jnp.where(lane % HD < quarter, back, ahead)
+
+
+def beside_kernel(left_ref, right_ref, out_ref):
+    width = left_ref.shape[1]
+    out_ref[:, :width] = left_ref[...]
+    out_ref[:, width:] = right_ref[...]
+
+
+def beside(left, right):
+    rows, width = left.shape
+    whole = pl.BlockSpec(memory_space=pltpu.VMEM)
+    return pl.pallas_call(
+        beside_kernel,
+        in_specs=[whole, whole],
+        out_specs=whole,
+        out_shape=jax.ShapeDtypeStruct((rows, 2 * width), left.dtype),
+        compiler_params=pltpu.CompilerParams(vmem_limit_bytes=6 * 1024 * 1024),
+        cost_estimate=pl.CostEstimate(flops=10**8, bytes_accessed=0, transcendentals=0),
+        name="beside",
+    )(left, right)
 
 
 def row_block(place_ref, offset):
@@ -112,7 +132,7 @@
             pltpu.VMEM((blocks * width, inner), own_weights.dtype),
             pltpu.SemaphoreType.DMA((blocks,)),
         ],
-        compiler_params=pltpu.CompilerParams(vmem_limit_bytes=16 * 1024 * 1024),
+        compiler_params=pltpu.CompilerParams(vmem_limit_bytes=6 * 1024 * 1024),
         cost_estimate=pl.CostEstimate(flops=flops, bytes_accessed=0, transcendentals=0),
         name="ring_sums",
     )(place, own_weights, other_weights, *operands)
@@ -221,7 +241,7 @@
             jax.ShapeDtypeStruct((groups, prompts * (keep + 1), inner), jnp.float32),
             jax.ShapeDtypeStruct((EXTRA, inner), jnp.float32),
         ],
-        compiler_params=pltpu.CompilerParams(vmem_limit_bytes=24 * 1024 * 1024),
+        compiler_params=pltpu.CompilerParams(vmem_limit_bytes=8 * 1024 * 1024),
         name="span_states",
     )(place, *operands)
 
@@ -324,18 +344,24 @@
         axis=0,
     )
     new_first = sent(new_pair, onward)
-    main_weights = jnp.concatenate([key_weight, value_weight], axis=1)
+    a_list, b_list = [tokens, chain_a], [None, chain_b]
+    new_list = [new_first]
+    chain_a, first_position, log_decay = lax.optimization_barrier(
+        (chain_a, own_index * span_len, log_decay)
+    )
+    a_list[1] = chain_a
+    cosine, sine = tables(first_position, span_len, groups * span_len, heads)
+    lane_decay = jnp.repeat(log_decay, HD)[None, :]
+    new_first, cosine, sine, lane_decay = lax.optimization_barrier(
+        (new_first, cosine, sine, lane_decay)
+    )
+    chain_b = jnp.concatenate([chain_b, new_first], axis=0)
+    key_weight, value_weight, chain_b = lax.optimization_barrier(
+        (key_weight, value_weight, chain_b)
+    )
+    main_weights = beside(key_weight, value_weight)
     other_weights = sent(main_weights, partner)
-    other_tokens = sent(tokens, partner)
-    cosine, sine = tables(own_index * span_len, span_len, groups * span_len, heads)
-    lane_decay = jnp.repeat(log_decay, HD)[None, :]
-    chain_a, cosine, sine, lane_decay = lax.optimization_barrier(
-        (chain_a, cosine, sine, lane_decay)
-    )
-
-    a_list, b_list = [tokens, chain_a], [other_tokens, chain_b]
-    new_list = [new_first]
-    chain_b = jnp.concatenate([chain_b, new_first], axis=0)
+    b_list[0] = sent(tokens, partner)
     for _ in range(2, reach + 1):
         chain_a = sent(chain_a, onward)
         chain_b = sent(chain_b, onward)

time: 137 us -> 139 us (1.015)
  starting transfers between devices: 88.6 us -> 85 us
  local copies, waits for them, and re-layouts: 9.57 us -> 12.7 us
    ppermute x22, starting transfers between devices: 88.6 us -> 85 us  [sent(): return lax.ppermute(value, 'tp', pairs)]
    unnamed x41 -> x40, local copies, waits for them, and re-layouts: 8.46 us -> 11.2 us
  transfers between devices with their start and end apart: 22 -> 22, of which waited for: 6 -> 5; matrix products, arithmetic and copies ran while one was open for 4% -> 3% of each run, Pallas kernels for 7% -> 7%
where the time goes in v7:
time: 139 us; the launch traced here: 137 us
  starting transfers between devices  85 us (61%)
  Pallas kernels  15.5 us (11%)
  blocking collectives  13.4 us (10%)
  local copies, waits for them, and re-layouts  12.7 us (9%)
  waiting for transfers between devices  7.78 us (6%)
  other arithmetic  1.83 us (1%)
    ppermute x22, starting transfers between devices, sent(): return lax.ppermute(value, 'tp', pairs)  85 us
    all_to_all x1, blocking collectives, body(): lax.all_to_all(messages, 'sp', split_axis=0, concat_axis=0, tiled=True)  13.4 us
    pallas_call x4, Pallas kernels, ring_sums(): pl.pallas_call(functools.partial(sums_kernel, offsets, span_len, bool(bef...  12.1 us
    unnamed x40, local copies, waits for them, and re-layouts  11.2 us
    ppermute x22, waiting for transfers between devices, sent(): return lax.ppermute(value, 'tp', pairs)  7.78 us
  transfers between devices with their start and end apart: 22, of which 5 were waited for; matrix products, arithmetic and copies ran while one was open for 3% of the time, Pallas kernels for 7%

profile of v7, /device:TPU:1, one launch (start us, length us, event | category | flops | bytes accessed | tf_op | source)
XLA Modules:
  0.0 137.4 jit_solution(16586414684074802547)
XLA Ops:
  0.6 11.9 %collective-permute-start.3 = (bf16[1536,128]{1,0:T(8,128)(2,1)}, bf16[1536,128]{1,0:T(8,128)(2,1)}, u32[]{:S(2)}, u32[]{:S(2)}) collective-permute-start(bf16[1536,128]{1,0:T(8,128)(2,1)} %bitcast.3.refs_0_), channel_id=1, source_target_pairs={{0,2},{1,31},{2,4},{3,1},{4,6},{5,3},{6,8},{7,5},{8,10},{9,7},{10,... | collective-permute-start | bytes 1179656 | tf_op jit(solution)/shard_map/ppermute | solution.py:329
  12.6 1.9 %collective-permute-start = (bf16[1536,128]{1,0:T(8,128)(2,1)}, bf16[1536,128]{1,0:T(8,128)(2,1)S(1)}, u32[]{:S(2)}, u32[]{:S(2)}) collective-permute-start(bf16[1536,128]{1,0:T(8,128)(2,1)} %bitcast.3.refs_0_), channel_id=1, source_target_pairs={{1,2},{0,31},{3,4},{2,1},{5,6},{4,3},{7,8},{6,5},{9,10},{8,7},{11,... | collective-permute-start | bytes 1179656 | tf_op jit(solution)/shard_map/ppermute | solution.py:329
  14.5 3.0 %collective-permute-start.1 = (bf16[3,1,128]{2,0,1:T(4,128)(2,1)}, bf16[3,1,128]{2,0,1:T(4,128)(2,1)S(1)}, u32[]{:S(2)}, u32[]{:S(2)}) collective-permute-start(bf16[3,1,128]{2,0,1:T(4,128)(2,1)} %param.7), channel_id=1, source_target_pairs={{0,1},{1,0},{2,3},{3,2},{4,5},{5,4},{6,7},{7,6},{8,9},{9,8},{10,11... | collective-permute-start | bytes 2312 | tf_op jit(solution)/shard_map/ppermute | solution.py:329
  19.2 2.6 %collective-permute-start.2 = (bf16[32,128]{1,0:T(8,128)(2,1)S(1)}, bf16[32,128]{1,0:T(8,128)(2,1)S(1)}, u32[]{:S(2)}, u32[]{:S(2)}) collective-permute-start(bf16[32,128]{1,0:T(8,128)(2,1)S(1)} %pad_maximum_fusion.1.here_new_ref), channel_id=1, source_target_pairs={{0,2},{1,31},{2,4},{3,1},{4,6},{5,3},{6,8},{7,5},{8,10},{9,7},{10,... | collective-permute-start | bytes 24584 | tf_op jit(solution)/shard_map/ppermute | solution.py:329
  23.8 3.7 %collective-permute-start.11 = (bf16[1568,128]{1,0:T(8,128)(2,1)S(1)}, bf16[1568,128]{1,0:T(8,128)(2,1)S(1)}, u32[]{:S(2)}, u32[]{:S(2)}) collective-permute-start(bf16[1568,128]{1,0:T(8,128)(2,1)S(1)} %pad_maximum_fusion), channel_id=1, source_target_pairs={{0,2},{1,31},{2,4},{3,1},{4,6},{5,3},{6,8},{7,5},{8,10},{9,7},{10,... | collective-permute-start | bytes 1204232 | tf_op jit(solution)/shard_map/ppermute | solution.py:329
  27.5 1.2 copy-done.1
  28.8 1.2 copy-done.2
  30.3 2.7 %collective-permute-start.4 = (bf16[4096,256]{1,0:T(8,128)(2,1)S(1)}, bf16[4096,256]{1,0:T(8,128)(2,1)}, u32[]{:S(2)}, u32[]{:S(2)}) collective-permute-start(bf16[4096,256]{1,0:T(8,128)(2,1)S(1)} %beside.1.own_w_ref.main_ref), channel_id=1, source_target_pairs={{0,1},{1,0},{2,3},{3,2},{4,5},{5,4},{6,7},{7,6},{8,9},{9,8},{10,11... | collective-permute-start | bytes 6291464 | tf_op jit(solution)/shard_map/ppermute | solution.py:329
  33.0 4.9 %collective-permute-start.5 = (bf16[1536,128]{1,0:T(8,128)(2,1)}, bf16[1536,128]{1,0:T(8,128)(2,1)S(1)}, u32[]{:S(2)}, u32[]{:S(2)}) collective-permute-start(bf16[1536,128]{1,0:T(8,128)(2,1)} %collective-permute-done.3.refs_0_), channel_id=1, source_target_pairs={{0,2},{1,31},{2,4},{3,1},{4,6},{5,3},{6,8},{7,5},{8,10},{9,7},{10,... | collective-permute-start | bytes 1179656 | tf_op jit(solution)/shard_map/ppermute | solution.py:329
  37.9 1.9 %collective-permute-start.12 = (bf16[1568,128]{1,0:T(8,128)(2,1)S(1)}, bf16[1568,128]{1,0:T(8,128)(2,1)S(1)}, u32[]{:S(2)}, u32[]{:S(2)}) collective-permute-start(bf16[1568,128]{1,0:T(8,128)(2,1)S(1)} %collective-permute-done.11.refs_3_), channel_id=1, source_target_pairs={{0,2},{1,31},{2,4},{3,1},{4,6},{5,3},{6,8},{7,5},{8,10},{9,7},{10,... | collective-permute-start | bytes 1204232 | tf_op jit(solution)/shard_map/ppermute | solution.py:329
  40.6 2.3 %collective-permute-done.5.refs_1_ = bf16[1536,128]{1,0:T(8,128)(2,1)S(1)} collective-permute-done((bf16[1536,128]{1,0:T(8,128)(2,1)}, bf16[1536,128]{1,0:T(8,128)(2,1)S(1)}, u32[]{:S(2)}, u32[]{:S(2)}) %collective-permute-start.5) | collective-permute-done | bytes 393248 | tf_op jit(solution)/shard_map/ppermute | solution.py:329
  42.9 4.9 %collective-permute-start.6 = (bf16[1536,128]{1,0:T(8,128)(2,1)S(1)}, bf16[1536,128]{1,0:T(8,128)(2,1)S(1)}, u32[]{:S(2)}, u32[]{:S(2)}) collective-permute-start(bf16[1536,128]{1,0:T(8,128)(2,1)S(1)} %collective-permute-done.5.refs_1_), channel_id=1, source_target_pairs={{0,2},{1,31},{2,4},{3,1},{4,6},{5,3},{6,8},{7,5},{8,10},{9,7},{10,... | collective-permute-start | bytes 1179656 | tf_op jit(solution)/shard_map/ppermute | solution.py:329
  48.6 3.5 %collective-permute-start.13 = (bf16[1568,128]{1,0:T(8,128)(2,1)S(1)}, bf16[1568,128]{1,0:T(8,128)(2,1)S(1)}, u32[]{:S(2)}, u32[]{:S(2)}) collective-permute-start(bf16[1568,128]{1,0:T(8,128)(2,1)S(1)} %collective-permute-done.12.refs_4_), channel_id=1, source_target_pairs={{0,2},{1,31},{2,4},{3,1},{4,6},{5,3},{6,8},{7,5},{8,10},{9,7},{10,... | collective-permute-start | bytes 1204232 | tf_op jit(solution)/shard_map/ppermute | solution.py:329
  52.5 5.0 %collective-permute-start.7 = (bf16[1536,128]{1,0:T(8,128)(2,1)S(1)}, bf16[1536,128]{1,0:T(8,128)(2,1)S(1)}, u32[]{:S(2)}, u32[]{:S(2)}) collective-permute-start(bf16[1536,128]{1,0:T(8,128)(2,1)S(1)} %collective-permute-done.6.refs_1_), channel_id=1, source_target_pairs={{0,2},{1,31},{2,4},{3,1},{4,6},{5,3},{6,8},{7,5},{8,10},{9,7},{10,... | collective-permute-start | bytes 1179656 | tf_op jit(solution)/shard_map/ppermute | solution.py:329
  58.3 3.6 %collective-permute-start.14 = (bf16[1568,128]{1,0:T(8,128)(2,1)S(1)}, bf16[1568,128]{1,0:T(8,128)(2,1)S(1)}, u32[]{:S(2)}, u32[]{:S(2)}) collective-permute-start(bf16[1568,128]{1,0:T(8,128)(2,1)S(1)} %collective-permute-done.13.refs_5_), channel_id=1, source_target_pairs={{0,2},{1,31},{2,4},{3,1},{4,6},{5,3},{6,8},{7,5},{8,10},{9,7},{10,... | collective-permute-start | bytes 1204232 | tf_op jit(solution)/shard_map/ppermute | solution.py:329
  62.7 4.6 %collective-permute-start.8 = (bf16[1536,128]{1,0:T(8,128)(2,1)S(1)}, bf16[1536,128]{1,0:T(8,128)(2,1)S(1)}, u32[]{:S(2)}, u32[]{:S(2)}) collective-permute-start(bf16[1536,128]{1,0:T(8,128)(2,1)S(1)} %collective-permute-done.7.refs_2_), channel_id=1, source_target_pairs={{0,2},{1,31},{2,4},{3,1},{4,6},{5,3},{6,8},{7,5},{8,10},{9,7},{10,... | collective-permute-start | bytes 1179656 | tf_op jit(solution)/shard_map/ppermute | solution.py:329
  68.0 3.7 %collective-permute-start.15 = (bf16[1568,128]{1,0:T(8,128)(2,1)S(1)}, bf16[1568,128]{1,0:T(8,128)(2,1)}, u32[]{:S(2)}, u32[]{:S(2)}) collective-permute-start(bf16[1568,128]{1,0:T(8,128)(2,1)S(1)} %collective-permute-done.14.refs_2_), channel_id=1, source_target_pairs={{0,2},{1,31},{2,4},{3,1},{4,6},{5,3},{6,8},{7,5},{8,10},{9,7},{10,... | collective-permute-start | bytes 1204232 | tf_op jit(solution)/shard_map/ppermute | solution.py:329
  72.5 4.5 %collective-permute-start.9 = (bf16[1536,128]{1,0:T(8,128)(2,1)S(1)}, bf16[1536,128]{1,0:T(8,128)(2,1)}, u32[]{:S(2)}, u32[]{:S(2)}) collective-permute-start(bf16[1536,128]{1,0:T(8,128)(2,1)S(1)} %collective-permute-done.8.refs_0_), channel_id=1, source_target_pairs={{0,2},{1,31},{2,4},{3,1},{4,6},{5,3},{6,8},{7,5},{8,10},{9,7},{10,... | collective-permute-start | bytes 1179656 | tf_op jit(solution)/shard_map/ppermute | solution.py:329
  77.8 3.6 %collective-permute-start.17 = (bf16[1536,128]{1,0:T(8,128)(2,1)}, bf16[1536,128]{1,0:T(8,128)(2,1)}, u32[]{:S(2)}, u32[]{:S(2)}) collective-permute-start(bf16[1536,128]{1,0:T(8,128)(2,1)} %bitcast.3.refs_0_), channel_id=1, source_target_pairs={{0,1},{1,0},{2,3},{3,2},{4,5},{5,4},{6,7},{7,6},{8,9},{9,8},{10,11... | collective-permute-start | bytes 1179656 | tf_op jit(solution)/shard_map/ppermute | solution.py:329
  81.4 4.9 %collective-permute-start.16 = (bf16[1568,128]{1,0:T(8,128)(2,1)}, bf16[1568,128]{1,0:T(8,128)(2,1)}, u32[]{:S(2)}, u32[]{:S(2)}) collective-permute-start(bf16[1568,128]{1,0:T(8,128)(2,1)} %collective-permute-done.15.refs_3_), channel_id=1, source_target_pairs={{0,2},{1,31},{2,4},{3,1},{4,6},{5,3},{6,8},{7,5},{8,10},{9,7},{10,... | collective-permute-start | bytes 1204232 | tf_op jit(solution)/shard_map/ppermute | solution.py:329
  86.2 1.9 %collective-permute-start.10 = (bf16[1536,128]{1,0:T(8,128)(2,1)}, bf16[1536,128]{1,0:T(8,128)(2,1)}, u32[]{:S(2)}, u32[]{:S(2)}) collective-permute-start(bf16[1536,128]{1,0:T(8,128)(2,1)} %collective-permute-done.9.refs_1_), channel_id=1, source_target_pairs={{0,2},{1,31},{2,4},{3,1},{4,6},{5,3},{6,8},{7,5},{8,10},{9,7},{10,... | collective-permute-start | bytes 1179656 | tf_op jit(solution)/shard_map/ppermute | solution.py:329
  90.3 3.0 %ring_sums.4 = (f32[1536,256]{1,0:T(8,128)S(1)}, f32[1536,256]{1,0:T(8,128)S(1)}) custom-call(s32[4]{0:T(128)S(1)} %pad_add_fusion.place_ref, bf16[4096,256]{1,0:T(8,128)(2,1)S(1)} %beside.1.own_w_ref.main_ref, bf16[4096,256]{1,0:T(8,128)(2,1)} %collective-permute-done.4.other_w_ref, bf16[1536,128]{1,0:T(8,128)(2,1)} %collective-permute-done.3.refs_0_, ...), custom_call_target="tpu_custom_call" | custom-call | flops 805306368 | tf_op jit(solution)/shard_map/ring_sums/pallas_call | solution.py:121
  93.4 3.3 %ring_sums.5 = (f32[1536,256]{1,0:T(8,128)S(1)}, f32[1536,256]{1,0:T(8,128)S(1)}) custom-call(s32[4]{0:T(128)S(1)} %pad_add_fusion.place_ref, bf16[4096,256]{1,0:T(8,128)(2,1)S(1)} %beside.1.own_w_ref.main_ref, bf16[4096,256]{1,0:T(8,128)(2,1)} %collective-permute-done.4.other_w_ref, bf16[1536,128]{1,0:T(8,128)(2,1)} %bitcast.3.refs_0_, ...), custom_call_target="tpu_custom_call" | custom-call | flops 1207959552 | tf_op jit(solution)/shard_map/ring_sums/pallas_call | solution.py:121
  96.7 3.0 %ring_sums.6 = (f32[1536,256]{1,0:T(8,128)S(1)}, f32[1536,256]{1,0:T(8,128)S(1)}) custom-call(s32[4]{0:T(128)S(1)} %pad_add_fusion.place_ref, bf16[4096,256]{1,0:T(8,128)(2,1)S(1)} %beside.1.own_w_ref.main_ref, bf16[4096,256]{1,0:T(8,128)(2,1)} %collective-permute-done.4.other_w_ref, bf16[1536,128]{1,0:T(8,128)(2,1)S(1)} %copy-done.14, ...), custom_call_target="tpu_custom_call" | custom-call | flops 805306368 | tf_op jit(solution)/shard_map/ring_sums/pallas_call | solution.py:121
  99.8 2.8 %ring_sums.7 = (f32[1536,256]{1,0:T(8,128)S(1)}, f32[1536,256]{1,0:T(8,128)S(1)}) custom-call(s32[4]{0:T(128)S(1)} %pad_add_fusion.place_ref, bf16[4096,256]{1,0:T(8,128)(2,1)S(1)} %beside.1.own_w_ref.main_ref, bf16[4096,256]{1,0:T(8,128)(2,1)} %collective-permute-done.4.other_w_ref, bf16[1536,128]{1,0:T(8,128)(2,1)} %collective-permute-done.10.refs_0_, ...), custom_call_target="tpu_custom_call" | custom-call | flops 402653184 | tf_op jit(solution)/shard_map/ring_sums/pallas_call | solution.py:121
  102.6 3.4 %collective-permute-start.18 = (f32[1536,256]{1,0:T(8,128)S(1)}, f32[1536,256]{1,0:T(8,128)S(1)}, u32[]{:S(2)}, u32[]{:S(2)}) collective-permute-start(f32[1536,256]{1,0:T(8,128)S(1)} %get-tuple-element.36), channel_id=1, source_target_pairs={{0,1},{1,0},{2,3},{3,2},{4,5},{5,4},{6,7},{7,6},{8,9},{9,8},{10,11... | collective-permute-start | bytes 4718600 | tf_op jit(solution)/shard_map/ppermute | solution.py:329
  106.7 4.8 %collective-permute-start.20 = (bf16[1536,128]{1,0:T(8,128)(2,1)}, bf16[1536,128]{1,0:T(8,128)(2,1)S(1)}, u32[]{:S(2)}, u32[]{:S(2)}) collective-permute-start(bf16[1536,128]{1,0:T(8,128)(2,1)} %collective-permute-done.10.refs_0_), channel_id=1, source_target_pairs={{0,2},{1,31},{2,4},{3,1},{4,6},{5,3},{6,8},{7,5},{8,10},{9,7},{10,... | collective-permute-start | bytes 1179656 | tf_op jit(solution)/shard_map/ppermute | solution.py:329
  111.6 1.9 %collective-permute-start.21 = (bf16[1568,128]{1,0:T(8,128)(2,1)}, bf16[1568,128]{1,0:T(8,128)(2,1)S(1)}, u32[]{:S(2)}, u32[]{:S(2)}) collective-permute-start(bf16[1568,128]{1,0:T(8,128)(2,1)} %collective-permute-done.16.refs_1_), channel_id=1, source_target_pairs={{0,2},{1,31},{2,4},{3,1},{4,6},{5,3},{6,8},{7,5},{8,10},{9,7},{10,... | collective-permute-start | bytes 1204232 | tf_op jit(solution)/shard_map/ppermute | solution.py:329
  114.9 1.9 %collective-permute-start.19 = (bf16[224,128]{1,0:T(8,128)(2,1)S(1)}, bf16[224,128]{1,0:T(8,128)(2,1)S(1)}, u32[]{:S(2)}, u32[]{:S(2)}) collective-permute-start(bf16[224,128]{1,0:T(8,128)(2,1)S(1)} %constant_dynamic-update-slice_fusion.mine_new_ref), channel_id=1, source_target_pairs={{0,1},{1,0},{2,3},{3,2},{4,5},{5,4},{6,7},{7,6},{8,9},{9,8},{10,11... | collective-permute-start | bytes 172040 | tf_op jit(solution)/shard_map/ppermute | solution.py:329
  118.0 2.9 %collective-permute-done.21.last_b_ref = bf16[1568,128]{1,0:T(8,128)(2,1)S(1)} collective-permute-done((bf16[1568,128]{1,0:T(8,128)(2,1)}, bf16[1568,128]{1,0:T(8,128)(2,1)S(1)}, u32[]{:S(2)}, u32[]{:S(2)}) %collective-permute-start.21) | collective-permute-done | bytes 401440 | tf_op jit(solution)/shard_map/ppermute | solution.py:329
  120.9 2.3 %span_states.1 = (f32[16,15,128]{2,1,0:T(8,128)S(1)}, f32[16,128]{1,0:T(8,128)S(1)}) custom-call(s32[4]{0:T(128)S(1)} %pad_add_fusion.place_ref, f32[1536,256]{1,0:T(8,128)S(1)} %get-tuple-element.35.total_ref, f32[1536,256]{1,0:T(8,128)S(1)} %collective-permute-done.18.arrived_ref, bf16[32,128]{1,0:T(8,128)(2,1)S(1)} %pad_maximum_fusion.1.here_new_ref, ...), custom_call_target="tpu_custom_call" | custom-call | tf_op jit(solution)/shard_map/span_states/pallas_call | solution.py:236
  123.2 13.4 %all_to_all.5.arrived_ref = f32[16,15,128]{2,1,0:T(8,128)S(1)} all-to-all(f32[16,15,128]{2,1,0:T(8,128)S(1)} %get-tuple-element.40), channel_id=1, replica_groups=mesh['sp'=16,'tp'=32] {'sp'}, dimensions={0} | all-to-all | bytes 245760 | tf_op jit(solution)/shard_map/all_to_all | solution.py:407
  (71 shorter events, 15.9 us)
Async XLA Ops:
  0.6 21.3 %collective-permute-start.3 = (bf16[1536,128]{1,0:T(8,128)(2,1)}, bf16[1536,128]{1,0:T(8,128)(2,1)}, u32[]{:S(2)}, u32[]{:S(2)}) collective-permute-start(bf16[1536,128]{1,0:T(8,128)(2,1)} %bitcast.3.refs_0_), channel_id=1, source_target_pairs={{0,2},{1,31},{2,4},{3,1},{4,6},{5,3},{6,8},{7,5},{8,10},{9,7},{10,... | collective-permute-start | bytes 1179656 | tf_op jit(solution)/shard_map/ppermute | solution.py:329
  12.6 11.2 %collective-permute-start = (bf16[1536,128]{1,0:T(8,128)(2,1)}, bf16[1536,128]{1,0:T(8,128)(2,1)S(1)}, u32[]{:S(2)}, u32[]{:S(2)}) collective-permute-start(bf16[1536,128]{1,0:T(8,128)(2,1)} %bitcast.3.refs_0_), channel_id=1, source_target_pairs={{1,2},{0,31},{3,4},{2,1},{5,6},{4,3},{7,8},{6,5},{9,10},{8,7},{11,... | collective-permute-start | bytes 1179656 | tf_op jit(solution)/shard_map/ppermute | solution.py:329
  14.5 4.0 %collective-permute-start.1 = (bf16[3,1,128]{2,0,1:T(4,128)(2,1)}, bf16[3,1,128]{2,0,1:T(4,128)(2,1)S(1)}, u32[]{:S(2)}, u32[]{:S(2)}) collective-permute-start(bf16[3,1,128]{2,0,1:T(4,128)(2,1)} %param.7), channel_id=1, source_target_pairs={{0,1},{1,0},{2,3},{3,2},{4,5},{5,4},{6,7},{7,6},{8,9},{9,8},{10,11... | collective-permute-start | bytes 2312 | tf_op jit(solution)/shard_map/ppermute | solution.py:329
  19.2 4.5 %collective-permute-start.2 = (bf16[32,128]{1,0:T(8,128)(2,1)S(1)}, bf16[32,128]{1,0:T(8,128)(2,1)S(1)}, u32[]{:S(2)}, u32[]{:S(2)}) collective-permute-start(bf16[32,128]{1,0:T(8,128)(2,1)S(1)} %pad_maximum_fusion.1.here_new_ref), channel_id=1, source_target_pairs={{0,2},{1,31},{2,4},{3,1},{4,6},{5,3},{6,8},{7,5},{8,10},{9,7},{10,... | collective-permute-start | bytes 24584 | tf_op jit(solution)/shard_map/ppermute | solution.py:329
  23.8 14.1 %collective-permute-start.11 = (bf16[1568,128]{1,0:T(8,128)(2,1)S(1)}, bf16[1568,128]{1,0:T(8,128)(2,1)S(1)}, u32[]{:S(2)}, u32[]{:S(2)}) collective-permute-start(bf16[1568,128]{1,0:T(8,128)(2,1)S(1)} %pad_maximum_fusion), channel_id=1, source_target_pairs={{0,2},{1,31},{2,4},{3,1},{4,6},{5,3},{6,8},{7,5},{8,10},{9,7},{10,... | collective-permute-start | bytes 1204232 | tf_op jit(solution)/shard_map/ppermute | solution.py:329
  27.5 1.2 copy-start.1
  28.8 1.2 copy-start.2
  30.3 57.9 %collective-permute-start.4 = (bf16[4096,256]{1,0:T(8,128)(2,1)S(1)}, bf16[4096,256]{1,0:T(8,128)(2,1)}, u32[]{:S(2)}, u32[]{:S(2)}) collective-permute-start(bf16[4096,256]{1,0:T(8,128)(2,1)S(1)} %beside.1.own_w_ref.main_ref), channel_id=1, source_target_pairs={{0,1},{1,0},{2,3},{3,2},{4,5},{5,4},{6,7},{7,6},{8,9},{9,8},{10,11... | collective-permute-start | bytes 6291464 | tf_op jit(solution)/shard_map/ppermute | solution.py:329
  33.0 9.9 %collective-permute-start.5 = (bf16[1536,128]{1,0:T(8,128)(2,1)}, bf16[1536,128]{1,0:T(8,128)(2,1)S(1)}, u32[]{:S(2)}, u32[]{:S(2)}) collective-permute-start(bf16[1536,128]{1,0:T(8,128)(2,1)} %collective-permute-done.3.refs_0_), channel_id=1, source_target_pairs={{0,2},{1,31},{2,4},{3,1},{4,6},{5,3},{6,8},{7,5},{8,10},{9,7},{10,... | collective-permute-start | bytes 1179656 | tf_op jit(solution)/shard_map/ppermute | solution.py:329
  37.9 10.7 %collective-permute-start.12 = (bf16[1568,128]{1,0:T(8,128)(2,1)S(1)}, bf16[1568,128]{1,0:T(8,128)(2,1)S(1)}, u32[]{:S(2)}, u32[]{:S(2)}) collective-permute-start(bf16[1568,128]{1,0:T(8,128)(2,1)S(1)} %collective-permute-done.11.refs_3_), channel_id=1, source_target_pairs={{0,2},{1,31},{2,4},{3,1},{4,6},{5,3},{6,8},{7,5},{8,10},{9,7},{10,... | collective-permute-start | bytes 1204232 | tf_op jit(solution)/shard_map/ppermute | solution.py:329
  42.9 9.6 %collective-permute-start.6 = (bf16[1536,128]{1,0:T(8,128)(2,1)S(1)}, bf16[1536,128]{1,0:T(8,128)(2,1)S(1)}, u32[]{:S(2)}, u32[]{:S(2)}) collective-permute-start(bf16[1536,128]{1,0:T(8,128)(2,1)S(1)} %collective-permute-done.5.refs_1_), channel_id=1, source_target_pairs={{0,2},{1,31},{2,4},{3,1},{4,6},{5,3},{6,8},{7,5},{8,10},{9,7},{10,... | collective-permute-start | bytes 1179656 | tf_op jit(solution)/shard_map/ppermute | solution.py:329
  48.6 9.7 %collective-permute-start.13 = (bf16[1568,128]{1,0:T(8,128)(2,1)S(1)}, bf16[1568,128]{1,0:T(8,128)(2,1)S(1)}, u32[]{:S(2)}, u32[]{:S(2)}) collective-permute-start(bf16[1568,128]{1,0:T(8,128)(2,1)S(1)} %collective-permute-done.12.refs_4_), channel_id=1, source_target_pairs={{0,2},{1,31},{2,4},{3,1},{4,6},{5,3},{6,8},{7,5},{8,10},{9,7},{10,... | collective-permute-start | bytes 1204232 | tf_op jit(solution)/shard_map/ppermute | solution.py:329
  52.5 10.2 %collective-permute-start.7 = (bf16[1536,128]{1,0:T(8,128)(2,1)S(1)}, bf16[1536,128]{1,0:T(8,128)(2,1)S(1)}, u32[]{:S(2)}, u32[]{:S(2)}) collective-permute-start(bf16[1536,128]{1,0:T(8,128)(2,1)S(1)} %collective-permute-done.6.refs_1_), channel_id=1, source_target_pairs={{0,2},{1,31},{2,4},{3,1},{4,6},{5,3},{6,8},{7,5},{8,10},{9,7},{10,... | collective-permute-start | bytes 1179656 | tf_op jit(solution)/shard_map/ppermute | solution.py:329
  58.3 9.7 %collective-permute-start.14 = (bf16[1568,128]{1,0:T(8,128)(2,1)S(1)}, bf16[1568,128]{1,0:T(8,128)(2,1)S(1)}, u32[]{:S(2)}, u32[]{:S(2)}) collective-permute-start(bf16[1568,128]{1,0:T(8,128)(2,1)S(1)} %collective-permute-done.13.refs_5_), channel_id=1, source_target_pairs={{0,2},{1,31},{2,4},{3,1},{4,6},{5,3},{6,8},{7,5},{8,10},{9,7},{10,... | collective-permute-start | bytes 1204232 | tf_op jit(solution)/shard_map/ppermute | solution.py:329
  62.7 9.8 %collective-permute-start.8 = (bf16[1536,128]{1,0:T(8,128)(2,1)S(1)}, bf16[1536,128]{1,0:T(8,128)(2,1)S(1)}, u32[]{:S(2)}, u32[]{:S(2)}) collective-permute-start(bf16[1536,128]{1,0:T(8,128)(2,1)S(1)} %collective-permute-done.7.refs_2_), channel_id=1, source_target_pairs={{0,2},{1,31},{2,4},{3,1},{4,6},{5,3},{6,8},{7,5},{8,10},{9,7},{10,... | collective-permute-start | bytes 1179656 | tf_op jit(solution)/shard_map/ppermute | solution.py:329
  68.0 13.3 %collective-permute-start.15 = (bf16[1568,128]{1,0:T(8,128)(2,1)S(1)}, bf16[1568,128]{1,0:T(8,128)(2,1)}, u32[]{:S(2)}, u32[]{:S(2)}) collective-permute-start(bf16[1568,128]{1,0:T(8,128)(2,1)S(1)} %collective-permute-done.14.refs_2_), channel_id=1, source_target_pairs={{0,2},{1,31},{2,4},{3,1},{4,6},{5,3},{6,8},{7,5},{8,10},{9,7},{10,... | collective-permute-start | bytes 1204232 | tf_op jit(solution)/shard_map/ppermute | solution.py:329
  72.5 13.7 %collective-permute-start.9 = (bf16[1536,128]{1,0:T(8,128)(2,1)S(1)}, bf16[1536,128]{1,0:T(8,128)(2,1)}, u32[]{:S(2)}, u32[]{:S(2)}) collective-permute-start(bf16[1536,128]{1,0:T(8,128)(2,1)S(1)} %collective-permute-done.8.refs_0_), channel_id=1, source_target_pairs={{0,2},{1,31},{2,4},{3,1},{4,6},{5,3},{6,8},{7,5},{8,10},{9,7},{10,... | collective-permute-start | bytes 1179656 | tf_op jit(solution)/shard_map/ppermute | solution.py:329
  77.8 15.6 %collective-permute-start.17 = (bf16[1536,128]{1,0:T(8,128)(2,1)}, bf16[1536,128]{1,0:T(8,128)(2,1)}, u32[]{:S(2)}, u32[]{:S(2)}) collective-permute-start(bf16[1536,128]{1,0:T(8,128)(2,1)} %bitcast.3.refs_0_), channel_id=1, source_target_pairs={{0,1},{1,0},{2,3},{3,2},{4,5},{5,4},{6,7},{7,6},{8,9},{9,8},{10,11... | collective-permute-start | bytes 1179656 | tf_op jit(solution)/shard_map/ppermute | solution.py:329
  81.4 18.4 %collective-permute-start.16 = (bf16[1568,128]{1,0:T(8,128)(2,1)}, bf16[1568,128]{1,0:T(8,128)(2,1)}, u32[]{:S(2)}, u32[]{:S(2)}) collective-permute-start(bf16[1568,128]{1,0:T(8,128)(2,1)} %collective-permute-done.15.refs_3_), channel_id=1, source_target_pairs={{0,2},{1,31},{2,4},{3,1},{4,6},{5,3},{6,8},{7,5},{8,10},{9,7},{10,... | collective-permute-start | bytes 1204232 | tf_op jit(solution)/shard_map/ppermute | solution.py:329
  86.2 13.5 %collective-permute-start.10 = (bf16[1536,128]{1,0:T(8,128)(2,1)}, bf16[1536,128]{1,0:T(8,128)(2,1)}, u32[]{:S(2)}, u32[]{:S(2)}) collective-permute-start(bf16[1536,128]{1,0:T(8,128)(2,1)} %collective-permute-done.9.refs_1_), channel_id=1, source_target_pairs={{0,2},{1,31},{2,4},{3,1},{4,6},{5,3},{6,8},{7,5},{8,10},{9,7},{10,... | collective-permute-start | bytes 1179656 | tf_op jit(solution)/shard_map/ppermute | solution.py:329
  88.2 5.1 %copy-start.4 = (bf16[1568,128]{1,0:T(8,128)(2,1)S(1)}, bf16[1568,128]{1,0:T(8,128)(2,1)}, u32[]{:S(2)}) copy-start(bf16[1568,128]{1,0:T(8,128)(2,1)} %copy-done.3) | copy-start | bytes 1204228
  88.3 1.1 copy-start.6
  89.3 1.0 copy-start.16
  90.3 3.0 %copy-start.10 = (bf16[1536,128]{1,0:T(8,128)(2,1)S(1)}, bf16[1536,128]{1,0:T(8,128)(2,1)}, u32[]{:S(2)}) copy-start(bf16[1536,128]{1,0:T(8,128)(2,1)} %copy-done.9) | copy-start | bytes 1179652
  90.3 3.0 %copy-start.12 = (bf16[1536,128]{1,0:T(8,128)(2,1)S(1)}, bf16[1536,128]{1,0:T(8,128)(2,1)}, u32[]{:S(2)}) copy-start(bf16[1536,128]{1,0:T(8,128)(2,1)} %copy-done.11) | copy-start | bytes 1179652
  93.4 3.3 %copy-start.8 = (bf16[1568,128]{1,0:T(8,128)(2,1)S(1)}, bf16[1568,128]{1,0:T(8,128)(2,1)}, u32[]{:S(2)}) copy-start(bf16[1568,128]{1,0:T(8,128)(2,1)} %copy-done.7) | copy-start | bytes 1204228
  93.4 3.3 %copy-start.14 = (bf16[1536,128]{1,0:T(8,128)(2,1)S(1)}, bf16[1536,128]{1,0:T(8,128)(2,1)}, u32[]{:S(2)}) copy-start(bf16[1536,128]{1,0:T(8,128)(2,1)} %copy-done.13) | copy-start | bytes 1179652
  99.8 21.2 %copy-start = (bf16[4096,128]{1,0:T(8,128)(2,1)S(1)}, bf16[4096,128]{1,0:T(8,128)(2,1)}, u32[]{:S(2)}) copy-start(bf16[4096,128]{1,0:T(8,128)(2,1)} %query_w_ref.1) | copy-start | bytes 3145732
  102.6 18.3 %collective-permute-start.18 = (f32[1536,256]{1,0:T(8,128)S(1)}, f32[1536,256]{1,0:T(8,128)S(1)}, u32[]{:S(2)}, u32[]{:S(2)}) collective-permute-start(f32[1536,256]{1,0:T(8,128)S(1)} %get-tuple-element.36), channel_id=1, source_target_pairs={{0,1},{1,0},{2,3},{3,2},{4,5},{5,4},{6,7},{7,6},{8,9},{9,8},{10,11... | collective-permute-start | bytes 4718600 | tf_op jit(solution)/shard_map/ppermute | solution.py:329
  106.7 11.3 %collective-permute-start.20 = (bf16[1536,128]{1,0:T(8,128)(2,1)}, bf16[1536,128]{1,0:T(8,128)(2,1)S(1)}, u32[]{:S(2)}, u32[]{:S(2)}) collective-permute-start(bf16[1536,128]{1,0:T(8,128)(2,1)} %collective-permute-done.10.refs_0_), channel_id=1, source_target_pairs={{0,2},{1,31},{2,4},{3,1},{4,6},{5,3},{6,8},{7,5},{8,10},{9,7},{10,... | collective-permute-start | bytes 1179656 | tf_op jit(solution)/shard_map/ppermute | solution.py:329
  111.6 9.3 %collective-permute-start.21 = (bf16[1568,128]{1,0:T(8,128)(2,1)}, bf16[1568,128]{1,0:T(8,128)(2,1)S(1)}, u32[]{:S(2)}, u32[]{:S(2)}) collective-permute-start(bf16[1568,128]{1,0:T(8,128)(2,1)} %collective-permute-done.16.refs_1_), channel_id=1, source_target_pairs={{0,2},{1,31},{2,4},{3,1},{4,6},{5,3},{6,8},{7,5},{8,10},{9,7},{10,... | collective-permute-start | bytes 1204232 | tf_op jit(solution)/shard_map/ppermute | solution.py:329
  114.9 3.1 %collective-permute-start.19 = (bf16[224,128]{1,0:T(8,128)(2,1)S(1)}, bf16[224,128]{1,0:T(8,128)(2,1)S(1)}, u32[]{:S(2)}, u32[]{:S(2)}) collective-permute-start(bf16[224,128]{1,0:T(8,128)(2,1)S(1)} %constant_dynamic-update-slice_fusion.mine_new_ref), channel_id=1, source_target_pairs={{0,1},{1,0},{2,3},{3,2},{4,5},{5,4},{6,7},{7,6},{8,9},{9,8},{10,11... | collective-permute-start | bytes 172040 | tf_op jit(solution)/shard_map/ppermute | solution.py:329
  (7 other events, 5.3 us)

commit v8 on v7

--- a/solution.py
+++ b/solution.py
@@ -140,6 +140,7 @@
 
 def state_kernel(
     place_ref,
+    rate_ref,
     total_ref,
     arrived_ref,
     here_new_ref,
@@ -151,7 +152,6 @@
     query_w_ref,
     cos_ref,
     sin_ref,
-    lane_ref,
     out_ref,
     own_ref,
 ):
@@ -163,7 +163,10 @@
     span_len = rows // prompts
     reach = mine_new_ref.shape[0] // (2 * EXTRA) + 1
     lane = lax.broadcasted_iota(jnp.int32, (HD, inner), 1)
-    lane_decay = lane_ref[...]
+    row_lane = lax.broadcasted_iota(jnp.int32, (1, inner), 1)
+    lane_decay = jnp.full((1, inner), rate_ref[0], jnp.float32)
+    for h in range(1, inner // HD):
+        lane_decay = jnp.where(row_lane // HD == h, rate_ref[h], lane_decay)
     distance = ((groups - 1 - place_ref[2]) * span_len).astype(jnp.float32)
     carried = jnp.exp(lane_decay * distance)
     one = jnp.exp(lane_decay)
@@ -230,12 +233,12 @@
             out_ref[g, prompts * keep + s : prompts * keep + s + 1, :] = read
 
 
-def span_states(prompts, groups, inner, place, *operands):
+def span_states(prompts, groups, inner, place, *operands, decay):
     keep = HD // groups
     whole = pl.BlockSpec(memory_space=pltpu.VMEM)
     return pl.pallas_call(
         state_kernel,
-        in_specs=[pl.BlockSpec(memory_space=pltpu.SMEM)] + [whole] * len(operands),
+        in_specs=[pl.BlockSpec(memory_space=pltpu.SMEM)] * 2 + [whole] * len(operands),
         out_specs=[whole, whole],
         out_shape=[
             jax.ShapeDtypeStruct((groups, prompts * (keep + 1), inner), jnp.float32),
@@ -243,7 +246,7 @@
         ],
         compiler_params=pltpu.CompilerParams(vmem_limit_bytes=8 * 1024 * 1024),
         name="span_states",
-    )(place, *operands)
+    )(place, decay, *operands)
 
 
 def finish_kernel(arrived_ref, own_ref, state_ref, read_ref):
@@ -346,15 +349,10 @@
     new_first = sent(new_pair, onward)
     a_list, b_list = [tokens, chain_a], [None, chain_b]
     new_list = [new_first]
-    chain_a, first_position, log_decay = lax.optimization_barrier(
-        (chain_a, own_index * span_len, log_decay)
-    )
+    chain_a, first_position = lax.optimization_barrier((chain_a, own_index * span_len))
     a_list[1] = chain_a
     cosine, sine = tables(first_position, span_len, groups * span_len, heads)
-    lane_decay = jnp.repeat(log_decay, HD)[None, :]
-    new_first, cosine, sine, lane_decay = lax.optimization_barrier(
-        (new_first, cosine, sine, lane_decay)
-    )
+    new_first, cosine, sine = lax.optimization_barrier((new_first, cosine, sine))
     chain_b = jnp.concatenate([chain_b, new_first], axis=0)
     key_weight, value_weight, chain_b = lax.optimization_barrier(
         (key_weight, value_weight, chain_b)
@@ -402,7 +400,7 @@
         query_weight,
         cosine,
         sine,
-        lane_decay,
+        decay=log_decay,
     )
     arrived = lax.all_to_all(messages, "sp", split_axis=0, concat_axis=0, tiled=True)
     return tuple(finish(arrived, own_term, prompts, heads, HD // groups))

time: 139 us -> 138 us (level)
  local copies, waits for them, and re-layouts: 12.7 us -> 10.7 us
    unnamed x40 -> x42, local copies, waits for them, and re-layouts: 11.2 us -> 9.98 us
  transfers between devices with their start and end apart: 22 -> 22, of which waited for: 5 -> 6; matrix products, arithmetic and copies ran while one was open for 3% -> 3% of each run, Pallas kernels for 7% -> 7%
where the time goes in v8:
time: 138 us; the launch traced here: 136 us
  starting transfers between devices  85.1 us (62%)
  Pallas kernels  15.6 us (11%)
  blocking collectives  13.4 us (10%)
  local copies, waits for them, and re-layouts  10.7 us (8%)
  waiting for transfers between devices  8.49 us (6%)
  other arithmetic  1.83 us (1%)
    ppermute x22, starting transfers between devices, sent(): return lax.ppermute(value, 'tp', pairs)  85.1 us
    all_to_all x1, blocking collectives, body(): lax.all_to_all(messages, 'sp', split_axis=0, concat_axis=0, tiled=True)  13.4 us
    pallas_call x4, Pallas kernels, ring_sums(): pl.pallas_call(functools.partial(sums_kernel, offsets, span_len, bool(bef...  12.2 us
    unnamed x42, local copies, waits for them, and re-layouts  9.98 us
    ppermute x22, waiting for transfers between devices, sent(): return lax.ppermute(value, 'tp', pairs)  8.49 us
  transfers between devices with their start and end apart: 22, of which 6 were waited for; matrix products, arithmetic and copies ran while one was open for 3% of the time, Pallas kernels for 7%

profile of v8, /device:TPU:1, one launch (start us, length us, event | category | flops | bytes accessed | tf_op | source)
XLA Modules:
  0.0 136.2 jit_solution(3384144894110104097)
XLA Ops:
  0.6 11.9 %collective-permute-start.3 = (bf16[1536,128]{1,0:T(8,128)(2,1)}, bf16[1536,128]{1,0:T(8,128)(2,1)}, u32[]{:S(2)}, u32[]{:S(2)}) collective-permute-start(bf16[1536,128]{1,0:T(8,128)(2,1)} %bitcast.3.refs_0_), channel_id=1, source_target_pairs={{0,2},{1,31},{2,4},{3,1},{4,6},{5,3},{6,8},{7,5},{8,10},{9,7},{10,... | collective-permute-start | bytes 1179656 | tf_op jit(solution)/shard_map/ppermute | solution.py:332
  12.6 1.9 %collective-permute-start = (bf16[1536,128]{1,0:T(8,128)(2,1)}, bf16[1536,128]{1,0:T(8,128)(2,1)S(1)}, u32[]{:S(2)}, u32[]{:S(2)}) collective-permute-start(bf16[1536,128]{1,0:T(8,128)(2,1)} %bitcast.3.refs_0_), channel_id=1, source_target_pairs={{1,2},{0,31},{3,4},{2,1},{5,6},{4,3},{7,8},{6,5},{9,10},{8,7},{11,... | collective-permute-start | bytes 1179656 | tf_op jit(solution)/shard_map/ppermute | solution.py:332
  14.5 3.0 %collective-permute-start.1 = (bf16[3,1,128]{2,0,1:T(4,128)(2,1)}, bf16[3,1,128]{2,0,1:T(4,128)(2,1)S(1)}, u32[]{:S(2)}, u32[]{:S(2)}) collective-permute-start(bf16[3,1,128]{2,0,1:T(4,128)(2,1)} %param.7), channel_id=1, source_target_pairs={{0,1},{1,0},{2,3},{3,2},{4,5},{5,4},{6,7},{7,6},{8,9},{9,8},{10,11... | collective-permute-start | bytes 2312 | tf_op jit(solution)/shard_map/ppermute | solution.py:332
  19.2 2.6 %collective-permute-start.2 = (bf16[32,128]{1,0:T(8,128)(2,1)S(1)}, bf16[32,128]{1,0:T(8,128)(2,1)S(1)}, u32[]{:S(2)}, u32[]{:S(2)}) collective-permute-start(bf16[32,128]{1,0:T(8,128)(2,1)S(1)} %pad_maximum_fusion.1.here_new_ref), channel_id=1, source_target_pairs={{0,2},{1,31},{2,4},{3,1},{4,6},{5,3},{6,8},{7,5},{8,10},{9,7},{10,... | collective-permute-start | bytes 24584 | tf_op jit(solution)/shard_map/ppermute | solution.py:332
  23.7 3.8 %collective-permute-start.11 = (bf16[1568,128]{1,0:T(8,128)(2,1)S(1)}, bf16[1568,128]{1,0:T(8,128)(2,1)S(1)}, u32[]{:S(2)}, u32[]{:S(2)}) collective-permute-start(bf16[1568,128]{1,0:T(8,128)(2,1)S(1)} %pad_maximum_fusion), channel_id=1, source_target_pairs={{0,2},{1,31},{2,4},{3,1},{4,6},{5,3},{6,8},{7,5},{8,10},{9,7},{10,... | collective-permute-start | bytes 1204232 | tf_op jit(solution)/shard_map/ppermute | solution.py:332
  27.6 1.2 copy-done.2
  29.1 2.7 %collective-permute-start.4 = (bf16[4096,256]{1,0:T(8,128)(2,1)S(1)}, bf16[4096,256]{1,0:T(8,128)(2,1)}, u32[]{:S(2)}, u32[]{:S(2)}) collective-permute-start(bf16[4096,256]{1,0:T(8,128)(2,1)S(1)} %beside.1.own_w_ref.main_ref), channel_id=1, source_target_pairs={{0,1},{1,0},{2,3},{3,2},{4,5},{5,4},{6,7},{7,6},{8,9},{9,8},{10,11... | collective-permute-start | bytes 6291464 | tf_op jit(solution)/shard_map/ppermute | solution.py:332
  31.8 4.9 %collective-permute-start.5 = (bf16[1536,128]{1,0:T(8,128)(2,1)}, bf16[1536,128]{1,0:T(8,128)(2,1)S(1)}, u32[]{:S(2)}, u32[]{:S(2)}) collective-permute-start(bf16[1536,128]{1,0:T(8,128)(2,1)} %collective-permute-done.3.refs_0_), channel_id=1, source_target_pairs={{0,2},{1,31},{2,4},{3,1},{4,6},{5,3},{6,8},{7,5},{8,10},{9,7},{10,... | collective-permute-start | bytes 1179656 | tf_op jit(solution)/shard_map/ppermute | solution.py:332
  36.7 1.9 %collective-permute-start.12 = (bf16[1568,128]{1,0:T(8,128)(2,1)S(1)}, bf16[1568,128]{1,0:T(8,128)(2,1)S(1)}, u32[]{:S(2)}, u32[]{:S(2)}) collective-permute-start(bf16[1568,128]{1,0:T(8,128)(2,1)S(1)} %collective-permute-done.11.refs_3_), channel_id=1, source_target_pairs={{0,2},{1,31},{2,4},{3,1},{4,6},{5,3},{6,8},{7,5},{8,10},{9,7},{10,... | collective-permute-start | bytes 1204232 | tf_op jit(solution)/shard_map/ppermute | solution.py:332
  39.4 2.3 %collective-permute-done.5.refs_1_ = bf16[1536,128]{1,0:T(8,128)(2,1)S(1)} collective-permute-done((bf16[1536,128]{1,0:T(8,128)(2,1)}, bf16[1536,128]{1,0:T(8,128)(2,1)S(1)}, u32[]{:S(2)}, u32[]{:S(2)}) %collective-permute-start.5) | collective-permute-done | bytes 393248 | tf_op jit(solution)/shard_map/ppermute | solution.py:332
  41.7 4.9 %collective-permute-start.6 = (bf16[1536,128]{1,0:T(8,128)(2,1)S(1)}, bf16[1536,128]{1,0:T(8,128)(2,1)S(1)}, u32[]{:S(2)}, u32[]{:S(2)}) collective-permute-start(bf16[1536,128]{1,0:T(8,128)(2,1)S(1)} %collective-permute-done.5.refs_1_), channel_id=1, source_target_pairs={{0,2},{1,31},{2,4},{3,1},{4,6},{5,3},{6,8},{7,5},{8,10},{9,7},{10,... | collective-permute-start | bytes 1179656 | tf_op jit(solution)/shard_map/ppermute | solution.py:332
  47.4 3.5 %collective-permute-start.13 = (bf16[1568,128]{1,0:T(8,128)(2,1)S(1)}, bf16[1568,128]{1,0:T(8,128)(2,1)S(1)}, u32[]{:S(2)}, u32[]{:S(2)}) collective-permute-start(bf16[1568,128]{1,0:T(8,128)(2,1)S(1)} %collective-permute-done.12.refs_4_), channel_id=1, source_target_pairs={{0,2},{1,31},{2,4},{3,1},{4,6},{5,3},{6,8},{7,5},{8,10},{9,7},{10,... | collective-permute-start | bytes 1204232 | tf_op jit(solution)/shard_map/ppermute | solution.py:332
  51.3 5.0 %collective-permute-start.7 = (bf16[1536,128]{1,0:T(8,128)(2,1)S(1)}, bf16[1536,128]{1,0:T(8,128)(2,1)S(1)}, u32[]{:S(2)}, u32[]{:S(2)}) collective-permute-start(bf16[1536,128]{1,0:T(8,128)(2,1)S(1)} %collective-permute-done.6.refs_1_), channel_id=1, source_target_pairs={{0,2},{1,31},{2,4},{3,1},{4,6},{5,3},{6,8},{7,5},{8,10},{9,7},{10,... | collective-permute-start | bytes 1179656 | tf_op jit(solution)/shard_map/ppermute | solution.py:332
  57.1 3.6 %collective-permute-start.14 = (bf16[1568,128]{1,0:T(8,128)(2,1)S(1)}, bf16[1568,128]{1,0:T(8,128)(2,1)S(1)}, u32[]{:S(2)}, u32[]{:S(2)}) collective-permute-start(bf16[1568,128]{1,0:T(8,128)(2,1)S(1)} %collective-permute-done.13.refs_5_), channel_id=1, source_target_pairs={{0,2},{1,31},{2,4},{3,1},{4,6},{5,3},{6,8},{7,5},{8,10},{9,7},{10,... | collective-permute-start | bytes 1204232 | tf_op jit(solution)/shard_map/ppermute | solution.py:332
  61.5 4.6 %collective-permute-start.8 = (bf16[1536,128]{1,0:T(8,128)(2,1)S(1)}, bf16[1536,128]{1,0:T(8,128)(2,1)S(1)}, u32[]{:S(2)}, u32[]{:S(2)}) collective-permute-start(bf16[1536,128]{1,0:T(8,128)(2,1)S(1)} %collective-permute-done.7.refs_2_), channel_id=1, source_target_pairs={{0,2},{1,31},{2,4},{3,1},{4,6},{5,3},{6,8},{7,5},{8,10},{9,7},{10,... | collective-permute-start | bytes 1179656 | tf_op jit(solution)/shard_map/ppermute | solution.py:332
  66.8 3.7 %collective-permute-start.15 = (bf16[1568,128]{1,0:T(8,128)(2,1)S(1)}, bf16[1568,128]{1,0:T(8,128)(2,1)}, u32[]{:S(2)}, u32[]{:S(2)}) collective-permute-start(bf16[1568,128]{1,0:T(8,128)(2,1)S(1)} %collective-permute-done.14.refs_2_), channel_id=1, source_target_pairs={{0,2},{1,31},{2,4},{3,1},{4,6},{5,3},{6,8},{7,5},{8,10},{9,7},{10,... | collective-permute-start | bytes 1204232 | tf_op jit(solution)/shard_map/ppermute | solution.py:332
  71.3 4.5 %collective-permute-start.9 = (bf16[1536,128]{1,0:T(8,128)(2,1)S(1)}, bf16[1536,128]{1,0:T(8,128)(2,1)}, u32[]{:S(2)}, u32[]{:S(2)}) collective-permute-start(bf16[1536,128]{1,0:T(8,128)(2,1)S(1)} %collective-permute-done.8.refs_0_), channel_id=1, source_target_pairs={{0,2},{1,31},{2,4},{3,1},{4,6},{5,3},{6,8},{7,5},{8,10},{9,7},{10,... | collective-permute-start | bytes 1179656 | tf_op jit(solution)/shard_map/ppermute | solution.py:332
  76.5 3.6 %collective-permute-start.17 = (bf16[1536,128]{1,0:T(8,128)(2,1)}, bf16[1536,128]{1,0:T(8,128)(2,1)}, u32[]{:S(2)}, u32[]{:S(2)}) collective-permute-start(bf16[1536,128]{1,0:T(8,128)(2,1)} %bitcast.3.refs_0_), channel_id=1, source_target_pairs={{0,1},{1,0},{2,3},{3,2},{4,5},{5,4},{6,7},{7,6},{8,9},{9,8},{10,11... | collective-permute-start | bytes 1179656 | tf_op jit(solution)/shard_map/ppermute | solution.py:332
  80.1 4.9 %collective-permute-start.16 = (bf16[1568,128]{1,0:T(8,128)(2,1)}, bf16[1568,128]{1,0:T(8,128)(2,1)}, u32[]{:S(2)}, u32[]{:S(2)}) collective-permute-start(bf16[1568,128]{1,0:T(8,128)(2,1)} %collective-permute-done.15.refs_3_), channel_id=1, source_target_pairs={{0,2},{1,31},{2,4},{3,1},{4,6},{5,3},{6,8},{7,5},{8,10},{9,7},{10,... | collective-permute-start | bytes 1204232 | tf_op jit(solution)/shard_map/ppermute | solution.py:332
  85.0 1.9 %collective-permute-start.10 = (bf16[1536,128]{1,0:T(8,128)(2,1)}, bf16[1536,128]{1,0:T(8,128)(2,1)}, u32[]{:S(2)}, u32[]{:S(2)}) collective-permute-start(bf16[1536,128]{1,0:T(8,128)(2,1)} %collective-permute-done.9.refs_1_), channel_id=1, source_target_pairs={{0,2},{1,31},{2,4},{3,1},{4,6},{5,3},{6,8},{7,5},{8,10},{9,7},{10,... | collective-permute-start | bytes 1179656 | tf_op jit(solution)/shard_map/ppermute | solution.py:332
  89.1 3.0 %ring_sums.4 = (f32[1536,256]{1,0:T(8,128)S(1)}, f32[1536,256]{1,0:T(8,128)S(1)}) custom-call(s32[4]{0:T(128)S(1)} %pad_add_fusion.place_ref, bf16[4096,256]{1,0:T(8,128)(2,1)S(1)} %beside.1.own_w_ref.main_ref, bf16[4096,256]{1,0:T(8,128)(2,1)} %collective-permute-done.4.other_w_ref, bf16[1536,128]{1,0:T(8,128)(2,1)} %collective-permute-done.3.refs_0_, ...), custom_call_target="tpu_custom_call" | custom-call | flops 805306368 | tf_op jit(solution)/shard_map/ring_sums/pallas_call | solution.py:121
  92.1 3.3 %ring_sums.5 = (f32[1536,256]{1,0:T(8,128)S(1)}, f32[1536,256]{1,0:T(8,128)S(1)}) custom-call(s32[4]{0:T(128)S(1)} %pad_add_fusion.place_ref, bf16[4096,256]{1,0:T(8,128)(2,1)S(1)} %beside.1.own_w_ref.main_ref, bf16[4096,256]{1,0:T(8,128)(2,1)} %collective-permute-done.4.other_w_ref, bf16[1536,128]{1,0:T(8,128)(2,1)} %bitcast.3.refs_0_, ...), custom_call_target="tpu_custom_call" | custom-call | flops 1207959552 | tf_op jit(solution)/shard_map/ring_sums/pallas_call | solution.py:121
  95.5 3.0 %ring_sums.6 = (f32[1536,256]{1,0:T(8,128)S(1)}, f32[1536,256]{1,0:T(8,128)S(1)}) custom-call(s32[4]{0:T(128)S(1)} %pad_add_fusion.place_ref, bf16[4096,256]{1,0:T(8,128)(2,1)S(1)} %beside.1.own_w_ref.main_ref, bf16[4096,256]{1,0:T(8,128)(2,1)} %collective-permute-done.4.other_w_ref, bf16[1536,128]{1,0:T(8,128)(2,1)S(1)} %copy-done.14, ...), custom_call_target="tpu_custom_call" | custom-call | flops 805306368 | tf_op jit(solution)/shard_map/ring_sums/pallas_call | solution.py:121
  98.6 2.8 %ring_sums.7 = (f32[1536,256]{1,0:T(8,128)S(1)}, f32[1536,256]{1,0:T(8,128)S(1)}) custom-call(s32[4]{0:T(128)S(1)} %pad_add_fusion.place_ref, bf16[4096,256]{1,0:T(8,128)(2,1)S(1)} %beside.1.own_w_ref.main_ref, bf16[4096,256]{1,0:T(8,128)(2,1)} %collective-permute-done.4.other_w_ref, bf16[1536,128]{1,0:T(8,128)(2,1)} %collective-permute-done.10.refs_0_, ...), custom_call_target="tpu_custom_call" | custom-call | flops 402653184 | tf_op jit(solution)/shard_map/ring_sums/pallas_call | solution.py:121
  101.4 3.4 %collective-permute-start.18 = (f32[1536,256]{1,0:T(8,128)S(1)}, f32[1536,256]{1,0:T(8,128)S(1)}, u32[]{:S(2)}, u32[]{:S(2)}) collective-permute-start(f32[1536,256]{1,0:T(8,128)S(1)} %get-tuple-element.33), channel_id=1, source_target_pairs={{0,1},{1,0},{2,3},{3,2},{4,5},{5,4},{6,7},{7,6},{8,9},{9,8},{10,11... | collective-permute-start | bytes 4718600 | tf_op jit(solution)/shard_map/ppermute | solution.py:332
  105.6 4.8 %collective-permute-start.20 = (bf16[1536,128]{1,0:T(8,128)(2,1)}, bf16[1536,128]{1,0:T(8,128)(2,1)S(1)}, u32[]{:S(2)}, u32[]{:S(2)}) collective-permute-start(bf16[1536,128]{1,0:T(8,128)(2,1)} %collective-permute-done.10.refs_0_), channel_id=1, source_target_pairs={{0,2},{1,31},{2,4},{3,1},{4,6},{5,3},{6,8},{7,5},{8,10},{9,7},{10,... | collective-permute-start | bytes 1179656 | tf_op jit(solution)/shard_map/ppermute | solution.py:332
  110.4 1.9 %collective-permute-start.21 = (bf16[1568,128]{1,0:T(8,128)(2,1)}, bf16[1568,128]{1,0:T(8,128)(2,1)S(1)}, u32[]{:S(2)}, u32[]{:S(2)}) collective-permute-start(bf16[1568,128]{1,0:T(8,128)(2,1)} %collective-permute-done.16.refs_1_), channel_id=1, source_target_pairs={{0,2},{1,31},{2,4},{3,1},{4,6},{5,3},{6,8},{7,5},{8,10},{9,7},{10,... | collective-permute-start | bytes 1204232 | tf_op jit(solution)/shard_map/ppermute | solution.py:332
  113.8 1.9 %collective-permute-start.19 = (bf16[224,128]{1,0:T(8,128)(2,1)S(1)}, bf16[224,128]{1,0:T(8,128)(2,1)S(1)}, u32[]{:S(2)}, u32[]{:S(2)}) collective-permute-start(bf16[224,128]{1,0:T(8,128)(2,1)S(1)} %constant_dynamic-update-slice_fusion.mine_new_ref), channel_id=1, source_target_pairs={{0,1},{1,0},{2,3},{3,2},{4,5},{5,4},{6,7},{7,6},{8,9},{9,8},{10,11... | collective-permute-start | bytes 172040 | tf_op jit(solution)/shard_map/ppermute | solution.py:332
  115.7 1.2 collective-permute-done.19.theirs_new_ref
  116.9 2.9 %collective-permute-done.21.last_b_ref = bf16[1568,128]{1,0:T(8,128)(2,1)S(1)} collective-permute-done((bf16[1568,128]{1,0:T(8,128)(2,1)}, bf16[1568,128]{1,0:T(8,128)(2,1)S(1)}, u32[]{:S(2)}, u32[]{:S(2)}) %collective-permute-start.21) | collective-permute-done | bytes 401440 | tf_op jit(solution)/shard_map/ppermute | solution.py:332
  119.7 2.3 %span_states.1 = (f32[16,15,128]{2,1,0:T(8,128)S(1)}, f32[16,128]{1,0:T(8,128)S(1)}) custom-call(s32[4]{0:T(128)S(1)} %pad_add_fusion.place_ref, f32[2]{0:T(128)S(1)} %copy-done.17, f32[1536,256]{1,0:T(8,128)S(1)} %get-tuple-element.32.total_ref, f32[1536,256]{1,0:T(8,128)S(1)} %collective-permute-done.18.arrived_ref, ...), custom_call_target="tpu_custom_call" | custom-call | tf_op jit(solution)/shard_map/span_states/pallas_call | solution.py:239
  122.0 13.4 %all_to_all.5.arrived_ref = f32[16,15,128]{2,1,0:T(8,128)S(1)} all-to-all(f32[16,15,128]{2,1,0:T(8,128)S(1)} %get-tuple-element.36), channel_id=1, replica_groups=mesh['sp'=16,'tp'=32] {'sp'}, dimensions={0} | all-to-all | bytes 245760 | tf_op jit(solution)/shard_map/all_to_all | solution.py:405
  (71 shorter events, 14.5 us)
Async XLA Ops:
  0.6 21.3 %collective-permute-start.3 = (bf16[1536,128]{1,0:T(8,128)(2,1)}, bf16[1536,128]{1,0:T(8,128)(2,1)}, u32[]{:S(2)}, u32[]{:S(2)}) collective-permute-start(bf16[1536,128]{1,0:T(8,128)(2,1)} %bitcast.3.refs_0_), channel_id=1, source_target_pairs={{0,2},{1,31},{2,4},{3,1},{4,6},{5,3},{6,8},{7,5},{8,10},{9,7},{10,... | collective-permute-start | bytes 1179656 | tf_op jit(solution)/shard_map/ppermute | solution.py:332
  12.6 11.1 %collective-permute-start = (bf16[1536,128]{1,0:T(8,128)(2,1)}, bf16[1536,128]{1,0:T(8,128)(2,1)S(1)}, u32[]{:S(2)}, u32[]{:S(2)}) collective-permute-start(bf16[1536,128]{1,0:T(8,128)(2,1)} %bitcast.3.refs_0_), channel_id=1, source_target_pairs={{1,2},{0,31},{3,4},{2,1},{5,6},{4,3},{7,8},{6,5},{9,10},{8,7},{11,... | collective-permute-start | bytes 1179656 | tf_op jit(solution)/shard_map/ppermute | solution.py:332
  14.5 4.0 %collective-permute-start.1 = (bf16[3,1,128]{2,0,1:T(4,128)(2,1)}, bf16[3,1,128]{2,0,1:T(4,128)(2,1)S(1)}, u32[]{:S(2)}, u32[]{:S(2)}) collective-permute-start(bf16[3,1,128]{2,0,1:T(4,128)(2,1)} %param.7), channel_id=1, source_target_pairs={{0,1},{1,0},{2,3},{3,2},{4,5},{5,4},{6,7},{7,6},{8,9},{9,8},{10,11... | collective-permute-start | bytes 2312 | tf_op jit(solution)/shard_map/ppermute | solution.py:332
  17.6 10.0 %copy-start.1 = (bf16[4096,128]{1,0:T(8,128)(2,1)S(1)}, bf16[4096,128]{1,0:T(8,128)(2,1)}, u32[]{:S(2)}) copy-start(bf16[4096,128]{1,0:T(8,128)(2,1)} %left_ref) | copy-start | bytes 3145732
  19.2 4.4 %collective-permute-start.2 = (bf16[32,128]{1,0:T(8,128)(2,1)S(1)}, bf16[32,128]{1,0:T(8,128)(2,1)S(1)}, u32[]{:S(2)}, u32[]{:S(2)}) collective-permute-start(bf16[32,128]{1,0:T(8,128)(2,1)S(1)} %pad_maximum_fusion.1.here_new_ref), channel_id=1, source_target_pairs={{0,2},{1,31},{2,4},{3,1},{4,6},{5,3},{6,8},{7,5},{8,10},{9,7},{10,... | collective-permute-start | bytes 24584 | tf_op jit(solution)/shard_map/ppermute | solution.py:332
  23.7 13.0 %collective-permute-start.11 = (bf16[1568,128]{1,0:T(8,128)(2,1)S(1)}, bf16[1568,128]{1,0:T(8,128)(2,1)S(1)}, u32[]{:S(2)}, u32[]{:S(2)}) collective-permute-start(bf16[1568,128]{1,0:T(8,128)(2,1)S(1)} %pad_maximum_fusion), channel_id=1, source_target_pairs={{0,2},{1,31},{2,4},{3,1},{4,6},{5,3},{6,8},{7,5},{8,10},{9,7},{10,... | collective-permute-start | bytes 1204232 | tf_op jit(solution)/shard_map/ppermute | solution.py:332
  27.5 1.2 copy-start.2
  29.1 57.9 %collective-permute-start.4 = (bf16[4096,256]{1,0:T(8,128)(2,1)S(1)}, bf16[4096,256]{1,0:T(8,128)(2,1)}, u32[]{:S(2)}, u32[]{:S(2)}) collective-permute-start(bf16[4096,256]{1,0:T(8,128)(2,1)S(1)} %beside.1.own_w_ref.main_ref), channel_id=1, source_target_pairs={{0,1},{1,0},{2,3},{3,2},{4,5},{5,4},{6,7},{7,6},{8,9},{9,8},{10,11... | collective-permute-start | bytes 6291464 | tf_op jit(solution)/shard_map/ppermute | solution.py:332
  31.8 9.9 %collective-permute-start.5 = (bf16[1536,128]{1,0:T(8,128)(2,1)}, bf16[1536,128]{1,0:T(8,128)(2,1)S(1)}, u32[]{:S(2)}, u32[]{:S(2)}) collective-permute-start(bf16[1536,128]{1,0:T(8,128)(2,1)} %collective-permute-done.3.refs_0_), channel_id=1, source_target_pairs={{0,2},{1,31},{2,4},{3,1},{4,6},{5,3},{6,8},{7,5},{8,10},{9,7},{10,... | collective-permute-start | bytes 1179656 | tf_op jit(solution)/shard_map/ppermute | solution.py:332
  36.7 10.7 %collective-permute-start.12 = (bf16[1568,128]{1,0:T(8,128)(2,1)S(1)}, bf16[1568,128]{1,0:T(8,128)(2,1)S(1)}, u32[]{:S(2)}, u32[]{:S(2)}) collective-permute-start(bf16[1568,128]{1,0:T(8,128)(2,1)S(1)} %collective-permute-done.11.refs_3_), channel_id=1, source_target_pairs={{0,2},{1,31},{2,4},{3,1},{4,6},{5,3},{6,8},{7,5},{8,10},{9,7},{10,... | collective-permute-start | bytes 1204232 | tf_op jit(solution)/shard_map/ppermute | solution.py:332
  41.7 9.6 %collective-permute-start.6 = (bf16[1536,128]{1,0:T(8,128)(2,1)S(1)}, bf16[1536,128]{1,0:T(8,128)(2,1)S(1)}, u32[]{:S(2)}, u32[]{:S(2)}) collective-permute-start(bf16[1536,128]{1,0:T(8,128)(2,1)S(1)} %collective-permute-done.5.refs_1_), channel_id=1, source_target_pairs={{0,2},{1,31},{2,4},{3,1},{4,6},{5,3},{6,8},{7,5},{8,10},{9,7},{10,... | collective-permute-start | bytes 1179656 | tf_op jit(solution)/shard_map/ppermute | solution.py:332
  47.4 9.7 %collective-permute-start.13 = (bf16[1568,128]{1,0:T(8,128)(2,1)S(1)}, bf16[1568,128]{1,0:T(8,128)(2,1)S(1)}, u32[]{:S(2)}, u32[]{:S(2)}) collective-permute-start(bf16[1568,128]{1,0:T(8,128)(2,1)S(1)} %collective-permute-done.12.refs_4_), channel_id=1, source_target_pairs={{0,2},{1,31},{2,4},{3,1},{4,6},{5,3},{6,8},{7,5},{8,10},{9,7},{10,... | collective-permute-start | bytes 1204232 | tf_op jit(solution)/shard_map/ppermute | solution.py:332
  51.3 10.2 %collective-permute-start.7 = (bf16[1536,128]{1,0:T(8,128)(2,1)S(1)}, bf16[1536,128]{1,0:T(8,128)(2,1)S(1)}, u32[]{:S(2)}, u32[]{:S(2)}) collective-permute-start(bf16[1536,128]{1,0:T(8,128)(2,1)S(1)} %collective-permute-done.6.refs_1_), channel_id=1, source_target_pairs={{0,2},{1,31},{2,4},{3,1},{4,6},{5,3},{6,8},{7,5},{8,10},{9,7},{10,... | collective-permute-start | bytes 1179656 | tf_op jit(solution)/shard_map/ppermute | solution.py:332
  57.1 9.7 %collective-permute-start.14 = (bf16[1568,128]{1,0:T(8,128)(2,1)S(1)}, bf16[1568,128]{1,0:T(8,128)(2,1)S(1)}, u32[]{:S(2)}, u32[]{:S(2)}) collective-permute-start(bf16[1568,128]{1,0:T(8,128)(2,1)S(1)} %collective-permute-done.13.refs_5_), channel_id=1, source_target_pairs={{0,2},{1,31},{2,4},{3,1},{4,6},{5,3},{6,8},{7,5},{8,10},{9,7},{10,... | collective-permute-start | bytes 1204232 | tf_op jit(solution)/shard_map/ppermute | solution.py:332
  61.5 9.8 %collective-permute-start.8 = (bf16[1536,128]{1,0:T(8,128)(2,1)S(1)}, bf16[1536,128]{1,0:T(8,128)(2,1)S(1)}, u32[]{:S(2)}, u32[]{:S(2)}) collective-permute-start(bf16[1536,128]{1,0:T(8,128)(2,1)S(1)} %collective-permute-done.7.refs_2_), channel_id=1, source_target_pairs={{0,2},{1,31},{2,4},{3,1},{4,6},{5,3},{6,8},{7,5},{8,10},{9,7},{10,... | collective-permute-start | bytes 1179656 | tf_op jit(solution)/shard_map/ppermute | solution.py:332
  66.8 13.3 %collective-permute-start.15 = (bf16[1568,128]{1,0:T(8,128)(2,1)S(1)}, bf16[1568,128]{1,0:T(8,128)(2,1)}, u32[]{:S(2)}, u32[]{:S(2)}) collective-permute-start(bf16[1568,128]{1,0:T(8,128)(2,1)S(1)} %collective-permute-done.14.refs_2_), channel_id=1, source_target_pairs={{0,2},{1,31},{2,4},{3,1},{4,6},{5,3},{6,8},{7,5},{8,10},{9,7},{10,... | collective-permute-start | bytes 1204232 | tf_op jit(solution)/shard_map/ppermute | solution.py:332
  71.3 13.7 %collective-permute-start.9 = (bf16[1536,128]{1,0:T(8,128)(2,1)S(1)}, bf16[1536,128]{1,0:T(8,128)(2,1)}, u32[]{:S(2)}, u32[]{:S(2)}) collective-permute-start(bf16[1536,128]{1,0:T(8,128)(2,1)S(1)} %collective-permute-done.8.refs_0_), channel_id=1, source_target_pairs={{0,2},{1,31},{2,4},{3,1},{4,6},{5,3},{6,8},{7,5},{8,10},{9,7},{10,... | collective-permute-start | bytes 1179656 | tf_op jit(solution)/shard_map/ppermute | solution.py:332
  76.5 15.6 %collective-permute-start.17 = (bf16[1536,128]{1,0:T(8,128)(2,1)}, bf16[1536,128]{1,0:T(8,128)(2,1)}, u32[]{:S(2)}, u32[]{:S(2)}) collective-permute-start(bf16[1536,128]{1,0:T(8,128)(2,1)} %bitcast.3.refs_0_), channel_id=1, source_target_pairs={{0,1},{1,0},{2,3},{3,2},{4,5},{5,4},{6,7},{7,6},{8,9},{9,8},{10,11... | collective-permute-start | bytes 1179656 | tf_op jit(solution)/shard_map/ppermute | solution.py:332
  80.1 18.4 %collective-permute-start.16 = (bf16[1568,128]{1,0:T(8,128)(2,1)}, bf16[1568,128]{1,0:T(8,128)(2,1)}, u32[]{:S(2)}, u32[]{:S(2)}) collective-permute-start(bf16[1568,128]{1,0:T(8,128)(2,1)} %collective-permute-done.15.refs_3_), channel_id=1, source_target_pairs={{0,2},{1,31},{2,4},{3,1},{4,6},{5,3},{6,8},{7,5},{8,10},{9,7},{10,... | collective-permute-start | bytes 1204232 | tf_op jit(solution)/shard_map/ppermute | solution.py:332
  85.0 13.5 %collective-permute-start.10 = (bf16[1536,128]{1,0:T(8,128)(2,1)}, bf16[1536,128]{1,0:T(8,128)(2,1)}, u32[]{:S(2)}, u32[]{:S(2)}) collective-permute-start(bf16[1536,128]{1,0:T(8,128)(2,1)} %collective-permute-done.9.refs_1_), channel_id=1, source_target_pairs={{0,2},{1,31},{2,4},{3,1},{4,6},{5,3},{6,8},{7,5},{8,10},{9,7},{10,... | collective-permute-start | bytes 1179656 | tf_op jit(solution)/shard_map/ppermute | solution.py:332
  87.0 5.1 %copy-start.4 = (bf16[1568,128]{1,0:T(8,128)(2,1)S(1)}, bf16[1568,128]{1,0:T(8,128)(2,1)}, u32[]{:S(2)}) copy-start(bf16[1568,128]{1,0:T(8,128)(2,1)} %copy-done.3) | copy-start | bytes 1204228
  87.0 1.1 copy-start.6
  89.1 3.0 %copy-start.10 = (bf16[1536,128]{1,0:T(8,128)(2,1)S(1)}, bf16[1536,128]{1,0:T(8,128)(2,1)}, u32[]{:S(2)}) copy-start(bf16[1536,128]{1,0:T(8,128)(2,1)} %copy-done.9) | copy-start | bytes 1179652
  89.1 3.0 %copy-start.12 = (bf16[1536,128]{1,0:T(8,128)(2,1)S(1)}, bf16[1536,128]{1,0:T(8,128)(2,1)}, u32[]{:S(2)}) copy-start(bf16[1536,128]{1,0:T(8,128)(2,1)} %copy-done.11) | copy-start | bytes 1179652
  92.1 3.3 %copy-start.8 = (bf16[1568,128]{1,0:T(8,128)(2,1)S(1)}, bf16[1568,128]{1,0:T(8,128)(2,1)}, u32[]{:S(2)}) copy-start(bf16[1568,128]{1,0:T(8,128)(2,1)} %copy-done.7) | copy-start | bytes 1204228
  92.1 3.3 %copy-start.14 = (bf16[1536,128]{1,0:T(8,128)(2,1)S(1)}, bf16[1536,128]{1,0:T(8,128)(2,1)}, u32[]{:S(2)}) copy-start(bf16[1536,128]{1,0:T(8,128)(2,1)} %copy-done.13) | copy-start | bytes 1179652
  98.6 21.2 %copy-start = (bf16[4096,128]{1,0:T(8,128)(2,1)S(1)}, bf16[4096,128]{1,0:T(8,128)(2,1)}, u32[]{:S(2)}) copy-start(bf16[4096,128]{1,0:T(8,128)(2,1)} %query_w_ref.1) | copy-start | bytes 3145732
  98.6 21.2 %copy-start.17 = (f32[2]{0:T(128)S(1)}, f32[2]{0:T(128)}, u32[]{:S(2)}) copy-start(f32[2]{0:T(128)} %rate_ref.1) | copy-start | bytes 28
  101.4 18.3 %collective-permute-start.18 = (f32[1536,256]{1,0:T(8,128)S(1)}, f32[1536,256]{1,0:T(8,128)S(1)}, u32[]{:S(2)}, u32[]{:S(2)}) collective-permute-start(f32[1536,256]{1,0:T(8,128)S(1)} %get-tuple-element.33), channel_id=1, source_target_pairs={{0,1},{1,0},{2,3},{3,2},{4,5},{5,4},{6,7},{7,6},{8,9},{9,8},{10,11... | collective-permute-start | bytes 4718600 | tf_op jit(solution)/shard_map/ppermute | solution.py:332
  105.6 11.3 %collective-permute-start.20 = (bf16[1536,128]{1,0:T(8,128)(2,1)}, bf16[1536,128]{1,0:T(8,128)(2,1)S(1)}, u32[]{:S(2)}, u32[]{:S(2)}) collective-permute-start(bf16[1536,128]{1,0:T(8,128)(2,1)} %collective-permute-done.10.refs_0_), channel_id=1, source_target_pairs={{0,2},{1,31},{2,4},{3,1},{4,6},{5,3},{6,8},{7,5},{8,10},{9,7},{10,... | collective-permute-start | bytes 1179656 | tf_op jit(solution)/shard_map/ppermute | solution.py:332
  110.4 9.3 %collective-permute-start.21 = (bf16[1568,128]{1,0:T(8,128)(2,1)}, bf16[1568,128]{1,0:T(8,128)(2,1)S(1)}, u32[]{:S(2)}, u32[]{:S(2)}) collective-permute-start(bf16[1568,128]{1,0:T(8,128)(2,1)} %collective-permute-done.16.refs_1_), channel_id=1, source_target_pairs={{0,2},{1,31},{2,4},{3,1},{4,6},{5,3},{6,8},{7,5},{8,10},{9,7},{10,... | collective-permute-start | bytes 1204232 | tf_op jit(solution)/shard_map/ppermute | solution.py:332
  113.8 3.1 %collective-permute-start.19 = (bf16[224,128]{1,0:T(8,128)(2,1)S(1)}, bf16[224,128]{1,0:T(8,128)(2,1)S(1)}, u32[]{:S(2)}, u32[]{:S(2)}) collective-permute-start(bf16[224,128]{1,0:T(8,128)(2,1)S(1)} %constant_dynamic-update-slice_fusion.mine_new_ref), channel_id=1, source_target_pairs={{0,1},{1,0},{2,3},{3,2},{4,5},{5,4},{6,7},{7,6},{8,9},{9,8},{10,11... | collective-permute-start | bytes 172040 | tf_op jit(solution)/shard_map/ppermute | solution.py:332
  (8 other events, 6.3 us)

commit v9 on v8

--- a/solution.py
+++ b/solution.py
@@ -146,8 +146,10 @@
     here_new_ref,
     mine_new_ref,
     theirs_new_ref,
-    last_a_ref,
-    last_b_ref,
+    tail_a_ref,
+    tail_b_ref,
+    passed_a_ref,
+    passed_b_ref,
     main_ref,
     query_w_ref,
     cos_ref,
@@ -155,7 +157,7 @@
     out_ref,
     own_ref,
 ):
-    rows, width = last_a_ref.shape
+    rows, width = tail_a_ref.shape
     inner = query_w_ref.shape[1]
     groups, out_rows, _ = out_ref.shape
     keep = HD // groups
@@ -182,7 +184,7 @@
         pieces += pair(mine_new_ref, (k - 1) * 2 * EXTRA)
         pieces += pair(theirs_new_ref, (k - 1) * 2 * EXTRA)
         order += [k, -k]
-    pieces += pair(last_b_ref, rows)
+    pieces += [x + y for x, y in zip(pair(tail_b_ref, rows), pair(passed_b_ref, rows))]
     order.append(reach)
     entries = jnp.concatenate(pieces, axis=1)
     plane_rows = [at_rows(row_block(place_ref, k), 2 * width) for k in order]
@@ -210,12 +212,18 @@
     own_ref[...] = score * new_value
     columns = jnp.transpose(query)
 
-    last_weights = stacked(place_ref, main_ref, [reach], width)
+    last_weights = main_ref[at_rows(row_block(place_ref, reach), 2 * width), :]
     cosine = cos_ref[:span_len, :]
     sine = sin_ref[:span_len, :]
     for s in range(prompts):
         at = pl.ds(s * span_len, span_len)
-        last = jnp.concatenate([last_a_ref[at, :], last_b_ref[at, :]], axis=1)
+        last = jnp.concatenate(
+            [
+                tail_b_ref[at, :] + passed_b_ref[at, :],
+                tail_a_ref[at, :] + passed_a_ref[at, :],
+            ],
+            axis=1,
+        )
         total = total_ref[at, :] + arrived_ref[at, :]
         total += jnp.dot(last, last_weights, preferred_element_type=jnp.float32)
         keys = total[:, :inner]
@@ -360,12 +368,16 @@
     main_weights = beside(key_weight, value_weight)
     other_weights = sent(main_weights, partner)
     b_list[0] = sent(tokens, partner)
-    for _ in range(2, reach + 1):
+    for _ in range(2, reach):
         chain_a = sent(chain_a, onward)
         chain_b = sent(chain_b, onward)
         a_list.append(chain_a)
         b_list.append(chain_b)
         new_list.append(chain_b[rows:])
+    down = [(2 * z + 1, 2 * ((z - 1) % planes) + 1) for z in range(planes)]
+    inward = [(2 * z + 1, 2 * z) for z in range(planes)]
+    tail_a = sent(chain_a, down)
+    tail_b = sent(chain_b, down)
     sums = ()
     for offsets in ((1, 2), (0, 3, 4), (5, 6), (7,)):
         sums = ring_sums(
@@ -381,8 +393,10 @@
     own, other = sums
 
     arrived = sent(other, partner)
-    mine_new = jnp.concatenate(new_list[:-1], axis=0)
+    mine_new = jnp.concatenate(new_list, axis=0)
     theirs_new = sent(mine_new, partner)
+    passed_a = sent(tail_a, inward)
+    passed_b = sent(tail_b, inward)
 
     messages, own_term = span_states(
         prompts,
@@ -394,8 +408,10 @@
         new_pair,
         mine_new,
         theirs_new,
-        a_list[-1],
-        b_list[-1],
+        tail_a,
+        tail_b,
+        passed_a,
+        passed_b,
         main_weights,
         query_weight,
         cosine,

time: 138 us -> 143 us (1.036)
  waiting for transfers between devices: 8.49 us -> 11.7 us
  starting transfers between devices: 85.1 us -> 87.7 us
    ppermute x22 -> x24, waiting for transfers between devices: 8.49 us -> 11.7 us  [sent(): return lax.ppermute(value, 'tp', pairs)]
    ppermute x22 -> x24, starting transfers between devices: 85.1 us -> 87.7 us  [sent(): return lax.ppermute(value, 'tp', pairs)]
  transfers between devices with their start and end apart: 22 -> 24, of which waited for: 6 -> 7; matrix products, arithmetic and copies ran while one was open for 3% -> 3% of each run, Pallas kernels for 7% -> 7%
where the time goes in v9:
time: 143 us; the launch traced here: 142 us
  starting transfers between devices  87.7 us (61%)
  Pallas kernels  15.6 us (11%)
  blocking collectives  13.4 us (9%)
  waiting for transfers between devices  11.7 us (8%)
  local copies, waits for them, and re-layouts  10.7 us (7%)
  other arithmetic  1.83 us (1%)
    ppermute x24, starting transfers between devices, sent(): return lax.ppermute(value, 'tp', pairs)  87.7 us
    all_to_all x1, blocking collectives, body(): lax.all_to_all(messages, 'sp', split_axis=0, concat_axis=0, tiled=True)  13.4 us
    pallas_call x4, Pallas kernels, ring_sums(): pl.pallas_call(functools.partial(sums_kernel, offsets, span_len, bool(bef...  12.1 us
    ppermute x24, waiting for transfers between devices, sent(): return lax.ppermute(value, 'tp', pairs)  11.7 us
    unnamed x42, local copies, waits for them, and re-layouts  10 us
  transfers between devices with their start and end apart: 24, of which 7 were waited for; matrix products, arithmetic and copies ran while one was open for 3% of the time, Pallas kernels for 7%

profile of v9, /device:TPU:1, one launch (start us, length us, event | category | flops | bytes accessed | tf_op | source)
XLA Modules:
  0.0 142.0 jit_solution(4384269642012389831)
XLA Ops:
  0.6 11.9 %collective-permute-start.3 = (bf16[1536,128]{1,0:T(8,128)(2,1)}, bf16[1536,128]{1,0:T(8,128)(2,1)}, u32[]{:S(2)}, u32[]{:S(2)}) collective-permute-start(bf16[1536,128]{1,0:T(8,128)(2,1)} %bitcast.3.refs_0_), channel_id=1, source_target_pairs={{0,2},{1,31},{2,4},{3,1},{4,6},{5,3},{6,8},{7,5},{8,10},{9,7},{10,... | collective-permute-start | bytes 1179656 | tf_op jit(solution)/shard_map/ppermute | solution.py:340
  12.6 1.9 %collective-permute-start = (bf16[1536,128]{1,0:T(8,128)(2,1)}, bf16[1536,128]{1,0:T(8,128)(2,1)S(1)}, u32[]{:S(2)}, u32[]{:S(2)}) collective-permute-start(bf16[1536,128]{1,0:T(8,128)(2,1)} %bitcast.3.refs_0_), channel_id=1, source_target_pairs={{1,2},{0,31},{3,4},{2,1},{5,6},{4,3},{7,8},{6,5},{9,10},{8,7},{11,... | collective-permute-start | bytes 1179656 | tf_op jit(solution)/shard_map/ppermute | solution.py:340
  14.5 3.0 %collective-permute-start.1 = (bf16[3,1,128]{2,0,1:T(4,128)(2,1)}, bf16[3,1,128]{2,0,1:T(4,128)(2,1)S(1)}, u32[]{:S(2)}, u32[]{:S(2)}) collective-permute-start(bf16[3,1,128]{2,0,1:T(4,128)(2,1)} %param.7), channel_id=1, source_target_pairs={{0,1},{1,0},{2,3},{3,2},{4,5},{5,4},{6,7},{7,6},{8,9},{9,8},{10,11... | collective-permute-start | bytes 2312 | tf_op jit(solution)/shard_map/ppermute | solution.py:340
  19.2 2.6 %collective-permute-start.2 = (bf16[32,128]{1,0:T(8,128)(2,1)S(1)}, bf16[32,128]{1,0:T(8,128)(2,1)S(1)}, u32[]{:S(2)}, u32[]{:S(2)}) collective-permute-start(bf16[32,128]{1,0:T(8,128)(2,1)S(1)} %pad_maximum_fusion.1.here_new_ref), channel_id=1, source_target_pairs={{0,2},{1,31},{2,4},{3,1},{4,6},{5,3},{6,8},{7,5},{8,10},{9,7},{10,... | collective-permute-start | bytes 24584 | tf_op jit(solution)/shard_map/ppermute | solution.py:340
  23.7 3.8 %collective-permute-start.11 = (bf16[1568,128]{1,0:T(8,128)(2,1)S(1)}, bf16[1568,128]{1,0:T(8,128)(2,1)S(1)}, u32[]{:S(2)}, u32[]{:S(2)}) collective-permute-start(bf16[1568,128]{1,0:T(8,128)(2,1)S(1)} %pad_maximum_fusion), channel_id=1, source_target_pairs={{0,2},{1,31},{2,4},{3,1},{4,6},{5,3},{6,8},{7,5},{8,10},{9,7},{10,... | collective-permute-start | bytes 1204232 | tf_op jit(solution)/shard_map/ppermute | solution.py:340
  29.1 2.7 %collective-permute-start.4 = (bf16[4096,256]{1,0:T(8,128)(2,1)S(1)}, bf16[4096,256]{1,0:T(8,128)(2,1)}, u32[]{:S(2)}, u32[]{:S(2)}) collective-permute-start(bf16[4096,256]{1,0:T(8,128)(2,1)S(1)} %beside.1.own_w_ref.main_ref), channel_id=1, source_target_pairs={{0,1},{1,0},{2,3},{3,2},{4,5},{5,4},{6,7},{7,6},{8,9},{9,8},{10,11... | collective-permute-start | bytes 6291464 | tf_op jit(solution)/shard_map/ppermute | solution.py:340
  31.8 4.9 %collective-permute-start.5 = (bf16[1536,128]{1,0:T(8,128)(2,1)}, bf16[1536,128]{1,0:T(8,128)(2,1)S(1)}, u32[]{:S(2)}, u32[]{:S(2)}) collective-permute-start(bf16[1536,128]{1,0:T(8,128)(2,1)} %collective-permute-done.3.refs_0_), channel_id=1, source_target_pairs={{0,2},{1,31},{2,4},{3,1},{4,6},{5,3},{6,8},{7,5},{8,10},{9,7},{10,... | collective-permute-start | bytes 1179656 | tf_op jit(solution)/shard_map/ppermute | solution.py:340
  36.7 1.9 %collective-permute-start.12 = (bf16[1568,128]{1,0:T(8,128)(2,1)S(1)}, bf16[1568,128]{1,0:T(8,128)(2,1)S(1)}, u32[]{:S(2)}, u32[]{:S(2)}) collective-permute-start(bf16[1568,128]{1,0:T(8,128)(2,1)S(1)} %collective-permute-done.11.refs_3_), channel_id=1, source_target_pairs={{0,2},{1,31},{2,4},{3,1},{4,6},{5,3},{6,8},{7,5},{8,10},{9,7},{10,... | collective-permute-start | bytes 1204232 | tf_op jit(solution)/shard_map/ppermute | solution.py:340
  39.4 2.3 %collective-permute-done.5.refs_1_ = bf16[1536,128]{1,0:T(8,128)(2,1)S(1)} collective-permute-done((bf16[1536,128]{1,0:T(8,128)(2,1)}, bf16[1536,128]{1,0:T(8,128)(2,1)S(1)}, u32[]{:S(2)}, u32[]{:S(2)}) %collective-permute-start.5) | collective-permute-done | bytes 393248 | tf_op jit(solution)/shard_map/ppermute | solution.py:340
  41.7 4.9 %collective-permute-start.6 = (bf16[1536,128]{1,0:T(8,128)(2,1)S(1)}, bf16[1536,128]{1,0:T(8,128)(2,1)S(1)}, u32[]{:S(2)}, u32[]{:S(2)}) collective-permute-start(bf16[1536,128]{1,0:T(8,128)(2,1)S(1)} %collective-permute-done.5.refs_1_), channel_id=1, source_target_pairs={{0,2},{1,31},{2,4},{3,1},{4,6},{5,3},{6,8},{7,5},{8,10},{9,7},{10,... | collective-permute-start | bytes 1179656 | tf_op jit(solution)/shard_map/ppermute | solution.py:340
  47.4 3.5 %collective-permute-start.13 = (bf16[1568,128]{1,0:T(8,128)(2,1)S(1)}, bf16[1568,128]{1,0:T(8,128)(2,1)S(1)}, u32[]{:S(2)}, u32[]{:S(2)}) collective-permute-start(bf16[1568,128]{1,0:T(8,128)(2,1)S(1)} %collective-permute-done.12.refs_4_), channel_id=1, source_target_pairs={{0,2},{1,31},{2,4},{3,1},{4,6},{5,3},{6,8},{7,5},{8,10},{9,7},{10,... | collective-permute-start | bytes 1204232 | tf_op jit(solution)/shard_map/ppermute | solution.py:340
  51.3 5.0 %collective-permute-start.7 = (bf16[1536,128]{1,0:T(8,128)(2,1)S(1)}, bf16[1536,128]{1,0:T(8,128)(2,1)S(1)}, u32[]{:S(2)}, u32[]{:S(2)}) collective-permute-start(bf16[1536,128]{1,0:T(8,128)(2,1)S(1)} %collective-permute-done.6.refs_1_), channel_id=1, source_target_pairs={{0,2},{1,31},{2,4},{3,1},{4,6},{5,3},{6,8},{7,5},{8,10},{9,7},{10,... | collective-permute-start | bytes 1179656 | tf_op jit(solution)/shard_map/ppermute | solution.py:340
  57.1 3.6 %collective-permute-start.14 = (bf16[1568,128]{1,0:T(8,128)(2,1)S(1)}, bf16[1568,128]{1,0:T(8,128)(2,1)S(1)}, u32[]{:S(2)}, u32[]{:S(2)}) collective-permute-start(bf16[1568,128]{1,0:T(8,128)(2,1)S(1)} %collective-permute-done.13.refs_5_), channel_id=1, source_target_pairs={{0,2},{1,31},{2,4},{3,1},{4,6},{5,3},{6,8},{7,5},{8,10},{9,7},{10,... | collective-permute-start | bytes 1204232 | tf_op jit(solution)/shard_map/ppermute | solution.py:340
  61.5 4.6 %collective-permute-start.8 = (bf16[1536,128]{1,0:T(8,128)(2,1)S(1)}, bf16[1536,128]{1,0:T(8,128)(2,1)S(1)}, u32[]{:S(2)}, u32[]{:S(2)}) collective-permute-start(bf16[1536,128]{1,0:T(8,128)(2,1)S(1)} %collective-permute-done.7.refs_2_), channel_id=1, source_target_pairs={{0,2},{1,31},{2,4},{3,1},{4,6},{5,3},{6,8},{7,5},{8,10},{9,7},{10,... | collective-permute-start | bytes 1179656 | tf_op jit(solution)/shard_map/ppermute | solution.py:340
  66.8 3.7 %collective-permute-start.15 = (bf16[1568,128]{1,0:T(8,128)(2,1)S(1)}, bf16[1568,128]{1,0:T(8,128)(2,1)}, u32[]{:S(2)}, u32[]{:S(2)}) collective-permute-start(bf16[1568,128]{1,0:T(8,128)(2,1)S(1)} %collective-permute-done.14.refs_2_), channel_id=1, source_target_pairs={{0,2},{1,31},{2,4},{3,1},{4,6},{5,3},{6,8},{7,5},{8,10},{9,7},{10,... | collective-permute-start | bytes 1204232 | tf_op jit(solution)/shard_map/ppermute | solution.py:340
  71.3 4.5 %collective-permute-start.9 = (bf16[1536,128]{1,0:T(8,128)(2,1)S(1)}, bf16[1536,128]{1,0:T(8,128)(2,1)}, u32[]{:S(2)}, u32[]{:S(2)}) collective-permute-start(bf16[1536,128]{1,0:T(8,128)(2,1)S(1)} %collective-permute-done.8.refs_0_), channel_id=1, source_target_pairs={{0,2},{1,31},{2,4},{3,1},{4,6},{5,3},{6,8},{7,5},{8,10},{9,7},{10,... | collective-permute-start | bytes 1179656 | tf_op jit(solution)/shard_map/ppermute | solution.py:340
  76.5 3.6 %collective-permute-start.17 = (bf16[1536,128]{1,0:T(8,128)(2,1)}, bf16[1536,128]{1,0:T(8,128)(2,1)}, u32[]{:S(2)}, u32[]{:S(2)}) collective-permute-start(bf16[1536,128]{1,0:T(8,128)(2,1)} %bitcast.3.refs_0_), channel_id=1, source_target_pairs={{0,1},{1,0},{2,3},{3,2},{4,5},{5,4},{6,7},{7,6},{8,9},{9,8},{10,11... | collective-permute-start | bytes 1179656 | tf_op jit(solution)/shard_map/ppermute | solution.py:340
  80.1 4.9 %collective-permute-start.16 = (bf16[1568,128]{1,0:T(8,128)(2,1)}, bf16[1568,128]{1,0:T(8,128)(2,1)}, u32[]{:S(2)}, u32[]{:S(2)}) collective-permute-start(bf16[1568,128]{1,0:T(8,128)(2,1)} %collective-permute-done.15.refs_3_), channel_id=1, source_target_pairs={{0,2},{1,31},{2,4},{3,1},{4,6},{5,3},{6,8},{7,5},{8,10},{9,7},{10,... | collective-permute-start | bytes 1204232 | tf_op jit(solution)/shard_map/ppermute | solution.py:340
  85.0 1.9 %collective-permute-start.10 = (bf16[1536,128]{1,0:T(8,128)(2,1)}, bf16[1536,128]{1,0:T(8,128)(2,1)}, u32[]{:S(2)}, u32[]{:S(2)}) collective-permute-start(bf16[1536,128]{1,0:T(8,128)(2,1)} %collective-permute-done.9.refs_1_), channel_id=1, source_target_pairs={{0,2},{1,31},{2,4},{3,1},{4,6},{5,3},{6,8},{7,5},{8,10},{9,7},{10,... | collective-permute-start | bytes 1179656 | tf_op jit(solution)/shard_map/ppermute | solution.py:340
  89.1 3.0 %ring_sums.4 = (f32[1536,256]{1,0:T(8,128)S(1)}, f32[1536,256]{1,0:T(8,128)S(1)}) custom-call(s32[4]{0:T(128)S(1)} %pad_add_fusion.place_ref, bf16[4096,256]{1,0:T(8,128)(2,1)S(1)} %beside.1.own_w_ref.main_ref, bf16[4096,256]{1,0:T(8,128)(2,1)} %collective-permute-done.4.other_w_ref, bf16[1536,128]{1,0:T(8,128)(2,1)} %collective-permute-done.3.refs_0_, ...), custom_call_target="tpu_custom_call" | custom-call | flops 805306368 | tf_op jit(solution)/shard_map/ring_sums/pallas_call | solution.py:121
  92.2 3.3 %ring_sums.5 = (f32[1536,256]{1,0:T(8,128)S(1)}, f32[1536,256]{1,0:T(8,128)S(1)}) custom-call(s32[4]{0:T(128)S(1)} %pad_add_fusion.place_ref, bf16[4096,256]{1,0:T(8,128)(2,1)S(1)} %beside.1.own_w_ref.main_ref, bf16[4096,256]{1,0:T(8,128)(2,1)} %collective-permute-done.4.other_w_ref, bf16[1536,128]{1,0:T(8,128)(2,1)} %bitcast.3.refs_0_, ...), custom_call_target="tpu_custom_call" | custom-call | flops 1207959552 | tf_op jit(solution)/shard_map/ring_sums/pallas_call | solution.py:121
  95.5 3.0 %ring_sums.6 = (f32[1536,256]{1,0:T(8,128)S(1)}, f32[1536,256]{1,0:T(8,128)S(1)}) custom-call(s32[4]{0:T(128)S(1)} %pad_add_fusion.place_ref, bf16[4096,256]{1,0:T(8,128)(2,1)S(1)} %beside.1.own_w_ref.main_ref, bf16[4096,256]{1,0:T(8,128)(2,1)} %collective-permute-done.4.other_w_ref, bf16[1536,128]{1,0:T(8,128)(2,1)S(1)} %copy-done.14, ...), custom_call_target="tpu_custom_call" | custom-call | flops 805306368 | tf_op jit(solution)/shard_map/ring_sums/pallas_call | solution.py:121
  98.6 2.8 %ring_sums.7 = (f32[1536,256]{1,0:T(8,128)S(1)}, f32[1536,256]{1,0:T(8,128)S(1)}) custom-call(s32[4]{0:T(128)S(1)} %pad_add_fusion.place_ref, bf16[4096,256]{1,0:T(8,128)(2,1)S(1)} %beside.1.own_w_ref.main_ref, bf16[4096,256]{1,0:T(8,128)(2,1)} %collective-permute-done.4.other_w_ref, bf16[1536,128]{1,0:T(8,128)(2,1)} %collective-permute-done.10.refs_0_, ...), custom_call_target="tpu_custom_call" | custom-call | flops 402653184 | tf_op jit(solution)/shard_map/ring_sums/pallas_call | solution.py:121
  101.4 3.4 %collective-permute-start.18 = (f32[1536,256]{1,0:T(8,128)S(1)}, f32[1536,256]{1,0:T(8,128)S(1)}, u32[]{:S(2)}, u32[]{:S(2)}) collective-permute-start(f32[1536,256]{1,0:T(8,128)S(1)} %get-tuple-element.33), channel_id=1, source_target_pairs={{0,1},{1,0},{2,3},{3,2},{4,5},{5,4},{6,7},{7,6},{8,9},{9,8},{10,11... | collective-permute-start | bytes 4718600 | tf_op jit(solution)/shard_map/ppermute | solution.py:340
  105.5 4.8 %collective-permute-start.20 = (bf16[1536,128]{1,0:T(8,128)(2,1)}, bf16[1536,128]{1,0:T(8,128)(2,1)S(1)}, u32[]{:S(2)}, u32[]{:S(2)}) collective-permute-start(bf16[1536,128]{1,0:T(8,128)(2,1)} %collective-permute-done.10.refs_0_), channel_id=1, source_target_pairs={{1,31},{3,1},{5,3},{7,5},{9,7},{11,9},{13,11},{15,13},{17,15},{19,... | collective-permute-start | bytes 1179656 | tf_op jit(solution)/shard_map/ppermute | solution.py:340
  110.4 1.9 %collective-permute-start.21 = (bf16[1568,128]{1,0:T(8,128)(2,1)}, bf16[1568,128]{1,0:T(8,128)(2,1)S(1)}, u32[]{:S(2)}, u32[]{:S(2)}) collective-permute-start(bf16[1568,128]{1,0:T(8,128)(2,1)} %collective-permute-done.16.refs_1_), channel_id=1, source_target_pairs={{1,31},{3,1},{5,3},{7,5},{9,7},{11,9},{13,11},{15,13},{17,15},{19,... | collective-permute-start | bytes 1204232 | tf_op jit(solution)/shard_map/ppermute | solution.py:340
  112.3 3.1 %collective-permute-done.20.tail_a_ref = bf16[1536,128]{1,0:T(8,128)(2,1)S(1)} collective-permute-done((bf16[1536,128]{1,0:T(8,128)(2,1)}, bf16[1536,128]{1,0:T(8,128)(2,1)S(1)}, u32[]{:S(2)}, u32[]{:S(2)}) %collective-permute-start.20) | collective-permute-done | bytes 393248 | tf_op jit(solution)/shard_map/ppermute | solution.py:340
  116.7 3.0 %collective-permute-done.21.tail_b_ref = bf16[1568,128]{1,0:T(8,128)(2,1)S(1)} collective-permute-done((bf16[1568,128]{1,0:T(8,128)(2,1)}, bf16[1568,128]{1,0:T(8,128)(2,1)S(1)}, u32[]{:S(2)}, u32[]{:S(2)}) %collective-permute-start.21) | collective-permute-done | bytes 401440 | tf_op jit(solution)/shard_map/ppermute | solution.py:340
  119.7 1.3 collective-permute-start.23
  122.4 1.9 %collective-permute-start.19 = (bf16[224,128]{1,0:T(8,128)(2,1)S(1)}, bf16[224,128]{1,0:T(8,128)(2,1)S(1)}, u32[]{:S(2)}, u32[]{:S(2)}) collective-permute-start(bf16[224,128]{1,0:T(8,128)(2,1)S(1)} %constant_dynamic-update-slice_fusion.mine_new_ref), channel_id=1, source_target_pairs={{0,1},{1,0},{2,3},{3,2},{4,5},{5,4},{6,7},{7,6},{8,9},{9,8},{10,11... | collective-permute-start | bytes 172040 | tf_op jit(solution)/shard_map/ppermute | solution.py:340
  125.6 2.3 %span_states.1 = (f32[16,15,128]{2,1,0:T(8,128)S(1)}, f32[16,128]{1,0:T(8,128)S(1)}) custom-call(s32[4]{0:T(128)S(1)} %pad_add_fusion.place_ref, f32[2]{0:T(128)S(1)} %copy-done.17, f32[1536,256]{1,0:T(8,128)S(1)} %get-tuple-element.32.total_ref, f32[1536,256]{1,0:T(8,128)S(1)} %collective-permute-done.18.arrived_ref, ...), custom_call_target="tpu_custom_call" | custom-call | tf_op jit(solution)/shard_map/span_states/pallas_call | solution.py:247
  127.9 13.4 %all_to_all.5.arrived_ref = f32[16,15,128]{2,1,0:T(8,128)S(1)} all-to-all(f32[16,15,128]{2,1,0:T(8,128)S(1)} %get-tuple-element.36), channel_id=1, replica_groups=mesh['sp'=16,'tp'=32] {'sp'}, dimensions={0} | all-to-all | bytes 245760 | tf_op jit(solution)/shard_map/all_to_all | solution.py:421
  (75 shorter events, 18.3 us)
Async XLA Ops:
  0.6 21.3 %collective-permute-start.3 = (bf16[1536,128]{1,0:T(8,128)(2,1)}, bf16[1536,128]{1,0:T(8,128)(2,1)}, u32[]{:S(2)}, u32[]{:S(2)}) collective-permute-start(bf16[1536,128]{1,0:T(8,128)(2,1)} %bitcast.3.refs_0_), channel_id=1, source_target_pairs={{0,2},{1,31},{2,4},{3,1},{4,6},{5,3},{6,8},{7,5},{8,10},{9,7},{10,... | collective-permute-start | bytes 1179656 | tf_op jit(solution)/shard_map/ppermute | solution.py:340
  12.6 11.1 %collective-permute-start = (bf16[1536,128]{1,0:T(8,128)(2,1)}, bf16[1536,128]{1,0:T(8,128)(2,1)S(1)}, u32[]{:S(2)}, u32[]{:S(2)}) collective-permute-start(bf16[1536,128]{1,0:T(8,128)(2,1)} %bitcast.3.refs_0_), channel_id=1, source_target_pairs={{1,2},{0,31},{3,4},{2,1},{5,6},{4,3},{7,8},{6,5},{9,10},{8,7},{11,... | collective-permute-start | bytes 1179656 | tf_op jit(solution)/shard_map/ppermute | solution.py:340
  14.5 4.0 %collective-permute-start.1 = (bf16[3,1,128]{2,0,1:T(4,128)(2,1)}, bf16[3,1,128]{2,0,1:T(4,128)(2,1)S(1)}, u32[]{:S(2)}, u32[]{:S(2)}) collective-permute-start(bf16[3,1,128]{2,0,1:T(4,128)(2,1)} %param.7), channel_id=1, source_target_pairs={{0,1},{1,0},{2,3},{3,2},{4,5},{5,4},{6,7},{7,6},{8,9},{9,8},{10,11... | collective-permute-start | bytes 2312 | tf_op jit(solution)/shard_map/ppermute | solution.py:340
  17.6 10.0 %copy-start.1 = (bf16[4096,128]{1,0:T(8,128)(2,1)S(1)}, bf16[4096,128]{1,0:T(8,128)(2,1)}, u32[]{:S(2)}) copy-start(bf16[4096,128]{1,0:T(8,128)(2,1)} %left_ref) | copy-start | bytes 3145732
  19.2 4.4 %collective-permute-start.2 = (bf16[32,128]{1,0:T(8,128)(2,1)S(1)}, bf16[32,128]{1,0:T(8,128)(2,1)S(1)}, u32[]{:S(2)}, u32[]{:S(2)}) collective-permute-start(bf16[32,128]{1,0:T(8,128)(2,1)S(1)} %pad_maximum_fusion.1.here_new_ref), channel_id=1, source_target_pairs={{0,2},{1,31},{2,4},{3,1},{4,6},{5,3},{6,8},{7,5},{8,10},{9,7},{10,... | collective-permute-start | bytes 24584 | tf_op jit(solution)/shard_map/ppermute | solution.py:340
  23.7 13.0 %collective-permute-start.11 = (bf16[1568,128]{1,0:T(8,128)(2,1)S(1)}, bf16[1568,128]{1,0:T(8,128)(2,1)S(1)}, u32[]{:S(2)}, u32[]{:S(2)}) collective-permute-start(bf16[1568,128]{1,0:T(8,128)(2,1)S(1)} %pad_maximum_fusion), channel_id=1, source_target_pairs={{0,2},{1,31},{2,4},{3,1},{4,6},{5,3},{6,8},{7,5},{8,10},{9,7},{10,... | collective-permute-start | bytes 1204232 | tf_op jit(solution)/shard_map/ppermute | solution.py:340
  29.1 57.9 %collective-permute-start.4 = (bf16[4096,256]{1,0:T(8,128)(2,1)S(1)}, bf16[4096,256]{1,0:T(8,128)(2,1)}, u32[]{:S(2)}, u32[]{:S(2)}) collective-permute-start(bf16[4096,256]{1,0:T(8,128)(2,1)S(1)} %beside.1.own_w_ref.main_ref), channel_id=1, source_target_pairs={{0,1},{1,0},{2,3},{3,2},{4,5},{5,4},{6,7},{7,6},{8,9},{9,8},{10,11... | collective-permute-start | bytes 6291464 | tf_op jit(solution)/shard_map/ppermute | solution.py:340
  31.8 9.9 %collective-permute-start.5 = (bf16[1536,128]{1,0:T(8,128)(2,1)}, bf16[1536,128]{1,0:T(8,128)(2,1)S(1)}, u32[]{:S(2)}, u32[]{:S(2)}) collective-permute-start(bf16[1536,128]{1,0:T(8,128)(2,1)} %collective-permute-done.3.refs_0_), channel_id=1, source_target_pairs={{0,2},{1,31},{2,4},{3,1},{4,6},{5,3},{6,8},{7,5},{8,10},{9,7},{10,... | collective-permute-start | bytes 1179656 | tf_op jit(solution)/shard_map/ppermute | solution.py:340
  36.7 10.7 %collective-permute-start.12 = (bf16[1568,128]{1,0:T(8,128)(2,1)S(1)}, bf16[1568,128]{1,0:T(8,128)(2,1)S(1)}, u32[]{:S(2)}, u32[]{:S(2)}) collective-permute-start(bf16[1568,128]{1,0:T(8,128)(2,1)S(1)} %collective-permute-done.11.refs_3_), channel_id=1, source_target_pairs={{0,2},{1,31},{2,4},{3,1},{4,6},{5,3},{6,8},{7,5},{8,10},{9,7},{10,... | collective-permute-start | bytes 1204232 | tf_op jit(solution)/shard_map/ppermute | solution.py:340
  41.7 9.6 %collective-permute-start.6 = (bf16[1536,128]{1,0:T(8,128)(2,1)S(1)}, bf16[1536,128]{1,0:T(8,128)(2,1)S(1)}, u32[]{:S(2)}, u32[]{:S(2)}) collective-permute-start(bf16[1536,128]{1,0:T(8,128)(2,1)S(1)} %collective-permute-done.5.refs_1_), channel_id=1, source_target_pairs={{0,2},{1,31},{2,4},{3,1},{4,6},{5,3},{6,8},{7,5},{8,10},{9,7},{10,... | collective-permute-start | bytes 1179656 | tf_op jit(solution)/shard_map/ppermute | solution.py:340
  47.4 9.7 %collective-permute-start.13 = (bf16[1568,128]{1,0:T(8,128)(2,1)S(1)}, bf16[1568,128]{1,0:T(8,128)(2,1)S(1)}, u32[]{:S(2)}, u32[]{:S(2)}) collective-permute-start(bf16[1568,128]{1,0:T(8,128)(2,1)S(1)} %collective-permute-done.12.refs_4_), channel_id=1, source_target_pairs={{0,2},{1,31},{2,4},{3,1},{4,6},{5,3},{6,8},{7,5},{8,10},{9,7},{10,... | collective-permute-start | bytes 1204232 | tf_op jit(solution)/shard_map/ppermute | solution.py:340
  51.3 10.2 %collective-permute-start.7 = (bf16[1536,128]{1,0:T(8,128)(2,1)S(1)}, bf16[1536,128]{1,0:T(8,128)(2,1)S(1)}, u32[]{:S(2)}, u32[]{:S(2)}) collective-permute-start(bf16[1536,128]{1,0:T(8,128)(2,1)S(1)} %collective-permute-done.6.refs_1_), channel_id=1, source_target_pairs={{0,2},{1,31},{2,4},{3,1},{4,6},{5,3},{6,8},{7,5},{8,10},{9,7},{10,... | collective-permute-start | bytes 1179656 | tf_op jit(solution)/shard_map/ppermute | solution.py:340
  57.1 9.7 %collective-permute-start.14 = (bf16[1568,128]{1,0:T(8,128)(2,1)S(1)}, bf16[1568,128]{1,0:T(8,128)(2,1)S(1)}, u32[]{:S(2)}, u32[]{:S(2)}) collective-permute-start(bf16[1568,128]{1,0:T(8,128)(2,1)S(1)} %collective-permute-done.13.refs_5_), channel_id=1, source_target_pairs={{0,2},{1,31},{2,4},{3,1},{4,6},{5,3},{6,8},{7,5},{8,10},{9,7},{10,... | collective-permute-start | bytes 1204232 | tf_op jit(solution)/shard_map/ppermute | solution.py:340
  61.5 9.8 %collective-permute-start.8 = (bf16[1536,128]{1,0:T(8,128)(2,1)S(1)}, bf16[1536,128]{1,0:T(8,128)(2,1)S(1)}, u32[]{:S(2)}, u32[]{:S(2)}) collective-permute-start(bf16[1536,128]{1,0:T(8,128)(2,1)S(1)} %collective-permute-done.7.refs_2_), channel_id=1, source_target_pairs={{0,2},{1,31},{2,4},{3,1},{4,6},{5,3},{6,8},{7,5},{8,10},{9,7},{10,... | collective-permute-start | bytes 1179656 | tf_op jit(solution)/shard_map/ppermute | solution.py:340
  66.8 13.3 %collective-permute-start.15 = (bf16[1568,128]{1,0:T(8,128)(2,1)S(1)}, bf16[1568,128]{1,0:T(8,128)(2,1)}, u32[]{:S(2)}, u32[]{:S(2)}) collective-permute-start(bf16[1568,128]{1,0:T(8,128)(2,1)S(1)} %collective-permute-done.14.refs_2_), channel_id=1, source_target_pairs={{0,2},{1,31},{2,4},{3,1},{4,6},{5,3},{6,8},{7,5},{8,10},{9,7},{10,... | collective-permute-start | bytes 1204232 | tf_op jit(solution)/shard_map/ppermute | solution.py:340
  71.3 13.7 %collective-permute-start.9 = (bf16[1536,128]{1,0:T(8,128)(2,1)S(1)}, bf16[1536,128]{1,0:T(8,128)(2,1)}, u32[]{:S(2)}, u32[]{:S(2)}) collective-permute-start(bf16[1536,128]{1,0:T(8,128)(2,1)S(1)} %collective-permute-done.8.refs_0_), channel_id=1, source_target_pairs={{0,2},{1,31},{2,4},{3,1},{4,6},{5,3},{6,8},{7,5},{8,10},{9,7},{10,... | collective-permute-start | bytes 1179656 | tf_op jit(solution)/shard_map/ppermute | solution.py:340
  76.5 15.6 %collective-permute-start.17 = (bf16[1536,128]{1,0:T(8,128)(2,1)}, bf16[1536,128]{1,0:T(8,128)(2,1)}, u32[]{:S(2)}, u32[]{:S(2)}) collective-permute-start(bf16[1536,128]{1,0:T(8,128)(2,1)} %bitcast.3.refs_0_), channel_id=1, source_target_pairs={{0,1},{1,0},{2,3},{3,2},{4,5},{5,4},{6,7},{7,6},{8,9},{9,8},{10,11... | collective-permute-start | bytes 1179656 | tf_op jit(solution)/shard_map/ppermute | solution.py:340
  80.1 18.4 %collective-permute-start.16 = (bf16[1568,128]{1,0:T(8,128)(2,1)}, bf16[1568,128]{1,0:T(8,128)(2,1)}, u32[]{:S(2)}, u32[]{:S(2)}) collective-permute-start(bf16[1568,128]{1,0:T(8,128)(2,1)} %collective-permute-done.15.refs_3_), channel_id=1, source_target_pairs={{0,2},{1,31},{2,4},{3,1},{4,6},{5,3},{6,8},{7,5},{8,10},{9,7},{10,... | collective-permute-start | bytes 1204232 | tf_op jit(solution)/shard_map/ppermute | solution.py:340
  85.0 13.5 %collective-permute-start.10 = (bf16[1536,128]{1,0:T(8,128)(2,1)}, bf16[1536,128]{1,0:T(8,128)(2,1)}, u32[]{:S(2)}, u32[]{:S(2)}) collective-permute-start(bf16[1536,128]{1,0:T(8,128)(2,1)} %collective-permute-done.9.refs_1_), channel_id=1, source_target_pairs={{0,2},{1,31},{2,4},{3,1},{4,6},{5,3},{6,8},{7,5},{8,10},{9,7},{10,... | collective-permute-start | bytes 1179656 | tf_op jit(solution)/shard_map/ppermute | solution.py:340
  87.0 5.1 %copy-start.4 = (bf16[1568,128]{1,0:T(8,128)(2,1)S(1)}, bf16[1568,128]{1,0:T(8,128)(2,1)}, u32[]{:S(2)}) copy-start(bf16[1568,128]{1,0:T(8,128)(2,1)} %copy-done.3) | copy-start | bytes 1204228
  89.1 3.0 %copy-start.10 = (bf16[1536,128]{1,0:T(8,128)(2,1)S(1)}, bf16[1536,128]{1,0:T(8,128)(2,1)}, u32[]{:S(2)}) copy-start(bf16[1536,128]{1,0:T(8,128)(2,1)} %copy-done.9) | copy-start | bytes 1179652
  89.1 3.0 %copy-start.12 = (bf16[1536,128]{1,0:T(8,128)(2,1)S(1)}, bf16[1536,128]{1,0:T(8,128)(2,1)}, u32[]{:S(2)}) copy-start(bf16[1536,128]{1,0:T(8,128)(2,1)} %copy-done.11) | copy-start | bytes 1179652
  92.1 3.3 %copy-start.8 = (bf16[1568,128]{1,0:T(8,128)(2,1)S(1)}, bf16[1568,128]{1,0:T(8,128)(2,1)}, u32[]{:S(2)}) copy-start(bf16[1568,128]{1,0:T(8,128)(2,1)} %copy-done.7) | copy-start | bytes 1204228
  92.1 3.3 %copy-start.14 = (bf16[1536,128]{1,0:T(8,128)(2,1)S(1)}, bf16[1536,128]{1,0:T(8,128)(2,1)}, u32[]{:S(2)}) copy-start(bf16[1536,128]{1,0:T(8,128)(2,1)} %copy-done.13) | copy-start | bytes 1179652
  98.5 27.0 %copy-start = (bf16[4096,128]{1,0:T(8,128)(2,1)S(1)}, bf16[4096,128]{1,0:T(8,128)(2,1)}, u32[]{:S(2)}) copy-start(bf16[4096,128]{1,0:T(8,128)(2,1)} %query_w_ref.1) | copy-start | bytes 3145732
  98.6 27.0 %copy-start.17 = (f32[2]{0:T(128)S(1)}, f32[2]{0:T(128)}, u32[]{:S(2)}) copy-start(f32[2]{0:T(128)} %rate_ref.1) | copy-start | bytes 28
  101.4 24.2 %collective-permute-start.18 = (f32[1536,256]{1,0:T(8,128)S(1)}, f32[1536,256]{1,0:T(8,128)S(1)}, u32[]{:S(2)}, u32[]{:S(2)}) collective-permute-start(f32[1536,256]{1,0:T(8,128)S(1)} %get-tuple-element.33), channel_id=1, source_target_pairs={{0,1},{1,0},{2,3},{3,2},{4,5},{5,4},{6,7},{7,6},{8,9},{9,8},{10,11... | collective-permute-start | bytes 4718600 | tf_op jit(solution)/shard_map/ppermute | solution.py:340
  105.5 9.9 %collective-permute-start.20 = (bf16[1536,128]{1,0:T(8,128)(2,1)}, bf16[1536,128]{1,0:T(8,128)(2,1)S(1)}, u32[]{:S(2)}, u32[]{:S(2)}) collective-permute-start(bf16[1536,128]{1,0:T(8,128)(2,1)} %collective-permute-done.10.refs_0_), channel_id=1, source_target_pairs={{1,31},{3,1},{5,3},{7,5},{9,7},{11,9},{13,11},{15,13},{17,15},{19,... | collective-permute-start | bytes 1179656 | tf_op jit(solution)/shard_map/ppermute | solution.py:340
  110.4 9.3 %collective-permute-start.21 = (bf16[1568,128]{1,0:T(8,128)(2,1)}, bf16[1568,128]{1,0:T(8,128)(2,1)S(1)}, u32[]{:S(2)}, u32[]{:S(2)}) collective-permute-start(bf16[1568,128]{1,0:T(8,128)(2,1)} %collective-permute-done.16.refs_1_), channel_id=1, source_target_pairs={{1,31},{3,1},{5,3},{7,5},{9,7},{11,9},{13,11},{15,13},{17,15},{19,... | collective-permute-start | bytes 1204232 | tf_op jit(solution)/shard_map/ppermute | solution.py:340
  115.4 10.1 %collective-permute-start.22 = (bf16[1536,128]{1,0:T(8,128)(2,1)S(1)}, bf16[1536,128]{1,0:T(8,128)(2,1)S(1)}, u32[]{:S(2)}, u32[]{:S(2)}) collective-permute-start(bf16[1536,128]{1,0:T(8,128)(2,1)S(1)} %collective-permute-done.20.tail_a_ref), channel_id=1, source_target_pairs={{1,0},{3,2},{5,4},{7,6},{9,8},{11,10},{13,12},{15,14},{17,16},{19,... | collective-permute-start | bytes 1179656 | tf_op jit(solution)/shard_map/ppermute | solution.py:340
  119.7 5.9 %collective-permute-start.23 = (bf16[1568,128]{1,0:T(8,128)(2,1)S(1)}, bf16[1568,128]{1,0:T(8,128)(2,1)S(1)}, u32[]{:S(2)}, u32[]{:S(2)}) collective-permute-start(bf16[1568,128]{1,0:T(8,128)(2,1)S(1)} %collective-permute-done.21.tail_b_ref), channel_id=1, source_target_pairs={{1,0},{3,2},{5,4},{7,6},{9,8},{11,10},{13,12},{15,14},{17,16},{19,... | collective-permute-start | bytes 1204232 | tf_op jit(solution)/shard_map/ppermute | solution.py:340
  122.4 3.1 %collective-permute-start.19 = (bf16[224,128]{1,0:T(8,128)(2,1)S(1)}, bf16[224,128]{1,0:T(8,128)(2,1)S(1)}, u32[]{:S(2)}, u32[]{:S(2)}) collective-permute-start(bf16[224,128]{1,0:T(8,128)(2,1)S(1)} %constant_dynamic-update-slice_fusion.mine_new_ref), channel_id=1, source_target_pairs={{0,1},{1,0},{2,3},{3,2},{4,5},{5,4},{6,7},{7,6},{8,9},{9,8},{10,11... | collective-permute-start | bytes 172040 | tf_op jit(solution)/shard_map/ppermute | solution.py:340
  (10 other events, 8.6 us)

commit v10 on v8

--- a/solution.py
+++ b/solution.py
@@ -64,9 +64,11 @@
 def sums_kernel(offsets, span_len, has_before, place_ref, own_w_ref, other_w_ref, *refs):
     count = len(offsets)
     a_refs, b_refs, rest = refs[:count], refs[count : 2 * count], refs[2 * count :]
-    before = rest[:2] if has_before else ()
-    own_ref, other_ref, held, landed = rest[len(before) :]
+    before, rest = (rest[:2], rest[2:]) if has_before else ((), rest)
+    tails, (own_ref, other_ref, held, landed) = rest[:-4], rest[-4:]
     rows, width = a_refs[0].shape
+    for i, tail_ref in enumerate(tails):
+        other_ref[rows:, i * width : (i + 1) * width] = tail_ref[...].astype(jnp.float32)
     core = place_ref[1]
     hops = [i for i in range(count) if offsets[i] > 0]
 
@@ -111,11 +113,14 @@
     summed(other_ref, before[1] if before else None, hops, lambda: held[...])
 
 
-def ring_sums(offsets, span_len, place, own_weights, other_weights, a_list, b_list, before):
+def ring_sums(
+    offsets, span_len, place, own_weights, other_weights, a_list, b_list, before, tails=()
+):
     rows, width = a_list[0].shape
     inner = own_weights.shape[1]
     whole = pl.BlockSpec(memory_space=pltpu.VMEM)
-    operands = [*a_list, *b_list, *before]
+    operands = [*a_list, *b_list, *before, *tails]
+    more = tails[0].shape[0] if tails else 0
     blocks = 2 * sum(1 for offset in offsets if offset > 0)
     flops = 2 * rows * 2 * inner * 2 * width * len(offsets)
     return pl.pallas_call(
@@ -127,7 +132,10 @@
         ]
         + [whole] * len(operands),
         out_specs=[whole, whole],
-        out_shape=[jax.ShapeDtypeStruct((rows, inner), jnp.float32)] * 2,
+        out_shape=[
+            jax.ShapeDtypeStruct((rows, inner), jnp.float32),
+            jax.ShapeDtypeStruct((rows + more, inner), jnp.float32),
+        ],
         scratch_shapes=[
             pltpu.VMEM((blocks * width, inner), own_weights.dtype),
             pltpu.SemaphoreType.DMA((blocks,)),
@@ -145,9 +153,13 @@
     arrived_ref,
     here_new_ref,
     mine_new_ref,
+    near_new_ref,
     theirs_new_ref,
-    last_a_ref,
+    far_new_ref,
+    last_up_ref,
+    last_down_ref,
     last_b_ref,
+    passed_a_ref,
     main_ref,
     query_w_ref,
     cos_ref,
@@ -155,13 +167,14 @@
     out_ref,
     own_ref,
 ):
-    rows, width = last_a_ref.shape
+    rows, width = last_up_ref.shape
     inner = query_w_ref.shape[1]
     groups, out_rows, _ = out_ref.shape
     keep = HD // groups
     prompts = out_rows // (keep + 1)
     span_len = rows // prompts
-    reach = mine_new_ref.shape[0] // (2 * EXTRA) + 1
+    swapped = mine_new_ref.shape[0] // (2 * EXTRA)
+    reach = swapped + near_new_ref.shape[0] // (2 * EXTRA) + 1
     lane = lax.broadcasted_iota(jnp.int32, (HD, inner), 1)
     row_lane = lax.broadcasted_iota(jnp.int32, (1, inner), 1)
     lane_decay = jnp.full((1, inner), rate_ref[0], jnp.float32)
@@ -178,11 +191,18 @@
 
     pieces = pair(here_new_ref, 0)
     order = [0]
-    for k in range(1, reach):
+    for k in range(1, swapped + 1):
         pieces += pair(mine_new_ref, (k - 1) * 2 * EXTRA)
         pieces += pair(theirs_new_ref, (k - 1) * 2 * EXTRA)
         order += [k, -k]
-    pieces += pair(last_b_ref, rows)
+    late = arrived_ref[rows:, :].astype(jnp.bfloat16)
+    for k in range(swapped + 1, reach):
+        i = k - swapped - 1
+        pieces += pair(near_new_ref, i * 2 * EXTRA)
+        theirs = late[:, i * width : (i + 1) * width]
+        pieces += [theirs[:EXTRA], theirs[EXTRA:]]
+        order += [k, -k]
+    pieces += pair(far_new_ref, 0)
     order.append(reach)
     entries = jnp.concatenate(pieces, axis=1)
     plane_rows = [at_rows(row_block(place_ref, k), 2 * width) for k in order]
@@ -215,7 +235,9 @@
     sine = sin_ref[:span_len, :]
     for s in range(prompts):
         at = pl.ds(s * span_len, span_len)
-        last = jnp.concatenate([last_a_ref[at, :], last_b_ref[at, :]], axis=1)
+        other = last_b_ref[at, :] + passed_a_ref[at, :]
+        mine = last_up_ref[at, :] + last_down_ref[at, :]
+        last = jnp.concatenate([mine, other], axis=1)
         total = total_ref[at, :] + arrived_ref[at, :]
         total += jnp.dot(last, last_weights, preferred_element_type=jnp.float32)
         keys = total[:, :inner]
@@ -360,12 +382,24 @@
     main_weights = beside(key_weight, value_weight)
     other_weights = sent(main_weights, partner)
     b_list[0] = sent(tokens, partner)
-    for _ in range(2, reach + 1):
+    for _ in range(2, reach):
         chain_a = sent(chain_a, onward)
         chain_b = sent(chain_b, onward)
         a_list.append(chain_a)
         b_list.append(chain_b)
         new_list.append(chain_b[rows:])
+    down = [(2 * z + 1, 2 * ((z - 1) % planes) + 1) for z in range(planes)]
+    inward = [(2 * z + 1, 2 * z) for z in range(planes)]
+    up = [(2 * z, 2 * ((z + 1) % planes)) for z in range(planes)]
+    last_up = sent(chain_a, up)
+    last_down = sent(chain_a, down)
+    last_b = sent(chain_b, down)
+    far_new = sent(new_list[-1], onward)
+    mine_new = jnp.concatenate(new_list[: reach - 3], axis=0)
+    theirs_new = sent(mine_new, partner)
+    near_list = new_list[reach - 3 :]
+    near_new = jnp.concatenate(near_list, axis=0)
+
     sums = ()
     for offsets in ((1, 2), (0, 3, 4), (5, 6), (7,)):
         sums = ring_sums(
@@ -377,12 +411,12 @@
             [a_list[k] for k in offsets],
             [b_list[k] for k in offsets],
             sums,
+            near_list if offsets[-1] == reach - 1 else (),
         )
     own, other = sums
 
     arrived = sent(other, partner)
-    mine_new = jnp.concatenate(new_list[:-1], axis=0)
-    theirs_new = sent(mine_new, partner)
+    passed_a = sent(last_down, inward)
 
     messages, own_term = span_states(
         prompts,
@@ -393,9 +427,13 @@
         arrived,
         new_pair,
         mine_new,
+        near_new,
         theirs_new,
-        a_list[-1],
-        b_list[-1],
+        far_new,
+        last_up,
+        last_down,
+        last_b,
+        passed_a,
         main_weights,
         query_weight,
         cosine,

time: 138 us -> 144 us (1.043)
  starting transfers between devices: 85.1 us -> 92.2 us
    ppermute x22 -> x25, starting transfers between devices: 85.1 us -> 92.2 us  [sent(): return lax.ppermute(value, 'tp', pairs)]
    ppermute x22 -> x25, waiting for transfers between devices: 8.49 us -> 7.64 us  [sent(): return lax.ppermute(value, 'tp', pairs)]
    unnamed x42 -> x44, local copies, waits for them, and re-layouts: 9.98 us -> 10.3 us
  transfers between devices with their start and end apart: 22 -> 25, of which waited for: 6 -> 7; matrix products, arithmetic and copies ran while one was open for 3% -> 3% of each run, Pallas kernels for 7% -> 6%
where the time goes in v10:
time: 144 us; the launch traced here: 143 us
  starting transfers between devices  92.2 us (64%)
  Pallas kernels  15.1 us (10%)
  blocking collectives  13.4 us (9%)
  local copies, waits for them, and re-layouts  11.7 us (8%)
  waiting for transfers between devices  7.64 us (5%)
  other arithmetic  1.84 us (1%)
    ppermute x25, starting transfers between devices, sent(): return lax.ppermute(value, 'tp', pairs)  92.2 us
    all_to_all x1, blocking collectives, body(): lax.all_to_all(messages, 'sp', split_axis=0, concat_axis=0, tiled=True)  13.4 us
    pallas_call x4, Pallas kernels, ring_sums(): pl.pallas_call(functools.partial(sums_kernel, offsets, span_len, bool(bef...  11.6 us
    unnamed x44, local copies, waits for them, and re-layouts  10.3 us
    ppermute x25, waiting for transfers between devices, sent(): return lax.ppermute(value, 'tp', pairs)  7.64 us
  transfers between devices with their start and end apart: 25, of which 7 were waited for; matrix products, arithmetic and copies ran while one was open for 3% of the time, Pallas kernels for 6%

profile of v10, /device:TPU:1, one launch (start us, length us, event | category | flops | bytes accessed | tf_op | source)
XLA Modules:
  0.0 143.0 jit_solution(4585959119871502565)
XLA Ops:
  0.6 11.9 %collective-permute-start.3 = (bf16[1536,128]{1,0:T(8,128)(2,1)}, bf16[1536,128]{1,0:T(8,128)(2,1)S(1)}, u32[]{:S(2)}, u32[]{:S(2)}) collective-permute-start(bf16[1536,128]{1,0:T(8,128)(2,1)} %bitcast.3.refs_0_), channel_id=1, source_target_pairs={{0,2},{1,31},{2,4},{3,1},{4,6},{5,3},{6,8},{7,5},{8,10},{9,7},{10,... | collective-permute-start | bytes 1179656 | tf_op jit(solution)/shard_map/ppermute | solution.py:354
  12.6 1.9 %collective-permute-start = (bf16[1536,128]{1,0:T(8,128)(2,1)}, bf16[1536,128]{1,0:T(8,128)(2,1)S(1)}, u32[]{:S(2)}, u32[]{:S(2)}) collective-permute-start(bf16[1536,128]{1,0:T(8,128)(2,1)} %bitcast.3.refs_0_), channel_id=1, source_target_pairs={{1,2},{0,31},{3,4},{2,1},{5,6},{4,3},{7,8},{6,5},{9,10},{8,7},{11,... | collective-permute-start | bytes 1179656 | tf_op jit(solution)/shard_map/ppermute | solution.py:354
  14.5 3.0 %collective-permute-start.1 = (bf16[3,1,128]{2,0,1:T(4,128)(2,1)}, bf16[3,1,128]{2,0,1:T(4,128)(2,1)S(1)}, u32[]{:S(2)}, u32[]{:S(2)}) collective-permute-start(bf16[3,1,128]{2,0,1:T(4,128)(2,1)} %param.7), channel_id=1, source_target_pairs={{0,1},{1,0},{2,3},{3,2},{4,5},{5,4},{6,7},{7,6},{8,9},{9,8},{10,11... | collective-permute-start | bytes 2312 | tf_op jit(solution)/shard_map/ppermute | solution.py:354
  19.2 2.6 %collective-permute-start.2 = (bf16[32,128]{1,0:T(8,128)(2,1)S(1)}, bf16[32,128]{1,0:T(8,128)(2,1)S(1)}, u32[]{:S(2)}, u32[]{:S(2)}) collective-permute-start(bf16[32,128]{1,0:T(8,128)(2,1)S(1)} %pad_maximum_fusion.2.here_new_ref), channel_id=1, source_target_pairs={{0,2},{1,31},{2,4},{3,1},{4,6},{5,3},{6,8},{7,5},{8,10},{9,7},{10,... | collective-permute-start | bytes 24584 | tf_op jit(solution)/shard_map/ppermute | solution.py:354
  23.7 3.8 %collective-permute-start.11 = (bf16[1568,128]{1,0:T(8,128)(2,1)S(1)}, bf16[1568,128]{1,0:T(8,128)(2,1)S(1)}, u32[]{:S(2)}, u32[]{:S(2)}) collective-permute-start(bf16[1568,128]{1,0:T(8,128)(2,1)S(1)} %pad_maximum_fusion), channel_id=1, source_target_pairs={{0,2},{1,31},{2,4},{3,1},{4,6},{5,3},{6,8},{7,5},{8,10},{9,7},{10,... | collective-permute-start | bytes 1204232 | tf_op jit(solution)/shard_map/ppermute | solution.py:354
  29.1 2.7 %collective-permute-start.4 = (bf16[4096,256]{1,0:T(8,128)(2,1)S(1)}, bf16[4096,256]{1,0:T(8,128)(2,1)}, u32[]{:S(2)}, u32[]{:S(2)}) collective-permute-start(bf16[4096,256]{1,0:T(8,128)(2,1)S(1)} %beside.1.own_w_ref.main_ref), channel_id=1, source_target_pairs={{0,1},{1,0},{2,3},{3,2},{4,5},{5,4},{6,7},{7,6},{8,9},{9,8},{10,11... | collective-permute-start | bytes 6291464 | tf_op jit(solution)/shard_map/ppermute | solution.py:354
  31.8 4.9 %collective-permute-start.5 = (bf16[1536,128]{1,0:T(8,128)(2,1)S(1)}, bf16[1536,128]{1,0:T(8,128)(2,1)S(1)}, u32[]{:S(2)}, u32[]{:S(2)}) collective-permute-start(bf16[1536,128]{1,0:T(8,128)(2,1)S(1)} %collective-permute-done.3.refs_0_), channel_id=1, source_target_pairs={{0,2},{1,31},{2,4},{3,1},{4,6},{5,3},{6,8},{7,5},{8,10},{9,7},{10,... | collective-permute-start | bytes 1179656 | tf_op jit(solution)/shard_map/ppermute | solution.py:354
  36.7 1.9 %collective-permute-start.12 = (bf16[1568,128]{1,0:T(8,128)(2,1)S(1)}, bf16[1568,128]{1,0:T(8,128)(2,1)S(1)}, u32[]{:S(2)}, u32[]{:S(2)}) collective-permute-start(bf16[1568,128]{1,0:T(8,128)(2,1)S(1)} %collective-permute-done.11.refs_3_), channel_id=1, source_target_pairs={{0,2},{1,31},{2,4},{3,1},{4,6},{5,3},{6,8},{7,5},{8,10},{9,7},{10,... | collective-permute-start | bytes 1204232 | tf_op jit(solution)/shard_map/ppermute | solution.py:354
  39.4 2.0 %collective-permute-done.5.refs_1_ = bf16[1536,128]{1,0:T(8,128)(2,1)S(1)} collective-permute-done((bf16[1536,128]{1,0:T(8,128)(2,1)S(1)}, bf16[1536,128]{1,0:T(8,128)(2,1)S(1)}, u32[]{:S(2)}, u32[]{:S(2)}) %collective-permute-start.5) | collective-permute-done | bytes 393248 | tf_op jit(solution)/shard_map/ppermute | solution.py:354
  41.4 5.0 %collective-permute-start.6 = (bf16[1536,128]{1,0:T(8,128)(2,1)S(1)}, bf16[1536,128]{1,0:T(8,128)(2,1)S(1)}, u32[]{:S(2)}, u32[]{:S(2)}) collective-permute-start(bf16[1536,128]{1,0:T(8,128)(2,1)S(1)} %collective-permute-done.5.refs_1_), channel_id=1, source_target_pairs={{0,2},{1,31},{2,4},{3,1},{4,6},{5,3},{6,8},{7,5},{8,10},{9,7},{10,... | collective-permute-start | bytes 1179656 | tf_op jit(solution)/shard_map/ppermute | solution.py:354
  47.2 3.5 %collective-permute-start.13 = (bf16[1568,128]{1,0:T(8,128)(2,1)S(1)}, bf16[1568,128]{1,0:T(8,128)(2,1)S(1)}, u32[]{:S(2)}, u32[]{:S(2)}) collective-permute-start(bf16[1568,128]{1,0:T(8,128)(2,1)S(1)} %collective-permute-done.12.refs_4_), channel_id=1, source_target_pairs={{0,2},{1,31},{2,4},{3,1},{4,6},{5,3},{6,8},{7,5},{8,10},{9,7},{10,... | collective-permute-start | bytes 1204232 | tf_op jit(solution)/shard_map/ppermute | solution.py:354
  51.5 4.7 %collective-permute-start.7 = (bf16[1536,128]{1,0:T(8,128)(2,1)S(1)}, bf16[1536,128]{1,0:T(8,128)(2,1)S(1)}, u32[]{:S(2)}, u32[]{:S(2)}) collective-permute-start(bf16[1536,128]{1,0:T(8,128)(2,1)S(1)} %collective-permute-done.6.refs_1_), channel_id=1, source_target_pairs={{0,2},{1,31},{2,4},{3,1},{4,6},{5,3},{6,8},{7,5},{8,10},{9,7},{10,... | collective-permute-start | bytes 1179656 | tf_op jit(solution)/shard_map/ppermute | solution.py:354
  56.9 3.6 %collective-permute-start.14 = (bf16[1568,128]{1,0:T(8,128)(2,1)S(1)}, bf16[1568,128]{1,0:T(8,128)(2,1)S(1)}, u32[]{:S(2)}, u32[]{:S(2)}) collective-permute-start(bf16[1568,128]{1,0:T(8,128)(2,1)S(1)} %collective-permute-done.13.refs_5_), channel_id=1, source_target_pairs={{0,2},{1,31},{2,4},{3,1},{4,6},{5,3},{6,8},{7,5},{8,10},{9,7},{10,... | collective-permute-start | bytes 1204232 | tf_op jit(solution)/shard_map/ppermute | solution.py:354
  60.8 5.0 %collective-permute-start.8 = (bf16[1536,128]{1,0:T(8,128)(2,1)S(1)}, bf16[1536,128]{1,0:T(8,128)(2,1)S(1)}, u32[]{:S(2)}, u32[]{:S(2)}) collective-permute-start(bf16[1536,128]{1,0:T(8,128)(2,1)S(1)} %collective-permute-done.7.refs_2_), channel_id=1, source_target_pairs={{0,2},{1,31},{2,4},{3,1},{4,6},{5,3},{6,8},{7,5},{8,10},{9,7},{10,... | collective-permute-start | bytes 1179656 | tf_op jit(solution)/shard_map/ppermute | solution.py:354
  66.6 3.7 %collective-permute-start.15 = (bf16[1568,128]{1,0:T(8,128)(2,1)S(1)}, bf16[1568,128]{1,0:T(8,128)(2,1)}, u32[]{:S(2)}, u32[]{:S(2)}) collective-permute-start(bf16[1568,128]{1,0:T(8,128)(2,1)S(1)} %collective-permute-done.14.refs_2_), channel_id=1, source_target_pairs={{0,2},{1,31},{2,4},{3,1},{4,6},{5,3},{6,8},{7,5},{8,10},{9,7},{10,... | collective-permute-start | bytes 1204232 | tf_op jit(solution)/shard_map/ppermute | solution.py:354
  71.1 4.5 %collective-permute-start.9 = (bf16[1536,128]{1,0:T(8,128)(2,1)S(1)}, bf16[1536,128]{1,0:T(8,128)(2,1)}, u32[]{:S(2)}, u32[]{:S(2)}) collective-permute-start(bf16[1536,128]{1,0:T(8,128)(2,1)S(1)} %collective-permute-done.8.refs_0_), channel_id=1, source_target_pairs={{0,2},{1,31},{2,4},{3,1},{4,6},{5,3},{6,8},{7,5},{8,10},{9,7},{10,... | collective-permute-start | bytes 1179656 | tf_op jit(solution)/shard_map/ppermute | solution.py:354
  76.3 3.6 %collective-permute-start.17 = (bf16[1536,128]{1,0:T(8,128)(2,1)}, bf16[1536,128]{1,0:T(8,128)(2,1)}, u32[]{:S(2)}, u32[]{:S(2)}) collective-permute-start(bf16[1536,128]{1,0:T(8,128)(2,1)} %bitcast.3.refs_0_), channel_id=1, source_target_pairs={{0,1},{1,0},{2,3},{3,2},{4,5},{5,4},{6,7},{7,6},{8,9},{9,8},{10,11... | collective-permute-start | bytes 1179656 | tf_op jit(solution)/shard_map/ppermute | solution.py:354
  79.9 4.9 %collective-permute-start.16 = (bf16[1568,128]{1,0:T(8,128)(2,1)}, bf16[1568,128]{1,0:T(8,128)(2,1)}, u32[]{:S(2)}, u32[]{:S(2)}) collective-permute-start(bf16[1568,128]{1,0:T(8,128)(2,1)} %collective-permute-done.15.refs_3_), channel_id=1, source_target_pairs={{0,2},{1,31},{2,4},{3,1},{4,6},{5,3},{6,8},{7,5},{8,10},{9,7},{10,... | collective-permute-start | bytes 1204232 | tf_op jit(solution)/shard_map/ppermute | solution.py:354
  84.8 1.9 %collective-permute-start.10 = (bf16[1536,128]{1,0:T(8,128)(2,1)}, bf16[1536,128]{1,0:T(8,128)(2,1)}, u32[]{:S(2)}, u32[]{:S(2)}) collective-permute-start(bf16[1536,128]{1,0:T(8,128)(2,1)} %collective-permute-done.9.refs_1_), channel_id=1, source_target_pairs={{0,2},{1,31},{2,4},{3,1},{4,6},{5,3},{6,8},{7,5},{8,10},{9,7},{10,... | collective-permute-start | bytes 1179656 | tf_op jit(solution)/shard_map/ppermute | solution.py:354
  90.6 2.5 %ring_sums.4 = (f32[1536,256]{1,0:T(8,128)S(1)}, f32[1536,256]{1,0:T(8,128)S(1)}) custom-call(s32[4]{0:T(128)S(1)} %pad_add_fusion.place_ref, bf16[4096,256]{1,0:T(8,128)(2,1)S(1)} %beside.1.own_w_ref.main_ref, bf16[4096,256]{1,0:T(8,128)(2,1)} %collective-permute-done.4.other_w_ref, bf16[1536,128]{1,0:T(8,128)(2,1)S(1)} %copy-done.16, ...), custom_call_target="tpu_custom_call" | custom-call | flops 805306368 | tf_op jit(solution)/shard_map/ring_sums/pallas_call | solution.py:126
  93.1 3.3 %ring_sums.5 = (f32[1536,256]{1,0:T(8,128)S(1)}, f32[1536,256]{1,0:T(8,128)S(1)}) custom-call(s32[4]{0:T(128)S(1)} %pad_add_fusion.place_ref, bf16[4096,256]{1,0:T(8,128)(2,1)S(1)} %beside.1.own_w_ref.main_ref, bf16[4096,256]{1,0:T(8,128)(2,1)} %collective-permute-done.4.other_w_ref, bf16[1536,128]{1,0:T(8,128)(2,1)} %bitcast.3.refs_0_, ...), custom_call_target="tpu_custom_call" | custom-call | flops 1207959552 | tf_op jit(solution)/shard_map/ring_sums/pallas_call | solution.py:126
  96.5 3.0 %ring_sums.6 = (f32[1536,256]{1,0:T(8,128)S(1)}, f32[1536,256]{1,0:T(8,128)S(1)}) custom-call(s32[4]{0:T(128)S(1)} %pad_add_fusion.place_ref, bf16[4096,256]{1,0:T(8,128)(2,1)S(1)} %beside.1.own_w_ref.main_ref, bf16[4096,256]{1,0:T(8,128)(2,1)} %collective-permute-done.4.other_w_ref, bf16[1536,128]{1,0:T(8,128)(2,1)S(1)} %copy-done.14, ...), custom_call_target="tpu_custom_call" | custom-call | flops 805306368 | tf_op jit(solution)/shard_map/ring_sums/pallas_call | solution.py:126
  100.2 2.8 %ring_sums.7 = (f32[1536,256]{1,0:T(8,128)S(1)}, f32[1568,256]{1,0:T(8,128)S(1)}) custom-call(s32[4]{0:T(128)S(1)} %pad_add_fusion.place_ref, bf16[4096,256]{1,0:T(8,128)(2,1)S(1)} %beside.1.own_w_ref.main_ref, bf16[4096,256]{1,0:T(8,128)(2,1)} %collective-permute-done.4.other_w_ref, bf16[1536,128]{1,0:T(8,128)(2,1)} %collective-permute-done.10.refs_0_, ...), custom_call_target="tpu_custom_call" | custom-call | flops 402653184 | tf_op jit(solution)/shard_map/ring_sums/pallas_call | solution.py:126
  103.0 3.4 %collective-permute-start.18 = (f32[1568,256]{1,0:T(8,128)S(1)}, f32[1568,256]{1,0:T(8,128)S(1)}, u32[]{:S(2)}, u32[]{:S(2)}) collective-permute-start(f32[1568,256]{1,0:T(8,128)S(1)} %get-tuple-element.33), channel_id=1, source_target_pairs={{0,1},{1,0},{2,3},{3,2},{4,5},{5,4},{6,7},{7,6},{8,9},{9,8},{10,11... | collective-permute-start | bytes 4816904 | tf_op jit(solution)/shard_map/ppermute | solution.py:354
  106.5 4.9 %collective-permute-start.22 = (bf16[1536,128]{1,0:T(8,128)(2,1)}, bf16[1536,128]{1,0:T(8,128)(2,1)S(1)}, u32[]{:S(2)}, u32[]{:S(2)}) collective-permute-start(bf16[1536,128]{1,0:T(8,128)(2,1)} %collective-permute-done.10.refs_0_), channel_id=1, source_target_pairs={{1,31},{3,1},{5,3},{7,5},{9,7},{11,9},{13,11},{15,13},{17,15},{19,... | collective-permute-start | bytes 1179656 | tf_op jit(solution)/shard_map/ppermute | solution.py:354
  112.7 1.9 %collective-permute-start.23 = (bf16[1568,128]{1,0:T(8,128)(2,1)}, bf16[1568,128]{1,0:T(8,128)(2,1)S(1)}, u32[]{:S(2)}, u32[]{:S(2)}) collective-permute-start(bf16[1568,128]{1,0:T(8,128)(2,1)} %collective-permute-done.16.refs_1_), channel_id=1, source_target_pairs={{1,31},{3,1},{5,3},{7,5},{9,7},{11,9},{13,11},{15,13},{17,15},{19,... | collective-permute-start | bytes 1204232 | tf_op jit(solution)/shard_map/ppermute | solution.py:354
  114.6 1.7 %collective-permute-done.22.last_down_ref = bf16[1536,128]{1,0:T(8,128)(2,1)S(1)} collective-permute-done((bf16[1536,128]{1,0:T(8,128)(2,1)}, bf16[1536,128]{1,0:T(8,128)(2,1)S(1)}, u32[]{:S(2)}, u32[]{:S(2)}) %collective-permute-start.22) | collective-permute-done | bytes 393248 | tf_op jit(solution)/shard_map/ppermute | solution.py:354
  116.3 1.3 collective-permute-start.24
  117.7 1.9 %collective-permute-start.19 = (bf16[160,128]{1,0:T(8,128)(2,1)S(1)}, bf16[160,128]{1,0:T(8,128)(2,1)S(1)}, u32[]{:S(2)}, u32[]{:S(2)}) collective-permute-start(bf16[160,128]{1,0:T(8,128)(2,1)S(1)} %constant_dynamic-update-slice_fusion.mine_new_ref), channel_id=1, source_target_pairs={{0,1},{1,0},{2,3},{3,2},{4,5},{5,4},{6,7},{7,6},{8,9},{9,8},{10,11... | collective-permute-start | bytes 122888 | tf_op jit(solution)/shard_map/ppermute | solution.py:354
  120.8 4.9 %collective-permute-start.20 = (bf16[32,128]{1,0:T(8,128)(2,1)S(1)}, bf16[32,128]{1,0:T(8,128)(2,1)S(1)}, u32[]{:S(2)}, u32[]{:S(2)}) collective-permute-start(bf16[32,128]{1,0:T(8,128)(2,1)S(1)} %slice.25.refs_5_), channel_id=1, source_target_pairs={{0,2},{1,31},{2,4},{3,1},{4,6},{5,3},{6,8},{7,5},{8,10},{9,7},{10,... | collective-permute-start | bytes 24584 | tf_op jit(solution)/shard_map/ppermute | solution.py:354
  126.5 2.3 %span_states.1 = (f32[16,15,128]{2,1,0:T(8,128)S(1)}, f32[16,128]{1,0:T(8,128)S(1)}) custom-call(s32[4]{0:T(128)S(1)} %pad_add_fusion.place_ref, f32[2]{0:T(128)S(1)} %copy-done.19, f32[1536,256]{1,0:T(8,128)S(1)} %get-tuple-element.32.total_ref, f32[1568,256]{1,0:T(8,128)S(1)} %collective-permute-done.18.arrived_ref, ...), custom_call_target="tpu_custom_call" | custom-call | tf_op jit(solution)/shard_map/span_states/pallas_call | solution.py:261
  128.8 13.4 %all_to_all.5.arrived_ref = f32[16,15,128]{2,1,0:T(8,128)S(1)} all-to-all(f32[16,15,128]{2,1,0:T(8,128)S(1)} %get-tuple-element.36), channel_id=1, replica_groups=mesh['sp'=16,'tp'=32] {'sp'}, dimensions={0} | all-to-all | bytes 245760 | tf_op jit(solution)/shard_map/all_to_all | solution.py:443
  (82 shorter events, 19.3 us)
Async XLA Ops:
  0.6 21.3 %collective-permute-start.3 = (bf16[1536,128]{1,0:T(8,128)(2,1)}, bf16[1536,128]{1,0:T(8,128)(2,1)S(1)}, u32[]{:S(2)}, u32[]{:S(2)}) collective-permute-start(bf16[1536,128]{1,0:T(8,128)(2,1)} %bitcast.3.refs_0_), channel_id=1, source_target_pairs={{0,2},{1,31},{2,4},{3,1},{4,6},{5,3},{6,8},{7,5},{8,10},{9,7},{10,... | collective-permute-start | bytes 1179656 | tf_op jit(solution)/shard_map/ppermute | solution.py:354
  12.6 11.1 %collective-permute-start = (bf16[1536,128]{1,0:T(8,128)(2,1)}, bf16[1536,128]{1,0:T(8,128)(2,1)S(1)}, u32[]{:S(2)}, u32[]{:S(2)}) collective-permute-start(bf16[1536,128]{1,0:T(8,128)(2,1)} %bitcast.3.refs_0_), channel_id=1, source_target_pairs={{1,2},{0,31},{3,4},{2,1},{5,6},{4,3},{7,8},{6,5},{9,10},{8,7},{11,... | collective-permute-start | bytes 1179656 | tf_op jit(solution)/shard_map/ppermute | solution.py:354
  14.5 4.0 %collective-permute-start.1 = (bf16[3,1,128]{2,0,1:T(4,128)(2,1)}, bf16[3,1,128]{2,0,1:T(4,128)(2,1)S(1)}, u32[]{:S(2)}, u32[]{:S(2)}) collective-permute-start(bf16[3,1,128]{2,0,1:T(4,128)(2,1)} %param.7), channel_id=1, source_target_pairs={{0,1},{1,0},{2,3},{3,2},{4,5},{5,4},{6,7},{7,6},{8,9},{9,8},{10,11... | collective-permute-start | bytes 2312 | tf_op jit(solution)/shard_map/ppermute | solution.py:354
  17.6 10.0 %copy-start.1 = (bf16[4096,128]{1,0:T(8,128)(2,1)S(1)}, bf16[4096,128]{1,0:T(8,128)(2,1)}, u32[]{:S(2)}) copy-start(bf16[4096,128]{1,0:T(8,128)(2,1)} %left_ref) | copy-start | bytes 3145732
  19.2 4.4 %collective-permute-start.2 = (bf16[32,128]{1,0:T(8,128)(2,1)S(1)}, bf16[32,128]{1,0:T(8,128)(2,1)S(1)}, u32[]{:S(2)}, u32[]{:S(2)}) collective-permute-start(bf16[32,128]{1,0:T(8,128)(2,1)S(1)} %pad_maximum_fusion.2.here_new_ref), channel_id=1, source_target_pairs={{0,2},{1,31},{2,4},{3,1},{4,6},{5,3},{6,8},{7,5},{8,10},{9,7},{10,... | collective-permute-start | bytes 24584 | tf_op jit(solution)/shard_map/ppermute | solution.py:354
  21.9 9.9 %copy-start.15 = (bf16[1536,128]{1,0:T(8,128)(2,1)}, bf16[1536,128]{1,0:T(8,128)(2,1)S(1)}, u32[]{:S(2)}) copy-start(bf16[1536,128]{1,0:T(8,128)(2,1)S(1)} %collective-permute-done.3.refs_0_) | copy-start | bytes 1179652
  23.7 13.0 %collective-permute-start.11 = (bf16[1568,128]{1,0:T(8,128)(2,1)S(1)}, bf16[1568,128]{1,0:T(8,128)(2,1)S(1)}, u32[]{:S(2)}, u32[]{:S(2)}) collective-permute-start(bf16[1568,128]{1,0:T(8,128)(2,1)S(1)} %pad_maximum_fusion), channel_id=1, source_target_pairs={{0,2},{1,31},{2,4},{3,1},{4,6},{5,3},{6,8},{7,5},{8,10},{9,7},{10,... | collective-permute-start | bytes 1204232 | tf_op jit(solution)/shard_map/ppermute | solution.py:354
  29.1 58.4 %collective-permute-start.4 = (bf16[4096,256]{1,0:T(8,128)(2,1)S(1)}, bf16[4096,256]{1,0:T(8,128)(2,1)}, u32[]{:S(2)}, u32[]{:S(2)}) collective-permute-start(bf16[4096,256]{1,0:T(8,128)(2,1)S(1)} %beside.1.own_w_ref.main_ref), channel_id=1, source_target_pairs={{0,1},{1,0},{2,3},{3,2},{4,5},{5,4},{6,7},{7,6},{8,9},{9,8},{10,11... | collective-permute-start | bytes 6291464 | tf_op jit(solution)/shard_map/ppermute | solution.py:354
  31.8 9.6 %collective-permute-start.5 = (bf16[1536,128]{1,0:T(8,128)(2,1)S(1)}, bf16[1536,128]{1,0:T(8,128)(2,1)S(1)}, u32[]{:S(2)}, u32[]{:S(2)}) collective-permute-start(bf16[1536,128]{1,0:T(8,128)(2,1)S(1)} %collective-permute-done.3.refs_0_), channel_id=1, source_target_pairs={{0,2},{1,31},{2,4},{3,1},{4,6},{5,3},{6,8},{7,5},{8,10},{9,7},{10,... | collective-permute-start | bytes 1179656 | tf_op jit(solution)/shard_map/ppermute | solution.py:354
  36.7 10.5 %collective-permute-start.12 = (bf16[1568,128]{1,0:T(8,128)(2,1)S(1)}, bf16[1568,128]{1,0:T(8,128)(2,1)S(1)}, u32[]{:S(2)}, u32[]{:S(2)}) collective-permute-start(bf16[1568,128]{1,0:T(8,128)(2,1)S(1)} %collective-permute-done.11.refs_3_), channel_id=1, source_target_pairs={{0,2},{1,31},{2,4},{3,1},{4,6},{5,3},{6,8},{7,5},{8,10},{9,7},{10,... | collective-permute-start | bytes 1204232 | tf_op jit(solution)/shard_map/ppermute | solution.py:354
  41.4 10.1 %collective-permute-start.6 = (bf16[1536,128]{1,0:T(8,128)(2,1)S(1)}, bf16[1536,128]{1,0:T(8,128)(2,1)S(1)}, u32[]{:S(2)}, u32[]{:S(2)}) collective-permute-start(bf16[1536,128]{1,0:T(8,128)(2,1)S(1)} %collective-permute-done.5.refs_1_), channel_id=1, source_target_pairs={{0,2},{1,31},{2,4},{3,1},{4,6},{5,3},{6,8},{7,5},{8,10},{9,7},{10,... | collective-permute-start | bytes 1179656 | tf_op jit(solution)/shard_map/ppermute | solution.py:354
  47.2 9.7 %collective-permute-start.13 = (bf16[1568,128]{1,0:T(8,128)(2,1)S(1)}, bf16[1568,128]{1,0:T(8,128)(2,1)S(1)}, u32[]{:S(2)}, u32[]{:S(2)}) collective-permute-start(bf16[1568,128]{1,0:T(8,128)(2,1)S(1)} %collective-permute-done.12.refs_4_), channel_id=1, source_target_pairs={{0,2},{1,31},{2,4},{3,1},{4,6},{5,3},{6,8},{7,5},{8,10},{9,7},{10,... | collective-permute-start | bytes 1204232 | tf_op jit(solution)/shard_map/ppermute | solution.py:354
  51.5 9.4 %collective-permute-start.7 = (bf16[1536,128]{1,0:T(8,128)(2,1)S(1)}, bf16[1536,128]{1,0:T(8,128)(2,1)S(1)}, u32[]{:S(2)}, u32[]{:S(2)}) collective-permute-start(bf16[1536,128]{1,0:T(8,128)(2,1)S(1)} %collective-permute-done.6.refs_1_), channel_id=1, source_target_pairs={{0,2},{1,31},{2,4},{3,1},{4,6},{5,3},{6,8},{7,5},{8,10},{9,7},{10,... | collective-permute-start | bytes 1179656 | tf_op jit(solution)/shard_map/ppermute | solution.py:354
  56.9 9.7 %collective-permute-start.14 = (bf16[1568,128]{1,0:T(8,128)(2,1)S(1)}, bf16[1568,128]{1,0:T(8,128)(2,1)S(1)}, u32[]{:S(2)}, u32[]{:S(2)}) collective-permute-start(bf16[1568,128]{1,0:T(8,128)(2,1)S(1)} %collective-permute-done.13.refs_5_), channel_id=1, source_target_pairs={{0,2},{1,31},{2,4},{3,1},{4,6},{5,3},{6,8},{7,5},{8,10},{9,7},{10,... | collective-permute-start | bytes 1204232 | tf_op jit(solution)/shard_map/ppermute | solution.py:354
  60.8 10.3 %collective-permute-start.8 = (bf16[1536,128]{1,0:T(8,128)(2,1)S(1)}, bf16[1536,128]{1,0:T(8,128)(2,1)S(1)}, u32[]{:S(2)}, u32[]{:S(2)}) collective-permute-start(bf16[1536,128]{1,0:T(8,128)(2,1)S(1)} %collective-permute-done.7.refs_2_), channel_id=1, source_target_pairs={{0,2},{1,31},{2,4},{3,1},{4,6},{5,3},{6,8},{7,5},{8,10},{9,7},{10,... | collective-permute-start | bytes 1179656 | tf_op jit(solution)/shard_map/ppermute | solution.py:354
  66.6 13.3 %collective-permute-start.15 = (bf16[1568,128]{1,0:T(8,128)(2,1)S(1)}, bf16[1568,128]{1,0:T(8,128)(2,1)}, u32[]{:S(2)}, u32[]{:S(2)}) collective-permute-start(bf16[1568,128]{1,0:T(8,128)(2,1)S(1)} %collective-permute-done.14.refs_2_), channel_id=1, source_target_pairs={{0,2},{1,31},{2,4},{3,1},{4,6},{5,3},{6,8},{7,5},{8,10},{9,7},{10,... | collective-permute-start | bytes 1204232 | tf_op jit(solution)/shard_map/ppermute | solution.py:354
  71.1 13.7 %collective-permute-start.9 = (bf16[1536,128]{1,0:T(8,128)(2,1)S(1)}, bf16[1536,128]{1,0:T(8,128)(2,1)}, u32[]{:S(2)}, u32[]{:S(2)}) collective-permute-start(bf16[1536,128]{1,0:T(8,128)(2,1)S(1)} %collective-permute-done.8.refs_0_), channel_id=1, source_target_pairs={{0,2},{1,31},{2,4},{3,1},{4,6},{5,3},{6,8},{7,5},{8,10},{9,7},{10,... | collective-permute-start | bytes 1179656 | tf_op jit(solution)/shard_map/ppermute | solution.py:354
  76.3 16.7 %collective-permute-start.17 = (bf16[1536,128]{1,0:T(8,128)(2,1)}, bf16[1536,128]{1,0:T(8,128)(2,1)}, u32[]{:S(2)}, u32[]{:S(2)}) collective-permute-start(bf16[1536,128]{1,0:T(8,128)(2,1)} %bitcast.3.refs_0_), channel_id=1, source_target_pairs={{0,1},{1,0},{2,3},{3,2},{4,5},{5,4},{6,7},{7,6},{8,9},{9,8},{10,11... | collective-permute-start | bytes 1179656 | tf_op jit(solution)/shard_map/ppermute | solution.py:354
  79.9 19.6 %collective-permute-start.16 = (bf16[1568,128]{1,0:T(8,128)(2,1)}, bf16[1568,128]{1,0:T(8,128)(2,1)}, u32[]{:S(2)}, u32[]{:S(2)}) collective-permute-start(bf16[1568,128]{1,0:T(8,128)(2,1)} %collective-permute-done.15.refs_3_), channel_id=1, source_target_pairs={{0,2},{1,31},{2,4},{3,1},{4,6},{5,3},{6,8},{7,5},{8,10},{9,7},{10,... | collective-permute-start | bytes 1204232 | tf_op jit(solution)/shard_map/ppermute | solution.py:354
  84.8 15.4 %collective-permute-start.10 = (bf16[1536,128]{1,0:T(8,128)(2,1)}, bf16[1536,128]{1,0:T(8,128)(2,1)}, u32[]{:S(2)}, u32[]{:S(2)}) collective-permute-start(bf16[1536,128]{1,0:T(8,128)(2,1)} %collective-permute-done.9.refs_1_), channel_id=1, source_target_pairs={{0,2},{1,31},{2,4},{3,1},{4,6},{5,3},{6,8},{7,5},{8,10},{9,7},{10,... | collective-permute-start | bytes 1179656 | tf_op jit(solution)/shard_map/ppermute | solution.py:354
  87.5 5.5 %copy-start.4 = (bf16[1568,128]{1,0:T(8,128)(2,1)S(1)}, bf16[1568,128]{1,0:T(8,128)(2,1)}, u32[]{:S(2)}) copy-start(bf16[1568,128]{1,0:T(8,128)(2,1)} %copy-done.3) | copy-start | bytes 1204228
  93.1 3.4 %copy-start.8 = (bf16[1568,128]{1,0:T(8,128)(2,1)S(1)}, bf16[1568,128]{1,0:T(8,128)(2,1)}, u32[]{:S(2)}) copy-start(bf16[1568,128]{1,0:T(8,128)(2,1)} %copy-done.7) | copy-start | bytes 1204228
  93.1 3.4 %copy-start.14 = (bf16[1536,128]{1,0:T(8,128)(2,1)S(1)}, bf16[1536,128]{1,0:T(8,128)(2,1)}, u32[]{:S(2)}) copy-start(bf16[1536,128]{1,0:T(8,128)(2,1)} %copy-done.13) | copy-start | bytes 1179652
  100.2 26.3 %copy-start = (bf16[4096,128]{1,0:T(8,128)(2,1)S(1)}, bf16[4096,128]{1,0:T(8,128)(2,1)}, u32[]{:S(2)}) copy-start(bf16[4096,128]{1,0:T(8,128)(2,1)} %query_w_ref.1) | copy-start | bytes 3145732
  100.2 26.3 %copy-start.19 = (f32[2]{0:T(128)S(1)}, f32[2]{0:T(128)}, u32[]{:S(2)}) copy-start(f32[2]{0:T(128)} %rate_ref.1) | copy-start | bytes 28
  103.0 23.5 %collective-permute-start.18 = (f32[1568,256]{1,0:T(8,128)S(1)}, f32[1568,256]{1,0:T(8,128)S(1)}, u32[]{:S(2)}, u32[]{:S(2)}) collective-permute-start(f32[1568,256]{1,0:T(8,128)S(1)} %get-tuple-element.33), channel_id=1, source_target_pairs={{0,1},{1,0},{2,3},{3,2},{4,5},{5,4},{6,7},{7,6},{8,9},{9,8},{10,11... | collective-permute-start | bytes 4816904 | tf_op jit(solution)/shard_map/ppermute | solution.py:354
  106.5 9.9 %collective-permute-start.22 = (bf16[1536,128]{1,0:T(8,128)(2,1)}, bf16[1536,128]{1,0:T(8,128)(2,1)S(1)}, u32[]{:S(2)}, u32[]{:S(2)}) collective-permute-start(bf16[1536,128]{1,0:T(8,128)(2,1)} %collective-permute-done.10.refs_0_), channel_id=1, source_target_pairs={{1,31},{3,1},{5,3},{7,5},{9,7},{11,9},{13,11},{15,13},{17,15},{19,... | collective-permute-start | bytes 1179656 | tf_op jit(solution)/shard_map/ppermute | solution.py:354
  112.0 14.4 %collective-permute-start.21 = (bf16[1536,128]{1,0:T(8,128)(2,1)}, bf16[1536,128]{1,0:T(8,128)(2,1)S(1)}, u32[]{:S(2)}, u32[]{:S(2)}) collective-permute-start(bf16[1536,128]{1,0:T(8,128)(2,1)} %collective-permute-done.10.refs_0_), channel_id=1, source_target_pairs={{0,2},{2,4},{4,6},{6,8},{8,10},{10,12},{12,14},{14,16},{16,18},{18... | collective-permute-start | bytes 1179656 | tf_op jit(solution)/shard_map/ppermute | solution.py:354
  112.7 13.8 %collective-permute-start.23 = (bf16[1568,128]{1,0:T(8,128)(2,1)}, bf16[1568,128]{1,0:T(8,128)(2,1)S(1)}, u32[]{:S(2)}, u32[]{:S(2)}) collective-permute-start(bf16[1568,128]{1,0:T(8,128)(2,1)} %collective-permute-done.16.refs_1_), channel_id=1, source_target_pairs={{1,31},{3,1},{5,3},{7,5},{9,7},{11,9},{13,11},{15,13},{17,15},{19,... | collective-permute-start | bytes 1204232 | tf_op jit(solution)/shard_map/ppermute | solution.py:354
  116.3 10.1 %collective-permute-start.24 = (bf16[1536,128]{1,0:T(8,128)(2,1)S(1)}, bf16[1536,128]{1,0:T(8,128)(2,1)S(1)}, u32[]{:S(2)}, u32[]{:S(2)}) collective-permute-start(bf16[1536,128]{1,0:T(8,128)(2,1)S(1)} %collective-permute-done.22.last_down_ref), channel_id=1, source_target_pairs={{1,0},{3,2},{5,4},{7,6},{9,8},{11,10},{13,12},{15,14},{17,16},{19,... | collective-permute-start | bytes 1179656 | tf_op jit(solution)/shard_map/ppermute | solution.py:354
  117.7 3.1 %collective-permute-start.19 = (bf16[160,128]{1,0:T(8,128)(2,1)S(1)}, bf16[160,128]{1,0:T(8,128)(2,1)S(1)}, u32[]{:S(2)}, u32[]{:S(2)}) collective-permute-start(bf16[160,128]{1,0:T(8,128)(2,1)S(1)} %constant_dynamic-update-slice_fusion.mine_new_ref), channel_id=1, source_target_pairs={{0,1},{1,0},{2,3},{3,2},{4,5},{5,4},{6,7},{7,6},{8,9},{9,8},{10,11... | collective-permute-start | bytes 122888 | tf_op jit(solution)/shard_map/ppermute | solution.py:354
  120.8 5.7 %collective-permute-start.20 = (bf16[32,128]{1,0:T(8,128)(2,1)S(1)}, bf16[32,128]{1,0:T(8,128)(2,1)S(1)}, u32[]{:S(2)}, u32[]{:S(2)}) collective-permute-start(bf16[32,128]{1,0:T(8,128)(2,1)S(1)} %slice.25.refs_5_), channel_id=1, source_target_pairs={{0,2},{1,31},{2,4},{3,1},{4,6},{5,3},{6,8},{7,5},{8,10},{9,7},{10,... | collective-permute-start | bytes 24584 | tf_op jit(solution)/shard_map/ppermute | solution.py:354
  (13 other events, 14.6 us)

commit v11 on v8

--- a/solution.py
+++ b/solution.py
@@ -138,13 +138,48 @@
     )(place, own_weights, other_weights, *operands)
 
 
+def pair(ref, start):
+    return [ref[start : start + EXTRA, :], ref[start + EXTRA : start + 2 * EXTRA, :]]
+
+
+def new_rows_product(place_ref, main_ref, query_w_ref, pieces, order):
+    width = pieces[0].shape[1]
+    plane_rows = [at_rows(row_block(place_ref, k), 2 * width) for k in order]
+    weights = jnp.concatenate(
+        [jnp.concatenate([main_ref[at, :], query_w_ref[at, :]], axis=1) for at in plane_rows], axis=0
+    )
+    entries = jnp.concatenate(pieces, axis=1)
+    return jnp.dot(entries, weights, preferred_element_type=jnp.float32)
+
+
+def new_kernel(place_ref, here_new_ref, mine_new_ref, main_ref, query_w_ref, out_ref):
+    pieces = pair(here_new_ref, 0)
+    order = [0]
+    for k in range(1, mine_new_ref.shape[0] // (2 * EXTRA) + 1):
+        pieces += pair(mine_new_ref, (k - 1) * 2 * EXTRA)
+        order.append(k)
+    out_ref[...] = new_rows_product(place_ref, main_ref, query_w_ref, pieces, order)
+
+
+def new_sums(place, here_new, mine_new, main_weights, query_weight):
+    whole = pl.BlockSpec(memory_space=pltpu.VMEM)
+    inner = main_weights.shape[1] + query_weight.shape[1]
+    return pl.pallas_call(
+        new_kernel,
+        in_specs=[pl.BlockSpec(memory_space=pltpu.SMEM)] + [whole] * 4,
+        out_specs=whole,
+        out_shape=jax.ShapeDtypeStruct((EXTRA, inner), jnp.float32),
+        compiler_params=pltpu.CompilerParams(vmem_limit_bytes=6 * 1024 * 1024),
+        name="new_sums",
+    )(place, here_new, mine_new, main_weights, query_weight)
+
+
 def state_kernel(
     place_ref,
     rate_ref,
     total_ref,
     arrived_ref,
-    here_new_ref,
-    mine_new_ref,
+    early_ref,
     theirs_new_ref,
     last_a_ref,
     last_b_ref,
@@ -161,7 +196,7 @@
     keep = HD // groups
     prompts = out_rows // (keep + 1)
     span_len = rows // prompts
-    reach = mine_new_ref.shape[0] // (2 * EXTRA) + 1
+    reach = theirs_new_ref.shape[0] // (2 * EXTRA) + 1
     lane = lax.broadcasted_iota(jnp.int32, (HD, inner), 1)
     row_lane = lax.broadcasted_iota(jnp.int32, (1, inner), 1)
     lane_decay = jnp.full((1, inner), rate_ref[0], jnp.float32)
@@ -173,23 +208,13 @@
     to_end = lax.broadcasted_iota(jnp.int32, (span_len, inner), 0)
     decay = jnp.exp((span_len - 1 - to_end).astype(jnp.float32) * lane_decay)
 
-    def pair(ref, start):
-        return [ref[start : start + EXTRA, :], ref[start + EXTRA : start + 2 * EXTRA, :]]
-
-    pieces = pair(here_new_ref, 0)
-    order = [0]
+    pieces, order = [], []
     for k in range(1, reach):
-        pieces += pair(mine_new_ref, (k - 1) * 2 * EXTRA)
         pieces += pair(theirs_new_ref, (k - 1) * 2 * EXTRA)
-        order += [k, -k]
+        order.append(-k)
     pieces += pair(last_b_ref, rows)
     order.append(reach)
-    entries = jnp.concatenate(pieces, axis=1)
-    plane_rows = [at_rows(row_block(place_ref, k), 2 * width) for k in order]
-    weights = jnp.concatenate(
-        [jnp.concatenate([main_ref[at, :], query_w_ref[at, :]], axis=1) for at in plane_rows], axis=0
-    )
-    fresh = jnp.dot(entries, weights, preferred_element_type=jnp.float32)
+    fresh = early_ref[...] + new_rows_product(place_ref, main_ref, query_w_ref, pieces, order)
     new_cos = cos_ref[span_len : span_len + 1, :]
     new_sin = sin_ref[span_len : span_len + 1, :]
     new_key = fresh[:, :inner]
@@ -384,6 +409,7 @@
     mine_new = jnp.concatenate(new_list[:-1], axis=0)
     theirs_new = sent(mine_new, partner)
 
+    early = new_sums(place, new_pair, mine_new, main_weights, query_weight)
     messages, own_term = span_states(
         prompts,
         groups,
@@ -391,8 +417,7 @@
         place,
         own,
         arrived,
-        new_pair,
-        mine_new,
+        early,
         theirs_new,
         a_list[-1],
         b_list[-1],

time: 138 us -> 137 us (level)
  transfers between devices with their start and end apart: 22 -> 22, of which waited for: 6 -> 6; matrix products, arithmetic and copies ran while one was open for 3% -> 3% of each run, Pallas kernels for 7% -> 8%
where the time goes in v11:
time: 137 us; the launch traced here: 136 us
  starting transfers between devices  85.2 us (62%)
  Pallas kernels  16.2 us (12%)
  blocking collectives  13.4 us (10%)
  local copies, waits for them, and re-layouts  10.7 us (8%)
  waiting for transfers between devices  7.48 us (5%)
  other arithmetic  1.83 us (1%)
    ppermute x22, starting transfers between devices, sent(): return lax.ppermute(value, 'tp', pairs)  85.2 us
    all_to_all x1, blocking collectives, body(): lax.all_to_all(messages, 'sp', split_axis=0, concat_axis=0, tiled=True)  13.4 us
    pallas_call x4, Pallas kernels, ring_sums(): pl.pallas_call(functools.partial(sums_kernel, offsets, span_len, bool(bef...  12.1 us
    unnamed x42, local copies, waits for them, and re-layouts  9.98 us
    ppermute x22, waiting for transfers between devices, sent(): return lax.ppermute(value, 'tp', pairs)  7.48 us
  transfers between devices with their start and end apart: 22, of which 6 were waited for; matrix products, arithmetic and copies ran while one was open for 3% of the time, Pallas kernels for 8%

profile of v11, /device:TPU:1, one launch (start us, length us, event | category | flops | bytes accessed | tf_op | source)
XLA Modules:
  0.0 135.9 jit_solution(8232318861217426009)
XLA Ops:
  0.6 11.9 %collective-permute-start.3 = (bf16[1536,128]{1,0:T(8,128)(2,1)}, bf16[1536,128]{1,0:T(8,128)(2,1)}, u32[]{:S(2)}, u32[]{:S(2)}) collective-permute-start(bf16[1536,128]{1,0:T(8,128)(2,1)} %bitcast.3.refs_0_), channel_id=1, source_target_pairs={{0,2},{1,31},{2,4},{3,1},{4,6},{5,3},{6,8},{7,5},{8,10},{9,7},{10,... | collective-permute-start | bytes 1179656 | tf_op jit(solution)/shard_map/ppermute | solution.py:357
  12.6 1.9 %collective-permute-start = (bf16[1536,128]{1,0:T(8,128)(2,1)}, bf16[1536,128]{1,0:T(8,128)(2,1)S(1)}, u32[]{:S(2)}, u32[]{:S(2)}) collective-permute-start(bf16[1536,128]{1,0:T(8,128)(2,1)} %bitcast.3.refs_0_), channel_id=1, source_target_pairs={{1,2},{0,31},{3,4},{2,1},{5,6},{4,3},{7,8},{6,5},{9,10},{8,7},{11,... | collective-permute-start | bytes 1179656 | tf_op jit(solution)/shard_map/ppermute | solution.py:357
  14.5 3.0 %collective-permute-start.1 = (bf16[3,1,128]{2,0,1:T(4,128)(2,1)}, bf16[3,1,128]{2,0,1:T(4,128)(2,1)S(1)}, u32[]{:S(2)}, u32[]{:S(2)}) collective-permute-start(bf16[3,1,128]{2,0,1:T(4,128)(2,1)} %param.7), channel_id=1, source_target_pairs={{0,1},{1,0},{2,3},{3,2},{4,5},{5,4},{6,7},{7,6},{8,9},{9,8},{10,11... | collective-permute-start | bytes 2312 | tf_op jit(solution)/shard_map/ppermute | solution.py:357
  19.2 2.6 %collective-permute-start.2 = (bf16[32,128]{1,0:T(8,128)(2,1)S(1)}, bf16[32,128]{1,0:T(8,128)(2,1)S(1)}, u32[]{:S(2)}, u32[]{:S(2)}) collective-permute-start(bf16[32,128]{1,0:T(8,128)(2,1)S(1)} %pad_maximum_fusion.1.here_new_ref), channel_id=1, source_target_pairs={{0,2},{1,31},{2,4},{3,1},{4,6},{5,3},{6,8},{7,5},{8,10},{9,7},{10,... | collective-permute-start | bytes 24584 | tf_op jit(solution)/shard_map/ppermute | solution.py:357
  23.7 3.8 %collective-permute-start.11 = (bf16[1568,128]{1,0:T(8,128)(2,1)S(1)}, bf16[1568,128]{1,0:T(8,128)(2,1)S(1)}, u32[]{:S(2)}, u32[]{:S(2)}) collective-permute-start(bf16[1568,128]{1,0:T(8,128)(2,1)S(1)} %pad_maximum_fusion), channel_id=1, source_target_pairs={{0,2},{1,31},{2,4},{3,1},{4,6},{5,3},{6,8},{7,5},{8,10},{9,7},{10,... | collective-permute-start | bytes 1204232 | tf_op jit(solution)/shard_map/ppermute | solution.py:357
  27.6 1.2 copy-done.2
  29.1 2.7 %collective-permute-start.4 = (bf16[4096,256]{1,0:T(8,128)(2,1)S(1)}, bf16[4096,256]{1,0:T(8,128)(2,1)}, u32[]{:S(2)}, u32[]{:S(2)}) collective-permute-start(bf16[4096,256]{1,0:T(8,128)(2,1)S(1)} %beside.1.own_w_ref.main_ref), channel_id=1, source_target_pairs={{0,1},{1,0},{2,3},{3,2},{4,5},{5,4},{6,7},{7,6},{8,9},{9,8},{10,11... | collective-permute-start | bytes 6291464 | tf_op jit(solution)/shard_map/ppermute | solution.py:357
  31.8 4.9 %collective-permute-start.5 = (bf16[1536,128]{1,0:T(8,128)(2,1)}, bf16[1536,128]{1,0:T(8,128)(2,1)S(1)}, u32[]{:S(2)}, u32[]{:S(2)}) collective-permute-start(bf16[1536,128]{1,0:T(8,128)(2,1)} %collective-permute-done.3.refs_0_), channel_id=1, source_target_pairs={{0,2},{1,31},{2,4},{3,1},{4,6},{5,3},{6,8},{7,5},{8,10},{9,7},{10,... | collective-permute-start | bytes 1179656 | tf_op jit(solution)/shard_map/ppermute | solution.py:357
  36.7 1.9 %collective-permute-start.12 = (bf16[1568,128]{1,0:T(8,128)(2,1)S(1)}, bf16[1568,128]{1,0:T(8,128)(2,1)S(1)}, u32[]{:S(2)}, u32[]{:S(2)}) collective-permute-start(bf16[1568,128]{1,0:T(8,128)(2,1)S(1)} %collective-permute-done.11.refs_3_), channel_id=1, source_target_pairs={{0,2},{1,31},{2,4},{3,1},{4,6},{5,3},{6,8},{7,5},{8,10},{9,7},{10,... | collective-permute-start | bytes 1204232 | tf_op jit(solution)/shard_map/ppermute | solution.py:357
  39.4 2.3 %collective-permute-done.5.refs_1_ = bf16[1536,128]{1,0:T(8,128)(2,1)S(1)} collective-permute-done((bf16[1536,128]{1,0:T(8,128)(2,1)}, bf16[1536,128]{1,0:T(8,128)(2,1)S(1)}, u32[]{:S(2)}, u32[]{:S(2)}) %collective-permute-start.5) | collective-permute-done | bytes 393248 | tf_op jit(solution)/shard_map/ppermute | solution.py:357
  41.7 4.9 %collective-permute-start.6 = (bf16[1536,128]{1,0:T(8,128)(2,1)S(1)}, bf16[1536,128]{1,0:T(8,128)(2,1)S(1)}, u32[]{:S(2)}, u32[]{:S(2)}) collective-permute-start(bf16[1536,128]{1,0:T(8,128)(2,1)S(1)} %collective-permute-done.5.refs_1_), channel_id=1, source_target_pairs={{0,2},{1,31},{2,4},{3,1},{4,6},{5,3},{6,8},{7,5},{8,10},{9,7},{10,... | collective-permute-start | bytes 1179656 | tf_op jit(solution)/shard_map/ppermute | solution.py:357
  47.4 3.5 %collective-permute-start.13 = (bf16[1568,128]{1,0:T(8,128)(2,1)S(1)}, bf16[1568,128]{1,0:T(8,128)(2,1)S(1)}, u32[]{:S(2)}, u32[]{:S(2)}) collective-permute-start(bf16[1568,128]{1,0:T(8,128)(2,1)S(1)} %collective-permute-done.12.refs_4_), channel_id=1, source_target_pairs={{0,2},{1,31},{2,4},{3,1},{4,6},{5,3},{6,8},{7,5},{8,10},{9,7},{10,... | collective-permute-start | bytes 1204232 | tf_op jit(solution)/shard_map/ppermute | solution.py:357
  51.3 5.0 %collective-permute-start.7 = (bf16[1536,128]{1,0:T(8,128)(2,1)S(1)}, bf16[1536,128]{1,0:T(8,128)(2,1)S(1)}, u32[]{:S(2)}, u32[]{:S(2)}) collective-permute-start(bf16[1536,128]{1,0:T(8,128)(2,1)S(1)} %collective-permute-done.6.refs_1_), channel_id=1, source_target_pairs={{0,2},{1,31},{2,4},{3,1},{4,6},{5,3},{6,8},{7,5},{8,10},{9,7},{10,... | collective-permute-start | bytes 1179656 | tf_op jit(solution)/shard_map/ppermute | solution.py:357
  57.1 3.6 %collective-permute-start.14 = (bf16[1568,128]{1,0:T(8,128)(2,1)S(1)}, bf16[1568,128]{1,0:T(8,128)(2,1)S(1)}, u32[]{:S(2)}, u32[]{:S(2)}) collective-permute-start(bf16[1568,128]{1,0:T(8,128)(2,1)S(1)} %collective-permute-done.13.refs_5_), channel_id=1, source_target_pairs={{0,2},{1,31},{2,4},{3,1},{4,6},{5,3},{6,8},{7,5},{8,10},{9,7},{10,... | collective-permute-start | bytes 1204232 | tf_op jit(solution)/shard_map/ppermute | solution.py:357
  61.5 4.6 %collective-permute-start.8 = (bf16[1536,128]{1,0:T(8,128)(2,1)S(1)}, bf16[1536,128]{1,0:T(8,128)(2,1)S(1)}, u32[]{:S(2)}, u32[]{:S(2)}) collective-permute-start(bf16[1536,128]{1,0:T(8,128)(2,1)S(1)} %collective-permute-done.7.refs_2_), channel_id=1, source_target_pairs={{0,2},{1,31},{2,4},{3,1},{4,6},{5,3},{6,8},{7,5},{8,10},{9,7},{10,... | collective-permute-start | bytes 1179656 | tf_op jit(solution)/shard_map/ppermute | solution.py:357
  66.8 3.7 %collective-permute-start.15 = (bf16[1568,128]{1,0:T(8,128)(2,1)S(1)}, bf16[1568,128]{1,0:T(8,128)(2,1)}, u32[]{:S(2)}, u32[]{:S(2)}) collective-permute-start(bf16[1568,128]{1,0:T(8,128)(2,1)S(1)} %collective-permute-done.14.refs_2_), channel_id=1, source_target_pairs={{0,2},{1,31},{2,4},{3,1},{4,6},{5,3},{6,8},{7,5},{8,10},{9,7},{10,... | collective-permute-start | bytes 1204232 | tf_op jit(solution)/shard_map/ppermute | solution.py:357
  71.3 4.5 %collective-permute-start.9 = (bf16[1536,128]{1,0:T(8,128)(2,1)S(1)}, bf16[1536,128]{1,0:T(8,128)(2,1)}, u32[]{:S(2)}, u32[]{:S(2)}) collective-permute-start(bf16[1536,128]{1,0:T(8,128)(2,1)S(1)} %collective-permute-done.8.refs_0_), channel_id=1, source_target_pairs={{0,2},{1,31},{2,4},{3,1},{4,6},{5,3},{6,8},{7,5},{8,10},{9,7},{10,... | collective-permute-start | bytes 1179656 | tf_op jit(solution)/shard_map/ppermute | solution.py:357
  76.5 3.6 %collective-permute-start.17 = (bf16[1536,128]{1,0:T(8,128)(2,1)}, bf16[1536,128]{1,0:T(8,128)(2,1)}, u32[]{:S(2)}, u32[]{:S(2)}) collective-permute-start(bf16[1536,128]{1,0:T(8,128)(2,1)} %bitcast.3.refs_0_), channel_id=1, source_target_pairs={{0,1},{1,0},{2,3},{3,2},{4,5},{5,4},{6,7},{7,6},{8,9},{9,8},{10,11... | collective-permute-start | bytes 1179656 | tf_op jit(solution)/shard_map/ppermute | solution.py:357
  80.1 4.9 %collective-permute-start.16 = (bf16[1568,128]{1,0:T(8,128)(2,1)}, bf16[1568,128]{1,0:T(8,128)(2,1)}, u32[]{:S(2)}, u32[]{:S(2)}) collective-permute-start(bf16[1568,128]{1,0:T(8,128)(2,1)} %collective-permute-done.15.refs_3_), channel_id=1, source_target_pairs={{0,2},{1,31},{2,4},{3,1},{4,6},{5,3},{6,8},{7,5},{8,10},{9,7},{10,... | collective-permute-start | bytes 1204232 | tf_op jit(solution)/shard_map/ppermute | solution.py:357
  85.0 1.9 %collective-permute-start.10 = (bf16[1536,128]{1,0:T(8,128)(2,1)}, bf16[1536,128]{1,0:T(8,128)(2,1)}, u32[]{:S(2)}, u32[]{:S(2)}) collective-permute-start(bf16[1536,128]{1,0:T(8,128)(2,1)} %collective-permute-done.9.refs_1_), channel_id=1, source_target_pairs={{0,2},{1,31},{2,4},{3,1},{4,6},{5,3},{6,8},{7,5},{8,10},{9,7},{10,... | collective-permute-start | bytes 1179656 | tf_op jit(solution)/shard_map/ppermute | solution.py:357
  87.0 1.0 copy-done.6
  89.1 3.0 %ring_sums.4 = (f32[1536,256]{1,0:T(8,128)S(1)}, f32[1536,256]{1,0:T(8,128)S(1)}) custom-call(s32[4]{0:T(128)S(1)} %pad_add_fusion.place_ref, bf16[4096,256]{1,0:T(8,128)(2,1)S(1)} %beside.1.own_w_ref.main_ref, bf16[4096,256]{1,0:T(8,128)(2,1)} %collective-permute-done.4.other_w_ref, bf16[1536,128]{1,0:T(8,128)(2,1)} %collective-permute-done.3.refs_0_, ...), custom_call_target="tpu_custom_call" | custom-call | flops 805306368 | tf_op jit(solution)/shard_map/ring_sums/pallas_call | solution.py:121
  92.1 3.3 %ring_sums.5 = (f32[1536,256]{1,0:T(8,128)S(1)}, f32[1536,256]{1,0:T(8,128)S(1)}) custom-call(s32[4]{0:T(128)S(1)} %pad_add_fusion.place_ref, bf16[4096,256]{1,0:T(8,128)(2,1)S(1)} %beside.1.own_w_ref.main_ref, bf16[4096,256]{1,0:T(8,128)(2,1)} %collective-permute-done.4.other_w_ref, bf16[1536,128]{1,0:T(8,128)(2,1)} %bitcast.3.refs_0_, ...), custom_call_target="tpu_custom_call" | custom-call | flops 1207959552 | tf_op jit(solution)/shard_map/ring_sums/pallas_call | solution.py:121
  95.5 3.0 %ring_sums.6 = (f32[1536,256]{1,0:T(8,128)S(1)}, f32[1536,256]{1,0:T(8,128)S(1)}) custom-call(s32[4]{0:T(128)S(1)} %pad_add_fusion.place_ref, bf16[4096,256]{1,0:T(8,128)(2,1)S(1)} %beside.1.own_w_ref.main_ref, bf16[4096,256]{1,0:T(8,128)(2,1)} %collective-permute-done.4.other_w_ref, bf16[1536,128]{1,0:T(8,128)(2,1)S(1)} %copy-done.14, ...), custom_call_target="tpu_custom_call" | custom-call | flops 805306368 | tf_op jit(solution)/shard_map/ring_sums/pallas_call | solution.py:121
  98.5 2.8 %ring_sums.7 = (f32[1536,256]{1,0:T(8,128)S(1)}, f32[1536,256]{1,0:T(8,128)S(1)}) custom-call(s32[4]{0:T(128)S(1)} %pad_add_fusion.place_ref, bf16[4096,256]{1,0:T(8,128)(2,1)S(1)} %beside.1.own_w_ref.main_ref, bf16[4096,256]{1,0:T(8,128)(2,1)} %collective-permute-done.4.other_w_ref, bf16[1536,128]{1,0:T(8,128)(2,1)} %collective-permute-done.10.refs_0_, ...), custom_call_target="tpu_custom_call" | custom-call | flops 402653184 | tf_op jit(solution)/shard_map/ring_sums/pallas_call | solution.py:121
  101.4 3.4 %collective-permute-start.18 = (f32[1536,256]{1,0:T(8,128)S(1)}, f32[1536,256]{1,0:T(8,128)S(1)}, u32[]{:S(2)}, u32[]{:S(2)}) collective-permute-start(f32[1536,256]{1,0:T(8,128)S(1)} %get-tuple-element.33), channel_id=1, source_target_pairs={{0,1},{1,0},{2,3},{3,2},{4,5},{5,4},{6,7},{7,6},{8,9},{9,8},{10,11... | collective-permute-start | bytes 4718600 | tf_op jit(solution)/shard_map/ppermute | solution.py:357
  105.5 4.8 %collective-permute-start.20 = (bf16[1536,128]{1,0:T(8,128)(2,1)}, bf16[1536,128]{1,0:T(8,128)(2,1)S(1)}, u32[]{:S(2)}, u32[]{:S(2)}) collective-permute-start(bf16[1536,128]{1,0:T(8,128)(2,1)} %collective-permute-done.10.refs_0_), channel_id=1, source_target_pairs={{0,2},{1,31},{2,4},{3,1},{4,6},{5,3},{6,8},{7,5},{8,10},{9,7},{10,... | collective-permute-start | bytes 1179656 | tf_op jit(solution)/shard_map/ppermute | solution.py:357
  110.4 1.9 %collective-permute-start.21 = (bf16[1568,128]{1,0:T(8,128)(2,1)}, bf16[1568,128]{1,0:T(8,128)(2,1)S(1)}, u32[]{:S(2)}, u32[]{:S(2)}) collective-permute-start(bf16[1568,128]{1,0:T(8,128)(2,1)} %collective-permute-done.16.refs_1_), channel_id=1, source_target_pairs={{0,2},{1,31},{2,4},{3,1},{4,6},{5,3},{6,8},{7,5},{8,10},{9,7},{10,... | collective-permute-start | bytes 1204232 | tf_op jit(solution)/shard_map/ppermute | solution.py:357
  113.7 2.0 %collective-permute-start.19 = (bf16[224,128]{1,0:T(8,128)(2,1)S(1)}, bf16[224,128]{1,0:T(8,128)(2,1)S(1)}, u32[]{:S(2)}, u32[]{:S(2)}) collective-permute-start(bf16[224,128]{1,0:T(8,128)(2,1)S(1)} %constant_dynamic-update-slice_fusion.mine_new_ref), channel_id=1, source_target_pairs={{0,1},{1,0},{2,3},{3,2},{4,5},{5,4},{6,7},{7,6},{8,9},{9,8},{10,11... | collective-permute-start | bytes 172040 | tf_op jit(solution)/shard_map/ppermute | solution.py:357
  117.0 2.7 %collective-permute-done.21.last_b_ref = bf16[1568,128]{1,0:T(8,128)(2,1)S(1)} collective-permute-done((bf16[1568,128]{1,0:T(8,128)(2,1)}, bf16[1568,128]{1,0:T(8,128)(2,1)S(1)}, u32[]{:S(2)}, u32[]{:S(2)}) %collective-permute-start.21) | collective-permute-done | bytes 401440 | tf_op jit(solution)/shard_map/ppermute | solution.py:357
  119.7 2.1 %span_states.1 = (f32[16,15,128]{2,1,0:T(8,128)S(1)}, f32[16,128]{1,0:T(8,128)S(1)}) custom-call(s32[4]{0:T(128)S(1)} %pad_add_fusion.place_ref, f32[2]{0:T(128)S(1)} %copy-done.17, f32[1536,256]{1,0:T(8,128)S(1)} %get-tuple-element.32.total_ref, f32[1536,256]{1,0:T(8,128)S(1)} %collective-permute-done.18.arrived_ref, f32[16,384]{1,0:T(8,128)S(1)} %new_sums.1.early_ref, ...), custom_call_target="tpu_custom_call" | custom-call | tf_op jit(solution)/shard_map/span_states/pallas_call | solution.py:264
  121.8 13.4 %all_to_all.5.arrived_ref = f32[16,15,128]{2,1,0:T(8,128)S(1)} all-to-all(f32[16,15,128]{2,1,0:T(8,128)S(1)} %get-tuple-element.36), channel_id=1, replica_groups=mesh['sp'=16,'tp'=32] {'sp'}, dimensions={0} | all-to-all | bytes 245760 | tf_op jit(solution)/shard_map/all_to_all | solution.py:430
  (72 shorter events, 14.7 us)
Async XLA Ops:
  0.6 21.3 %collective-permute-start.3 = (bf16[1536,128]{1,0:T(8,128)(2,1)}, bf16[1536,128]{1,0:T(8,128)(2,1)}, u32[]{:S(2)}, u32[]{:S(2)}) collective-permute-start(bf16[1536,128]{1,0:T(8,128)(2,1)} %bitcast.3.refs_0_), channel_id=1, source_target_pairs={{0,2},{1,31},{2,4},{3,1},{4,6},{5,3},{6,8},{7,5},{8,10},{9,7},{10,... | collective-permute-start | bytes 1179656 | tf_op jit(solution)/shard_map/ppermute | solution.py:357
  12.6 11.1 %collective-permute-start = (bf16[1536,128]{1,0:T(8,128)(2,1)}, bf16[1536,128]{1,0:T(8,128)(2,1)S(1)}, u32[]{:S(2)}, u32[]{:S(2)}) collective-permute-start(bf16[1536,128]{1,0:T(8,128)(2,1)} %bitcast.3.refs_0_), channel_id=1, source_target_pairs={{1,2},{0,31},{3,4},{2,1},{5,6},{4,3},{7,8},{6,5},{9,10},{8,7},{11,... | collective-permute-start | bytes 1179656 | tf_op jit(solution)/shard_map/ppermute | solution.py:357
  14.5 4.0 %collective-permute-start.1 = (bf16[3,1,128]{2,0,1:T(4,128)(2,1)}, bf16[3,1,128]{2,0,1:T(4,128)(2,1)S(1)}, u32[]{:S(2)}, u32[]{:S(2)}) collective-permute-start(bf16[3,1,128]{2,0,1:T(4,128)(2,1)} %param.7), channel_id=1, source_target_pairs={{0,1},{1,0},{2,3},{3,2},{4,5},{5,4},{6,7},{7,6},{8,9},{9,8},{10,11... | collective-permute-start | bytes 2312 | tf_op jit(solution)/shard_map/ppermute | solution.py:357
  17.6 10.0 %copy-start.1 = (bf16[4096,128]{1,0:T(8,128)(2,1)S(1)}, bf16[4096,128]{1,0:T(8,128)(2,1)}, u32[]{:S(2)}) copy-start(bf16[4096,128]{1,0:T(8,128)(2,1)} %left_ref) | copy-start | bytes 3145732
  19.2 4.4 %collective-permute-start.2 = (bf16[32,128]{1,0:T(8,128)(2,1)S(1)}, bf16[32,128]{1,0:T(8,128)(2,1)S(1)}, u32[]{:S(2)}, u32[]{:S(2)}) collective-permute-start(bf16[32,128]{1,0:T(8,128)(2,1)S(1)} %pad_maximum_fusion.1.here_new_ref), channel_id=1, source_target_pairs={{0,2},{1,31},{2,4},{3,1},{4,6},{5,3},{6,8},{7,5},{8,10},{9,7},{10,... | collective-permute-start | bytes 24584 | tf_op jit(solution)/shard_map/ppermute | solution.py:357
  23.7 13.0 %collective-permute-start.11 = (bf16[1568,128]{1,0:T(8,128)(2,1)S(1)}, bf16[1568,128]{1,0:T(8,128)(2,1)S(1)}, u32[]{:S(2)}, u32[]{:S(2)}) collective-permute-start(bf16[1568,128]{1,0:T(8,128)(2,1)S(1)} %pad_maximum_fusion), channel_id=1, source_target_pairs={{0,2},{1,31},{2,4},{3,1},{4,6},{5,3},{6,8},{7,5},{8,10},{9,7},{10,... | collective-permute-start | bytes 1204232 | tf_op jit(solution)/shard_map/ppermute | solution.py:357
  27.5 1.2 copy-start.2
  29.1 57.9 %collective-permute-start.4 = (bf16[4096,256]{1,0:T(8,128)(2,1)S(1)}, bf16[4096,256]{1,0:T(8,128)(2,1)}, u32[]{:S(2)}, u32[]{:S(2)}) collective-permute-start(bf16[4096,256]{1,0:T(8,128)(2,1)S(1)} %beside.1.own_w_ref.main_ref), channel_id=1, source_target_pairs={{0,1},{1,0},{2,3},{3,2},{4,5},{5,4},{6,7},{7,6},{8,9},{9,8},{10,11... | collective-permute-start | bytes 6291464 | tf_op jit(solution)/shard_map/ppermute | solution.py:357
  31.8 9.9 %collective-permute-start.5 = (bf16[1536,128]{1,0:T(8,128)(2,1)}, bf16[1536,128]{1,0:T(8,128)(2,1)S(1)}, u32[]{:S(2)}, u32[]{:S(2)}) collective-permute-start(bf16[1536,128]{1,0:T(8,128)(2,1)} %collective-permute-done.3.refs_0_), channel_id=1, source_target_pairs={{0,2},{1,31},{2,4},{3,1},{4,6},{5,3},{6,8},{7,5},{8,10},{9,7},{10,... | collective-permute-start | bytes 1179656 | tf_op jit(solution)/shard_map/ppermute | solution.py:357
  36.7 10.7 %collective-permute-start.12 = (bf16[1568,128]{1,0:T(8,128)(2,1)S(1)}, bf16[1568,128]{1,0:T(8,128)(2,1)S(1)}, u32[]{:S(2)}, u32[]{:S(2)}) collective-permute-start(bf16[1568,128]{1,0:T(8,128)(2,1)S(1)} %collective-permute-done.11.refs_3_), channel_id=1, source_target_pairs={{0,2},{1,31},{2,4},{3,1},{4,6},{5,3},{6,8},{7,5},{8,10},{9,7},{10,... | collective-permute-start | bytes 1204232 | tf_op jit(solution)/shard_map/ppermute | solution.py:357
  41.7 9.6 %collective-permute-start.6 = (bf16[1536,128]{1,0:T(8,128)(2,1)S(1)}, bf16[1536,128]{1,0:T(8,128)(2,1)S(1)}, u32[]{:S(2)}, u32[]{:S(2)}) collective-permute-start(bf16[1536,128]{1,0:T(8,128)(2,1)S(1)} %collective-permute-done.5.refs_1_), channel_id=1, source_target_pairs={{0,2},{1,31},{2,4},{3,1},{4,6},{5,3},{6,8},{7,5},{8,10},{9,7},{10,... | collective-permute-start | bytes 1179656 | tf_op jit(solution)/shard_map/ppermute | solution.py:357
  47.4 9.7 %collective-permute-start.13 = (bf16[1568,128]{1,0:T(8,128)(2,1)S(1)}, bf16[1568,128]{1,0:T(8,128)(2,1)S(1)}, u32[]{:S(2)}, u32[]{:S(2)}) collective-permute-start(bf16[1568,128]{1,0:T(8,128)(2,1)S(1)} %collective-permute-done.12.refs_4_), channel_id=1, source_target_pairs={{0,2},{1,31},{2,4},{3,1},{4,6},{5,3},{6,8},{7,5},{8,10},{9,7},{10,... | collective-permute-start | bytes 1204232 | tf_op jit(solution)/shard_map/ppermute | solution.py:357
  51.3 10.2 %collective-permute-start.7 = (bf16[1536,128]{1,0:T(8,128)(2,1)S(1)}, bf16[1536,128]{1,0:T(8,128)(2,1)S(1)}, u32[]{:S(2)}, u32[]{:S(2)}) collective-permute-start(bf16[1536,128]{1,0:T(8,128)(2,1)S(1)} %collective-permute-done.6.refs_1_), channel_id=1, source_target_pairs={{0,2},{1,31},{2,4},{3,1},{4,6},{5,3},{6,8},{7,5},{8,10},{9,7},{10,... | collective-permute-start | bytes 1179656 | tf_op jit(solution)/shard_map/ppermute | solution.py:357
  57.1 9.7 %collective-permute-start.14 = (bf16[1568,128]{1,0:T(8,128)(2,1)S(1)}, bf16[1568,128]{1,0:T(8,128)(2,1)S(1)}, u32[]{:S(2)}, u32[]{:S(2)}) collective-permute-start(bf16[1568,128]{1,0:T(8,128)(2,1)S(1)} %collective-permute-done.13.refs_5_), channel_id=1, source_target_pairs={{0,2},{1,31},{2,4},{3,1},{4,6},{5,3},{6,8},{7,5},{8,10},{9,7},{10,... | collective-permute-start | bytes 1204232 | tf_op jit(solution)/shard_map/ppermute | solution.py:357
  61.5 9.8 %collective-permute-start.8 = (bf16[1536,128]{1,0:T(8,128)(2,1)S(1)}, bf16[1536,128]{1,0:T(8,128)(2,1)S(1)}, u32[]{:S(2)}, u32[]{:S(2)}) collective-permute-start(bf16[1536,128]{1,0:T(8,128)(2,1)S(1)} %collective-permute-done.7.refs_2_), channel_id=1, source_target_pairs={{0,2},{1,31},{2,4},{3,1},{4,6},{5,3},{6,8},{7,5},{8,10},{9,7},{10,... | collective-permute-start | bytes 1179656 | tf_op jit(solution)/shard_map/ppermute | solution.py:357
  66.8 13.3 %collective-permute-start.15 = (bf16[1568,128]{1,0:T(8,128)(2,1)S(1)}, bf16[1568,128]{1,0:T(8,128)(2,1)}, u32[]{:S(2)}, u32[]{:S(2)}) collective-permute-start(bf16[1568,128]{1,0:T(8,128)(2,1)S(1)} %collective-permute-done.14.refs_2_), channel_id=1, source_target_pairs={{0,2},{1,31},{2,4},{3,1},{4,6},{5,3},{6,8},{7,5},{8,10},{9,7},{10,... | collective-permute-start | bytes 1204232 | tf_op jit(solution)/shard_map/ppermute | solution.py:357
  71.3 13.7 %collective-permute-start.9 = (bf16[1536,128]{1,0:T(8,128)(2,1)S(1)}, bf16[1536,128]{1,0:T(8,128)(2,1)}, u32[]{:S(2)}, u32[]{:S(2)}) collective-permute-start(bf16[1536,128]{1,0:T(8,128)(2,1)S(1)} %collective-permute-done.8.refs_0_), channel_id=1, source_target_pairs={{0,2},{1,31},{2,4},{3,1},{4,6},{5,3},{6,8},{7,5},{8,10},{9,7},{10,... | collective-permute-start | bytes 1179656 | tf_op jit(solution)/shard_map/ppermute | solution.py:357
  76.5 15.6 %collective-permute-start.17 = (bf16[1536,128]{1,0:T(8,128)(2,1)}, bf16[1536,128]{1,0:T(8,128)(2,1)}, u32[]{:S(2)}, u32[]{:S(2)}) collective-permute-start(bf16[1536,128]{1,0:T(8,128)(2,1)} %bitcast.3.refs_0_), channel_id=1, source_target_pairs={{0,1},{1,0},{2,3},{3,2},{4,5},{5,4},{6,7},{7,6},{8,9},{9,8},{10,11... | collective-permute-start | bytes 1179656 | tf_op jit(solution)/shard_map/ppermute | solution.py:357
  80.1 18.4 %collective-permute-start.16 = (bf16[1568,128]{1,0:T(8,128)(2,1)}, bf16[1568,128]{1,0:T(8,128)(2,1)}, u32[]{:S(2)}, u32[]{:S(2)}) collective-permute-start(bf16[1568,128]{1,0:T(8,128)(2,1)} %collective-permute-done.15.refs_3_), channel_id=1, source_target_pairs={{0,2},{1,31},{2,4},{3,1},{4,6},{5,3},{6,8},{7,5},{8,10},{9,7},{10,... | collective-permute-start | bytes 1204232 | tf_op jit(solution)/shard_map/ppermute | solution.py:357
  85.0 13.5 %collective-permute-start.10 = (bf16[1536,128]{1,0:T(8,128)(2,1)}, bf16[1536,128]{1,0:T(8,128)(2,1)}, u32[]{:S(2)}, u32[]{:S(2)}) collective-permute-start(bf16[1536,128]{1,0:T(8,128)(2,1)} %collective-permute-done.9.refs_1_), channel_id=1, source_target_pairs={{0,2},{1,31},{2,4},{3,1},{4,6},{5,3},{6,8},{7,5},{8,10},{9,7},{10,... | collective-permute-start | bytes 1179656 | tf_op jit(solution)/shard_map/ppermute | solution.py:357
  87.0 5.1 %copy-start.4 = (bf16[1568,128]{1,0:T(8,128)(2,1)S(1)}, bf16[1568,128]{1,0:T(8,128)(2,1)}, u32[]{:S(2)}) copy-start(bf16[1568,128]{1,0:T(8,128)(2,1)} %copy-done.3) | copy-start | bytes 1204228
  87.0 1.1 copy-start.6
  89.1 3.0 %copy-start.10 = (bf16[1536,128]{1,0:T(8,128)(2,1)S(1)}, bf16[1536,128]{1,0:T(8,128)(2,1)}, u32[]{:S(2)}) copy-start(bf16[1536,128]{1,0:T(8,128)(2,1)} %copy-done.9) | copy-start | bytes 1179652
  89.1 3.0 %copy-start.12 = (bf16[1536,128]{1,0:T(8,128)(2,1)S(1)}, bf16[1536,128]{1,0:T(8,128)(2,1)}, u32[]{:S(2)}) copy-start(bf16[1536,128]{1,0:T(8,128)(2,1)} %copy-done.11) | copy-start | bytes 1179652
  92.1 3.3 %copy-start.8 = (bf16[1568,128]{1,0:T(8,128)(2,1)S(1)}, bf16[1568,128]{1,0:T(8,128)(2,1)}, u32[]{:S(2)}) copy-start(bf16[1568,128]{1,0:T(8,128)(2,1)} %copy-done.7) | copy-start | bytes 1204228
  92.1 3.3 %copy-start.14 = (bf16[1536,128]{1,0:T(8,128)(2,1)S(1)}, bf16[1536,128]{1,0:T(8,128)(2,1)}, u32[]{:S(2)}) copy-start(bf16[1536,128]{1,0:T(8,128)(2,1)} %copy-done.13) | copy-start | bytes 1179652
  98.5 17.2 %copy-start = (bf16[4096,128]{1,0:T(8,128)(2,1)S(1)}, bf16[4096,128]{1,0:T(8,128)(2,1)}, u32[]{:S(2)}) copy-start(bf16[4096,128]{1,0:T(8,128)(2,1)} %query_w_ref.3) | copy-start | bytes 3145732
  101.4 18.3 %collective-permute-start.18 = (f32[1536,256]{1,0:T(8,128)S(1)}, f32[1536,256]{1,0:T(8,128)S(1)}, u32[]{:S(2)}, u32[]{:S(2)}) collective-permute-start(f32[1536,256]{1,0:T(8,128)S(1)} %get-tuple-element.33), channel_id=1, source_target_pairs={{0,1},{1,0},{2,3},{3,2},{4,5},{5,4},{6,7},{7,6},{8,9},{9,8},{10,11... | collective-permute-start | bytes 4718600 | tf_op jit(solution)/shard_map/ppermute | solution.py:357
  105.5 11.4 %collective-permute-start.20 = (bf16[1536,128]{1,0:T(8,128)(2,1)}, bf16[1536,128]{1,0:T(8,128)(2,1)S(1)}, u32[]{:S(2)}, u32[]{:S(2)}) collective-permute-start(bf16[1536,128]{1,0:T(8,128)(2,1)} %collective-permute-done.10.refs_0_), channel_id=1, source_target_pairs={{0,2},{1,31},{2,4},{3,1},{4,6},{5,3},{6,8},{7,5},{8,10},{9,7},{10,... | collective-permute-start | bytes 1179656 | tf_op jit(solution)/shard_map/ppermute | solution.py:357
  110.4 9.3 %collective-permute-start.21 = (bf16[1568,128]{1,0:T(8,128)(2,1)}, bf16[1568,128]{1,0:T(8,128)(2,1)S(1)}, u32[]{:S(2)}, u32[]{:S(2)}) collective-permute-start(bf16[1568,128]{1,0:T(8,128)(2,1)} %collective-permute-done.16.refs_1_), channel_id=1, source_target_pairs={{0,2},{1,31},{2,4},{3,1},{4,6},{5,3},{6,8},{7,5},{8,10},{9,7},{10,... | collective-permute-start | bytes 1204232 | tf_op jit(solution)/shard_map/ppermute | solution.py:357
  113.7 6.0 %copy-start.17 = (f32[2]{0:T(128)S(1)}, f32[2]{0:T(128)}, u32[]{:S(2)}) copy-start(f32[2]{0:T(128)} %rate_ref.1) | copy-start | bytes 28
  113.7 3.3 %collective-permute-start.19 = (bf16[224,128]{1,0:T(8,128)(2,1)S(1)}, bf16[224,128]{1,0:T(8,128)(2,1)S(1)}, u32[]{:S(2)}, u32[]{:S(2)}) collective-permute-start(bf16[224,128]{1,0:T(8,128)(2,1)S(1)} %constant_dynamic-update-slice_fusion.mine_new_ref), channel_id=1, source_target_pairs={{0,1},{1,0},{2,3},{3,2},{4,5},{5,4},{6,7},{7,6},{8,9},{9,8},{10,11... | collective-permute-start | bytes 172040 | tf_op jit(solution)/shard_map/ppermute | solution.py:357
  (8 other events, 6.3 us)

commit v12 on v11

--- a/solution.py
+++ b/solution.py
@@ -152,7 +152,21 @@
     return jnp.dot(entries, weights, preferred_element_type=jnp.float32)
 
 
-def new_kernel(place_ref, here_new_ref, mine_new_ref, main_ref, query_w_ref, out_ref):
+def lane_rates(rate_ref, inner):
+    row_lane = lax.broadcasted_iota(jnp.int32, (1, inner), 1)
+    lane_decay = jnp.full((1, inner), rate_ref[0], jnp.float32)
+    for h in range(1, inner // HD):
+        lane_decay = jnp.where(row_lane // HD == h, rate_ref[h], lane_decay)
+    return lane_decay
+
+
+def new_kernel(
+    place_ref, rate_ref, here_new_ref, mine_new_ref, main_ref, query_w_ref, out_ref, decay_ref
+):
+    span_len, inner = decay_ref.shape
+    to_end = lax.broadcasted_iota(jnp.int32, (span_len, inner), 0)
+    to_end = (span_len - 1 - to_end).astype(jnp.float32)
+    decay_ref[...] = jnp.exp(to_end * lane_rates(rate_ref, inner))
     pieces = pair(here_new_ref, 0)
     order = [0]
     for k in range(1, mine_new_ref.shape[0] // (2 * EXTRA) + 1):
@@ -161,17 +175,20 @@
     out_ref[...] = new_rows_product(place_ref, main_ref, query_w_ref, pieces, order)
 
 
-def new_sums(place, here_new, mine_new, main_weights, query_weight):
+def new_sums(place, decay, span_len, here_new, mine_new, main_weights, query_weight):
     whole = pl.BlockSpec(memory_space=pltpu.VMEM)
     inner = main_weights.shape[1] + query_weight.shape[1]
     return pl.pallas_call(
         new_kernel,
-        in_specs=[pl.BlockSpec(memory_space=pltpu.SMEM)] + [whole] * 4,
-        out_specs=whole,
-        out_shape=jax.ShapeDtypeStruct((EXTRA, inner), jnp.float32),
+        in_specs=[pl.BlockSpec(memory_space=pltpu.SMEM)] * 2 + [whole] * 4,
+        out_specs=[whole, whole],
+        out_shape=[
+            jax.ShapeDtypeStruct((EXTRA, inner), jnp.float32),
+            jax.ShapeDtypeStruct((span_len, query_weight.shape[1]), jnp.float32),
+        ],
         compiler_params=pltpu.CompilerParams(vmem_limit_bytes=6 * 1024 * 1024),
         name="new_sums",
-    )(place, here_new, mine_new, main_weights, query_weight)
+    )(place, decay, here_new, mine_new, main_weights, query_weight)
 
 
 def state_kernel(
@@ -180,6 +197,7 @@
     total_ref,
     arrived_ref,
     early_ref,
+    decay_ref,
     theirs_new_ref,
     last_a_ref,
     last_b_ref,
@@ -198,15 +216,11 @@
     span_len = rows // prompts
     reach = theirs_new_ref.shape[0] // (2 * EXTRA) + 1
     lane = lax.broadcasted_iota(jnp.int32, (HD, inner), 1)
-    row_lane = lax.broadcasted_iota(jnp.int32, (1, inner), 1)
-    lane_decay = jnp.full((1, inner), rate_ref[0], jnp.float32)
-    for h in range(1, inner // HD):
-        lane_decay = jnp.where(row_lane // HD == h, rate_ref[h], lane_decay)
+    lane_decay = lane_rates(rate_ref, inner)
     distance = ((groups - 1 - place_ref[2]) * span_len).astype(jnp.float32)
     carried = jnp.exp(lane_decay * distance)
     one = jnp.exp(lane_decay)
-    to_end = lax.broadcasted_iota(jnp.int32, (span_len, inner), 0)
-    decay = jnp.exp((span_len - 1 - to_end).astype(jnp.float32) * lane_decay)
+    decay = decay_ref[...]
 
     pieces, order = [], []
     for k in range(1, reach):
@@ -409,7 +423,9 @@
     mine_new = jnp.concatenate(new_list[:-1], axis=0)
     theirs_new = sent(mine_new, partner)
 
-    early = new_sums(place, new_pair, mine_new, main_weights, query_weight)
+    early = new_sums(
+        place, log_decay, span_len, new_pair, mine_new, main_weights, query_weight
+    )
     messages, own_term = span_states(
         prompts,
         groups,
@@ -417,7 +433,7 @@
         place,
         own,
         arrived,
-        early,
+        *early,
         theirs_new,
         a_list[-1],
         b_list[-1],

time: 137 us -> 137 us (level)
  no operation moved by 1% of the time
where the time goes in v12:
time: 137 us; the launch traced here: 136 us
  starting transfers between devices  85.1 us (62%)
  Pallas kernels  16.2 us (12%)
  blocking collectives  13.4 us (10%)
  local copies, waits for them, and re-layouts  10.7 us (8%)
  waiting for transfers between devices  7.59 us (6%)
  other arithmetic  1.83 us (1%)
    ppermute x22, starting transfers between devices, sent(): return lax.ppermute(value, 'tp', pairs)  85.1 us
    all_to_all x1, blocking collectives, body(): lax.all_to_all(messages, 'sp', split_axis=0, concat_axis=0, tiled=True)  13.4 us
    pallas_call x4, Pallas kernels, ring_sums(): pl.pallas_call(functools.partial(sums_kernel, offsets, span_len, bool(bef...  12.2 us
    unnamed x42, local copies, waits for them, and re-layouts  9.98 us
    ppermute x22, waiting for transfers between devices, sent(): return lax.ppermute(value, 'tp', pairs)  7.59 us
  transfers between devices with their start and end apart: 22, of which 6 were waited for; matrix products, arithmetic and copies ran while one was open for 3% of the time, Pallas kernels for 8%

profile of v12, /device:TPU:1, one launch (start us, length us, event | category | flops | bytes accessed | tf_op | source)
XLA Modules:
  0.0 136.0 jit_solution(13310093874371626842)
XLA Ops:
  0.6 11.9 %collective-permute-start.3 = (bf16[1536,128]{1,0:T(8,128)(2,1)}, bf16[1536,128]{1,0:T(8,128)(2,1)}, u32[]{:S(2)}, u32[]{:S(2)}) collective-permute-start(bf16[1536,128]{1,0:T(8,128)(2,1)} %bitcast.3.refs_0_), channel_id=1, source_target_pairs={{0,2},{1,31},{2,4},{3,1},{4,6},{5,3},{6,8},{7,5},{8,10},{9,7},{10,... | collective-permute-start | bytes 1179656 | tf_op jit(solution)/shard_map/ppermute | solution.py:371
  12.6 1.9 %collective-permute-start = (bf16[1536,128]{1,0:T(8,128)(2,1)}, bf16[1536,128]{1,0:T(8,128)(2,1)S(1)}, u32[]{:S(2)}, u32[]{:S(2)}) collective-permute-start(bf16[1536,128]{1,0:T(8,128)(2,1)} %bitcast.3.refs_0_), channel_id=1, source_target_pairs={{1,2},{0,31},{3,4},{2,1},{5,6},{4,3},{7,8},{6,5},{9,10},{8,7},{11,... | collective-permute-start | bytes 1179656 | tf_op jit(solution)/shard_map/ppermute | solution.py:371
  14.5 3.0 %collective-permute-start.1 = (bf16[3,1,128]{2,0,1:T(4,128)(2,1)}, bf16[3,1,128]{2,0,1:T(4,128)(2,1)S(1)}, u32[]{:S(2)}, u32[]{:S(2)}) collective-permute-start(bf16[3,1,128]{2,0,1:T(4,128)(2,1)} %param.7), channel_id=1, source_target_pairs={{0,1},{1,0},{2,3},{3,2},{4,5},{5,4},{6,7},{7,6},{8,9},{9,8},{10,11... | collective-permute-start | bytes 2312 | tf_op jit(solution)/shard_map/ppermute | solution.py:371
  19.2 2.6 %collective-permute-start.2 = (bf16[32,128]{1,0:T(8,128)(2,1)S(1)}, bf16[32,128]{1,0:T(8,128)(2,1)S(1)}, u32[]{:S(2)}, u32[]{:S(2)}) collective-permute-start(bf16[32,128]{1,0:T(8,128)(2,1)S(1)} %pad_maximum_fusion.1.here_new_ref), channel_id=1, source_target_pairs={{0,2},{1,31},{2,4},{3,1},{4,6},{5,3},{6,8},{7,5},{8,10},{9,7},{10,... | collective-permute-start | bytes 24584 | tf_op jit(solution)/shard_map/ppermute | solution.py:371
  23.7 3.8 %collective-permute-start.11 = (bf16[1568,128]{1,0:T(8,128)(2,1)S(1)}, bf16[1568,128]{1,0:T(8,128)(2,1)S(1)}, u32[]{:S(2)}, u32[]{:S(2)}) collective-permute-start(bf16[1568,128]{1,0:T(8,128)(2,1)S(1)} %pad_maximum_fusion), channel_id=1, source_target_pairs={{0,2},{1,31},{2,4},{3,1},{4,6},{5,3},{6,8},{7,5},{8,10},{9,7},{10,... | collective-permute-start | bytes 1204232 | tf_op jit(solution)/shard_map/ppermute | solution.py:371
  27.6 1.2 copy-done.2
  29.1 2.7 %collective-permute-start.4 = (bf16[4096,256]{1,0:T(8,128)(2,1)S(1)}, bf16[4096,256]{1,0:T(8,128)(2,1)}, u32[]{:S(2)}, u32[]{:S(2)}) collective-permute-start(bf16[4096,256]{1,0:T(8,128)(2,1)S(1)} %beside.1.own_w_ref.main_ref), channel_id=1, source_target_pairs={{0,1},{1,0},{2,3},{3,2},{4,5},{5,4},{6,7},{7,6},{8,9},{9,8},{10,11... | collective-permute-start | bytes 6291464 | tf_op jit(solution)/shard_map/ppermute | solution.py:371
  31.8 4.9 %collective-permute-start.5 = (bf16[1536,128]{1,0:T(8,128)(2,1)}, bf16[1536,128]{1,0:T(8,128)(2,1)S(1)}, u32[]{:S(2)}, u32[]{:S(2)}) collective-permute-start(bf16[1536,128]{1,0:T(8,128)(2,1)} %collective-permute-done.3.refs_0_), channel_id=1, source_target_pairs={{0,2},{1,31},{2,4},{3,1},{4,6},{5,3},{6,8},{7,5},{8,10},{9,7},{10,... | collective-permute-start | bytes 1179656 | tf_op jit(solution)/shard_map/ppermute | solution.py:371
  36.7 1.9 %collective-permute-start.12 = (bf16[1568,128]{1,0:T(8,128)(2,1)S(1)}, bf16[1568,128]{1,0:T(8,128)(2,1)S(1)}, u32[]{:S(2)}, u32[]{:S(2)}) collective-permute-start(bf16[1568,128]{1,0:T(8,128)(2,1)S(1)} %collective-permute-done.11.refs_3_), channel_id=1, source_target_pairs={{0,2},{1,31},{2,4},{3,1},{4,6},{5,3},{6,8},{7,5},{8,10},{9,7},{10,... | collective-permute-start | bytes 1204232 | tf_op jit(solution)/shard_map/ppermute | solution.py:371
  39.4 2.3 %collective-permute-done.5.refs_1_ = bf16[1536,128]{1,0:T(8,128)(2,1)S(1)} collective-permute-done((bf16[1536,128]{1,0:T(8,128)(2,1)}, bf16[1536,128]{1,0:T(8,128)(2,1)S(1)}, u32[]{:S(2)}, u32[]{:S(2)}) %collective-permute-start.5) | collective-permute-done | bytes 393248 | tf_op jit(solution)/shard_map/ppermute | solution.py:371
  41.7 4.9 %collective-permute-start.6 = (bf16[1536,128]{1,0:T(8,128)(2,1)S(1)}, bf16[1536,128]{1,0:T(8,128)(2,1)S(1)}, u32[]{:S(2)}, u32[]{:S(2)}) collective-permute-start(bf16[1536,128]{1,0:T(8,128)(2,1)S(1)} %collective-permute-done.5.refs_1_), channel_id=1, source_target_pairs={{0,2},{1,31},{2,4},{3,1},{4,6},{5,3},{6,8},{7,5},{8,10},{9,7},{10,... | collective-permute-start | bytes 1179656 | tf_op jit(solution)/shard_map/ppermute | solution.py:371
  47.4 3.5 %collective-permute-start.13 = (bf16[1568,128]{1,0:T(8,128)(2,1)S(1)}, bf16[1568,128]{1,0:T(8,128)(2,1)S(1)}, u32[]{:S(2)}, u32[]{:S(2)}) collective-permute-start(bf16[1568,128]{1,0:T(8,128)(2,1)S(1)} %collective-permute-done.12.refs_4_), channel_id=1, source_target_pairs={{0,2},{1,31},{2,4},{3,1},{4,6},{5,3},{6,8},{7,5},{8,10},{9,7},{10,... | collective-permute-start | bytes 1204232 | tf_op jit(solution)/shard_map/ppermute | solution.py:371
  51.3 5.0 %collective-permute-start.7 = (bf16[1536,128]{1,0:T(8,128)(2,1)S(1)}, bf16[1536,128]{1,0:T(8,128)(2,1)S(1)}, u32[]{:S(2)}, u32[]{:S(2)}) collective-permute-start(bf16[1536,128]{1,0:T(8,128)(2,1)S(1)} %collective-permute-done.6.refs_1_), channel_id=1, source_target_pairs={{0,2},{1,31},{2,4},{3,1},{4,6},{5,3},{6,8},{7,5},{8,10},{9,7},{10,... | collective-permute-start | bytes 1179656 | tf_op jit(solution)/shard_map/ppermute | solution.py:371
  57.1 3.6 %collective-permute-start.14 = (bf16[1568,128]{1,0:T(8,128)(2,1)S(1)}, bf16[1568,128]{1,0:T(8,128)(2,1)S(1)}, u32[]{:S(2)}, u32[]{:S(2)}) collective-permute-start(bf16[1568,128]{1,0:T(8,128)(2,1)S(1)} %collective-permute-done.13.refs_5_), channel_id=1, source_target_pairs={{0,2},{1,31},{2,4},{3,1},{4,6},{5,3},{6,8},{7,5},{8,10},{9,7},{10,... | collective-permute-start | bytes 1204232 | tf_op jit(solution)/shard_map/ppermute | solution.py:371
  61.5 4.6 %collective-permute-start.8 = (bf16[1536,128]{1,0:T(8,128)(2,1)S(1)}, bf16[1536,128]{1,0:T(8,128)(2,1)S(1)}, u32[]{:S(2)}, u32[]{:S(2)}) collective-permute-start(bf16[1536,128]{1,0:T(8,128)(2,1)S(1)} %collective-permute-done.7.refs_2_), channel_id=1, source_target_pairs={{0,2},{1,31},{2,4},{3,1},{4,6},{5,3},{6,8},{7,5},{8,10},{9,7},{10,... | collective-permute-start | bytes 1179656 | tf_op jit(solution)/shard_map/ppermute | solution.py:371
  66.8 3.7 %collective-permute-start.15 = (bf16[1568,128]{1,0:T(8,128)(2,1)S(1)}, bf16[1568,128]{1,0:T(8,128)(2,1)}, u32[]{:S(2)}, u32[]{:S(2)}) collective-permute-start(bf16[1568,128]{1,0:T(8,128)(2,1)S(1)} %collective-permute-done.14.refs_2_), channel_id=1, source_target_pairs={{0,2},{1,31},{2,4},{3,1},{4,6},{5,3},{6,8},{7,5},{8,10},{9,7},{10,... | collective-permute-start | bytes 1204232 | tf_op jit(solution)/shard_map/ppermute | solution.py:371
  71.3 4.5 %collective-permute-start.9 = (bf16[1536,128]{1,0:T(8,128)(2,1)S(1)}, bf16[1536,128]{1,0:T(8,128)(2,1)}, u32[]{:S(2)}, u32[]{:S(2)}) collective-permute-start(bf16[1536,128]{1,0:T(8,128)(2,1)S(1)} %collective-permute-done.8.refs_0_), channel_id=1, source_target_pairs={{0,2},{1,31},{2,4},{3,1},{4,6},{5,3},{6,8},{7,5},{8,10},{9,7},{10,... | collective-permute-start | bytes 1179656 | tf_op jit(solution)/shard_map/ppermute | solution.py:371
  76.5 3.6 %collective-permute-start.17 = (bf16[1536,128]{1,0:T(8,128)(2,1)}, bf16[1536,128]{1,0:T(8,128)(2,1)}, u32[]{:S(2)}, u32[]{:S(2)}) collective-permute-start(bf16[1536,128]{1,0:T(8,128)(2,1)} %bitcast.3.refs_0_), channel_id=1, source_target_pairs={{0,1},{1,0},{2,3},{3,2},{4,5},{5,4},{6,7},{7,6},{8,9},{9,8},{10,11... | collective-permute-start | bytes 1179656 | tf_op jit(solution)/shard_map/ppermute | solution.py:371
  80.1 4.9 %collective-permute-start.16 = (bf16[1568,128]{1,0:T(8,128)(2,1)}, bf16[1568,128]{1,0:T(8,128)(2,1)}, u32[]{:S(2)}, u32[]{:S(2)}) collective-permute-start(bf16[1568,128]{1,0:T(8,128)(2,1)} %collective-permute-done.15.refs_3_), channel_id=1, source_target_pairs={{0,2},{1,31},{2,4},{3,1},{4,6},{5,3},{6,8},{7,5},{8,10},{9,7},{10,... | collective-permute-start | bytes 1204232 | tf_op jit(solution)/shard_map/ppermute | solution.py:371
  85.0 1.9 %collective-permute-start.10 = (bf16[1536,128]{1,0:T(8,128)(2,1)}, bf16[1536,128]{1,0:T(8,128)(2,1)}, u32[]{:S(2)}, u32[]{:S(2)}) collective-permute-start(bf16[1536,128]{1,0:T(8,128)(2,1)} %collective-permute-done.9.refs_1_), channel_id=1, source_target_pairs={{0,2},{1,31},{2,4},{3,1},{4,6},{5,3},{6,8},{7,5},{8,10},{9,7},{10,... | collective-permute-start | bytes 1179656 | tf_op jit(solution)/shard_map/ppermute | solution.py:371
  87.0 1.0 copy-done.6
  89.1 3.0 %ring_sums.4 = (f32[1536,256]{1,0:T(8,128)S(1)}, f32[1536,256]{1,0:T(8,128)S(1)}) custom-call(s32[4]{0:T(128)S(1)} %pad_add_fusion.place_ref, bf16[4096,256]{1,0:T(8,128)(2,1)S(1)} %beside.1.own_w_ref.main_ref, bf16[4096,256]{1,0:T(8,128)(2,1)} %collective-permute-done.4.other_w_ref, bf16[1536,128]{1,0:T(8,128)(2,1)} %collective-permute-done.3.refs_0_, ...), custom_call_target="tpu_custom_call" | custom-call | flops 805306368 | tf_op jit(solution)/shard_map/ring_sums/pallas_call | solution.py:121
  92.1 3.3 %ring_sums.5 = (f32[1536,256]{1,0:T(8,128)S(1)}, f32[1536,256]{1,0:T(8,128)S(1)}) custom-call(s32[4]{0:T(128)S(1)} %pad_add_fusion.place_ref, bf16[4096,256]{1,0:T(8,128)(2,1)S(1)} %beside.1.own_w_ref.main_ref, bf16[4096,256]{1,0:T(8,128)(2,1)} %collective-permute-done.4.other_w_ref, bf16[1536,128]{1,0:T(8,128)(2,1)} %bitcast.3.refs_0_, ...), custom_call_target="tpu_custom_call" | custom-call | flops 1207959552 | tf_op jit(solution)/shard_map/ring_sums/pallas_call | solution.py:121
  95.5 3.0 %ring_sums.6 = (f32[1536,256]{1,0:T(8,128)S(1)}, f32[1536,256]{1,0:T(8,128)S(1)}) custom-call(s32[4]{0:T(128)S(1)} %pad_add_fusion.place_ref, bf16[4096,256]{1,0:T(8,128)(2,1)S(1)} %beside.1.own_w_ref.main_ref, bf16[4096,256]{1,0:T(8,128)(2,1)} %collective-permute-done.4.other_w_ref, bf16[1536,128]{1,0:T(8,128)(2,1)S(1)} %copy-done.14, ...), custom_call_target="tpu_custom_call" | custom-call | flops 805306368 | tf_op jit(solution)/shard_map/ring_sums/pallas_call | solution.py:121
  98.6 2.8 %ring_sums.7 = (f32[1536,256]{1,0:T(8,128)S(1)}, f32[1536,256]{1,0:T(8,128)S(1)}) custom-call(s32[4]{0:T(128)S(1)} %pad_add_fusion.place_ref, bf16[4096,256]{1,0:T(8,128)(2,1)S(1)} %beside.1.own_w_ref.main_ref, bf16[4096,256]{1,0:T(8,128)(2,1)} %collective-permute-done.4.other_w_ref, bf16[1536,128]{1,0:T(8,128)(2,1)} %collective-permute-done.10.refs_0_, ...), custom_call_target="tpu_custom_call" | custom-call | flops 402653184 | tf_op jit(solution)/shard_map/ring_sums/pallas_call | solution.py:121
  101.4 3.4 %collective-permute-start.18 = (f32[1536,256]{1,0:T(8,128)S(1)}, f32[1536,256]{1,0:T(8,128)S(1)}, u32[]{:S(2)}, u32[]{:S(2)}) collective-permute-start(f32[1536,256]{1,0:T(8,128)S(1)} %get-tuple-element.35), channel_id=1, source_target_pairs={{0,1},{1,0},{2,3},{3,2},{4,5},{5,4},{6,7},{7,6},{8,9},{9,8},{10,11... | collective-permute-start | bytes 4718600 | tf_op jit(solution)/shard_map/ppermute | solution.py:371
  105.6 4.8 %collective-permute-start.20 = (bf16[1536,128]{1,0:T(8,128)(2,1)}, bf16[1536,128]{1,0:T(8,128)(2,1)S(1)}, u32[]{:S(2)}, u32[]{:S(2)}) collective-permute-start(bf16[1536,128]{1,0:T(8,128)(2,1)} %collective-permute-done.10.refs_0_), channel_id=1, source_target_pairs={{0,2},{1,31},{2,4},{3,1},{4,6},{5,3},{6,8},{7,5},{8,10},{9,7},{10,... | collective-permute-start | bytes 1179656 | tf_op jit(solution)/shard_map/ppermute | solution.py:371
  110.4 1.9 %collective-permute-start.21 = (bf16[1568,128]{1,0:T(8,128)(2,1)}, bf16[1568,128]{1,0:T(8,128)(2,1)S(1)}, u32[]{:S(2)}, u32[]{:S(2)}) collective-permute-start(bf16[1568,128]{1,0:T(8,128)(2,1)} %collective-permute-done.16.refs_1_), channel_id=1, source_target_pairs={{0,2},{1,31},{2,4},{3,1},{4,6},{5,3},{6,8},{7,5},{8,10},{9,7},{10,... | collective-permute-start | bytes 1204232 | tf_op jit(solution)/shard_map/ppermute | solution.py:371
  113.8 1.9 %collective-permute-start.19 = (bf16[224,128]{1,0:T(8,128)(2,1)S(1)}, bf16[224,128]{1,0:T(8,128)(2,1)S(1)}, u32[]{:S(2)}, u32[]{:S(2)}) collective-permute-start(bf16[224,128]{1,0:T(8,128)(2,1)S(1)} %constant_dynamic-update-slice_fusion.mine_new_ref), channel_id=1, source_target_pairs={{0,1},{1,0},{2,3},{3,2},{4,5},{5,4},{6,7},{7,6},{8,9},{9,8},{10,11... | collective-permute-start | bytes 172040 | tf_op jit(solution)/shard_map/ppermute | solution.py:371
  116.9 2.9 %collective-permute-done.21.last_b_ref = bf16[1568,128]{1,0:T(8,128)(2,1)S(1)} collective-permute-done((bf16[1568,128]{1,0:T(8,128)(2,1)}, bf16[1568,128]{1,0:T(8,128)(2,1)S(1)}, u32[]{:S(2)}, u32[]{:S(2)}) %collective-permute-start.21) | collective-permute-done | bytes 401440 | tf_op jit(solution)/shard_map/ppermute | solution.py:371
  119.7 2.1 %span_states.1 = (f32[16,15,128]{2,1,0:T(8,128)S(1)}, f32[16,128]{1,0:T(8,128)S(1)}) custom-call(s32[4]{0:T(128)S(1)} %pad_add_fusion.place_ref, f32[2]{0:T(128)S(1)} %copy-done.17, f32[1536,256]{1,0:T(8,128)S(1)} %get-tuple-element.34.total_ref, f32[1536,256]{1,0:T(8,128)S(1)} %collective-permute-done.18.arrived_ref, ...), custom_call_target="tpu_custom_call" | custom-call | tf_op jit(solution)/shard_map/span_states/pallas_call | solution.py:278
  121.8 13.4 %all_to_all.5.arrived_ref = f32[16,15,128]{2,1,0:T(8,128)S(1)} all-to-all(f32[16,15,128]{2,1,0:T(8,128)S(1)} %get-tuple-element.40), channel_id=1, replica_groups=mesh['sp'=16,'tp'=32] {'sp'}, dimensions={0} | all-to-all | bytes 245760 | tf_op jit(solution)/shard_map/all_to_all | solution.py:446
  (72 shorter events, 14.7 us)
Async XLA Ops:
  0.6 21.3 %collective-permute-start.3 = (bf16[1536,128]{1,0:T(8,128)(2,1)}, bf16[1536,128]{1,0:T(8,128)(2,1)}, u32[]{:S(2)}, u32[]{:S(2)}) collective-permute-start(bf16[1536,128]{1,0:T(8,128)(2,1)} %bitcast.3.refs_0_), channel_id=1, source_target_pairs={{0,2},{1,31},{2,4},{3,1},{4,6},{5,3},{6,8},{7,5},{8,10},{9,7},{10,... | collective-permute-start | bytes 1179656 | tf_op jit(solution)/shard_map/ppermute | solution.py:371
  12.6 11.1 %collective-permute-start = (bf16[1536,128]{1,0:T(8,128)(2,1)}, bf16[1536,128]{1,0:T(8,128)(2,1)S(1)}, u32[]{:S(2)}, u32[]{:S(2)}) collective-permute-start(bf16[1536,128]{1,0:T(8,128)(2,1)} %bitcast.3.refs_0_), channel_id=1, source_target_pairs={{1,2},{0,31},{3,4},{2,1},{5,6},{4,3},{7,8},{6,5},{9,10},{8,7},{11,... | collective-permute-start | bytes 1179656 | tf_op jit(solution)/shard_map/ppermute | solution.py:371
  14.5 4.0 %collective-permute-start.1 = (bf16[3,1,128]{2,0,1:T(4,128)(2,1)}, bf16[3,1,128]{2,0,1:T(4,128)(2,1)S(1)}, u32[]{:S(2)}, u32[]{:S(2)}) collective-permute-start(bf16[3,1,128]{2,0,1:T(4,128)(2,1)} %param.7), channel_id=1, source_target_pairs={{0,1},{1,0},{2,3},{3,2},{4,5},{5,4},{6,7},{7,6},{8,9},{9,8},{10,11... | collective-permute-start | bytes 2312 | tf_op jit(solution)/shard_map/ppermute | solution.py:371
  17.6 10.0 %copy-start.1 = (bf16[4096,128]{1,0:T(8,128)(2,1)S(1)}, bf16[4096,128]{1,0:T(8,128)(2,1)}, u32[]{:S(2)}) copy-start(bf16[4096,128]{1,0:T(8,128)(2,1)} %left_ref) | copy-start | bytes 3145732
  19.2 4.4 %collective-permute-start.2 = (bf16[32,128]{1,0:T(8,128)(2,1)S(1)}, bf16[32,128]{1,0:T(8,128)(2,1)S(1)}, u32[]{:S(2)}, u32[]{:S(2)}) collective-permute-start(bf16[32,128]{1,0:T(8,128)(2,1)S(1)} %pad_maximum_fusion.1.here_new_ref), channel_id=1, source_target_pairs={{0,2},{1,31},{2,4},{3,1},{4,6},{5,3},{6,8},{7,5},{8,10},{9,7},{10,... | collective-permute-start | bytes 24584 | tf_op jit(solution)/shard_map/ppermute | solution.py:371
  23.7 13.0 %collective-permute-start.11 = (bf16[1568,128]{1,0:T(8,128)(2,1)S(1)}, bf16[1568,128]{1,0:T(8,128)(2,1)S(1)}, u32[]{:S(2)}, u32[]{:S(2)}) collective-permute-start(bf16[1568,128]{1,0:T(8,128)(2,1)S(1)} %pad_maximum_fusion), channel_id=1, source_target_pairs={{0,2},{1,31},{2,4},{3,1},{4,6},{5,3},{6,8},{7,5},{8,10},{9,7},{10,... | collective-permute-start | bytes 1204232 | tf_op jit(solution)/shard_map/ppermute | solution.py:371
  27.5 1.2 copy-start.2
  29.1 57.9 %collective-permute-start.4 = (bf16[4096,256]{1,0:T(8,128)(2,1)S(1)}, bf16[4096,256]{1,0:T(8,128)(2,1)}, u32[]{:S(2)}, u32[]{:S(2)}) collective-permute-start(bf16[4096,256]{1,0:T(8,128)(2,1)S(1)} %beside.1.own_w_ref.main_ref), channel_id=1, source_target_pairs={{0,1},{1,0},{2,3},{3,2},{4,5},{5,4},{6,7},{7,6},{8,9},{9,8},{10,11... | collective-permute-start | bytes 6291464 | tf_op jit(solution)/shard_map/ppermute | solution.py:371
  31.8 9.9 %collective-permute-start.5 = (bf16[1536,128]{1,0:T(8,128)(2,1)}, bf16[1536,128]{1,0:T(8,128)(2,1)S(1)}, u32[]{:S(2)}, u32[]{:S(2)}) collective-permute-start(bf16[1536,128]{1,0:T(8,128)(2,1)} %collective-permute-done.3.refs_0_), channel_id=1, source_target_pairs={{0,2},{1,31},{2,4},{3,1},{4,6},{5,3},{6,8},{7,5},{8,10},{9,7},{10,... | collective-permute-start | bytes 1179656 | tf_op jit(solution)/shard_map/ppermute | solution.py:371
  36.7 10.7 %collective-permute-start.12 = (bf16[1568,128]{1,0:T(8,128)(2,1)S(1)}, bf16[1568,128]{1,0:T(8,128)(2,1)S(1)}, u32[]{:S(2)}, u32[]{:S(2)}) collective-permute-start(bf16[1568,128]{1,0:T(8,128)(2,1)S(1)} %collective-permute-done.11.refs_3_), channel_id=1, source_target_pairs={{0,2},{1,31},{2,4},{3,1},{4,6},{5,3},{6,8},{7,5},{8,10},{9,7},{10,... | collective-permute-start | bytes 1204232 | tf_op jit(solution)/shard_map/ppermute | solution.py:371
  41.7 9.6 %collective-permute-start.6 = (bf16[1536,128]{1,0:T(8,128)(2,1)S(1)}, bf16[1536,128]{1,0:T(8,128)(2,1)S(1)}, u32[]{:S(2)}, u32[]{:S(2)}) collective-permute-start(bf16[1536,128]{1,0:T(8,128)(2,1)S(1)} %collective-permute-done.5.refs_1_), channel_id=1, source_target_pairs={{0,2},{1,31},{2,4},{3,1},{4,6},{5,3},{6,8},{7,5},{8,10},{9,7},{10,... | collective-permute-start | bytes 1179656 | tf_op jit(solution)/shard_map/ppermute | solution.py:371
  47.4 9.7 %collective-permute-start.13 = (bf16[1568,128]{1,0:T(8,128)(2,1)S(1)}, bf16[1568,128]{1,0:T(8,128)(2,1)S(1)}, u32[]{:S(2)}, u32[]{:S(2)}) collective-permute-start(bf16[1568,128]{1,0:T(8,128)(2,1)S(1)} %collective-permute-done.12.refs_4_), channel_id=1, source_target_pairs={{0,2},{1,31},{2,4},{3,1},{4,6},{5,3},{6,8},{7,5},{8,10},{9,7},{10,... | collective-permute-start | bytes 1204232 | tf_op jit(solution)/shard_map/ppermute | solution.py:371
  51.3 10.2 %collective-permute-start.7 = (bf16[1536,128]{1,0:T(8,128)(2,1)S(1)}, bf16[1536,128]{1,0:T(8,128)(2,1)S(1)}, u32[]{:S(2)}, u32[]{:S(2)}) collective-permute-start(bf16[1536,128]{1,0:T(8,128)(2,1)S(1)} %collective-permute-done.6.refs_1_), channel_id=1, source_target_pairs={{0,2},{1,31},{2,4},{3,1},{4,6},{5,3},{6,8},{7,5},{8,10},{9,7},{10,... | collective-permute-start | bytes 1179656 | tf_op jit(solution)/shard_map/ppermute | solution.py:371
  57.1 9.7 %collective-permute-start.14 = (bf16[1568,128]{1,0:T(8,128)(2,1)S(1)}, bf16[1568,128]{1,0:T(8,128)(2,1)S(1)}, u32[]{:S(2)}, u32[]{:S(2)}) collective-permute-start(bf16[1568,128]{1,0:T(8,128)(2,1)S(1)} %collective-permute-done.13.refs_5_), channel_id=1, source_target_pairs={{0,2},{1,31},{2,4},{3,1},{4,6},{5,3},{6,8},{7,5},{8,10},{9,7},{10,... | collective-permute-start | bytes 1204232 | tf_op jit(solution)/shard_map/ppermute | solution.py:371
  61.5 9.8 %collective-permute-start.8 = (bf16[1536,128]{1,0:T(8,128)(2,1)S(1)}, bf16[1536,128]{1,0:T(8,128)(2,1)S(1)}, u32[]{:S(2)}, u32[]{:S(2)}) collective-permute-start(bf16[1536,128]{1,0:T(8,128)(2,1)S(1)} %collective-permute-done.7.refs_2_), channel_id=1, source_target_pairs={{0,2},{1,31},{2,4},{3,1},{4,6},{5,3},{6,8},{7,5},{8,10},{9,7},{10,... | collective-permute-start | bytes 1179656 | tf_op jit(solution)/shard_map/ppermute | solution.py:371
  66.8 13.3 %collective-permute-start.15 = (bf16[1568,128]{1,0:T(8,128)(2,1)S(1)}, bf16[1568,128]{1,0:T(8,128)(2,1)}, u32[]{:S(2)}, u32[]{:S(2)}) collective-permute-start(bf16[1568,128]{1,0:T(8,128)(2,1)S(1)} %collective-permute-done.14.refs_2_), channel_id=1, source_target_pairs={{0,2},{1,31},{2,4},{3,1},{4,6},{5,3},{6,8},{7,5},{8,10},{9,7},{10,... | collective-permute-start | bytes 1204232 | tf_op jit(solution)/shard_map/ppermute | solution.py:371
  71.3 13.7 %collective-permute-start.9 = (bf16[1536,128]{1,0:T(8,128)(2,1)S(1)}, bf16[1536,128]{1,0:T(8,128)(2,1)}, u32[]{:S(2)}, u32[]{:S(2)}) collective-permute-start(bf16[1536,128]{1,0:T(8,128)(2,1)S(1)} %collective-permute-done.8.refs_0_), channel_id=1, source_target_pairs={{0,2},{1,31},{2,4},{3,1},{4,6},{5,3},{6,8},{7,5},{8,10},{9,7},{10,... | collective-permute-start | bytes 1179656 | tf_op jit(solution)/shard_map/ppermute | solution.py:371
  76.5 15.6 %collective-permute-start.17 = (bf16[1536,128]{1,0:T(8,128)(2,1)}, bf16[1536,128]{1,0:T(8,128)(2,1)}, u32[]{:S(2)}, u32[]{:S(2)}) collective-permute-start(bf16[1536,128]{1,0:T(8,128)(2,1)} %bitcast.3.refs_0_), channel_id=1, source_target_pairs={{0,1},{1,0},{2,3},{3,2},{4,5},{5,4},{6,7},{7,6},{8,9},{9,8},{10,11... | collective-permute-start | bytes 1179656 | tf_op jit(solution)/shard_map/ppermute | solution.py:371
  80.1 18.4 %collective-permute-start.16 = (bf16[1568,128]{1,0:T(8,128)(2,1)}, bf16[1568,128]{1,0:T(8,128)(2,1)}, u32[]{:S(2)}, u32[]{:S(2)}) collective-permute-start(bf16[1568,128]{1,0:T(8,128)(2,1)} %collective-permute-done.15.refs_3_), channel_id=1, source_target_pairs={{0,2},{1,31},{2,4},{3,1},{4,6},{5,3},{6,8},{7,5},{8,10},{9,7},{10,... | collective-permute-start | bytes 1204232 | tf_op jit(solution)/shard_map/ppermute | solution.py:371
  85.0 13.5 %collective-permute-start.10 = (bf16[1536,128]{1,0:T(8,128)(2,1)}, bf16[1536,128]{1,0:T(8,128)(2,1)}, u32[]{:S(2)}, u32[]{:S(2)}) collective-permute-start(bf16[1536,128]{1,0:T(8,128)(2,1)} %collective-permute-done.9.refs_1_), channel_id=1, source_target_pairs={{0,2},{1,31},{2,4},{3,1},{4,6},{5,3},{6,8},{7,5},{8,10},{9,7},{10,... | collective-permute-start | bytes 1179656 | tf_op jit(solution)/shard_map/ppermute | solution.py:371
  87.0 5.1 %copy-start.4 = (bf16[1568,128]{1,0:T(8,128)(2,1)S(1)}, bf16[1568,128]{1,0:T(8,128)(2,1)}, u32[]{:S(2)}) copy-start(bf16[1568,128]{1,0:T(8,128)(2,1)} %copy-done.3) | copy-start | bytes 1204228
  87.0 1.1 copy-start.6
  89.1 3.0 %copy-start.10 = (bf16[1536,128]{1,0:T(8,128)(2,1)S(1)}, bf16[1536,128]{1,0:T(8,128)(2,1)}, u32[]{:S(2)}) copy-start(bf16[1536,128]{1,0:T(8,128)(2,1)} %copy-done.9) | copy-start | bytes 1179652
  89.1 3.0 %copy-start.12 = (bf16[1536,128]{1,0:T(8,128)(2,1)S(1)}, bf16[1536,128]{1,0:T(8,128)(2,1)}, u32[]{:S(2)}) copy-start(bf16[1536,128]{1,0:T(8,128)(2,1)} %copy-done.11) | copy-start | bytes 1179652
  92.1 3.3 %copy-start.8 = (bf16[1568,128]{1,0:T(8,128)(2,1)S(1)}, bf16[1568,128]{1,0:T(8,128)(2,1)}, u32[]{:S(2)}) copy-start(bf16[1568,128]{1,0:T(8,128)(2,1)} %copy-done.7) | copy-start | bytes 1204228
  92.1 3.3 %copy-start.14 = (bf16[1536,128]{1,0:T(8,128)(2,1)S(1)}, bf16[1536,128]{1,0:T(8,128)(2,1)}, u32[]{:S(2)}) copy-start(bf16[1536,128]{1,0:T(8,128)(2,1)} %copy-done.13) | copy-start | bytes 1179652
  98.6 17.1 %copy-start = (bf16[4096,128]{1,0:T(8,128)(2,1)S(1)}, bf16[4096,128]{1,0:T(8,128)(2,1)}, u32[]{:S(2)}) copy-start(bf16[4096,128]{1,0:T(8,128)(2,1)} %query_w_ref.3) | copy-start | bytes 3145732
  98.6 17.1 %copy-start.17 = (f32[2]{0:T(128)S(1)}, f32[2]{0:T(128)}, u32[]{:S(2)}) copy-start(f32[2]{0:T(128)} %rate_ref.3) | copy-start | bytes 28
  101.4 18.3 %collective-permute-start.18 = (f32[1536,256]{1,0:T(8,128)S(1)}, f32[1536,256]{1,0:T(8,128)S(1)}, u32[]{:S(2)}, u32[]{:S(2)}) collective-permute-start(f32[1536,256]{1,0:T(8,128)S(1)} %get-tuple-element.35), channel_id=1, source_target_pairs={{0,1},{1,0},{2,3},{3,2},{4,5},{5,4},{6,7},{7,6},{8,9},{9,8},{10,11... | collective-permute-start | bytes 4718600 | tf_op jit(solution)/shard_map/ppermute | solution.py:371
  105.6 11.3 %collective-permute-start.20 = (bf16[1536,128]{1,0:T(8,128)(2,1)}, bf16[1536,128]{1,0:T(8,128)(2,1)S(1)}, u32[]{:S(2)}, u32[]{:S(2)}) collective-permute-start(bf16[1536,128]{1,0:T(8,128)(2,1)} %collective-permute-done.10.refs_0_), channel_id=1, source_target_pairs={{0,2},{1,31},{2,4},{3,1},{4,6},{5,3},{6,8},{7,5},{8,10},{9,7},{10,... | collective-permute-start | bytes 1179656 | tf_op jit(solution)/shard_map/ppermute | solution.py:371
  110.4 9.3 %collective-permute-start.21 = (bf16[1568,128]{1,0:T(8,128)(2,1)}, bf16[1568,128]{1,0:T(8,128)(2,1)S(1)}, u32[]{:S(2)}, u32[]{:S(2)}) collective-permute-start(bf16[1568,128]{1,0:T(8,128)(2,1)} %collective-permute-done.16.refs_1_), channel_id=1, source_target_pairs={{0,2},{1,31},{2,4},{3,1},{4,6},{5,3},{6,8},{7,5},{8,10},{9,7},{10,... | collective-permute-start | bytes 1204232 | tf_op jit(solution)/shard_map/ppermute | solution.py:371
  113.8 3.1 %collective-permute-start.19 = (bf16[224,128]{1,0:T(8,128)(2,1)S(1)}, bf16[224,128]{1,0:T(8,128)(2,1)S(1)}, u32[]{:S(2)}, u32[]{:S(2)}) collective-permute-start(bf16[224,128]{1,0:T(8,128)(2,1)S(1)} %constant_dynamic-update-slice_fusion.mine_new_ref), channel_id=1, source_target_pairs={{0,1},{1,0},{2,3},{3,2},{4,5},{5,4},{6,7},{7,6},{8,9},{9,8},{10,11... | collective-permute-start | bytes 172040 | tf_op jit(solution)/shard_map/ppermute | solution.py:371
  (8 other events, 6.3 us)
